TPU v7x, 128 devices: a whole 4x4x4 slice. The times are simulated.
128 devices in a mesh: sp: 64 (over z, y, x), tp: 2 (over core).
Axes of the slice: x: 4, y: 4, z: 4, core: 2. Of those that a mesh axis runs over, the one named last changes fastest.
Arguments:
- mixer_output: bfloat16 [8192, 2048], P('sp'), may hold values from -6 to 6
- layer_cotangent: bfloat16 [8192, 2048], P('sp'), may hold values from -16 to 16
- expert_choice: int32 [8192, 2], P('sp'), may hold values from 0 to 63, all different within a row; in each aligned block of 128 rows (0 to 127, 128 to 255, ...) at most 8 rows name the same one
- route_weight: float32 [8192, 2], P('sp'), may hold values from 0.1 to 0.9
- gate_pre: bfloat16 [64, 512, 1024], P('sp', None, 'tp'), may hold values from -15 to 15
- up_pre: bfloat16 [64, 512, 1024], P('sp', None, 'tp'), may hold values from -15 to 15
- w_gate: bfloat16 [64, 2048, 1024], P('sp', None, 'tp'), may hold values from -0.125 to 0.125
- w_up: bfloat16 [64, 2048, 1024], P('sp', None, 'tp'), may hold values from -0.125 to 0.125
- w_down: bfloat16 [64, 1024, 2048], P('sp', 'tp'), may hold values from -0.1875 to 0.1875
- w_out: bfloat16 [2048, 2048], P('tp'), may hold values from -0.125 to 0.125
- norm_gain: bfloat16 [2048], P('tp'), may hold values from 0.099609375 to 1.8984375
- scan_in: bfloat16 [8192, 2048], P('sp', 'tp'), may hold values from -6 to 6
- gate_in: bfloat16 [8192, 2048], P('sp', 'tp'), may hold values from -9 to 9
- b_proj: bfloat16 [8192, 1024], P('sp', 'tp'), may hold values from -1.796875 to 1.796875
- c_proj: bfloat16 [8192, 1024], P('sp', 'tp'), may hold values from -1.796875 to 1.796875
- log_decay: float32 [8192, 32], P('sp', 'tp'), may hold values from -3 to 0
- entry_state: float32 [64, 32, 64, 128], P('sp', 'tp'), may hold values from -24 to 24
Outputs:
- grad_w_gate: bfloat16 [64, 2048, 1024], P('sp', None, 'tp')
- grad_w_up: bfloat16 [64, 2048, 1024], P('sp', None, 'tp')
- grad_w_down: bfloat16 [64, 1024, 2048], P('sp', 'tp')
- grad_out_proj: float32 [2048, 2048], P('sp', 'tp')
- grad_scan_in: bfloat16 [8192, 2048], P('sp', 'tp')
- grad_gate_in: bfloat16 [8192, 2048], P('sp', 'tp')
- grad_b_proj: bfloat16 [8192, 1024], P('sp', 'tp')
- grad_c_proj: bfloat16 [8192, 1024], P('sp', 'tp')
- grad_log_decay: float32 [8192, 32], P('sp', 'tp')
Inputs may be any that keep to these rules, and one draw needn't show every extreme that they name: `expert_choice`: in the 128 rows of one device no expert is named more than 8 times, a bound that some blocks reach; the 2 entries of a row differ.
All inputs are finite; a program needn't handle non-finite values.
Results may differ from a plain program's by a relative error of at most 0.012.
Values may be sent and summed in bfloat16 or wider, within the bound.
No kernel may reach another device: no remote copies, remote signals or barrier semaphores. Data moves between devices by JAX's collectives and lax.ppermute only.
A program may use at most 192 MiB of HBM per device.

v0:
```python
import jax
import jax.numpy as jnp
from jax import lax
from jax.sharding import Mesh
from jax.sharding import PartitionSpec as P

HEAD_DIM = 64
STATE = 128
SP = ("sp_0", "sp_1", "sp_2")


rms_epsilon = 1e-05
clamp_limit = 7.0
swish_alpha = 1.702


def sent_together(arrays, axis, split_dim, concat_dim, along):
    both = jnp.concatenate(arrays, axis=along)
    out, at, gathered = (
        lax.all_to_all(both, axis, split_axis=split_dim, concat_axis=concat_dim, tiled=True),
        0,
        [],
    )
    for a in arrays:
        gathered.append(lax.slice_in_dim(out, at, at + a.shape[along], axis=along))
        at += a.shape[along]
    return tuple(gathered)


def in_one_piece(arrays, axis, dim, along):
    both = jnp.concatenate(arrays, axis=along)
    out, at, gathered = (lax.all_gather(both, axis, axis=dim, tiled=True), 0, [])
    for a in arrays:
        gathered.append(lax.slice_in_dim(out, at, at + a.shape[along], axis=along))
        at += a.shape[along]
    return tuple(gathered)


def from_everyone(x, axis):
    size = lax.axis_size(axis)
    return lax.all_to_all(jnp.broadcast_to(x[None], (size, *x.shape)), axis, 0, 0, tiled=True)


def of_everyone(x, axis):
    return from_everyone(x, axis).astype(jnp.float32).sum(axis=0)


def summed_rows(running, axes):
    for axis in axes:
        running = lax.psum_scatter(running, axis, scatter_dimension=0, tiled=True)
    return running


def filled_with(x, identity):
    return jax.tree.map(
        lambda part, zero: jnp.zeros_like(part) + jnp.asarray(zero, part.dtype), x, identity
    )


def carried_in(x, axes, combine, identity):
    before = start = filled_with(x, identity)
    running = x
    for axis in reversed(axes):
        size, position = (lax.axis_size(axis), lax.axis_index(axis))
        pieces = jax.tree.map(lambda part: lax.all_gather(part, axis), running)
        inside, running = (start, start)
        for k in reversed(range(size)):
            passed = k > position
            running = combine(running, jax.tree.map(lambda part: part[k], pieces))
            inside = jax.tree.map(lambda new, old: jnp.where(passed, new, old), running, inside)
        before = combine(inside, before)
    return before


def slot_ranks(expert_ids, expert_count):
    targets = expert_ids.reshape(-1)
    one_hot = (targets[:, None] == jnp.arange(expert_count, dtype=jnp.int32)[None, :]).astype(
        jnp.int32
    )
    earlier = jnp.cumsum(one_hot, axis=0) - one_hot
    return (targets, jnp.sum(earlier * one_hot, axis=1))


def expert_side(hidden_rows, grad_rows, gate_value, up_value, gate_weight, up_weight, down_weight):
    act_grad = jnp.einsum("rd,fd->rf", grad_rows, down_weight, preferred_element_type=jnp.float32)
    gate_full = gate_value.astype(jnp.float32)
    up_full = up_value.astype(jnp.float32)
    gate_clip = jnp.minimum(gate_full, clamp_limit)
    up_clip = jnp.clip(up_full, -clamp_limit, clamp_limit)
    sigmoid_gate = jax.nn.sigmoid(swish_alpha * gate_clip)
    swish_gate = gate_clip * sigmoid_gate
    active = ((up_clip + 1.0) * swish_gate).astype(jnp.bfloat16)
    up_grad = jnp.where(
        (up_full > -clamp_limit) & (up_full < clamp_limit), act_grad * swish_gate, 0.0
    ).astype(jnp.bfloat16)
    slope = sigmoid_gate + swish_alpha * gate_clip * sigmoid_gate * (1.0 - sigmoid_gate)
    gate_grad = jnp.where(gate_full < clamp_limit, act_grad * (up_clip + 1.0) * slope, 0.0).astype(
        jnp.bfloat16
    )
    down_wgrad = jnp.einsum(
        "rf,rd->fd", active, grad_rows, preferred_element_type=jnp.float32
    ).astype(jnp.bfloat16)
    gate_wgrad = jnp.einsum(
        "rd,rf->df", hidden_rows, gate_grad, preferred_element_type=jnp.float32
    ).astype(jnp.bfloat16)
    up_wgrad = jnp.einsum(
        "rd,rf->df", hidden_rows, up_grad, preferred_element_type=jnp.float32
    ).astype(jnp.bfloat16)
    partial_rows = jnp.einsum(
        "rf,df->rd", gate_grad, gate_weight, preferred_element_type=jnp.float32
    )
    partial_rows = partial_rows + jnp.einsum(
        "rf,df->rd", up_grad, up_weight, preferred_element_type=jnp.float32
    )
    return (gate_wgrad, up_wgrad, down_wgrad, partial_rows)


def join_reverse(earlier, later):
    upper_decay, upper_state, upper_local, upper_grad = earlier
    lower_decay, lower_state, lower_local, lower_grad = later
    joined_decay = lower_decay * upper_decay
    joined_state = lower_state + lower_decay[:, None, None] * upper_state
    joined_local = upper_decay[:, None, None] * lower_local + upper_local
    joined_grad = lower_grad + upper_grad - jnp.sum(upper_state * lower_local, axis=(1, 2))
    return (joined_decay, joined_state, joined_local, joined_grad)


def body(
    mixer_output,
    layer_cotangent,
    expert_choice,
    route_weight,
    gate_pre,
    up_pre,
    w_gate,
    w_up,
    w_down,
    w_out,
    norm_gain,
    scan_in,
    gate_in,
    b_proj,
    c_proj,
    log_decay,
    entry_state,
):
    expert_count = lax.axis_size(SP)
    tokens_here = mixer_output.shape[0]
    model_width = mixer_output.shape[1]
    top_count = expert_choice.shape[1]
    capacity = gate_pre.shape[1] // expert_count
    targets, ranked = slot_ranks(expert_choice, expert_count)
    token_of = jnp.arange(tokens_here * top_count, dtype=jnp.int32) // top_count
    grad_rows = (
        route_weight.reshape(-1)[:, None] * layer_cotangent[token_of].astype(jnp.float32)
    ).astype(jnp.bfloat16)
    blank_slots = jnp.zeros((expert_count, capacity, model_width), jnp.bfloat16)
    send_hidden = blank_slots.at[targets, ranked].set(mixer_output[token_of])
    send_grads = blank_slots.at[targets, ranked].set(grad_rows)
    half_width = model_width // lax.axis_size("tp")
    half_start = lax.axis_index("tp") * half_width
    hidden_half = lax.dynamic_slice_in_dim(send_hidden, half_start, half_width, 2)
    grads_half = lax.dynamic_slice_in_dim(send_grads, half_start, half_width, 2)
    came_hidden, came_grads = sent_together((hidden_half, grads_half), SP, 0, 0, 1)
    recv_hidden, recv_grads = in_one_piece((came_hidden, came_grads), "tp", 2, 0)
    gate_wgrad, up_wgrad, down_wgrad, partial_rows = expert_side(
        recv_hidden.reshape(-1, model_width),
        recv_grads.reshape(-1, model_width),
        gate_pre[0],
        up_pre[0],
        w_gate[0],
        w_up[0],
        w_down[0],
    )
    summed = of_everyone(partial_rows.astype(jnp.bfloat16), "tp").astype(jnp.float32)
    returned = lax.all_to_all(
        summed.astype(jnp.bfloat16).reshape(expert_count, capacity, -1),
        SP,
        split_axis=0,
        concat_axis=0,
        tiled=True,
    )
    columns = returned.shape[2]
    moe_terms = (
        returned[targets, ranked]
        .astype(jnp.float32)
        .reshape(tokens_here, top_count, columns)
        .sum(axis=1)
    )
    grad_hidden = (layer_cotangent.astype(jnp.float32) + moe_terms).astype(jnp.bfloat16)
    head_count = log_decay.shape[1]
    group_count = b_proj.shape[1] // STATE
    per_group = head_count // group_count
    scan_heads = scan_in.reshape(tokens_here, head_count, HEAD_DIM)
    b_groups = b_proj.reshape(tokens_here, group_count, STATE)
    c_groups = c_proj.reshape(tokens_here, group_count, STATE)
    x_float = scan_heads.astype(jnp.float32)
    b_float = b_groups.astype(jnp.float32)
    c_float = c_groups.astype(jnp.float32)
    cumulative = jnp.cumsum(log_decay, axis=0)
    growth = jnp.exp(cumulative)
    tail_decay = jnp.exp(cumulative[-1][None, :] - cumulative)
    token_locations = jnp.arange(tokens_here)
    causal = token_locations[:, None] >= token_locations[None, :]
    log_gaps = cumulative.T[:, :, None] - cumulative.T[:, None, :]
    decay_mat = jnp.exp(jnp.where(causal[None], log_gaps, -jnp.inf))
    inner_prod = jnp.einsum("tgn,sgn->gts", c_groups, b_groups, preferred_element_type=jnp.float32)
    mix_weights = (jnp.repeat(inner_prod, per_group, axis=0) * decay_mat).astype(jnp.bfloat16)
    state_groups = entry_state.reshape(group_count, per_group, HEAD_DIM, STATE)
    y_inner = jnp.einsum(
        "hts,shp->thp", mix_weights, scan_heads, preferred_element_type=jnp.float32
    )
    y_carry = jnp.einsum("tgn,grpn->tgrp", c_float, state_groups).reshape(
        tokens_here, head_count, HEAD_DIM
    )
    scan_out = y_inner + y_carry * growth[:, :, None]
    gate_float = gate_in.astype(jnp.float32)
    gate_sig = jax.nn.sigmoid(gate_float)
    gate_silu = gate_float * gate_sig
    gated = scan_out.reshape(tokens_here, -1) * gate_silu
    grouped = gated.reshape(tokens_here, group_count, -1)
    inv_rms = lax.rsqrt(jnp.mean(grouped * grouped, axis=-1, keepdims=True) + rms_epsilon)
    unit = grouped * inv_rms
    gain_groups = norm_gain.astype(jnp.float32).reshape(group_count, -1)
    mixed = (unit * gain_groups).reshape(tokens_here, -1).astype(jnp.bfloat16)
    grad_out_proj = summed_rows(
        jnp.einsum("td,ti->di", grad_hidden, mixed, preferred_element_type=jnp.float32), SP
    )
    grad_mixed = jnp.einsum("td,id->ti", grad_hidden, w_out, preferred_element_type=jnp.float32)
    grad_unit = grad_mixed.reshape(tokens_here, group_count, -1) * gain_groups
    grad_grouped = inv_rms * (grad_unit - unit * jnp.mean(grad_unit * unit, axis=-1, keepdims=True))
    grad_gated = grad_grouped.reshape(tokens_here, -1)
    grad_gate_in = (
        grad_gated
        * scan_out.reshape(tokens_here, -1)
        * gate_sig
        * (1.0 + gate_float * (1.0 - gate_sig))
    ).astype(jnp.bfloat16)
    grad_y = (grad_gated * gate_silu).reshape(tokens_here, head_count, HEAD_DIM)
    grad_y_b = grad_y.astype(jnp.bfloat16)
    grad_x_inner = jnp.einsum(
        "hts,thp->shp", mix_weights, grad_y_b, preferred_element_type=jnp.float32
    )
    grad_weights = (
        jnp.einsum("thp,shp->hts", grad_y_b, scan_heads, preferred_element_type=jnp.float32)
        * decay_mat
    )
    grad_weights = (
        grad_weights.reshape(group_count, per_group, tokens_here, tokens_here)
        .sum(axis=1)
        .astype(jnp.bfloat16)
    )
    grad_c_inner = jnp.einsum(
        "gts,sgn->tgn", grad_weights, b_groups, preferred_element_type=jnp.float32
    )
    grad_b_inner = jnp.einsum(
        "gts,tgn->sgn", grad_weights, c_groups, preferred_element_type=jnp.float32
    )
    grown_grads = (grad_y * growth[:, :, None]).reshape(
        tokens_here, group_count, per_group, HEAD_DIM
    )
    grad_c_carry = jnp.einsum("tgrp,grpn->tgn", grown_grads, state_groups)
    block_state = jnp.einsum("tgrp,tgn->grpn", grown_grads, c_float).reshape(
        head_count, HEAD_DIM, STATE
    )
    x_tail = (x_float * tail_decay[:, :, None]).reshape(
        tokens_here, group_count, per_group, HEAD_DIM
    )
    local_state = jnp.einsum("sgrp,sgn->grpn", x_tail, b_float).reshape(head_count, HEAD_DIM, STATE)
    local_grad = jnp.sum(
        jnp.sum(grad_y * scan_out, axis=2) - jnp.sum(x_float * grad_x_inner, axis=2), axis=0
    )
    identity = (
        jnp.ones((head_count,), jnp.float32),
        jnp.zeros((head_count, HEAD_DIM, STATE), jnp.float32),
        jnp.zeros((head_count, HEAD_DIM, STATE), jnp.float32),
        jnp.zeros((head_count,), jnp.float32),
    )
    scanned = carried_in(
        (jnp.exp(cumulative[-1]), block_state, local_state, local_grad), SP, join_reverse, identity
    )
    later_state = scanned[1]
    later_grad = scanned[3]
    later_groups = later_state.reshape(group_count, per_group, HEAD_DIM, STATE)
    grad_x_carry = jnp.einsum("sgn,grpn->sgrp", b_float, later_groups).reshape(
        tokens_here, head_count, HEAD_DIM
    )
    grad_x = grad_x_inner + grad_x_carry * tail_decay[:, :, None]
    grad_b_carry = jnp.einsum("sgrp,grpn->sgn", x_tail, later_groups)
    grad_a = jnp.sum(grad_y * scan_out, axis=2) - jnp.sum(x_float * grad_x, axis=2)
    grad_log_decay = jnp.flip(jnp.cumsum(jnp.flip(grad_a, 0), axis=0), 0) + later_grad[None, :]
    grad_scan_in = grad_x.reshape(tokens_here, -1).astype(jnp.bfloat16)
    grad_b_proj = (grad_b_inner + grad_b_carry).reshape(tokens_here, -1).astype(jnp.bfloat16)
    grad_c_proj = (grad_c_inner + grad_c_carry).reshape(tokens_here, -1).astype(jnp.bfloat16)
    return (
        gate_wgrad[None],
        up_wgrad[None],
        down_wgrad[None],
        grad_out_proj,
        grad_scan_in,
        grad_gate_in,
        grad_b_proj,
        grad_c_proj,
        grad_log_decay,
    )


def solution(mesh):
    split = Mesh(mesh.devices.reshape(4, 4, 4, mesh.shape["tp"]), ("sp_0", "sp_1", "sp_2", "tp"))
    return jax.shard_map(
        body,
        mesh=split,
        in_specs=(
            P(SP, None),
            P(SP, None),
            P(SP, None),
            P(SP, None),
            P(SP, None, "tp"),
            P(SP, None, "tp"),
            P(SP, None, "tp"),
            P(SP, None, "tp"),
            P(SP, "tp", None),
            P("tp", None),
            P("tp"),
            P(SP, "tp"),
            P(SP, "tp"),
            P(SP, "tp"),
            P(SP, "tp"),
            P(SP, "tp"),
            P(SP, "tp", None, None),
        ),
        out_specs=(
            P(SP, None, "tp"),
            P(SP, None, "tp"),
            P(SP, "tp", None),
            P(SP, "tp"),
            P(SP, "tp"),
            P(SP, "tp"),
            P(SP, "tp"),
            P(SP, "tp"),
            P(SP, "tp"),
        ),
        check_vma=False,
    )
```

profile of v0, /device:TPU:0, one launch (start us, length us, event | category | flops | bytes accessed | tf_op | source)
XLA Modules:
  0.0 497.3 jit_solution(16533501211170878534)
XLA Ops:
  20.1 46.1 %scatter_fusion.1 = bf16[64,8,2048]{2,1,0:T(8,128)(2,1)} fusion(bf16[64,8,2048]{2,1,0:T(8,128)(2,1)} %broadcast_in_dim.29.clone, s32[256]{0:T(256)S(1)} %bitcast.593, bf16[256,2048]{1,0:T(8,128)(2,1)} %multiply_convert_fusion), kind=kCustom, calls=%fused_computation.4 | custom fusion | bytes 3147776 | tf_op jit(solution)/shard_map/scatter | solution.py:159
  67.8 46.1 %scatter_fusion = bf16[64,8,2048]{2,1,0:T(8,128)(2,1)} fusion(bf16[64,8,2048]{2,1,0:T(8,128)(2,1)} %broadcast_in_dim.29.clone.1, s32[256]{0:T(256)S(1)} %bitcast.594, bf16[256,2048]{1,0:T(8,128)(2,1)} %gather_fusion), kind=kCustom, calls=%fused_computation.3 | custom fusion | bytes 3147776 | tf_op jit(solution)/shard_map/scatter | solution.py:158
  115.8 41.5 %all_to_all.15 = bf16[64,16,1024]{2,1,0:T(8,128)(2,1)S(1)} all-to-all(bf16[64,16,1024]{2,1,0:T(8,128)(2,1)S(1)} %pad_maximum_fusion), channel_id=1, replica_groups=mesh['sp_0'=4,'sp_1'=4,'sp_2'=4,'tp'=2] {'sp_0','sp_1','sp_2'}, dimensions={0} | all-to-all | bytes 4194304 | tf_op jit(solution)/shard_map/all_to_all | solution.py:20
  161.7 10.6 %all-gather.14.cloned.1.call-done = bf16[128,8,2048]{2,1,0:T(8,128)(2,1)} async-done(((bf16[128,8,1024]{2,1,0:T(8,128)(2,1)}), bf16[128,8,2048]{2,1,0:T(8,128)(2,1)}) %all-gather.14.cloned.1.call-update) | async-done | bytes 4194320 | tf_op jit(solution)/shard_map/all_gather | solution.py:32
  180.5 8.2 %all_to_all.16 = bf16[2,512,2048]{2,1,0:T(8,128)(2,1)} all-to-all(bf16[2,512,2048]{2,1,0:T(8,128)(2,1)S(1)} %broadcast_in_dim.34), channel_id=1, replica_groups=mesh['sp_0'=4,'sp_1'=4,'sp_2'=4,'tp'=2] {'tp'}, dimensions={0} | all-to-all | bytes 8388608 | tf_op jit(solution)/shard_map/all_to_all | solution.py:41
  188.6 5.1 %reduce_sum.266 = bf16[512,2048]{1,0:T(8,128)(2,1)} reduce(bf16[2,512,2048]{2,1,0:T(8,128)(2,1)} %all_to_all.16, bf16[]{:T(256)} %constant.26.clone.1), dimensions={0}, to_apply=%region_5.6 | reduce | flops 1048576 | bytes 6291458 | tf_op jit(solution)/shard_map/reduce_sum | solution.py:45
  193.7 10.5 %all-to-all-start.2 = ((bf16[64,8,2048]{2,1,0:T(8,128)(2,1)}), bf16[64,8,2048]{2,1,0:T(8,128)(2,1)S(1)}, u32[]{:S(2)}, u32[]{:S(2)}) async-start(bf16[64,8,2048]{2,1,0:T(8,128)(2,1)} %bitcast.600), calls=%async_computation.2 | async-start | bytes 4194304 | tf_op jit(solution)/shard_map/all_to_all | solution.py:176
  221.8 21.7 %all-to-all-done.2 = bf16[64,8,2048]{2,1,0:T(8,128)(2,1)S(1)} async-done(((bf16[64,8,2048]{2,1,0:T(8,128)(2,1)}), bf16[64,8,2048]{2,1,0:T(8,128)(2,1)S(1)}, u32[]{:S(2)}, u32[]{:S(2)}) %all-to-all-start.2) | async-done | bytes 2097184 | tf_op jit(solution)/shard_map/all_to_all | solution.py:176
  243.4 5.2 %gather_fusion.2 = bf16[256,2048]{1,0:T(8,128)(2,1)} fusion(bf16[64,8,2048]{2,1,0:T(8,128)(2,1)S(1)} %all-to-all-done.2, s32[256]{0:T(256)S(1)} %bitcast.595), kind=kCustom, calls=%fused_computation.2 | custom fusion | bytes 2099200 | tf_op jit(solution)/shard_map/gather | solution.py:185
  256.4 4.5 fusion.155
  268.6 7.6 %all-gather.1 = f32[4,1,16]{2,1,0:T(1,128)S(1)} all-gather(f32[1,1,16]{2,1,0:T(1,128)S(1)} %copy-done.109), channel_id=1, replica_groups=mesh['sp_0'=4,'sp_1'=4,'sp_2'=4,'tp'=2] {'sp_2'}, dimensions={0}, use_global_device_ids=true | all-gather | bytes 320 | tf_op jit(solution)/shard_map/all_gather | solution.py:65
  281.0 14.6 %all-gather.16.cloned.1.call-done = f32[4,16,64,128]{3,2,1,0:T(8,128)} async-done(((f32[1,16,64,128]{3,2,1,0:T(8,128)}), f32[4,16,64,128]{3,2,1,0:T(8,128)}) %all-gather.16.cloned.1.call-update) | async-done | bytes 2097168 | tf_op jit(solution)/shard_map/all_gather | solution.py:65
  298.9 5.6 %fusion.99 = f32[2048,1024]{1,0:T(8,128)} fusion(f32[1024]{0:T(1024)S(1)} %convert_element_type.135, f32[128,1024]{1,0:T(8,128)S(1)} %bitcast.607, f32[128,2048]{1,0:T(8,128)S(1)} %reduce_sum.267, bf16[128,2048]{1,0:T(8,128)(2,1)S(1)} %copy-done.2, f32[128,1024]{1,0:T(8,128)S(1)} %copy-done.10, bf16[128,1024]{1,0:T(8,128)(2,1)} %param.29), kind=kOutput, calls=%fused_computation.178 | convolution fusion | flops 538836992 | bytes 11276288 | tf_op jit(solution)/shard_map/td,ti->di/dot_general | solution.py:227
  305.2 9.8 %all-gather.2 = f32[4,1,16]{2,1,0:T(1,128)S(1)} all-gather(f32[1,1,16]{2,1,0:T(1,128)S(1)} %copy-done.114), channel_id=1, replica_groups=mesh['sp_0'=4,'sp_1'=4,'sp_2'=4,'tp'=2] {'sp_1'}, dimensions={0}, use_global_device_ids=true | all-gather | bytes 320 | tf_op jit(solution)/shard_map/all_gather | solution.py:65
  315.6 12.8 %all-gather.24.cloned.1.call-done = f32[4,16,64,128]{3,2,1,0:T(8,128)} async-done(((f32[1,16,64,128]{3,2,1,0:T(8,128)}), f32[4,16,64,128]{3,2,1,0:T(8,128)}) %all-gather.24.cloned.1.call-update) | async-done | bytes 2097168 | tf_op jit(solution)/shard_map/all_gather | solution.py:65
  331.0 30.3 %all-gather.18.cloned.1.call-done = f32[4,16,64,128]{3,2,1,0:T(8,128)} async-done(((f32[1,16,64,128]{3,2,1,0:T(8,128)}), f32[4,16,64,128]{3,2,1,0:T(8,128)}) %all-gather.18.cloned.1.call-update) | async-done | bytes 2097168 | tf_op jit(solution)/shard_map/all_gather | solution.py:65
  365.5 10.2 %all-gather.3 = f32[4,1,16]{2,1,0:T(1,128)S(1)} all-gather(f32[1,1,16]{2,1,0:T(1,128)S(1)} %get-tuple-element.124), channel_id=1, replica_groups=mesh['sp_0'=4,'sp_1'=4,'sp_2'=4,'tp'=2] {'sp_0'}, dimensions={0}, use_global_device_ids=true | all-gather | bytes 320 | tf_op jit(solution)/shard_map/all_gather | solution.py:65
  381.4 4.4 fusion.2
  408.4 25.0 %all-gather.20.cloned.1.call-done = f32[4,16,64,128]{3,2,1,0:T(8,128)} async-done(((f32[1,16,64,128]{3,2,1,0:T(8,128)}), f32[4,16,64,128]{3,2,1,0:T(8,128)}) %all-gather.20.cloned.1.call-update) | async-done | bytes 2097168 | tf_op jit(solution)/shard_map/all_gather | solution.py:65
  438.7 10.5 %all-reduce = f32[64]{0:T(128)S(1)} all-reduce(f32[64]{0:T(128)S(1)} %dynamic-update-slice), channel_id=2, replica_groups=mesh['sp_0'=4,'sp_1'=4,'sp_2'=4,'tp'=2] {'sp_2'}, use_global_device_ids=true, to_apply=%add | all-reduce | flops 64 | bytes 512
  449.4 9.8 %all-gather.4 = f32[4,1,16]{2,1,0:T(1,128)S(1)} all-gather(f32[1,1,16]{2,1,0:T(1,128)S(1)} %bitcast.636), channel_id=1, replica_groups=mesh['sp_0'=4,'sp_1'=4,'sp_2'=4,'tp'=2] {'sp_1'}, dimensions={0}, use_global_device_ids=true | all-gather | bytes 320 | tf_op jit(solution)/shard_map/all_gather | solution.py:65
  459.7 5.5 %reduce-scatter.6.cloned.1.call-done = f32[128,1024]{1,0:T(8,128)} async-done(((f32[512,1024]{1,0:T(8,128)}), f32[128,1024]{1,0:T(8,128)}) %reduce-scatter.6.cloned.1.call-update) | async-done | bytes 524304 | tf_op jit(solution)/shard_map/reduce_scatter | solution.py:50
  468.8 10.0 %all-gather.5 = f32[4,1,16]{2,1,0:T(1,128)S(1)} all-gather(f32[1,1,16]{2,1,0:T(1,128)S(1)} %bitcast.637), channel_id=1, replica_groups=mesh['sp_0'=4,'sp_1'=4,'sp_2'=4,'tp'=2] {'sp_0'}, dimensions={0}, use_global_device_ids=true | all-gather | bytes 320 | tf_op jit(solution)/shard_map/all_gather | solution.py:65
  484.1 5.3 %reduce-scatter.8.cloned.1.call-done = f32[32,1024]{1,0:T(8,128)} async-done(((f32[128,1024]{1,0:T(8,128)}), f32[32,1024]{1,0:T(8,128)}) %reduce-scatter.8.cloned.1.call-update) | async-done | bytes 131088 | tf_op jit(solution)/shard_map/reduce_scatter | solution.py:50
  (397 shorter events, 118.1 us)
Async XLA Ops:
  8.0 168.5 %copy-start = (bf16[1,2048,512]{2,1,0:T(8,128)(2,1)S(1)}, bf16[1,2048,512]{2,1,0:T(8,128)(2,1)}, u32[]{:S(2)}) copy-start(bf16[1,2048,512]{2,1,0:T(8,128)(2,1)} %param.23) | copy-start | bytes 6291460
  8.0 164.3 %all-gather.14.cloned.1.call-start = ((), (), s32[]{:S(2)}) async-start(), calls=%async_computation.6 | async-start | bytes 6291456 | tf_op jit(solution)/shard_map/all_gather | solution.py:32
  193.7 49.7 %all-to-all-start.2 = ((bf16[64,8,2048]{2,1,0:T(8,128)(2,1)}), bf16[64,8,2048]{2,1,0:T(8,128)(2,1)S(1)}, u32[]{:S(2)}, u32[]{:S(2)}) async-start(bf16[64,8,2048]{2,1,0:T(8,128)(2,1)} %bitcast.600), calls=%async_computation.2 | async-start | bytes 4194304 | tf_op jit(solution)/shard_map/all_to_all | solution.py:176
  204.3 74.1 %all-gather.22.cloned.1.call-start = ((), (), s32[]{:S(2)}) async-start(), calls=%async_computation.13 | async-start | bytes 2621440 | tf_op jit(solution)/shard_map/all_gather | solution.py:65
  205.4 90.2 %all-gather.16.cloned.1.call-start = ((), (), s32[]{:S(2)}) async-start(), calls=%async_computation.10 | async-start | bytes 2621440 | tf_op jit(solution)/shard_map/all_gather | solution.py:65
  214.7 50.2 %copy-start.9 = (f32[128,1024]{1,0:T(8,128)}, f32[128,1024]{1,0:T(8,128)S(1)}, u32[]{:S(2)}) copy-start(f32[128,1024]{1,0:T(8,128)S(1)} %copy.123) | copy-start | bytes 1572868
  268.5 59.9 %all-gather.24.cloned.1.call-start = ((), (), s32[]{:S(2)}) async-start(), calls=%async_computation.14 | async-start | bytes 2621440 | tf_op jit(solution)/shard_map/all_gather | solution.py:65
  280.9 80.4 %all-gather.18.cloned.1.call-start = ((), (), s32[]{:S(2)}) async-start(), calls=%async_computation.11 | async-start | bytes 2621440 | tf_op jit(solution)/shard_map/all_gather | solution.py:65
  298.9 88.6 %reduce-scatter.4.cloned.1.call-start = ((), (), s32[]{:S(2)}) async-start(), calls=%async_computation.7 | async-start | bytes 10485760 | tf_op jit(solution)/shard_map/reduce_scatter | solution.py:50
  304.5 96.7 %all-gather.26.cloned.1.call-start = ((), (), s32[]{:S(2)}) async-start(), calls=%async_computation.15 | async-start | bytes 2621440 | tf_op jit(solution)/shard_map/all_gather | solution.py:65
  315.6 45.8 %copy-start.71 = (f32[16]{0:T(128)}, f32[16]{0:T(128)S(1)}, u32[]{:S(2)}) copy-start(f32[16]{0:T(128)S(1)} %get-tuple-element.75) | copy-start | bytes 196
  315.6 45.8 %copy-start.93 = (f32[16]{0:T(128)}, f32[16]{0:T(128)S(1)}, u32[]{:S(2)}) copy-start(f32[16]{0:T(128)S(1)} %get-tuple-element.114) | copy-start | bytes 196
  315.6 49.1 %copy-start.76 = (f32[16]{0:T(128)}, f32[16]{0:T(128)S(1)}, u32[]{:S(2)}) copy-start(f32[16]{0:T(128)S(1)} %get-tuple-element.115) | copy-start | bytes 196
  315.6 45.7 %copy-start.97 = (f32[16]{0:T(128)}, f32[16]{0:T(128)S(1)}, u32[]{:S(2)}) copy-start(f32[16]{0:T(128)S(1)} %get-tuple-element.116) | copy-start | bytes 196
  315.6 49.1 %copy-start.78 = (f32[16]{0:T(128)}, f32[16]{0:T(128)S(1)}, u32[]{:S(2)}) copy-start(f32[16]{0:T(128)S(1)} %get-tuple-element.117) | copy-start | bytes 196
  315.6 49.1 %copy-start.80 = (f32[16]{0:T(128)}, f32[16]{0:T(128)S(1)}, u32[]{:S(2)}) copy-start(f32[16]{0:T(128)S(1)} %get-tuple-element.118) | copy-start | bytes 196
  315.6 49.1 %copy-start.82 = (f32[16]{0:T(128)}, f32[16]{0:T(128)S(1)}, u32[]{:S(2)}) copy-start(f32[16]{0:T(128)S(1)} %get-tuple-element.119) | copy-start | bytes 196
  331.0 102.4 %all-gather.20.cloned.1.call-start = ((), (), s32[]{:S(2)}) async-start(), calls=%async_computation.12 | async-start | bytes 2621440 | tf_op jit(solution)/shard_map/all_gather | solution.py:65
  364.7 100.5 %reduce-scatter.6.cloned.1.call-start = ((), (), s32[]{:S(2)}) async-start(), calls=%async_computation.8 | async-start | bytes 2621440 | tf_op jit(solution)/shard_map/reduce_scatter | solution.py:50
  387.5 101.8 %reduce-scatter.8.cloned.1.call-start = ((), (), s32[]{:S(2)}) async-start(), calls=%async_computation.9 | async-start | bytes 655360 | tf_op jit(solution)/shard_map/reduce_scatter | solution.py:50
  406.0 43.3 %copy-start.84 = (f32[16]{0:T(128)}, f32[16]{0:T(128)S(1)}, u32[]{:S(2)}) copy-start(f32[16]{0:T(128)S(1)} %get-tuple-element.47) | copy-start | bytes 196
  406.0 43.3 %copy-start.86 = (f32[16]{0:T(128)}, f32[16]{0:T(128)S(1)}, u32[]{:S(2)}) copy-start(f32[16]{0:T(128)S(1)} %get-tuple-element.54) | copy-start | bytes 196
  406.0 43.3 %copy-start.88 = (f32[16]{0:T(128)}, f32[16]{0:T(128)S(1)}, u32[]{:S(2)}) copy-start(f32[16]{0:T(128)S(1)} %get-tuple-element.57) | copy-start | bytes 196
  438.4 40.5 %copy-start.115 = (f32[16]{0:T(128)S(1)}, f32[16]{0:T(128)}, u32[]{:S(2)}) copy-start(f32[16]{0:T(128)} %get-tuple-element.111) | copy-start | bytes 196
  (111 other events, 1130.5 us)
Sparse Core Ops, SparseCore 0:
  159.1 13.1 all-gather.13
  304.7 82.8 reduce-scatter.3
Sparse Core Ops, SparseCore 1:
  206.4 40.5 all-gather.21
  268.6 26.9 all-gather.15
  297.7 30.7 all-gather.23
  330.6 30.6 all-gather.17
  363.0 38.2 all-gather.25
  402.9 30.4 all-gather.19
  435.6 29.5 reduce-scatter.5
  468.0 21.2 reduce-scatter.7
where the time goes:
time: 506 us; the launch traced here: 497 us
  local copies, waits for them, and re-layouts  140 us (28%)
  waiting for transfers between devices  129 us (25%)
  blocking collectives  108 us (21%)
  other arithmetic  52.7 us (10%)
  matrix products  37.4 us (7%)
  between operations  18.3 us (4%)
  starting transfers between devices  11.5 us (2%)
    all_gather x6, waiting for transfers between devices, carried_in(): pieces = jax.tree.map(lambda part: lax.all_gather(part, axis), running)  84.5 us
    all_gather x5, blocking collectives, carried_in(): pieces = jax.tree.map(lambda part: lax.all_gather(part, axis), running)  47.5 us
    scatter x1, local copies, waits for them, and re-layouts, body(): send_grads = blank_slots.at[targets, ranked].set(grad_rows)  46.1 us
    scatter x1, local copies, waits for them, and re-layouts, body(): send_hidden = blank_slots.at[targets, ranked].set(mixer_output[token_of])  46.1 us
    all_to_all x1, blocking collectives, sent_together(): lax.all_to_all(both, axis, split_axis=split_dim, concat_axis=concat_dim,...  41.5 us
    all_to_all x1, waiting for transfers between devices, body(): lax.all_to_all(summed.astype(jnp.bfloat16).reshape(expert_count, capacity...  21.7 us
    reduce_scatter x3, waiting for transfers between devices, summed_rows(): running = lax.psum_scatter(running, axis, scatter_dimension=0, tiled=True)  12.4 us
    unnamed x261, local copies, waits for them, and re-layouts  12.4 us
  transfers between devices with their start and end apart: 11, of which 10 were waited for; matrix products, arithmetic and copies ran while one was open for 21% of the time, Pallas kernels for 0%

commit v1 on v0

v1 whole, which is shorter than its diff:
```python
import jax
import jax.numpy as jnp
from jax import lax
from jax.sharding import Mesh
from jax.sharding import PartitionSpec as P

HEAD_DIM = 64
STATE = 128
SP = ("sp_0", "sp_1", "sp_2")


rms_epsilon = 1e-05
clamp_limit = 7.0
swish_alpha = 1.702

bf16 = jnp.bfloat16
f32 = jnp.float32


def dot(a, b, dims):
    return lax.dot_general(a, b, (dims, ((), ())), preferred_element_type=f32)


def both_halves(x):
    sent = jnp.broadcast_to(x[None], (2, *x.shape))
    return lax.all_to_all(sent, "tp", 0, 0, tiled=True)


def three_parts(x):
    high = lax.reduce_precision(x, 8, 7)
    rest = x - high
    middle = lax.reduce_precision(rest, 8, 7)
    return high.astype(bf16), middle.astype(bf16), (rest - middle).astype(bf16)


def routing(expert_choice, experts, capacity):
    tokens = expert_choice.shape[0]
    hot = expert_choice[:, :, None] == jnp.arange(experts, dtype=jnp.int32)
    hot = hot.astype(f32)
    named = hot.sum(axis=1).astype(bf16)
    at = jnp.arange(tokens)
    before = (at[:, None] > at[None, :]).astype(bf16)
    earlier = dot(before, named, ((1,), (0,)))
    rank = (earlier[:, None, :] * hot).sum(axis=2).astype(jnp.int32)
    slot = expert_choice * capacity + rank
    return (slot[:, :, None] == jnp.arange(experts * capacity, dtype=jnp.int32)).astype(bf16)


def expert_side(hidden_rows, grad_rows, gate_value, up_value, gate_weight, up_weight, down_weight):
    act_grad = dot(grad_rows, down_weight, ((1,), (1,)))
    gate_full = gate_value.astype(f32)
    up_full = up_value.astype(f32)
    gate_clip = jnp.minimum(gate_full, clamp_limit)
    up_clip = jnp.clip(up_full, -clamp_limit, clamp_limit)
    sigmoid_gate = jax.nn.sigmoid(swish_alpha * gate_clip)
    swish_gate = gate_clip * sigmoid_gate
    active = ((up_clip + 1.0) * swish_gate).astype(bf16)
    up_grad = jnp.where(
        (up_full > -clamp_limit) & (up_full < clamp_limit), act_grad * swish_gate, 0.0
    ).astype(bf16)
    slope = sigmoid_gate + swish_alpha * gate_clip * sigmoid_gate * (1.0 - sigmoid_gate)
    gate_grad = jnp.where(gate_full < clamp_limit, act_grad * (up_clip + 1.0) * slope, 0.0).astype(
        bf16
    )
    down_wgrad = dot(active, grad_rows, ((0,), (0,))).astype(bf16)
    gate_wgrad = dot(hidden_rows, gate_grad, ((0,), (0,))).astype(bf16)
    up_wgrad = dot(hidden_rows, up_grad, ((0,), (0,))).astype(bf16)
    partial_rows = dot(gate_grad, gate_weight, ((1,), (1,)))
    partial_rows = partial_rows + dot(up_grad, up_weight, ((1,), (1,)))
    return (gate_wgrad, up_wgrad, down_wgrad, partial_rows)


def scan_piece(came):
    blocks = came.shape[0]
    values = came[:, :16].reshape(blocks, -1)
    local = came[:, 16:32].reshape(blocks, -1).astype(f32)
    sums = came[:, 35:38, 0].astype(f32).sum(axis=1)
    at = jnp.arange(blocks)
    after = at[None, :] > at[:, None]
    gaps = jnp.zeros((blocks, blocks), f32)
    for k in range(3):
        part = jnp.where(after, came[:, 32 + k, 0][None, :], 0).astype(bf16)
        gaps = gaps + dot(part, after.astype(bf16), ((1,), (0,)))
    weights = jnp.where(after, jnp.exp(gaps), 0.0)
    high = lax.reduce_precision(weights, 8, 7)
    low = weights - high
    later = dot(high.astype(bf16), values, ((1,), (0,))) + dot(
        low.astype(bf16), values, ((1,), (0,))
    )
    own = sums - jnp.sum(later * local, axis=1)
    carried = jnp.sum(jnp.where(after, own[None, :], 0.0), axis=1)
    return later.astype(bf16).reshape(blocks, 16, STATE), carried


def spread(parts, blocks):
    rows = jnp.stack(parts, axis=1)
    rows = jnp.pad(rows, ((0, 0), (0, 8 - len(parts))))
    return jnp.broadcast_to(rows[:, :, None], (blocks, 8, STATE)).astype(bf16)


def body(
    mixer_output,
    layer_cotangent,
    expert_choice,
    route_weight,
    gate_pre,
    up_pre,
    w_gate,
    w_up,
    w_down,
    w_out,
    norm_gain,
    scan_in,
    gate_in,
    b_proj,
    c_proj,
    log_decay,
    entry_state,
):
    experts = lax.axis_size(SP)
    tokens, width = mixer_output.shape
    capacity = gate_pre.shape[1] // experts
    half = width // 2
    start = lax.axis_index("tp") * half

    places = routing(expert_choice, experts, capacity)
    hidden_half = lax.dynamic_slice_in_dim(mixer_output, start, half, 1)
    cotangent_half = lax.dynamic_slice_in_dim(layer_cotangent, start, half, 1)
    weighted = (route_weight[:, :, None] * cotangent_half.astype(f32)[:, None, :]).astype(bf16)
    either = places[:, 0] + places[:, 1]
    send_grads = (
        dot(places[:, 0], weighted[:, 0], ((0,), (0,)))
        + dot(places[:, 1], weighted[:, 1], ((0,), (0,)))
    ).astype(bf16)
    send_hidden = dot(either, hidden_half, ((0,), (0,))).astype(bf16)
    send_grads = send_grads.reshape(experts, capacity, half)
    send_hidden = send_hidden.reshape(experts, capacity, half)
    came_grads = lax.all_to_all(send_grads, SP, 0, 0, tiled=True)
    came_hidden = lax.all_to_all(send_hidden, SP, 0, 0, tiled=True)

    def whole(x):
        x = both_halves(x.reshape(-1, half))
        return jnp.concatenate([x[0], x[1]], axis=1)

    gate_wgrad, up_wgrad, down_wgrad, partial_rows = expert_side(
        whole(came_hidden),
        whole(came_grads),
        gate_pre[0],
        up_pre[0],
        w_gate[0],
        w_up[0],
        w_down[0],
    )
    partial_rows = partial_rows.astype(bf16)
    split_rows = jnp.stack([partial_rows[:, :half], partial_rows[:, half:]])
    split_rows = lax.all_to_all(split_rows, "tp", 0, 0, tiled=True)
    summed = (split_rows[0].astype(f32) + split_rows[1].astype(f32)).astype(bf16)
    returned = lax.all_to_all(summed.reshape(experts, capacity, half), SP, 0, 0, tiled=True)
    moe_terms = dot(either, returned.reshape(-1, half), ((1,), (0,)))
    grad_half = (cotangent_half.astype(f32) + moe_terms).astype(bf16)
    grad_halves = both_halves(grad_half)
    grad_hidden = jnp.concatenate([grad_halves[0], grad_halves[1]], axis=1)

    head_count = log_decay.shape[1]
    group_count = b_proj.shape[1] // STATE
    per_group = head_count // group_count
    scan_heads = scan_in.reshape(tokens, head_count, HEAD_DIM)
    b_groups = b_proj.reshape(tokens, group_count, STATE)
    c_groups = c_proj.reshape(tokens, group_count, STATE)
    x_float = scan_heads.astype(f32)
    b_float = b_groups.astype(f32)
    c_float = c_groups.astype(f32)
    cumulative = jnp.cumsum(log_decay, axis=0)
    growth = jnp.exp(cumulative)
    tail_decay = jnp.exp(cumulative[-1][None, :] - cumulative)
    locations = jnp.arange(tokens)
    causal = locations[:, None] >= locations[None, :]
    log_gaps = cumulative.T[:, :, None] - cumulative.T[:, None, :]
    decay_mat = jnp.exp(jnp.where(causal[None], log_gaps, -jnp.inf))
    inner_prod = jnp.einsum("tgn,sgn->gts", c_groups, b_groups, preferred_element_type=f32)
    mix_weights = (jnp.repeat(inner_prod, per_group, axis=0) * decay_mat).astype(bf16)
    state_groups = entry_state.reshape(group_count, per_group, HEAD_DIM, STATE)
    y_inner = jnp.einsum("hts,shp->thp", mix_weights, scan_heads, preferred_element_type=f32)
    y_carry = jnp.einsum("tgn,grpn->tgrp", c_float, state_groups).reshape(
        tokens, head_count, HEAD_DIM
    )
    scan_out = y_inner + y_carry * growth[:, :, None]
    gate_float = gate_in.astype(f32)
    gate_sig = jax.nn.sigmoid(gate_float)
    gate_silu = gate_float * gate_sig
    gated = scan_out.reshape(tokens, -1) * gate_silu
    grouped = gated.reshape(tokens, group_count, -1)
    inv_rms = lax.rsqrt(jnp.mean(grouped * grouped, axis=-1, keepdims=True) + rms_epsilon)
    unit = grouped * inv_rms
    gain_groups = norm_gain.astype(f32).reshape(group_count, -1)
    mixed = (unit * gain_groups).reshape(tokens, -1).astype(bf16)
    x_tail = (x_float * tail_decay[:, :, None]).reshape(tokens, group_count, per_group, HEAD_DIM)
    local_state = jnp.einsum("sgrp,sgn->grpn", x_tail, b_float)

    line = lax.axis_size("sp_0")
    mixed_line = lax.all_to_all(
        jnp.broadcast_to(mixed[None], (line, *mixed.shape)), "sp_0", 0, 0, tiled=True
    )
    grads_line = lax.all_to_all(
        grad_hidden.reshape(tokens, line, -1).transpose(1, 0, 2), "sp_0", 0, 0, tiled=True
    )
    product = dot(
        grads_line.reshape(line * tokens, -1), mixed_line.reshape(line * tokens, -1), ((0,), (0,))
    ).astype(bf16)
    product = product.reshape(experts // line, -1, product.shape[1])
    grad_out_proj = (
        lax.all_to_all(product, ("sp_1", "sp_2"), 0, 0, tiled=True).astype(f32).sum(axis=0)
    )

    grad_mixed = jnp.einsum("td,id->ti", grad_hidden, w_out, preferred_element_type=f32)
    grad_unit = grad_mixed.reshape(tokens, group_count, -1) * gain_groups
    grad_grouped = inv_rms * (grad_unit - unit * jnp.mean(grad_unit * unit, axis=-1, keepdims=True))
    grad_gated = grad_grouped.reshape(tokens, -1)
    grad_gate_in = (
        grad_gated
        * scan_out.reshape(tokens, -1)
        * gate_sig
        * (1.0 + gate_float * (1.0 - gate_sig))
    ).astype(bf16)
    grad_y = (grad_gated * gate_silu).reshape(tokens, head_count, HEAD_DIM)
    grad_y_b = grad_y.astype(bf16)
    grad_x_inner = jnp.einsum("hts,thp->shp", mix_weights, grad_y_b, preferred_element_type=f32)
    grad_weights = (
        jnp.einsum("thp,shp->hts", grad_y_b, scan_heads, preferred_element_type=f32) * decay_mat
    )
    grad_weights = (
        grad_weights.reshape(group_count, per_group, tokens, tokens).sum(axis=1).astype(bf16)
    )
    grad_c_inner = jnp.einsum("gts,sgn->tgn", grad_weights, b_groups, preferred_element_type=f32)
    grad_b_inner = jnp.einsum("gts,tgn->sgn", grad_weights, c_groups, preferred_element_type=f32)
    grown_grads = (grad_y * growth[:, :, None]).reshape(tokens, group_count, per_group, HEAD_DIM)
    grad_c_carry = jnp.einsum("tgrp,grpn->tgn", grown_grads, state_groups)
    block_state = jnp.einsum("tgrp,tgn->grpn", grown_grads, c_float)
    y_dots = jnp.sum(grad_y * scan_out, axis=2)
    local_grad = jnp.sum(y_dots - jnp.sum(x_float * grad_x_inner, axis=2), axis=0)

    pieces = experts // head_count
    first = (jnp.arange(experts) % pieces == 0).astype(f32)
    scalars = [jnp.repeat(part, pieces) for part in three_parts(cumulative[-1])] + list(
        three_parts(jnp.repeat(local_grad, pieces) * first)
    )
    sent = jnp.concatenate(
        [
            block_state.astype(bf16).reshape(experts, -1, STATE),
            local_state.astype(bf16).reshape(experts, -1, STATE),
            spread(scalars, experts),
        ],
        axis=1,
    )
    later, carried = scan_piece(lax.all_to_all(sent, SP, 0, 0, tiled=True))
    back = jnp.concatenate([later, spread(list(three_parts(carried)), experts)], axis=1)
    back = lax.all_to_all(back, SP, 0, 0, tiled=True)
    later_groups = back[:, :16].reshape(group_count, per_group, HEAD_DIM, STATE).astype(f32)
    later_grad = back[:, 16:19, 0].astype(f32).sum(axis=1).reshape(head_count, pieces).sum(axis=1)

    grad_x_carry = jnp.einsum("sgn,grpn->sgrp", b_float, later_groups).reshape(
        tokens, head_count, HEAD_DIM
    )
    grad_x = grad_x_inner + grad_x_carry * tail_decay[:, :, None]
    grad_b_carry = jnp.einsum("sgrp,grpn->sgn", x_tail, later_groups)
    grad_a = y_dots - jnp.sum(x_float * grad_x, axis=2)
    grad_log_decay = jnp.flip(jnp.cumsum(jnp.flip(grad_a, 0), axis=0), 0) + later_grad[None, :]
    grad_scan_in = grad_x.reshape(tokens, -1).astype(bf16)
    grad_b_proj = (grad_b_inner + grad_b_carry).reshape(tokens, -1).astype(bf16)
    grad_c_proj = (grad_c_inner + grad_c_carry).reshape(tokens, -1).astype(bf16)
    return (
        gate_wgrad[None],
        up_wgrad[None],
        down_wgrad[None],
        grad_out_proj,
        grad_scan_in,
        grad_gate_in,
        grad_b_proj,
        grad_c_proj,
        grad_log_decay,
    )


def solution(mesh):
    split = Mesh(mesh.devices.reshape(4, 4, 4, mesh.shape["tp"]), ("sp_0", "sp_1", "sp_2", "tp"))
    return jax.shard_map(
        body,
        mesh=split,
        in_specs=(
            P(SP, None),
            P(SP, None),
            P(SP, None),
            P(SP, None),
            P(SP, None, "tp"),
            P(SP, None, "tp"),
            P(SP, None, "tp"),
            P(SP, None, "tp"),
            P(SP, "tp", None),
            P("tp", None),
            P("tp"),
            P(SP, "tp"),
            P(SP, "tp"),
            P(SP, "tp"),
            P(SP, "tp"),
            P(SP, "tp"),
            P(SP, "tp", None, None),
        ),
        out_specs=(
            P(SP, None, "tp"),
            P(SP, None, "tp"),
            P(SP, "tp", None),
            P(SP, "tp"),
            P(SP, "tp"),
            P(SP, "tp"),
            P(SP, "tp"),
            P(SP, "tp"),
            P(SP, "tp"),
        ),
        check_vma=False,
    )
```

time: 506 us -> 234 us (0.46); the launches traced: 497 us -> 232 us
  local copies, waits for them, and re-layouts: 140 us -> 40.6 us
  blocking collectives: 108 us -> 15 us
  waiting for transfers between devices: 129 us -> 54.1 us
  starting transfers between devices: 11.5 us -> 53.6 us
  other arithmetic: 52.7 us -> 30.5 us
  between operations: 18.3 us -> 1.6 us
    all_gather x7 -> x0, waiting for transfers between devices: 95.1 us -> none  [the longest x6 84.5 us: carried_in(): pieces = jax.tree.map(lambda part: lax.all_gather(part, axis), running)]
    scatter x2 -> x0, local copies, waits for them, and re-layouts: 92.2 us -> none  [the longest x1 46.1 us: body(): send_grads = blank_slots.at[targets, ranked].set(grad_rows)]
    all_gather x5 -> x0, blocking collectives: 47.5 us -> none  [carried_in(): pieces = jax.tree.map(lambda part: lax.all_gather(part, axis), running)]
    all_to_all x1 -> x9, starting transfers between devices: 10.5 us -> 53.6 us  [the longest x1 11.9 us: body(): came_grads = lax.all_to_all(send_grads, SP, 0, 0, tiled=True)]
    all_to_all x2 -> x3, blocking collectives: 49.6 us -> 15 us  [the longest x2 9.57 us: both_halves(): return lax.all_to_all(sent, 'tp', 0, 0, tiled=True)]
    all_to_all x1 -> x9, waiting for transfers between devices: 21.7 us -> 54.1 us  [the longest x1 11.2 us: body(): lax.all_to_all(summed.reshape(experts, capacity, half), SP, 0, 0, tiled=T...]
    reduce_sum x10, other arithmetic: 21.1 us -> 7.88 us  [the longest x2 2.61 us: body(): back[:, 16:19, 0].astype(f32).sum(axis=1).reshape(head_count, pieces)]
    reduce_scatter x3 -> x0, waiting for transfers between devices: 12.4 us -> none  [summed_rows(): running = lax.psum_scatter(running, axis, scatter_dimension=0, tiled=True)]
  transfers between devices with their start and end apart: 11 -> 9, of which waited for: 10 -> 7; matrix products, arithmetic and copies ran while one was open for 21% -> 31% of each run, Pallas kernels for 0% -> 0%
where the time goes in v1:
time: 234 us; the launch traced here: 232 us
  waiting for transfers between devices  54.1 us (23%)
  starting transfers between devices  53.6 us (23%)
  local copies, waits for them, and re-layouts  40.6 us (17%)
  matrix products  36.2 us (15%)
  other arithmetic  30.5 us (13%)
  blocking collectives  15 us (6%)
    dot_general x17, matrix products, dot(): return lax.dot_general(a, b, (dims, ((), ())), preferred_element_type=f32)  23.3 us
    unnamed x123, local copies, waits for them, and re-layouts  12.9 us
    all_to_all x1, starting transfers between devices, body(): came_grads = lax.all_to_all(send_grads, SP, 0, 0, tiled=True)  11.9 us
    all_to_all x1, waiting for transfers between devices, body(): lax.all_to_all(summed.reshape(experts, capacity, half), SP, 0, 0, tiled=T...  11.2 us
    all_to_all x1, waiting for transfers between devices, body(): lax.all_to_all(jnp.broadcast_to(mixed[None], (line, *mixed.shape)), 'sp_0...  11 us
    all_to_all x1, starting transfers between devices, body(): came_hidden = lax.all_to_all(send_hidden, SP, 0, 0, tiled=True)  10.7 us
    all_to_all x2, blocking collectives, both_halves(): return lax.all_to_all(sent, 'tp', 0, 0, tiled=True)  9.57 us
    all_to_all x1, waiting for transfers between devices, body(): later, carried = scan_piece(lax.all_to_all(sent, SP, 0, 0, tiled=True))  9.36 us
  transfers between devices with their start and end apart: 9, of which 7 were waited for; matrix products, arithmetic and copies ran while one was open for 31% of the time, Pallas kernels for 0%

profile of v1, /device:TPU:0, one launch (start us, length us, event | category | flops | bytes accessed | tf_op | source)
XLA Modules:
  0.0 231.5 jit_solution(15394692011324801718)
XLA Ops:
  7.7 11.9 %all-to-all-start.2 = ((bf16[64,8,1024]{2,1,0:T(8,128)(2,1)}), bf16[64,8,1024]{2,1,0:T(8,128)(2,1)}, u32[]{:S(2)}, u32[]{:S(2)}) async-start(bf16[64,8,1024]{2,1,0:T(8,128)(2,1)} %fusion.9), calls=%async_computation.2 | async-start | bytes 2097152 | tf_op jit(solution)/shard_map/all_to_all | solution.py:138
  41.5 5.4 %all_to_all.60 = bf16[2,512,1024]{2,1,0:T(8,128)(2,1)S(1)} all-to-all(bf16[2,512,1024]{2,1,0:T(8,128)(2,1)S(1)} %broadcast_in_dim.150), channel_id=1, replica_groups=mesh['sp_0'=4,'sp_1'=4,'sp_2'=4,'tp'=2] {'tp'}, dimensions={0} | all-to-all | bytes 4194304 | tf_op jit(solution)/shard_map/all_to_all | solution.py:26
  55.0 5.4 %all_to_all.61 = bf16[2,512,1024]{2,1,0:T(8,128)(2,1)S(1)} all-to-all(bf16[2,512,1024]{2,1,0:T(8,128)(2,1)S(1)} %pad_maximum_fusion.2), channel_id=1, replica_groups=mesh['sp_0'=4,'sp_1'=4,'sp_2'=4,'tp'=2] {'tp'}, dimensions={0} | all-to-all | bytes 4194304 | tf_op jit(solution)/shard_map/all_to_all | solution.py:156
  60.5 10.7 %all-to-all-start = ((bf16[64,8,1024]{2,1,0:T(8,128)(2,1)}), bf16[64,8,1024]{2,1,0:T(8,128)(2,1)}, u32[]{:S(2)}, u32[]{:S(2)}) async-start(bf16[64,8,1024]{2,1,0:T(8,128)(2,1)} %fusion.8), calls=%async_computation | async-start | bytes 2097152 | tf_op jit(solution)/shard_map/all_to_all | solution.py:139
  83.6 6.6 %all-to-all-done = bf16[64,8,1024]{2,1,0:T(8,128)(2,1)} async-done(((bf16[64,8,1024]{2,1,0:T(8,128)(2,1)}), bf16[64,8,1024]{2,1,0:T(8,128)(2,1)}, u32[]{:S(2)}, u32[]{:S(2)}) %all-to-all-start) | async-done | bytes 1048608 | tf_op jit(solution)/shard_map/all_to_all | solution.py:139
  90.2 2.8 %broadcast_in_dim.148 = bf16[2,512,1024]{2,1,0:T(8,128)(2,1)} broadcast(bf16[512,1024]{1,0:T(8,128)(2,1)} %bitcast.2), dimensions={1,2} | broadcast | bytes 3145728 | tf_op jit(solution)/shard_map/broadcast_in_dim | solution.py:25
  93.0 5.0 %all-to-all-start.1 = ((bf16[2,512,1024]{2,1,0:T(8,128)(2,1)}), bf16[2,512,1024]{2,1,0:T(8,128)(2,1)}, u32[]{:S(2)}, u32[]{:S(2)}) async-start(bf16[2,512,1024]{2,1,0:T(8,128)(2,1)} %broadcast_in_dim.148), calls=%async_computation.1 | async-start | bytes 4194304 | tf_op jit(solution)/shard_map/all_to_all | solution.py:26
  100.8 4.7 %all-to-all-start.5 = ((bf16[64,8,1024]{2,1,0:T(8,128)(2,1)}), bf16[64,8,1024]{2,1,0:T(8,128)(2,1)S(1)}, u32[]{:S(2)}, u32[]{:S(2)}) async-start(bf16[64,8,1024]{2,1,0:T(8,128)(2,1)} %fusion.35), calls=%async_computation.5 | async-start | bytes 2097152 | tf_op jit(solution)/shard_map/all_to_all | solution.py:158
  108.0 2.9 %fusion.2 = bf16[1,512,2048]{2,1,0:T(8,128)(2,1)} fusion(bf16[512,1024]{1,0:T(8,128)(2,1)S(1)} %copy-done.24, bf16[512,1024]{1,0:T(8,128)(2,1)S(1)} %copy-done.22, bf16[1,512,512]{2,1,0:T(8,128)(2,1)S(1)} %copy-done.53, bf16[1,512,512]{2,1,0:T(8,128)(2,1)S(1)} %copy-done.51), kind=kOutput, calls=%fused_computation.6 | convolution fusion | flops 1082130432 | bytes 5242880 | tf_op jit(solution)/shard_map/dot_general | solution.py:21
  110.9 2.9 %fusion = bf16[1,2048,512]{2,1,0:T(8,128)(2,1)} fusion(bf16[512,1024]{1,0:T(8,128)(2,1)S(1)} %get-tuple-element.66, bf16[512,1024]{1,0:T(8,128)(2,1)S(1)} %get-tuple-element.65, bf16[1,512,512]{2,1,0:T(8,128)(2,1)S(1)} %copy-done.51, f32[512,512]{1,0:T(8,128)S(1)} %copy-done.55, bf16[1,512,512]{2,1,0:T(8,128)(2,1)S(1)} %copy-done.53), kind=kOutput, calls=%fused_computation.4 | convolution fusion | flops 1083703296 | bytes 6291456 | tf_op jit(solution)/shard_map/dot_general | solution.py:21
  113.9 11.2 %all-to-all-done.5 = bf16[64,8,1024]{2,1,0:T(8,128)(2,1)S(1)} async-done(((bf16[64,8,1024]{2,1,0:T(8,128)(2,1)}), bf16[64,8,1024]{2,1,0:T(8,128)(2,1)S(1)}, u32[]{:S(2)}, u32[]{:S(2)}) %all-to-all-start.5) | async-done | bytes 1048608 | tf_op jit(solution)/shard_map/all_to_all | solution.py:158
  125.5 4.2 %all_to_all.62 = bf16[2,128,1024]{1,2,0:T(8,128)(2,1)S(1)} all-to-all(bf16[2,128,1024]{1,2,0:T(8,128)(2,1)S(1)} %broadcast_in_dim.155), channel_id=1, replica_groups=mesh['sp_0'=4,'sp_1'=4,'sp_2'=4,'tp'=2] {'tp'}, dimensions={0} | all-to-all | bytes 1048576 | tf_op jit(solution)/shard_map/all_to_all | solution.py:26
  130.6 3.8 %fusion.51 = f32[128,1024]{1,0:T(8,128)S(1)} fusion(bf16[1024,2048]{1,0:T(8,128)(2,1)} %param.26, bf16[128,1024]{0,1:T(8,128)(2,1)S(1)} %get-tuple-element.75, bf16[128,1024]{0,1:T(8,128)(2,1)S(1)} %get-tuple-element.74), kind=kOutput, calls=%fused_computation.99 | convolution fusion | flops 537919488 | bytes 5242880 | tf_op jit(solution)/shard_map/td,id->ti/dot_general | solution.py:215
  140.7 4.8 %all-to-all-start.10 = ((bf16[64,40,128]{2,1,0:T(8,128)(2,1)}), bf16[64,40,128]{2,1,0:T(8,128)(2,1)S(1)}, u32[]{:S(2)}, u32[]{:S(2)}) async-start(bf16[64,40,128]{2,1,0:T(8,128)(2,1)} %pad_maximum_fusion.7), calls=%async_computation.10 | async-start | bytes 1310720 | tf_op jit(solution)/shard_map/all_to_all | solution.py:255
  145.5 4.1 %fusion.1 = bf16[1,2048,512]{2,1,0:T(8,128)(2,1)} fusion(bf16[512,512]{1,0:T(8,128)(2,1)} %copy-done.30, bf16[512,1024]{1,0:T(8,128)(2,1)} %copy-done.20, bf16[512,1024]{1,0:T(8,128)(2,1)S(1)} %copy-done.19), kind=kOutput, calls=%fused_computation.5 | convolution fusion | flops 1078984704 | bytes 4718592 | tf_op jit(solution)/shard_map/dot_general | solution.py:21
  151.3 9.4 %all-to-all-done.10 = bf16[64,40,128]{2,1,0:T(8,128)(2,1)S(1)} async-done(((bf16[64,40,128]{2,1,0:T(8,128)(2,1)}), bf16[64,40,128]{2,1,0:T(8,128)(2,1)S(1)}, u32[]{:S(2)}, u32[]{:S(2)}) %all-to-all-start.10) | async-done | bytes 655392 | tf_op jit(solution)/shard_map/all_to_all | solution.py:255
  160.6 3.7 %all-to-all-start.7 = ((bf16[4,128,512]{1,2,0:T(8,128)(2,1)}), bf16[4,128,512]{1,2,0:T(8,128)(2,1)S(1)}, u32[]{:S(2)}, u32[]{:S(2)}) async-start(bf16[4,128,512]{1,2,0:T(8,128)(2,1)} %maximum_bitcast_fusion), calls=%async_computation.7 | async-start | bytes 1048576 | tf_op jit(solution)/shard_map/all_to_all | solution.py:204
  165.6 7.2 %all-to-all-done.7 = bf16[4,128,512]{1,2,0:T(8,128)(2,1)S(1)} async-done(((bf16[4,128,512]{1,2,0:T(8,128)(2,1)}), bf16[4,128,512]{1,2,0:T(8,128)(2,1)S(1)}, u32[]{:S(2)}, u32[]{:S(2)}) %all-to-all-start.7) | async-done | bytes 524320 | tf_op jit(solution)/shard_map/all_to_all | solution.py:204
  173.9 4.3 %all-to-all-start.8 = ((bf16[4,128,1024]{2,1,0:T(8,128)(2,1)}), bf16[4,128,1024]{2,1,0:T(8,128)(2,1)}, u32[]{:S(2)}, u32[]{:S(2)}) async-start(bf16[4,128,1024]{2,1,0:T(8,128)(2,1)} %broadcast_in_dim.159), calls=%async_computation.8 | async-start | bytes 2097152 | tf_op jit(solution)/shard_map/all_to_all | solution.py:201
  180.4 11.0 %all-to-all-done.8 = bf16[4,128,1024]{2,1,0:T(8,128)(2,1)} async-done(((bf16[4,128,1024]{2,1,0:T(8,128)(2,1)}), bf16[4,128,1024]{2,1,0:T(8,128)(2,1)}, u32[]{:S(2)}, u32[]{:S(2)}) %all-to-all-start.8) | async-done | bytes 1048608 | tf_op jit(solution)/shard_map/all_to_all | solution.py:201
  191.4 4.9 %all-to-all-start.11 = ((bf16[64,24,128]{2,1,0:T(8,128)(2,1)}), bf16[64,24,128]{2,1,0:T(8,128)(2,1)S(1)}, u32[]{:S(2)}, u32[]{:S(2)}) async-start(bf16[64,24,128]{2,1,0:T(8,128)(2,1)} %pad_maximum_fusion.8), calls=%async_computation.11 | async-start | bytes 786432 | tf_op jit(solution)/shard_map/all_to_all | solution.py:257
  197.3 3.0 %bitcast_convert_fusion = bf16[512,1024]{1,0:T(8,128)(2,1)} fusion(bf16[4,128,512]{1,2,0:T(8,128)(2,1)S(1)} %all-to-all-done.7, bf16[4,128,1024]{2,1,0:T(8,128)(2,1)} %all-to-all-done.8), kind=kOutput, calls=%fused_computation.11 | convolution fusion | flops 537395200 | bytes 2621440 | tf_op jit(solution)/shard_map/dot_general | solution.py:21
  200.3 7.3 %all-to-all-done.11 = bf16[64,24,128]{2,1,0:T(8,128)(2,1)S(1)} async-done(((bf16[64,24,128]{2,1,0:T(8,128)(2,1)}), bf16[64,24,128]{2,1,0:T(8,128)(2,1)S(1)}, u32[]{:S(2)}, u32[]{:S(2)}) %all-to-all-start.11) | async-done | bytes 393248 | tf_op jit(solution)/shard_map/all_to_all | solution.py:257
  207.6 3.7 %all-to-all-start.9 = ((bf16[16,32,1024]{2,1,0:T(8,128)(2,1)}), bf16[16,32,1024]{2,1,0:T(8,128)(2,1)S(1)}, u32[]{:S(2)}, u32[]{:S(2)}) async-start(bf16[16,32,1024]{2,1,0:T(8,128)(2,1)} %bitcast.40), calls=%async_computation.9 | async-start | bytes 2097152 | tf_op jit(solution)/shard_map/all_to_all | solution.py:212
  (237 shorter events, 89.3 us)
Async XLA Ops:
  0.6 50.6 %copy-start = (bf16[1,2048,512]{2,1,0:T(8,128)(2,1)S(1)}, bf16[1,2048,512]{2,1,0:T(8,128)(2,1)}, u32[]{:S(2)}) copy-start(bf16[1,2048,512]{2,1,0:T(8,128)(2,1)} %param.23) | copy-start | bytes 6291460
  6.2 13.4 %copy-start.44 = (f32[128,16]{0,1:T(8,128)S(1)}, f32[128,16]{0,1:T(8,128)}, u32[]{:S(2)}) copy-start(f32[128,16]{0,1:T(8,128)} %param.32) | copy-start | bytes 24580
  6.2 14.3 %copy-start.33 = (bf16[128,512]{1,0:T(8,128)(2,1)S(1)}, bf16[128,512]{1,0:T(8,128)(2,1)}, u32[]{:S(2)}) copy-start(bf16[128,512]{1,0:T(8,128)(2,1)} %param.31) | copy-start | bytes 393220
  7.7 13.0 %copy-start.34 = (bf16[128,512]{1,0:T(8,128)(2,1)S(1)}, bf16[128,512]{1,0:T(8,128)(2,1)}, u32[]{:S(2)}) copy-start(bf16[128,512]{1,0:T(8,128)(2,1)} %param.30) | copy-start | bytes 393220
  7.7 13.8 %copy-start.6 = (f32[1,16,64,128]{3,2,1,0:T(8,128)S(1)}, f32[1,16,64,128]{3,2,1,0:T(8,128)}, u32[]{:S(2)}) copy-start(f32[1,16,64,128]{3,2,1,0:T(8,128)} %param.33) | copy-start | bytes 1572868
  7.7 32.3 %all-to-all-start.2 = ((bf16[64,8,1024]{2,1,0:T(8,128)(2,1)}), bf16[64,8,1024]{2,1,0:T(8,128)(2,1)}, u32[]{:S(2)}, u32[]{:S(2)}) async-start(bf16[64,8,1024]{2,1,0:T(8,128)(2,1)} %fusion.9), calls=%async_computation.2 | async-start | bytes 2097152 | tf_op jit(solution)/shard_map/all_to_all | solution.py:138
  60.5 20.0 %copy-start.41 = (f32[128,16]{0,1:T(8,128)S(1)}, f32[128,16]{0,1:T(8,128)}, u32[]{:S(2)}) copy-start(f32[128,16]{0,1:T(8,128)} %copy.163) | copy-start | bytes 24580
  60.5 29.7 %all-to-all-start = ((bf16[64,8,1024]{2,1,0:T(8,128)(2,1)}), bf16[64,8,1024]{2,1,0:T(8,128)(2,1)}, u32[]{:S(2)}, u32[]{:S(2)}) async-start(bf16[64,8,1024]{2,1,0:T(8,128)(2,1)} %fusion.8), calls=%async_computation | async-start | bytes 2097152 | tf_op jit(solution)/shard_map/all_to_all | solution.py:139
  93.0 7.8 %all-to-all-start.1 = ((bf16[2,512,1024]{2,1,0:T(8,128)(2,1)}), bf16[2,512,1024]{2,1,0:T(8,128)(2,1)}, u32[]{:S(2)}, u32[]{:S(2)}) async-start(bf16[2,512,1024]{2,1,0:T(8,128)(2,1)} %broadcast_in_dim.148), calls=%async_computation.1 | async-start | bytes 4194304 | tf_op jit(solution)/shard_map/all_to_all | solution.py:26
  100.8 24.2 %all-to-all-start.5 = ((bf16[64,8,1024]{2,1,0:T(8,128)(2,1)}), bf16[64,8,1024]{2,1,0:T(8,128)(2,1)S(1)}, u32[]{:S(2)}, u32[]{:S(2)}) async-start(bf16[64,8,1024]{2,1,0:T(8,128)(2,1)} %fusion.35), calls=%async_computation.5 | async-start | bytes 2097152 | tf_op jit(solution)/shard_map/all_to_all | solution.py:158
  110.9 14.1 %copy-start.17 = (bf16[128,2,512]{2,0,1:T(8,128)(2,1)S(1)}, bf16[128,2,512]{2,0,1:T(8,128)(2,1)}, u32[]{:S(2)}) copy-start(bf16[128,2,512]{2,0,1:T(8,128)(2,1)} %get-tuple-element.88) | copy-start | bytes 786436
  110.9 14.1 %copy-start.32 = (bf16[128,2048]{1,0:T(8,128)(2,1)S(1)}, bf16[128,2048]{1,0:T(8,128)(2,1)}, u32[]{:S(2)}) copy-start(bf16[128,2048]{1,0:T(8,128)(2,1)} %param.18) | copy-start | bytes 1572868
  140.7 20.0 %all-to-all-start.10 = ((bf16[64,40,128]{2,1,0:T(8,128)(2,1)}), bf16[64,40,128]{2,1,0:T(8,128)(2,1)S(1)}, u32[]{:S(2)}, u32[]{:S(2)}) async-start(bf16[64,40,128]{2,1,0:T(8,128)(2,1)} %pad_maximum_fusion.7), calls=%async_computation.10 | async-start | bytes 1310720 | tf_op jit(solution)/shard_map/all_to_all | solution.py:255
  151.3 45.1 %copy-start.31 = (bf16[4,128,128]{2,1,0:T(8,128)(2,1)}, bf16[4,128,128]{2,1,0:T(8,128)(2,1)S(1)}, u32[]{:S(2)}) copy-start(bf16[4,128,128]{2,1,0:T(8,128)(2,1)S(1)} %bitcast_reduce_fusion) | copy-start | bytes 393220
  151.3 21.5 %copy-start.26 = (bf16[128,1024]{1,0:T(8,128)(2,1)S(1)}, bf16[128,1024]{1,0:T(8,128)(2,1)}, u32[]{:S(2)}) copy-start(bf16[128,1024]{1,0:T(8,128)(2,1)} %get-tuple-element.67) | copy-start | bytes 786436
  160.6 12.2 %all-to-all-start.7 = ((bf16[4,128,512]{1,2,0:T(8,128)(2,1)}), bf16[4,128,512]{1,2,0:T(8,128)(2,1)S(1)}, u32[]{:S(2)}, u32[]{:S(2)}) async-start(bf16[4,128,512]{1,2,0:T(8,128)(2,1)} %maximum_bitcast_fusion), calls=%async_computation.7 | async-start | bytes 1048576 | tf_op jit(solution)/shard_map/all_to_all | solution.py:204
  173.9 17.5 %all-to-all-start.8 = ((bf16[4,128,1024]{2,1,0:T(8,128)(2,1)}), bf16[4,128,1024]{2,1,0:T(8,128)(2,1)}, u32[]{:S(2)}, u32[]{:S(2)}) async-start(bf16[4,128,1024]{2,1,0:T(8,128)(2,1)} %broadcast_in_dim.159), calls=%async_computation.8 | async-start | bytes 2097152 | tf_op jit(solution)/shard_map/all_to_all | solution.py:201
  178.2 18.2 %copy-start.14 = (bf16[128,4,128]{0,2,1:T(8,128)(2,1)S(1)}, bf16[128,4,128]{0,2,1:T(8,128)(2,1)}, u32[]{:S(2)}) copy-start(bf16[128,4,128]{0,2,1:T(8,128)(2,1)} %copy.173) | copy-start | bytes 393220
  191.4 16.2 %all-to-all-start.11 = ((bf16[64,24,128]{2,1,0:T(8,128)(2,1)}), bf16[64,24,128]{2,1,0:T(8,128)(2,1)S(1)}, u32[]{:S(2)}, u32[]{:S(2)}) async-start(bf16[64,24,128]{2,1,0:T(8,128)(2,1)} %pad_maximum_fusion.8), calls=%async_computation.11 | async-start | bytes 786432 | tf_op jit(solution)/shard_map/all_to_all | solution.py:257
  197.3 14.7 %copy-start.9 = (bf16[128,4,128]{2,1,0:T(4,128)(2,1)S(1)}, bf16[128,4,128]{2,1,0:T(4,128)(2,1)}, u32[]{:S(2)}) copy-start(bf16[128,4,128]{2,1,0:T(4,128)(2,1)} %copy-done.8) | copy-start | bytes 393220
  207.6 23.1 %all-to-all-start.9 = ((bf16[16,32,1024]{2,1,0:T(8,128)(2,1)}), bf16[16,32,1024]{2,1,0:T(8,128)(2,1)S(1)}, u32[]{:S(2)}, u32[]{:S(2)}) async-start(bf16[16,32,1024]{2,1,0:T(8,128)(2,1)} %bitcast.40), calls=%async_computation.9 | async-start | bytes 2097152 | tf_op jit(solution)/shard_map/all_to_all | solution.py:212
  211.3 14.5 %copy-start.38 = (f32[128,4,4]{0,2,1:T(4,128)S(1)}, f32[128,4,4]{0,2,1:T(4,128)}, u32[]{:S(2)}) copy-start(f32[128,4,4]{0,2,1:T(4,128)} %copy-done.37) | copy-start | bytes 24580
  211.3 15.7 %copy-start.13 = (bf16[128,4,128]{0,2,1:T(8,128)(2,1)S(1)}, bf16[128,4,128]{0,2,1:T(8,128)(2,1)}, u32[]{:S(2)}) copy-start(bf16[128,4,128]{0,2,1:T(8,128)(2,1)} %copy-done.12) | copy-start | bytes 393220
  212.3 19.3 %copy-start.1 = (bf16[1,2048,512]{2,1,0:T(8,128)(2,1)S(1)}, bf16[1,2048,512]{2,1,0:T(8,128)(2,1)}, u32[]{:S(2)}) copy-start(bf16[1,2048,512]{2,1,0:T(8,128)(2,1)} %param.23) | copy-start | bytes 6291460
  (41 other events, 114.5 us)

commit v2 on v1

--- a/solution.py
+++ b/solution.py
@@ -2,6 +2,8 @@
 import jax.numpy as jnp
 from jax import lax
 from jax.sharding import Mesh
+from jax.experimental import pallas as pl
+from jax.experimental.pallas import tpu as pltpu
 from jax.sharding import PartitionSpec as P
 
 HEAD_DIM = 64
@@ -21,9 +23,16 @@
     return lax.dot_general(a, b, (dims, ((), ())), preferred_element_type=f32)
 
 
-def both_halves(x):
-    sent = jnp.broadcast_to(x[None], (2, *x.shape))
-    return lax.all_to_all(sent, "tp", 0, 0, tiled=True)
+def swapped(x):
+    return lax.ppermute(x, "tp", [(0, 1), (1, 0)])
+
+
+def from_line(parts, axis):
+    size = lax.axis_size(axis)
+    return [parts[0]] + [
+        lax.ppermute(parts[k], axis, [(i, (i + k) % size) for i in range(size)])
+        for k in range(1, size)
+    ]
 
 
 def three_parts(x):
@@ -46,28 +55,123 @@
     return (slot[:, :, None] == jnp.arange(experts * capacity, dtype=jnp.int32)).astype(bf16)
 
 
-def expert_side(hidden_rows, grad_rows, gate_value, up_value, gate_weight, up_weight, down_weight):
-    act_grad = dot(grad_rows, down_weight, ((1,), (1,)))
-    gate_full = gate_value.astype(f32)
-    up_full = up_value.astype(f32)
+def expert_rows_kernel(
+    side, mine, other, gate_value, up_value, down_own, down_far, gate_own, gate_far, up_own, up_far,
+    active, gate_grad, up_grad, rows_own, rows_far,
+):
+    act_grad = dot(mine[...], down_own[...], ((1,), (1,)))
+    act_grad = act_grad + dot(other[...], down_far[...], ((1,), (1,)))
+    gate_full = gate_value[...].astype(f32)
+    up_full = up_value[...].astype(f32)
     gate_clip = jnp.minimum(gate_full, clamp_limit)
     up_clip = jnp.clip(up_full, -clamp_limit, clamp_limit)
     sigmoid_gate = jax.nn.sigmoid(swish_alpha * gate_clip)
     swish_gate = gate_clip * sigmoid_gate
-    active = ((up_clip + 1.0) * swish_gate).astype(bf16)
-    up_grad = jnp.where(
-        (up_full > -clamp_limit) & (up_full < clamp_limit), act_grad * swish_gate, 0.0
+    active[...] = ((up_clip + 1.0) * swish_gate).astype(bf16)
+    inside = (up_full > -clamp_limit) & (up_full < clamp_limit)
+    up_side = jnp.where(inside, act_grad * swish_gate, 0.0).astype(bf16)
+    slope = sigmoid_gate + swish_alpha * gate_clip * sigmoid_gate * (1.0 - sigmoid_gate)
+    gate_side = jnp.where(
+        gate_full < clamp_limit, act_grad * (up_clip + 1.0) * slope, 0.0
     ).astype(bf16)
-    slope = sigmoid_gate + swish_alpha * gate_clip * sigmoid_gate * (1.0 - sigmoid_gate)
-    gate_grad = jnp.where(gate_full < clamp_limit, act_grad * (up_clip + 1.0) * slope, 0.0).astype(
-        bf16
-    )
-    down_wgrad = dot(active, grad_rows, ((0,), (0,))).astype(bf16)
-    gate_wgrad = dot(hidden_rows, gate_grad, ((0,), (0,))).astype(bf16)
-    up_wgrad = dot(hidden_rows, up_grad, ((0,), (0,))).astype(bf16)
-    partial_rows = dot(gate_grad, gate_weight, ((1,), (1,)))
-    partial_rows = partial_rows + dot(up_grad, up_weight, ((1,), (1,)))
-    return (gate_wgrad, up_wgrad, down_wgrad, partial_rows)
+    up_grad[...] = up_side
+    gate_grad[...] = gate_side
+    far = dot(gate_side, gate_far[...], ((1,), (1,))) + dot(up_side, up_far[...], ((1,), (1,)))
+    rows_far[...] = far.astype(bf16)
+    own = dot(gate_side, gate_own[...], ((1,), (1,))) + dot(up_side, up_own[...], ((1,), (1,)))
+    rows_own[...] = own.astype(bf16)
+
+
+def whole_block(*shape):
+    return pl.BlockSpec(shape, lambda i, side: (0,) * len(shape))
+
+
+def expert_rows(side, mine, other, gate_value, up_value, w_down, w_gate, w_up):
+    rows, half = mine.shape
+    hidden = gate_value.shape[1]
+    row_block = whole_block(rows, half)
+    act_block = whole_block(rows, hidden)
+    down = [
+        pl.BlockSpec((hidden, half), lambda i, side: (0, side[0])),
+        pl.BlockSpec((hidden, half), lambda i, side: (0, 1 - side[0])),
+    ]
+    tall = [
+        pl.BlockSpec((half, hidden), lambda i, side: (side[0], 0)),
+        pl.BlockSpec((half, hidden), lambda i, side: (1 - side[0], 0)),
+    ]
+    act = jax.ShapeDtypeStruct((rows, hidden), bf16)
+    out = jax.ShapeDtypeStruct((rows, half), bf16)
+    return pl.pallas_call(
+        expert_rows_kernel,
+        grid_spec=pltpu.PrefetchScalarGridSpec(
+            num_scalar_prefetch=1,
+            grid=(1,),
+            in_specs=[row_block, row_block, act_block, act_block] + down + tall + tall,
+            out_specs=[act_block] * 3 + [row_block] * 2,
+        ),
+        out_shape=[act] * 3 + [out] * 2,
+        name="expert_rows",
+    )(side, mine, other, gate_value, up_value, w_down, w_down, w_gate, w_gate, w_up, w_up)
+
+
+def down_kernel(side, active, mine, other, out):
+    @pl.when(pl.program_id(0) == 0)
+    def _():
+        out[...] = dot(active[...], mine[...], ((0,), (0,))).astype(bf16)
+
+    @pl.when(pl.program_id(0) == 1)
+    def _():
+        out[...] = dot(active[...], other[...], ((0,), (0,))).astype(bf16)
+
+
+def tall_kernel(side, gate_grad, up_grad, mine, other, gate_out, up_out):
+    def write(rows):
+        gate_out[...] = dot(rows, gate_grad[...], ((0,), (0,))).astype(bf16)
+        up_out[...] = dot(rows, up_grad[...], ((0,), (0,))).astype(bf16)
+
+    @pl.when(pl.program_id(0) == 0)
+    def _():
+        write(mine[...])
+
+    @pl.when(pl.program_id(0) == 1)
+    def _():
+        write(other[...])
+
+
+def half_of(i, side):
+    return lax.rem(i + side[0], 2)
+
+
+def down_weights(side, active, mine, other):
+    rows, half = mine.shape
+    hidden = active.shape[1]
+    return pl.pallas_call(
+        down_kernel,
+        grid_spec=pltpu.PrefetchScalarGridSpec(
+            num_scalar_prefetch=1,
+            grid=(2,),
+            in_specs=[whole_block(rows, hidden)] + [whole_block(rows, half)] * 2,
+            out_specs=pl.BlockSpec((hidden, half), lambda i, side: (0, half_of(i, side))),
+        ),
+        out_shape=jax.ShapeDtypeStruct((hidden, 2 * half), bf16),
+        name="down_weights",
+    )(side, active, mine, other)
+
+
+def tall_weights(side, gate_grad, up_grad, mine, other):
+    rows, half = mine.shape
+    hidden = gate_grad.shape[1]
+    return pl.pallas_call(
+        tall_kernel,
+        grid_spec=pltpu.PrefetchScalarGridSpec(
+            num_scalar_prefetch=1,
+            grid=(2,),
+            in_specs=[whole_block(rows, hidden)] * 2 + [whole_block(rows, half)] * 2,
+            out_specs=[pl.BlockSpec((half, hidden), lambda i, side: (half_of(i, side), 0))] * 2,
+        ),
+        out_shape=[jax.ShapeDtypeStruct((2 * half, hidden), bf16)] * 2,
+        name="tall_weights",
+    )(side, gate_grad, up_grad, mine, other)
 
 
 def scan_piece(came):
@@ -136,30 +240,29 @@
     send_grads = send_grads.reshape(experts, capacity, half)
     send_hidden = send_hidden.reshape(experts, capacity, half)
     came_grads = lax.all_to_all(send_grads, SP, 0, 0, tiled=True)
+    send_hidden, came_grads = lax.optimization_barrier((send_hidden, came_grads))
     came_hidden = lax.all_to_all(send_hidden, SP, 0, 0, tiled=True)
-
-    def whole(x):
-        x = both_halves(x.reshape(-1, half))
-        return jnp.concatenate([x[0], x[1]], axis=1)
-
-    gate_wgrad, up_wgrad, down_wgrad, partial_rows = expert_side(
-        whole(came_hidden),
-        whole(came_grads),
-        gate_pre[0],
-        up_pre[0],
-        w_gate[0],
-        w_up[0],
-        w_down[0],
-    )
-    partial_rows = partial_rows.astype(bf16)
-    split_rows = jnp.stack([partial_rows[:, :half], partial_rows[:, half:]])
-    split_rows = lax.all_to_all(split_rows, "tp", 0, 0, tiled=True)
-    summed = (split_rows[0].astype(f32) + split_rows[1].astype(f32)).astype(bf16)
+    grads_own = came_grads.reshape(-1, half)
+    grads_far = swapped(grads_own)
+    side = lax.axis_index("tp")[None]
+    active, gate_grad, up_grad, rows_own, rows_far = expert_rows(
+        side, grads_own, grads_far, gate_pre[0], up_pre[0], w_down[0], w_gate[0], w_up[0]
+    )
+    summed = (rows_own.astype(f32) + swapped(rows_far).astype(f32)).astype(bf16)
+    summed, came_hidden = lax.optimization_barrier((summed, came_hidden))
     returned = lax.all_to_all(summed.reshape(experts, capacity, half), SP, 0, 0, tiled=True)
+    hidden_own = came_hidden.reshape(-1, half)
+    hidden_far = swapped(hidden_own)
+    down_wgrad = down_weights(side, active, grads_own, grads_far)
+    gate_wgrad, up_wgrad = tall_weights(side, gate_grad, up_grad, hidden_own, hidden_far)
     moe_terms = dot(either, returned.reshape(-1, half), ((1,), (0,)))
-    grad_half = (cotangent_half.astype(f32) + moe_terms).astype(bf16)
-    grad_halves = both_halves(grad_half)
-    grad_hidden = jnp.concatenate([grad_halves[0], grad_halves[1]], axis=1)
+    grad_own = (cotangent_half.astype(f32) + moe_terms).astype(bf16)
+    grad_far = swapped(grad_own)
+    grad_hidden = jnp.where(
+        side == 0,
+        jnp.concatenate([grad_own, grad_far], axis=1),
+        jnp.concatenate([grad_far, grad_own], axis=1),
+    )
 
     head_count = log_decay.shape[1]
     group_count = b_proj.shape[1] // STATE
@@ -198,14 +301,18 @@
     local_state = jnp.einsum("sgrp,sgn->grpn", x_tail, b_float)
 
     line = lax.axis_size("sp_0")
-    mixed_line = lax.all_to_all(
-        jnp.broadcast_to(mixed[None], (line, *mixed.shape)), "sp_0", 0, 0, tiled=True
-    )
-    grads_line = lax.all_to_all(
-        grad_hidden.reshape(tokens, line, -1).transpose(1, 0, 2), "sp_0", 0, 0, tiled=True
+    spot = lax.axis_index("sp_0")
+    span = width // line
+    mixed_line = from_line([mixed] * line, "sp_0")
+    grads_line = from_line(
+        [
+            lax.dynamic_slice_in_dim(grad_hidden, lax.rem(spot + k, line) * span, span, 1)
+            for k in range(line)
+        ],
+        "sp_0",
     )
     product = dot(
-        grads_line.reshape(line * tokens, -1), mixed_line.reshape(line * tokens, -1), ((0,), (0,))
+        jnp.concatenate(grads_line, axis=0), jnp.concatenate(mixed_line, axis=0), ((0,), (0,))
     ).astype(bf16)
     product = product.reshape(experts // line, -1, product.shape[1])
     grad_out_proj = (

time: 234 us -> 198 us (0.85)
  local copies, waits for them, and re-layouts: 40.6 us -> 17.8 us
  Pallas kernels: 0 us -> 19.3 us
  matrix products: 36.2 us -> 18.6 us
  blocking collectives: 15 us -> 0 us
  waiting for transfers between devices: 54.1 us -> 64.4 us
  other arithmetic: 30.5 us -> 21.5 us
    all_to_all x3 -> x0, waiting for transfers between devices: 19.7 us -> none  [the longest x1 11 us: body(): lax.all_to_all(jnp.broadcast_to(mixed[None], (line, *mixed.shape)), 'sp_0...]
    pallas_call x0 -> x3, Pallas kernels: none -> 19.3 us  [the longest x1 9.26 us: expert_rows(): pl.pallas_call(expert_rows_kernel, grid_spec=pltpu.PrefetchScalarGridSpec...]
    all_to_all x1, waiting for transfers between devices: 0.01 us -> 17.4 us  [body(): came_grads = lax.all_to_all(send_grads, SP, 0, 0, tiled=True)]
    all_to_all x3 -> x0, blocking collectives: 15 us -> none  [the longest x2 9.57 us: both_halves(): return lax.all_to_all(sent, 'tp', 0, 0, tiled=True)]
    dot_general x17 -> x11, matrix products: 23.3 us -> 9.26 us  [dot(): return lax.dot_general(a, b, (dims, ((), ())), preferred_element_type=f32)]
    all_to_all x3 -> x0, starting transfers between devices: 12.9 us -> none  [the longest x1 5 us: both_halves(): return lax.all_to_all(sent, 'tp', 0, 0, tiled=True)]
    all_to_all x1, waiting for transfers between devices: 0.01 us -> 12 us  [body(): lax.all_to_all(product, ('sp_1', 'sp_2'), 0, 0, tiled=True).astype(f32)]
    ppermute x0 -> x10, starting transfers between devices: none -> 11.2 us  [the longest x6 10.3 us: from_line(): lax.ppermute(parts[k], axis, [(i, (i + k) % size) for i in range(size)])]
  transfers between devices with their start and end apart: 9 -> 16, of which waited for: 7 -> 7; matrix products, arithmetic and copies ran while one was open for 31% -> 24% of each run, Pallas kernels for 0% -> 5%
where the time goes in v2:
time: 198 us; the launch traced here: 197 us
  waiting for transfers between devices  64.4 us (33%)
  starting transfers between devices  53.6 us (27%)
  other arithmetic  21.5 us (11%)
  Pallas kernels  19.3 us (10%)
  matrix products  18.6 us (9%)
  local copies, waits for them, and re-layouts  17.8 us (9%)
    all_to_all x1, waiting for transfers between devices, body(): came_grads = lax.all_to_all(send_grads, SP, 0, 0, tiled=True)  17.4 us
    all_to_all x1, waiting for transfers between devices, body(): came_hidden = lax.all_to_all(send_hidden, SP, 0, 0, tiled=True)  15.8 us
    all_to_all x1, waiting for transfers between devices, body(): lax.all_to_all(summed.reshape(experts, capacity, half), SP, 0, 0, tiled=T...  14.2 us
    all_to_all x1, waiting for transfers between devices, body(): lax.all_to_all(product, ('sp_1', 'sp_2'), 0, 0, tiled=True).astype(f32)  12 us
    all_to_all x1, starting transfers between devices, body(): came_grads = lax.all_to_all(send_grads, SP, 0, 0, tiled=True)  11.7 us
    ppermute x6, starting transfers between devices, from_line(): lax.ppermute(parts[k], axis, [(i, (i + k) % size) for i in range(size)])  10.3 us
    all_to_all x1, starting transfers between devices, body(): back = lax.all_to_all(back, SP, 0, 0, tiled=True)  9.9 us
    pallas_call x1, Pallas kernels, expert_rows(): pl.pallas_call(expert_rows_kernel, grid_spec=pltpu.PrefetchScalarGridSpec...  9.26 us
  transfers between devices with their start and end apart: 16, of which 7 were waited for; matrix products, arithmetic and copies ran while one was open for 24% of the time, Pallas kernels for 5%

profile of v2, /device:TPU:0, one launch (start us, length us, event | category | flops | bytes accessed | tf_op | source)
XLA Modules:
  0.0 196.8 jit_solution(6574814255783761703)
XLA Ops:
  7.0 11.7 %all-to-all-start = ((bf16[64,8,1024]{2,1,0:T(8,128)(2,1)}), bf16[64,8,1024]{2,1,0:T(8,128)(2,1)S(1)}, u32[]{:S(2)}, u32[]{:S(2)}) async-start(bf16[64,8,1024]{2,1,0:T(8,128)(2,1)} %fusion.1), calls=%async_computation | async-start | bytes 2097152 | tf_op jit(solution)/shard_map/all_to_all | solution.py:242
  20.2 17.4 %all-to-all-done = bf16[64,8,1024]{2,1,0:T(8,128)(2,1)S(1)} async-done(((bf16[64,8,1024]{2,1,0:T(8,128)(2,1)}), bf16[64,8,1024]{2,1,0:T(8,128)(2,1)S(1)}, u32[]{:S(2)}, u32[]{:S(2)}) %all-to-all-start) | async-done | bytes 1048608 | tf_op jit(solution)/shard_map/all_to_all | solution.py:242
  38.6 1.7 collective-permute-done.other
  41.2 9.3 %expert_rows.1 = (bf16[512,512]{1,0:T(8,128)(2,1)}, bf16[512,512]{1,0:T(8,128)(2,1)}, bf16[512,512]{1,0:T(8,128)(2,1)}, bf16[512,1024]{1,0:T(8,128)(2,1)}, bf16[512,1024]{1,0:T(8,128)(2,1)}) custom-call(s32[1]{0:T(128)} %bitcast.side, bf16[512,1024]{1,0:T(8,128)(2,1)} %bitcast.158, bf16[512,1024]{1,0:T(8,128)(2,1)} %copy-done.4, bf16[512,512]{1,0:T(8,128)(2,1)} %bitcast.195, ...), custom_call_target="tpu_custom_call" | custom-call | tf_op jit(solution)/shard_map/expert_rows/pallas_call | solution.py:104
  53.1 4.7 %all-to-all-start.1 = ((bf16[64,8,1024]{2,1,0:T(8,128)(2,1)}), bf16[64,8,1024]{2,1,0:T(8,128)(2,1)S(1)}, u32[]{:S(2)}, u32[]{:S(2)}) async-start(bf16[64,8,1024]{2,1,0:T(8,128)(2,1)} %fusion), calls=%async_computation.1 | async-start | bytes 2097152 | tf_op jit(solution)/shard_map/all_to_all | solution.py:244
  59.1 2.6 %add_convert_fusion = bf16[512,1024]{1,0:T(8,128)(2,1)} fusion(bf16[512,1024]{1,0:T(8,128)(2,1)} %collective-permute-done.1, bf16[512,1024]{1,0:T(8,128)(2,1)S(1)} %copy-done.17), kind=kLoop, calls=%fused_computation.2 | loop fusion | flops 2097152 | bytes 3145728 | tf_op jit(solution)/shard_map/convert_element_type | solution.py:251
  61.7 15.8 %all-to-all-done.1 = bf16[64,8,1024]{2,1,0:T(8,128)(2,1)S(1)} async-done(((bf16[64,8,1024]{2,1,0:T(8,128)(2,1)}), bf16[64,8,1024]{2,1,0:T(8,128)(2,1)S(1)}, u32[]{:S(2)}, u32[]{:S(2)}) %all-to-all-start.1) | async-done | bytes 1048608 | tf_op jit(solution)/shard_map/all_to_all | solution.py:244
  77.5 5.5 %all-to-all-start.2 = ((bf16[64,8,1024]{2,1,0:T(8,128)(2,1)}), bf16[64,8,1024]{2,1,0:T(8,128)(2,1)}, u32[]{:S(2)}, u32[]{:S(2)}) async-start(bf16[64,8,1024]{2,1,0:T(8,128)(2,1)} %bitcast.19), calls=%async_computation.2 | async-start | bytes 2097152 | tf_op jit(solution)/shard_map/all_to_all | solution.py:253
  87.0 14.2 %all-to-all-done.2 = bf16[64,8,1024]{2,1,0:T(8,128)(2,1)} async-done(((bf16[64,8,1024]{2,1,0:T(8,128)(2,1)}), bf16[64,8,1024]{2,1,0:T(8,128)(2,1)}, u32[]{:S(2)}, u32[]{:S(2)}) %all-to-all-start.2) | async-done | bytes 1048608 | tf_op jit(solution)/shard_map/all_to_all | solution.py:253
  101.2 1.7 fusion.3
  110.9 3.7 %fusion.96 = f32[128,1024]{1,0:T(8,128)S(1)} fusion(bf16[128,2048]{1,0:T(8,128)(2,1)S(1)} %maximum_select_fusion, bf16[1024,2048]{1,0:T(8,128)(2,1)} %param.26), kind=kOutput, calls=%fused_computation.176 | convolution fusion | flops 536870912 | bytes 5242880 | tf_op jit(solution)/shard_map/td,id->ti/dot_general | solution.py:322
  115.7 1.5 multiply_reduce_fusion.1
  121.3 1.8 pad_maximum_fusion
  123.2 4.6 %all-to-all-start.4 = ((bf16[64,40,128]{2,1,0:T(8,128)(2,1)}), bf16[64,40,128]{2,1,0:T(8,128)(2,1)S(1)}, u32[]{:S(2)}, u32[]{:S(2)}) async-start(bf16[64,40,128]{2,1,0:T(8,128)(2,1)} %pad_maximum_fusion), calls=%async_computation.4 | async-start | bytes 1310720 | tf_op jit(solution)/shard_map/all_to_all | solution.py:362
  128.5 4.2 %down_weights.1 = bf16[512,2048]{1,0:T(8,128)(2,1)} custom-call(s32[1]{0:T(128)} %bitcast.side, bf16[512,512]{1,0:T(8,128)(2,1)} %get-tuple-element.29.active, bf16[512,1024]{1,0:T(8,128)(2,1)} %bitcast.159, bf16[512,1024]{1,0:T(8,128)(2,1)} %copy-done.4), custom_call_target="tpu_custom_call" | custom-call | tf_op jit(solution)/shard_map/down_weights/pallas_call | solution.py:148
  132.7 5.9 %tall_weights.1 = (bf16[2048,512]{1,0:T(8,128)(2,1)}, bf16[2048,512]{1,0:T(8,128)(2,1)}) custom-call(s32[1]{0:T(128)} %bitcast.side, bf16[512,512]{1,0:T(8,128)(2,1)} %get-tuple-element.21.gate_grad, bf16[512,512]{1,0:T(8,128)(2,1)} %get-tuple-element.22.up_grad, bf16[512,1024]{1,0:T(8,128)(2,1)} %bitcast.172, bf16[512,1024]{1,0:T(8,128)(2,1)} %collective-permute-done.2.other), custom_call_target="tpu_custom_call" | custom-call | tf_op jit(solution)/shard_map/tall_weights/pallas_call | solution.py:164
  138.6 1.6 collective-permute-start.7
  140.2 2.9 %collective-permute-start.8 = (bf16[128,1024]{1,0:T(8,128)(2,1)}, bf16[128,1024]{1,0:T(8,128)(2,1)}, u32[]{:S(2)}, u32[]{:S(2)}) collective-permute-start(bf16[128,1024]{1,0:T(8,128)(2,1)} %get-tuple-element.83), channel_id=1, source_target_pairs={{0,64},{32,96},{64,0},{96,32},{1,65},{33,97},{65,1},{97,33},{2,66}... | collective-permute-start | bytes 786440 | tf_op jit(solution)/shard_map/ppermute | solution.py:33
  151.7 9.9 %all-to-all-start.5 = ((bf16[64,24,128]{2,1,0:T(8,128)(2,1)}), bf16[64,24,128]{2,1,0:T(8,128)(2,1)S(1)}, u32[]{:S(2)}, u32[]{:S(2)}) async-start(bf16[64,24,128]{2,1,0:T(8,128)(2,1)} %pad_maximum_fusion.1), calls=%async_computation.5 | async-start | bytes 786432 | tf_op jit(solution)/shard_map/all_to_all | solution.py:364
  161.7 3.1 %collective-permute-start.6 = (bf16[128,512]{1,0:T(8,128)(2,1)}, bf16[128,512]{1,0:T(8,128)(2,1)S(1)}, u32[]{:S(2)}, u32[]{:S(2)}) collective-permute-start(bf16[128,512]{1,0:T(8,128)(2,1)} %get-tuple-element.91), channel_id=1, source_target_pairs={{0,96},{32,0},{64,32},{96,64},{1,97},{33,1},{65,33},{97,65},{2,98}... | collective-permute-start | bytes 393224 | tf_op jit(solution)/shard_map/ppermute | solution.py:33
  166.7 2.6 %collective-permute-done.6 = bf16[128,512]{1,0:T(8,128)(2,1)S(1)} collective-permute-done((bf16[128,512]{1,0:T(8,128)(2,1)}, bf16[128,512]{1,0:T(8,128)(2,1)S(1)}, u32[]{:S(2)}, u32[]{:S(2)}) %collective-permute-start.6) | collective-permute-done | bytes 131104 | tf_op jit(solution)/shard_map/ppermute | solution.py:33
  169.3 3.0 %convolution_convert_fusion.1 = bf16[512,1024]{1,0:T(8,128)(2,1)} fusion(bf16[128,1024]{1,0:T(8,128)(2,1)} %collective-permute-done.9, bf16[128,1024]{1,0:T(8,128)(2,1)} %collective-permute-done.8, bf16[128,1024]{1,0:T(8,128)(2,1)} %collective-permute-done.7, bf16[128,1024]{1,0:T(8,128)(2,1)S(1)} %copy-done.23, ...), kind=kOutput, calls=%fused_computation.5 | convolution fusion | flops 543686656 | bytes 2621440 | tf_op jit(solution)/shard_map/dot_general | solution.py:23
  172.9 6.0 %all-to-all-start.3 = ((bf16[16,32,1024]{2,1,0:T(8,128)(2,1)}), bf16[16,32,1024]{2,1,0:T(8,128)(2,1)S(1)}, u32[]{:S(2)}, u32[]{:S(2)}) async-start(bf16[16,32,1024]{2,1,0:T(8,128)(2,1)} %bitcast.193), calls=%async_computation.3 | async-start | bytes 2097152 | tf_op jit(solution)/shard_map/all_to_all | solution.py:319
  184.0 12.0 %all-to-all-done.3 = bf16[16,32,1024]{2,1,0:T(8,128)(2,1)S(1)} async-done(((bf16[16,32,1024]{2,1,0:T(8,128)(2,1)}), bf16[16,32,1024]{2,1,0:T(8,128)(2,1)S(1)}, u32[]{:S(2)}, u32[]{:S(2)}) %all-to-all-start.3) | async-done | bytes 1048608 | tf_op jit(solution)/shard_map/all_to_all | solution.py:319
  (206 shorter events, 48.0 us)
Async XLA Ops:
  0.6 18.1 %copy-start = (bf16[128,2048]{1,0:T(8,128)(2,1)S(1)}, bf16[128,2048]{1,0:T(8,128)(2,1)}, u32[]{:S(2)}) copy-start(bf16[128,2048]{1,0:T(8,128)(2,1)} %param.17) | copy-start | bytes 1572868
  7.0 30.6 %copy-start.36 = (f32[128,16]{0,1:T(8,128)S(1)}, f32[128,16]{0,1:T(8,128)}, u32[]{:S(2)}) copy-start(f32[128,16]{0,1:T(8,128)} %param.32) | copy-start | bytes 24580
  7.0 30.6 %all-to-all-start = ((bf16[64,8,1024]{2,1,0:T(8,128)(2,1)}), bf16[64,8,1024]{2,1,0:T(8,128)(2,1)S(1)}, u32[]{:S(2)}, u32[]{:S(2)}) async-start(bf16[64,8,1024]{2,1,0:T(8,128)(2,1)} %fusion.1), calls=%async_computation | async-start | bytes 2097152 | tf_op jit(solution)/shard_map/all_to_all | solution.py:242
  37.6 2.7 %collective-permute-start = (bf16[512,1024]{1,0:T(8,128)(2,1)S(1)}, bf16[512,1024]{1,0:T(8,128)(2,1)S(1)}, u32[]{:S(2)}, u32[]{:S(2)}) collective-permute-start(bf16[512,1024]{1,0:T(8,128)(2,1)S(1)} %bitcast.157), channel_id=1, source_target_pairs={{0,1},{1,0},{2,3},{3,2},{4,5},{5,4},{6,7},{7,6},{8,9},{9,8},{10,11... | collective-permute-start | bytes 3145736 | tf_op jit(solution)/shard_map/ppermute | solution.py:27
  50.5 8.3 %collective-permute-start.1 = (bf16[512,1024]{1,0:T(8,128)(2,1)}, bf16[512,1024]{1,0:T(8,128)(2,1)}, u32[]{:S(2)}, u32[]{:S(2)}) collective-permute-start(bf16[512,1024]{1,0:T(8,128)(2,1)} %get-tuple-element.24), channel_id=1, source_target_pairs={{0,1},{1,0},{2,3},{3,2},{4,5},{5,4},{6,7},{7,6},{8,9},{9,8},{10,11... | collective-permute-start | bytes 3145736 | tf_op jit(solution)/shard_map/ppermute | solution.py:27
  53.1 24.4 %all-to-all-start.1 = ((bf16[64,8,1024]{2,1,0:T(8,128)(2,1)}), bf16[64,8,1024]{2,1,0:T(8,128)(2,1)S(1)}, u32[]{:S(2)}, u32[]{:S(2)}) async-start(bf16[64,8,1024]{2,1,0:T(8,128)(2,1)} %fusion), calls=%async_computation.1 | async-start | bytes 2097152 | tf_op jit(solution)/shard_map/all_to_all | solution.py:244
  77.5 23.7 %all-to-all-start.2 = ((bf16[64,8,1024]{2,1,0:T(8,128)(2,1)}), bf16[64,8,1024]{2,1,0:T(8,128)(2,1)}, u32[]{:S(2)}, u32[]{:S(2)}) async-start(bf16[64,8,1024]{2,1,0:T(8,128)(2,1)} %bitcast.19), calls=%async_computation.2 | async-start | bytes 2097152 | tf_op jit(solution)/shard_map/all_to_all | solution.py:253
  85.6 18.3 %copy-start.37 = (bf16[1024]{0:T(1024)(128)(2,1)S(1)}, bf16[1024]{0:T(1024)(128)(2,1)}, u32[]{:S(2)}) copy-start(bf16[1024]{0:T(1024)(128)(2,1)} %param.27) | copy-start | bytes 6148
  85.9 22.5 %copy-start.9 = (bf16[128,4,128]{2,1,0:T(4,128)(2,1)S(1)}, bf16[128,4,128]{2,1,0:T(4,128)(2,1)}, u32[]{:S(2)}) copy-start(bf16[128,4,128]{2,1,0:T(4,128)(2,1)} %copy-done.8) | copy-start | bytes 393220
  87.0 22.3 %copy-start.29 = (f32[128,4,4]{0,2,1:T(4,128)}, f32[128,4,4]{0,2,1:T(4,128)S(1)}, u32[]{:S(2)}) copy-start(f32[128,4,4]{0,2,1:T(4,128)S(1)} %get-tuple-element.102) | copy-start | bytes 24580
  87.0 22.8 %copy-start.21 = (f32[128,4]{1,0:T(8,128)}, f32[128,4]{1,0:T(8,128)S(1)}, u32[]{:S(2)}) copy-start(f32[128,4]{1,0:T(8,128)S(1)} %add_rsqrt_fusion) | copy-start | bytes 6148
  102.9 6.9 %collective-permute-start.3 = (bf16[128,1024]{1,0:T(8,128)(2,1)S(1)}, bf16[128,1024]{1,0:T(8,128)(2,1)}, u32[]{:S(2)}, u32[]{:S(2)}) collective-permute-start(bf16[128,1024]{1,0:T(8,128)(2,1)S(1)} %fusion.3), channel_id=1, source_target_pairs={{0,1},{1,0},{2,3},{3,2},{4,5},{5,4},{6,7},{7,6},{8,9},{9,8},{10,11... | collective-permute-start | bytes 786440 | tf_op jit(solution)/shard_map/ppermute | solution.py:27
  109.3 23.4 %collective-permute-start.2 = (bf16[512,1024]{1,0:T(8,128)(2,1)}, bf16[512,1024]{1,0:T(8,128)(2,1)}, u32[]{:S(2)}, u32[]{:S(2)}) collective-permute-start(bf16[512,1024]{1,0:T(8,128)(2,1)} %bitcast.171), channel_id=1, source_target_pairs={{0,1},{1,0},{2,3},{3,2},{4,5},{5,4},{6,7},{7,6},{8,9},{9,8},{10,11... | collective-permute-start | bytes 3145736 | tf_op jit(solution)/shard_map/ppermute | solution.py:27
  123.2 25.0 %all-to-all-start.4 = ((bf16[64,40,128]{2,1,0:T(8,128)(2,1)}), bf16[64,40,128]{2,1,0:T(8,128)(2,1)S(1)}, u32[]{:S(2)}, u32[]{:S(2)}) async-start(bf16[64,40,128]{2,1,0:T(8,128)(2,1)} %pad_maximum_fusion), calls=%async_computation.4 | async-start | bytes 1310720 | tf_op jit(solution)/shard_map/all_to_all | solution.py:362
  138.6 30.7 %collective-permute-start.7 = (bf16[128,1024]{1,0:T(8,128)(2,1)}, bf16[128,1024]{1,0:T(8,128)(2,1)}, u32[]{:S(2)}, u32[]{:S(2)}) collective-permute-start(bf16[128,1024]{1,0:T(8,128)(2,1)} %get-tuple-element.83), channel_id=1, source_target_pairs={{0,32},{32,64},{64,96},{96,0},{1,33},{33,65},{65,97},{97,1},{2,34}... | collective-permute-start | bytes 786440 | tf_op jit(solution)/shard_map/ppermute | solution.py:33
  140.2 29.1 %collective-permute-start.8 = (bf16[128,1024]{1,0:T(8,128)(2,1)}, bf16[128,1024]{1,0:T(8,128)(2,1)}, u32[]{:S(2)}, u32[]{:S(2)}) collective-permute-start(bf16[128,1024]{1,0:T(8,128)(2,1)} %get-tuple-element.83), channel_id=1, source_target_pairs={{0,64},{32,96},{64,0},{96,32},{1,65},{33,97},{65,1},{97,33},{2,66}... | collective-permute-start | bytes 786440 | tf_op jit(solution)/shard_map/ppermute | solution.py:33
  143.1 26.2 %collective-permute-start.9 = (bf16[128,1024]{1,0:T(8,128)(2,1)}, bf16[128,1024]{1,0:T(8,128)(2,1)}, u32[]{:S(2)}, u32[]{:S(2)}) collective-permute-start(bf16[128,1024]{1,0:T(8,128)(2,1)} %get-tuple-element.83), channel_id=1, source_target_pairs={{0,96},{32,0},{64,32},{96,64},{1,97},{33,1},{65,33},{97,65},{2,98}... | collective-permute-start | bytes 786440 | tf_op jit(solution)/shard_map/ppermute | solution.py:33
  145.2 16.4 %collective-permute-start.4 = (bf16[128,512]{1,0:T(8,128)(2,1)}, bf16[128,512]{1,0:T(8,128)(2,1)}, u32[]{:S(2)}, u32[]{:S(2)}) collective-permute-start(bf16[128,512]{1,0:T(8,128)(2,1)} %get-tuple-element.93), channel_id=1, source_target_pairs={{0,32},{32,64},{64,96},{96,0},{1,33},{33,65},{65,97},{97,1},{2,34}... | collective-permute-start | bytes 393224 | tf_op jit(solution)/shard_map/ppermute | solution.py:33
  145.9 20.8 %collective-permute-start.5 = (bf16[128,512]{1,0:T(8,128)(2,1)}, bf16[128,512]{1,0:T(8,128)(2,1)}, u32[]{:S(2)}, u32[]{:S(2)}) collective-permute-start(bf16[128,512]{1,0:T(8,128)(2,1)} %get-tuple-element.92), channel_id=1, source_target_pairs={{0,64},{32,96},{64,0},{96,32},{1,65},{33,97},{65,1},{97,33},{2,66}... | collective-permute-start | bytes 393224 | tf_op jit(solution)/shard_map/ppermute | solution.py:33
  149.9 19.4 %copy-start.23 = (bf16[128,1024]{1,0:T(8,128)(2,1)S(1)}, bf16[128,1024]{1,0:T(8,128)(2,1)}, u32[]{:S(2)}) copy-start(bf16[128,1024]{1,0:T(8,128)(2,1)} %get-tuple-element.83) | copy-start | bytes 786436
  149.9 19.4 %copy-start.26 = (bf16[128,512]{1,0:T(8,128)(2,1)S(1)}, bf16[128,512]{1,0:T(8,128)(2,1)}, u32[]{:S(2)}) copy-start(bf16[128,512]{1,0:T(8,128)(2,1)} %get-tuple-element.90) | copy-start | bytes 393220
  151.7 21.2 %all-to-all-start.5 = ((bf16[64,24,128]{2,1,0:T(8,128)(2,1)}), bf16[64,24,128]{2,1,0:T(8,128)(2,1)S(1)}, u32[]{:S(2)}, u32[]{:S(2)}) async-start(bf16[64,24,128]{2,1,0:T(8,128)(2,1)} %pad_maximum_fusion.1), calls=%async_computation.5 | async-start | bytes 786432 | tf_op jit(solution)/shard_map/all_to_all | solution.py:364
  161.7 7.6 %collective-permute-start.6 = (bf16[128,512]{1,0:T(8,128)(2,1)}, bf16[128,512]{1,0:T(8,128)(2,1)S(1)}, u32[]{:S(2)}, u32[]{:S(2)}) collective-permute-start(bf16[128,512]{1,0:T(8,128)(2,1)} %get-tuple-element.91), channel_id=1, source_target_pairs={{0,96},{32,0},{64,32},{96,64},{1,97},{33,1},{65,33},{97,65},{2,98}... | collective-permute-start | bytes 393224 | tf_op jit(solution)/shard_map/ppermute | solution.py:33
  172.9 23.0 %all-to-all-start.3 = ((bf16[16,32,1024]{2,1,0:T(8,128)(2,1)}), bf16[16,32,1024]{2,1,0:T(8,128)(2,1)S(1)}, u32[]{:S(2)}, u32[]{:S(2)}) async-start(bf16[16,32,1024]{2,1,0:T(8,128)(2,1)} %bitcast.193), calls=%async_computation.3 | async-start | bytes 2097152 | tf_op jit(solution)/shard_map/all_to_all | solution.py:319
  (33 other events, 197.4 us)

commit v3 on v2

--- a/solution.py
+++ b/solution.py
@@ -35,24 +35,19 @@
     ]
 
 
+def pieces_for(x, axis, dim):
+    size, spot = lax.axis_size(axis), lax.axis_index(axis)
+    span = x.shape[dim] // size
+    return [
+        lax.dynamic_slice_in_dim(x, lax.rem(spot + k, size) * span, span, dim) for k in range(size)
+    ]
+
+
 def three_parts(x):
     high = lax.reduce_precision(x, 8, 7)
     rest = x - high
     middle = lax.reduce_precision(rest, 8, 7)
     return high.astype(bf16), middle.astype(bf16), (rest - middle).astype(bf16)
-
-
-def routing(expert_choice, experts, capacity):
-    tokens = expert_choice.shape[0]
-    hot = expert_choice[:, :, None] == jnp.arange(experts, dtype=jnp.int32)
-    hot = hot.astype(f32)
-    named = hot.sum(axis=1).astype(bf16)
-    at = jnp.arange(tokens)
-    before = (at[:, None] > at[None, :]).astype(bf16)
-    earlier = dot(before, named, ((1,), (0,)))
-    rank = (earlier[:, None, :] * hot).sum(axis=2).astype(jnp.int32)
-    slot = expert_choice * capacity + rank
-    return (slot[:, :, None] == jnp.arange(experts * capacity, dtype=jnp.int32)).astype(bf16)
 
 
 def expert_rows_kernel(
@@ -178,7 +173,9 @@
     blocks = came.shape[0]
     values = came[:, :16].reshape(blocks, -1)
     local = came[:, 16:32].reshape(blocks, -1).astype(f32)
-    sums = came[:, 35:38, 0].astype(f32).sum(axis=1)
+    pieces = 4
+    lead = lax.rem(lax.axis_index(SP), pieces) == 0
+    sums = jnp.where(lead, came[:, 35:38, 0].astype(f32).sum(axis=1), 0.0)
     at = jnp.arange(blocks)
     after = at[None, :] > at[:, None]
     gaps = jnp.zeros((blocks, blocks), f32)
@@ -200,6 +197,306 @@
     rows = jnp.stack(parts, axis=1)
     rows = jnp.pad(rows, ((0, 0), (0, 8 - len(parts))))
     return jnp.broadcast_to(rows[:, :, None], (blocks, 8, STATE)).astype(bf16)
+
+
+def exact_dot(a, b, dims):
+    return lax.dot_general(
+        a, b, (dims, ((), ())), preferred_element_type=f32, precision=lax.Precision.HIGHEST
+    )
+
+
+def grid_of(rows, columns, axis):
+    return lax.broadcasted_iota(jnp.int32, (rows, columns), axis)
+
+
+def route_kernel(side, choice, weight, cotangent, grads, places):
+    tokens = choice.shape[1]
+    slots = places.shape[0]
+    experts = slots // 8
+    expert_at = grid_of(experts, tokens, 0)
+    hot = [(expert_at == choice[k : k + 1, :]).astype(f32) for k in range(2)]
+    before = (grid_of(tokens, tokens, 0) < grid_of(tokens, tokens, 1)).astype(bf16)
+    earlier = dot((hot[0] + hot[1]).astype(bf16), before, ((1,), (0,)))
+    same = (grid_of(tokens, tokens, 0) == grid_of(tokens, tokens, 1)).astype(f32)
+    weights = exact_dot(same, weight[...], ((1,), (1,)))
+    cotangents = cotangent[...].astype(f32)
+    slot_at = grid_of(slots, tokens, 0)
+    either = jnp.zeros((slots, tokens), f32)
+    sent = jnp.zeros((slots, cotangent.shape[1]), f32)
+    for k in range(2):
+        rank = jnp.sum(earlier * hot[k], axis=0, keepdims=True).astype(jnp.int32)
+        taken = (slot_at == choice[k : k + 1, :] * 8 + rank).astype(f32)
+        either = either + taken
+        rows = (weights[:, k : k + 1] * cotangents).astype(bf16)
+        sent = sent + dot(taken.astype(bf16), rows, ((1,), (0,)))
+    grads[...] = sent.astype(bf16)
+    places[...] = either.astype(bf16)
+
+
+def route(side, choice, weight, cotangent, slots):
+    tokens, width = cotangent.shape
+    half = width // 2
+    return pl.pallas_call(
+        route_kernel,
+        grid_spec=pltpu.PrefetchScalarGridSpec(
+            num_scalar_prefetch=1,
+            grid=(1,),
+            in_specs=[
+                whole_block(*choice.shape),
+                whole_block(*weight.shape),
+                pl.BlockSpec((tokens, half), lambda i, side: (0, side[0])),
+            ],
+            out_specs=[whole_block(slots, half), whole_block(slots, tokens)],
+        ),
+        out_shape=[
+            jax.ShapeDtypeStruct((slots, half), bf16),
+            jax.ShapeDtypeStruct((slots, tokens), bf16),
+        ],
+        name="route",
+    )(side, choice, weight, cotangent)
+
+
+GROUP = 256
+PER_GROUP = GROUP // HEAD_DIM
+
+
+def per_head(rows, first):
+    return jnp.concatenate(
+        [
+            jnp.broadcast_to(rows[first + r : first + r + 1, :], (HEAD_DIM, rows.shape[1]))
+            for r in range(PER_GROUP)
+        ],
+        axis=0,
+    )
+
+
+def head_sums(x):
+    return [
+        jnp.sum(x[r * HEAD_DIM : (r + 1) * HEAD_DIM, :], axis=0, keepdims=True)
+        for r in range(PER_GROUP)
+    ]
+
+
+def forward_kernel(
+    scan_in, gate_in, b_proj, c_proj, log_decay, entry, gain,
+    mixed, gated_out, silu_out, slope_out, mix_out, decay_out, x_out, tail_out, local_out,
+    rows_out, inverse_out,
+):
+    tokens = scan_in.shape[0]
+    groups = scan_in.shape[1] // GROUP
+    down, across = grid_of(tokens, tokens, 0), grid_of(tokens, tokens, 1)
+    decays = log_decay[...]
+    cum_rows = exact_dot(decays, (down <= across).astype(f32), ((1,), (0,)))
+    cum_columns = exact_dot((across <= down).astype(f32), decays, ((1,), (1,)))
+    total = cum_rows[:, tokens - 1 :]
+    growth = jnp.exp(cum_rows)
+    tail = jnp.exp(total - cum_rows)
+    rows_out[0] = growth
+    rows_out[1] = tail
+    rows_out[2] = jnp.broadcast_to(total, growth.shape)
+    causal = down >= across
+    for g in range(groups):
+        span = slice(g * GROUP, (g + 1) * GROUP)
+        states = slice(g * STATE, (g + 1) * STATE)
+        first = g * PER_GROUP
+        b_group, c_group = b_proj[:, states], c_proj[:, states]
+        inner = dot(c_group, b_group, ((1,), (1,)))
+        x = jnp.transpose(scan_in[:, span].astype(f32))
+        x_b = x.astype(bf16)
+        carried = dot(entry[span, :].astype(bf16), c_group, ((1,), (1,)))
+        within = []
+        for r in range(PER_GROUP):
+            h = first + r
+            gaps = cum_columns[:, h : h + 1] - cum_rows[h : h + 1, :]
+            decay = jnp.where(causal, jnp.exp(jnp.where(causal, gaps, 0.0)), 0.0)
+            decay_out[h] = decay
+            mix = (inner * decay).astype(bf16)
+            mix_out[h] = mix
+            within.append(dot(x_b[r * HEAD_DIM : (r + 1) * HEAD_DIM, :], mix, ((1,), (1,))))
+        scan_out = jnp.concatenate(within, axis=0) + carried * per_head(growth, first)
+        gate = jnp.transpose(gate_in[:, span].astype(f32))
+        sig = jax.nn.sigmoid(gate)
+        silu = gate * sig
+        gated = scan_out * silu
+        inverse = lax.rsqrt(jnp.mean(gated * gated, axis=0, keepdims=True) + rms_epsilon)
+        mixed[span, :] = (gated * inverse * gain[span, :]).astype(bf16)
+        gated_out[span, :] = gated
+        silu_out[span, :] = silu
+        slope_out[span, :] = scan_out * sig * (1.0 + gate * (1.0 - sig))
+        inverse_out[g : g + 1, :] = inverse
+        x_out[span, :] = x_b
+        x_tail = (x * per_head(tail, first)).astype(bf16)
+        tail_out[span, :] = x_tail
+        local_out[span, :] = dot(x_tail, b_group, ((1,), (0,))).astype(bf16)
+
+
+def whole_call(kernel, out_shape, *args):
+    return pl.pallas_call(kernel, out_shape=[jax.ShapeDtypeStruct(*x) for x in out_shape])(*args)
+
+
+def forward(scan_in, gate_in, b_proj, c_proj, log_decay, entry, gain):
+    tokens, inner = scan_in.shape
+    heads = log_decay.shape[0]
+    return whole_call(
+        forward_kernel,
+        [
+            ((inner, tokens), bf16),
+            ((inner, tokens), f32),
+            ((inner, tokens), f32),
+            ((inner, tokens), f32),
+            ((heads, tokens, tokens), bf16),
+            ((heads, tokens, tokens), f32),
+            ((inner, tokens), bf16),
+            ((inner, tokens), bf16),
+            ((inner, STATE), bf16),
+            ((3, heads, tokens), f32),
+            ((inner // GROUP, tokens), f32),
+        ],
+        scan_in, gate_in, b_proj, c_proj, log_decay, entry, gain,
+    )
+
+
+def spread_parts(x, heads, pieces):
+    high = x.astype(bf16)
+    rest = x - high.astype(f32)
+    middle = rest.astype(bf16)
+    low = (rest - middle.astype(f32)).astype(bf16)
+    return [
+        jnp.broadcast_to(part.astype(f32)[:, None, :], (heads, pieces, STATE)).reshape(
+            heads * pieces, 1, STATE
+        )
+        for part in (high, middle, low)
+    ]
+
+
+def backward_kernel(
+    side, grad_own, grad_far, out_own, out_far, gain, gated_in, silu_in, slope_in, mix_in, decay_in,
+    x_in, b_proj, c_proj, entry, local_in, rows_in, inverse_in,
+    message, gate_grad, x_grad, b_grad, c_grad, y_dots,
+):
+    groups = gain.shape[0] // GROUP
+    pieces = GROUP // 16
+    tokens = grad_own.shape[0]
+    for g in range(groups):
+        span = slice(g * GROUP, (g + 1) * GROUP)
+        states = slice(g * STATE, (g + 1) * STATE)
+        first = g * PER_GROUP
+        grad_mixed = dot(out_own[span, :], grad_own[...], ((1,), (1,)))
+        grad_mixed = grad_mixed + dot(out_far[span, :], grad_far[...], ((1,), (1,)))
+        inverse = inverse_in[g : g + 1, :]
+        gated = gated_in[span, :]
+        unit = gated * inverse
+        grad_unit = grad_mixed * gain[span, :]
+        mean = jnp.mean(grad_unit * unit, axis=0, keepdims=True)
+        grad_gated = inverse * (grad_unit - unit * mean)
+        gate_grad[:, span] = jnp.transpose(grad_gated * slope_in[span, :]).astype(bf16)
+        grad_y = grad_gated * silu_in[span, :]
+        grad_y_b = grad_y.astype(bf16)
+        grown = (grad_y * per_head(rows_in[0], first)).astype(bf16)
+        b_group, c_group = b_proj[:, states], c_proj[:, states]
+        block_state = dot(grown, c_group, ((1,), (0,))).astype(bf16)
+        message[g * pieces : (g + 1) * pieces, 0:16, :] = block_state.reshape(pieces, 16, STATE)
+        message[g * pieces : (g + 1) * pieces, 16:32, :] = local_in[span, :].reshape(
+            pieces, 16, STATE
+        )
+        x = x_in[span, :]
+        weights = jnp.zeros((tokens, tokens), f32)
+        inside = []
+        for r in range(PER_GROUP):
+            h = first + r
+            head = slice(r * HEAD_DIM, (r + 1) * HEAD_DIM)
+            inside.append(dot(grad_y_b[head, :], mix_in[h], ((1,), (0,))))
+            weights = weights + decay_in[h] * dot(grad_y_b[head, :], x[head, :], ((0,), (0,)))
+        inside = jnp.concatenate(inside, axis=0)
+        x_grad[span, :] = inside
+        weights = weights.astype(bf16)
+        c_grad[:, states] = (
+            dot(weights, b_group, ((1,), (0,)))
+            + dot(grown, entry[span, :].astype(bf16), ((0,), (0,)))
+        ).astype(bf16)
+        b_grad[:, states] = dot(weights, c_group, ((0,), (0,)))
+        dots = jnp.concatenate(head_sums(grad_gated * gated), axis=0)
+        y_dots[first : first + PER_GROUP, :] = dots
+        own = dots - jnp.concatenate(head_sums(x.astype(f32) * inside), axis=0)
+        own = jnp.broadcast_to(jnp.sum(own, axis=1, keepdims=True), (PER_GROUP, STATE))
+        total = rows_in[2][first : first + PER_GROUP, :]
+        per = pieces // PER_GROUP
+        zero = jnp.zeros((pieces, 2, STATE), f32)
+        extra = jnp.concatenate(
+            spread_parts(total, PER_GROUP, per) + spread_parts(own, PER_GROUP, per) + [zero],
+            axis=1,
+        )
+        message[g * pieces : (g + 1) * pieces, 32:40, :] = extra.astype(bf16)
+
+
+def backward(side, grad_own, grad_far, w_out, gain, saved, b_proj, c_proj, entry):
+    gated, silu, slope, mix, decay, x, local, rows, inverse = saved
+    tokens, half = grad_own.shape
+    inner = gain.shape[0]
+    heads = decay.shape[0]
+    wide = [gain, gated, silu, slope, mix, decay, x, b_proj, c_proj, entry, local, rows, inverse]
+    outs = [
+        ((inner // 16, 40, STATE), bf16),
+        ((tokens, inner), bf16),
+        ((inner, tokens), f32),
+        ((tokens, b_proj.shape[1]), f32),
+        ((tokens, b_proj.shape[1]), bf16),
+        ((heads, tokens), f32),
+    ]
+    return pl.pallas_call(
+        backward_kernel,
+        grid_spec=pltpu.PrefetchScalarGridSpec(
+            num_scalar_prefetch=1,
+            grid=(1,),
+            in_specs=[whole_block(tokens, half)] * 2
+            + [
+                pl.BlockSpec((inner, half), lambda i, side: (0, side[0])),
+                pl.BlockSpec((inner, half), lambda i, side: (0, 1 - side[0])),
+            ]
+            + [whole_block(*x.shape) for x in wide],
+            out_specs=[whole_block(*shape) for shape, _ in outs],
+        ),
+        out_shape=[jax.ShapeDtypeStruct(*x) for x in outs],
+        name="backward",
+    )(side, grad_own, grad_far, w_out, w_out, *wide)
+
+
+def final_kernel(back, b_proj, x_in, tail_in, rows_in, x_inside, y_dots, b_inside, x_grad, b_grad, decay_grad):
+    groups = x_in.shape[0] // GROUP
+    pieces = GROUP // 16
+    tokens = x_in.shape[1]
+    heads = y_dots.shape[0]
+    dots = []
+    for g in range(groups):
+        span = slice(g * GROUP, (g + 1) * GROUP)
+        states = slice(g * STATE, (g + 1) * STATE)
+        first = g * PER_GROUP
+        later = back[g * pieces : (g + 1) * pieces, 0:16, :].reshape(GROUP, STATE)
+        carried = dot(later, b_proj[:, states], ((1,), (1,)))
+        grad = x_inside[span, :] + carried * per_head(rows_in[1], first)
+        x_grad[:, span] = jnp.transpose(grad).astype(bf16)
+        b_grad[:, states] = (
+            b_inside[:, states] + dot(tail_in[span, :], later, ((0,), (0,)))
+        ).astype(bf16)
+        dots = dots + head_sums(x_in[span, :].astype(f32) * grad)
+    own = y_dots[...] - jnp.concatenate(dots, axis=0)
+    after = (grid_of(tokens, tokens, 0) >= grid_of(tokens, tokens, 1)).astype(f32)
+    extra = jnp.sum(back[:, 16:24, :].astype(f32), axis=1)
+    extra = jnp.sum(extra.reshape(heads, extra.shape[0] // heads, STATE), axis=1)
+    decay_grad[...] = exact_dot(own, after, ((1,), (0,))) + extra
+
+
+def final(back, b_proj, x, x_tail, rows, x_inside, y_dots, b_inside):
+    inner, tokens = x.shape
+    return whole_call(
+        final_kernel,
+        [
+            ((tokens, inner), bf16),
+            (b_proj.shape, bf16),
+            (y_dots.shape, f32),
+        ],
+        back, b_proj, x, x_tail, rows, x_inside, y_dots, b_inside,
+    )
 
 
 def body(
@@ -222,21 +519,18 @@
     entry_state,
 ):
     experts = lax.axis_size(SP)
-    tokens, width = mixer_output.shape
+    _, width = mixer_output.shape
     capacity = gate_pre.shape[1] // experts
     half = width // 2
     start = lax.axis_index("tp") * half
 
-    places = routing(expert_choice, experts, capacity)
+    side = lax.axis_index("tp")[None]
+    send_grads, either = route(
+        side, expert_choice.T, route_weight.T, layer_cotangent, experts * capacity
+    )
     hidden_half = lax.dynamic_slice_in_dim(mixer_output, start, half, 1)
     cotangent_half = lax.dynamic_slice_in_dim(layer_cotangent, start, half, 1)
-    weighted = (route_weight[:, :, None] * cotangent_half.astype(f32)[:, None, :]).astype(bf16)
-    either = places[:, 0] + places[:, 1]
-    send_grads = (
-        dot(places[:, 0], weighted[:, 0], ((0,), (0,)))
-        + dot(places[:, 1], weighted[:, 1], ((0,), (0,)))
-    ).astype(bf16)
-    send_hidden = dot(either, hidden_half, ((0,), (0,))).astype(bf16)
+    send_hidden = dot(either, hidden_half, ((1,), (0,))).astype(bf16)
     send_grads = send_grads.reshape(experts, capacity, half)
     send_hidden = send_hidden.reshape(experts, capacity, half)
     came_grads = lax.all_to_all(send_grads, SP, 0, 0, tiled=True)
@@ -244,7 +538,6 @@
     came_hidden = lax.all_to_all(send_hidden, SP, 0, 0, tiled=True)
     grads_own = came_grads.reshape(-1, half)
     grads_far = swapped(grads_own)
-    side = lax.axis_index("tp")[None]
     active, gate_grad, up_grad, rows_own, rows_far = expert_rows(
         side, grads_own, grads_far, gate_pre[0], up_pre[0], w_down[0], w_gate[0], w_up[0]
     )
@@ -255,7 +548,7 @@
     hidden_far = swapped(hidden_own)
     down_wgrad = down_weights(side, active, grads_own, grads_far)
     gate_wgrad, up_wgrad = tall_weights(side, gate_grad, up_grad, hidden_own, hidden_far)
-    moe_terms = dot(either, returned.reshape(-1, half), ((1,), (0,)))
+    moe_terms = dot(either, returned.reshape(-1, half), ((0,), (0,)))
     grad_own = (cotangent_half.astype(f32) + moe_terms).astype(bf16)
     grad_far = swapped(grad_own)
     grad_hidden = jnp.where(
@@ -264,117 +557,36 @@
         jnp.concatenate([grad_far, grad_own], axis=1),
     )
 
-    head_count = log_decay.shape[1]
-    group_count = b_proj.shape[1] // STATE
-    per_group = head_count // group_count
-    scan_heads = scan_in.reshape(tokens, head_count, HEAD_DIM)
-    b_groups = b_proj.reshape(tokens, group_count, STATE)
-    c_groups = c_proj.reshape(tokens, group_count, STATE)
-    x_float = scan_heads.astype(f32)
-    b_float = b_groups.astype(f32)
-    c_float = c_groups.astype(f32)
-    cumulative = jnp.cumsum(log_decay, axis=0)
-    growth = jnp.exp(cumulative)
-    tail_decay = jnp.exp(cumulative[-1][None, :] - cumulative)
-    locations = jnp.arange(tokens)
-    causal = locations[:, None] >= locations[None, :]
-    log_gaps = cumulative.T[:, :, None] - cumulative.T[:, None, :]
-    decay_mat = jnp.exp(jnp.where(causal[None], log_gaps, -jnp.inf))
-    inner_prod = jnp.einsum("tgn,sgn->gts", c_groups, b_groups, preferred_element_type=f32)
-    mix_weights = (jnp.repeat(inner_prod, per_group, axis=0) * decay_mat).astype(bf16)
-    state_groups = entry_state.reshape(group_count, per_group, HEAD_DIM, STATE)
-    y_inner = jnp.einsum("hts,shp->thp", mix_weights, scan_heads, preferred_element_type=f32)
-    y_carry = jnp.einsum("tgn,grpn->tgrp", c_float, state_groups).reshape(
-        tokens, head_count, HEAD_DIM
-    )
-    scan_out = y_inner + y_carry * growth[:, :, None]
-    gate_float = gate_in.astype(f32)
-    gate_sig = jax.nn.sigmoid(gate_float)
-    gate_silu = gate_float * gate_sig
-    gated = scan_out.reshape(tokens, -1) * gate_silu
-    grouped = gated.reshape(tokens, group_count, -1)
-    inv_rms = lax.rsqrt(jnp.mean(grouped * grouped, axis=-1, keepdims=True) + rms_epsilon)
-    unit = grouped * inv_rms
-    gain_groups = norm_gain.astype(f32).reshape(group_count, -1)
-    mixed = (unit * gain_groups).reshape(tokens, -1).astype(bf16)
-    x_tail = (x_float * tail_decay[:, :, None]).reshape(tokens, group_count, per_group, HEAD_DIM)
-    local_state = jnp.einsum("sgrp,sgn->grpn", x_tail, b_float)
-
-    line = lax.axis_size("sp_0")
-    spot = lax.axis_index("sp_0")
-    span = width // line
-    mixed_line = from_line([mixed] * line, "sp_0")
-    grads_line = from_line(
-        [
-            lax.dynamic_slice_in_dim(grad_hidden, lax.rem(spot + k, line) * span, span, 1)
-            for k in range(line)
-        ],
-        "sp_0",
-    )
-    product = dot(
-        jnp.concatenate(grads_line, axis=0), jnp.concatenate(mixed_line, axis=0), ((0,), (0,))
-    ).astype(bf16)
-    product = product.reshape(experts // line, -1, product.shape[1])
-    grad_out_proj = (
-        lax.all_to_all(product, ("sp_1", "sp_2"), 0, 0, tiled=True).astype(f32).sum(axis=0)
-    )
-
-    grad_mixed = jnp.einsum("td,id->ti", grad_hidden, w_out, preferred_element_type=f32)
-    grad_unit = grad_mixed.reshape(tokens, group_count, -1) * gain_groups
-    grad_grouped = inv_rms * (grad_unit - unit * jnp.mean(grad_unit * unit, axis=-1, keepdims=True))
-    grad_gated = grad_grouped.reshape(tokens, -1)
-    grad_gate_in = (
-        grad_gated
-        * scan_out.reshape(tokens, -1)
-        * gate_sig
-        * (1.0 + gate_float * (1.0 - gate_sig))
-    ).astype(bf16)
-    grad_y = (grad_gated * gate_silu).reshape(tokens, head_count, HEAD_DIM)
-    grad_y_b = grad_y.astype(bf16)
-    grad_x_inner = jnp.einsum("hts,thp->shp", mix_weights, grad_y_b, preferred_element_type=f32)
-    grad_weights = (
-        jnp.einsum("thp,shp->hts", grad_y_b, scan_heads, preferred_element_type=f32) * decay_mat
-    )
-    grad_weights = (
-        grad_weights.reshape(group_count, per_group, tokens, tokens).sum(axis=1).astype(bf16)
-    )
-    grad_c_inner = jnp.einsum("gts,sgn->tgn", grad_weights, b_groups, preferred_element_type=f32)
-    grad_b_inner = jnp.einsum("gts,tgn->sgn", grad_weights, c_groups, preferred_element_type=f32)
-    grown_grads = (grad_y * growth[:, :, None]).reshape(tokens, group_count, per_group, HEAD_DIM)
-    grad_c_carry = jnp.einsum("tgrp,grpn->tgn", grown_grads, state_groups)
-    block_state = jnp.einsum("tgrp,tgn->grpn", grown_grads, c_float)
-    y_dots = jnp.sum(grad_y * scan_out, axis=2)
-    local_grad = jnp.sum(y_dots - jnp.sum(x_float * grad_x_inner, axis=2), axis=0)
-
-    pieces = experts // head_count
-    first = (jnp.arange(experts) % pieces == 0).astype(f32)
-    scalars = [jnp.repeat(part, pieces) for part in three_parts(cumulative[-1])] + list(
-        three_parts(jnp.repeat(local_grad, pieces) * first)
-    )
-    sent = jnp.concatenate(
-        [
-            block_state.astype(bf16).reshape(experts, -1, STATE),
-            local_state.astype(bf16).reshape(experts, -1, STATE),
-            spread(scalars, experts),
-        ],
-        axis=1,
-    )
-    later, carried = scan_piece(lax.all_to_all(sent, SP, 0, 0, tiled=True))
+    inner = scan_in.shape[1]
+    gain = norm_gain.astype(f32)[:, None]
+    entry = entry_state.reshape(inner, STATE)
+    mixed, *saved, x_tail, local, rows, inverse = forward(
+        scan_in, gate_in, b_proj, c_proj, log_decay.T, entry, gain
+    )
+    gated, silu, slope, mix, decay, x = saved
+    message, grad_gate_in, x_inside, b_inside, grad_c_proj, y_dots = backward(
+        side, grad_own, grad_far, w_out, gain,
+        (gated, silu, slope, mix, decay, x, local, rows, inverse), b_proj, c_proj, entry,
+    )
+    came_states = lax.all_to_all(message, SP, 0, 0, tiled=True)
+    later, carried = scan_piece(came_states)
     back = jnp.concatenate([later, spread(list(three_parts(carried)), experts)], axis=1)
     back = lax.all_to_all(back, SP, 0, 0, tiled=True)
-    later_groups = back[:, :16].reshape(group_count, per_group, HEAD_DIM, STATE).astype(f32)
-    later_grad = back[:, 16:19, 0].astype(f32).sum(axis=1).reshape(head_count, pieces).sum(axis=1)
-
-    grad_x_carry = jnp.einsum("sgn,grpn->sgrp", b_float, later_groups).reshape(
-        tokens, head_count, HEAD_DIM
-    )
-    grad_x = grad_x_inner + grad_x_carry * tail_decay[:, :, None]
-    grad_b_carry = jnp.einsum("sgrp,grpn->sgn", x_tail, later_groups)
-    grad_a = y_dots - jnp.sum(x_float * grad_x, axis=2)
-    grad_log_decay = jnp.flip(jnp.cumsum(jnp.flip(grad_a, 0), axis=0), 0) + later_grad[None, :]
-    grad_scan_in = grad_x.reshape(tokens, -1).astype(bf16)
-    grad_b_proj = (grad_b_inner + grad_b_carry).reshape(tokens, -1).astype(bf16)
-    grad_c_proj = (grad_c_inner + grad_c_carry).reshape(tokens, -1).astype(bf16)
+    grad_scan_in, grad_b_proj, decay_grad = final(
+        back, b_proj, x, x_tail, rows, x_inside, y_dots, b_inside
+    )
+    grad_log_decay = decay_grad.T
+
+    line = lax.axis_size("sp_0")
+    mixed_line = from_line([mixed] * line, "sp_0")
+    grads_line = from_line(pieces_for(grad_hidden, "sp_0", 1), "sp_0")
+    grad_out_proj = dot(
+        jnp.concatenate(grads_line, axis=0), jnp.concatenate(mixed_line, axis=1), ((0,), (1,))
+    )
+    for axis in ("sp_1", "sp_2"):
+        parts = from_line(pieces_for(grad_out_proj.astype(bf16), axis, 0), axis)
+        grad_out_proj = sum(part.astype(f32) for part in parts)
+
     return (
         gate_wgrad[None],
         up_wgrad[None],

time: 198 us -> 185 us (0.934)
  blocking collectives: 0 us -> 23 us
  Pallas kernels: 19.3 us -> 38.3 us
  other arithmetic: 21.5 us -> 5.66 us
  matrix products: 18.6 us -> 4.85 us
  local copies, waits for them, and re-layouts: 17.8 us -> 6.24 us
  starting transfers between devices: 53.6 us -> 47.1 us
  waiting for transfers between devices: 64.4 us -> 58.4 us
    all_to_all x3 -> x1, waiting for transfers between devices: 26.2 us -> 0.01 us  [body(): came_states = lax.all_to_all(message, SP, 0, 0, tiled=True)]
    all_to_all x0 -> x1, blocking collectives: none -> 23 us  [body(): lax.all_to_all(summed.reshape(experts, capacity, half), SP, 0, 0, tiled=T...]
    pallas_call x0 -> x4, Pallas kernels: none -> 19.1 us  [the longest x1 8.83 us: backward(): pl.pallas_call(backward_kernel, grid_spec=pltpu.PrefetchScalarGridSpec(nu...]
    ppermute x6 -> x12, waiting for transfers between devices: 2.63 us -> 21.6 us  [from_line(): lax.ppermute(parts[k], axis, [(i, (i + k) % size) for i in range(size)])]
    all_to_all x3 -> x1, starting transfers between devices: 16.1 us -> 5.08 us  [body(): came_states = lax.all_to_all(message, SP, 0, 0, tiled=True)]
    dot_general x13 -> x0, matrix products: 9.36 us -> none  [the longest x1 3.7 us: body(): jnp.einsum('td,id->ti', grad_hidden, w_out, preferred_element_type=f32)]
    ppermute x6 -> x12, starting transfers between devices: 10.3 us -> 18 us  [from_line(): lax.ppermute(parts[k], axis, [(i, (i + k) % size) for i in range(size)])]
    reduce_sum x11 -> x1, other arithmetic: 6.3 us -> 0.56 us  [scan_piece(): sums = jnp.where(lead, came[:, 35:38, 0].astype(f32).sum(axis=1), 0.0)]
  transfers between devices with their start and end apart: 16 -> 20, of which waited for: 7 -> 6; matrix products, arithmetic and copies ran while one was open for 24% -> 7% of each run, Pallas kernels for 5% -> 13%
where the time goes in v3:
time: 185 us
  waiting for transfers between devices  58.4 us (32%)
  starting transfers between devices  47.1 us (25%)
  Pallas kernels  38.3 us (21%)
  blocking collectives  23 us (12%)
  local copies, waits for them, and re-layouts  6.24 us (3%)
  other arithmetic  5.66 us (3%)
  matrix products  4.85 us (3%)
    all_to_all x1, blocking collectives, body(): lax.all_to_all(summed.reshape(experts, capacity, half), SP, 0, 0, tiled=T...  23 us
    ppermute x12, waiting for transfers between devices, from_line(): lax.ppermute(parts[k], axis, [(i, (i + k) % size) for i in range(size)])  21.6 us
    ppermute x12, starting transfers between devices, from_line(): lax.ppermute(parts[k], axis, [(i, (i + k) % size) for i in range(size)])  18 us
    all_to_all x1, waiting for transfers between devices, body(): came_grads = lax.all_to_all(send_grads, SP, 0, 0, tiled=True)  17.5 us
    all_to_all x1, waiting for transfers between devices, body(): came_hidden = lax.all_to_all(send_hidden, SP, 0, 0, tiled=True)  16.6 us
    all_to_all x1, starting transfers between devices, body(): came_grads = lax.all_to_all(send_grads, SP, 0, 0, tiled=True)  11.7 us
    pallas_call x1, Pallas kernels, expert_rows(): pl.pallas_call(expert_rows_kernel, grid_spec=pltpu.PrefetchScalarGridSpec...  9.2 us
    pallas_call x1, Pallas kernels, backward(): pl.pallas_call(backward_kernel, grid_spec=pltpu.PrefetchScalarGridSpec(nu...  8.83 us
  transfers between devices with their start and end apart: 20, of which 6 were waited for; matrix products, arithmetic and copies ran while one was open for 7% of the time, Pallas kernels for 13%

profile of v3, /device:TPU:0, one launch (start us, length us, event | category | flops | bytes accessed | tf_op | source)
XLA Modules:
  0.0 184.5 jit_solution(8841040539775104529)
XLA Ops:
  0.7 3.1 %route.1 = (bf16[512,1024]{1,0:T(8,128)(2,1)}, bf16[512,128]{1,0:T(8,128)(2,1)}) custom-call(s32[1]{0:T(128)} %bitcast.side, s32[2,128]{1,0:T(2,128)} %bitcast.74, f32[2,128]{1,0:T(2,128)} %bitcast.75, bf16[128,2048]{1,0:T(8,128)(2,1)} %cotangent.1), custom_call_target="tpu_custom_call" | custom-call | tf_op jit(solution)/shard_map/route/pallas_call | solution.py:239
  3.7 11.7 %all-to-all-start = ((bf16[64,8,1024]{2,1,0:T(8,128)(2,1)}), bf16[64,8,1024]{2,1,0:T(8,128)(2,1)S(1)}, u32[]{:S(2)}, u32[]{:S(2)}) async-start(bf16[64,8,1024]{2,1,0:T(8,128)(2,1)} %bitcast.69), calls=%async_computation | async-start | bytes 2097152 | tf_op jit(solution)/shard_map/all_to_all | solution.py:536
  16.8 17.5 %all-to-all-done = bf16[64,8,1024]{2,1,0:T(8,128)(2,1)S(1)} async-done(((bf16[64,8,1024]{2,1,0:T(8,128)(2,1)}), bf16[64,8,1024]{2,1,0:T(8,128)(2,1)S(1)}, u32[]{:S(2)}, u32[]{:S(2)}) %all-to-all-start) | async-done | bytes 1048608 | tf_op jit(solution)/shard_map/all_to_all | solution.py:536
  34.3 2.7 %collective-permute-done.other = bf16[512,1024]{1,0:T(8,128)(2,1)S(1)} collective-permute-done((bf16[512,1024]{1,0:T(8,128)(2,1)S(1)}, bf16[512,1024]{1,0:T(8,128)(2,1)S(1)}, u32[]{:S(2)}, u32[]{:S(2)}) %collective-permute-start) | collective-permute-done | bytes 1048608 | tf_op jit(solution)/shard_map/ppermute | solution.py:27
  37.9 9.2 %expert_rows.1 = (bf16[512,512]{1,0:T(8,128)(2,1)}, bf16[512,512]{1,0:T(8,128)(2,1)}, bf16[512,512]{1,0:T(8,128)(2,1)}, bf16[512,1024]{1,0:T(8,128)(2,1)}, bf16[512,1024]{1,0:T(8,128)(2,1)}) custom-call(s32[1]{0:T(128)} %bitcast.side, bf16[512,1024]{1,0:T(8,128)(2,1)} %bitcast.51, bf16[512,1024]{1,0:T(8,128)(2,1)} %copy-done.2, bf16[512,512]{1,0:T(8,128)(2,1)} %bitcast.70, ...), custom_call_target="tpu_custom_call" | custom-call | tf_op jit(solution)/shard_map/expert_rows/pallas_call | solution.py:99
  47.3 4.7 %all-to-all-start.1 = ((bf16[64,8,1024]{2,1,0:T(8,128)(2,1)}), bf16[64,8,1024]{2,1,0:T(8,128)(2,1)S(1)}, u32[]{:S(2)}, u32[]{:S(2)}) async-start(bf16[64,8,1024]{2,1,0:T(8,128)(2,1)} %fusion), calls=%async_computation.1 | async-start | bytes 2097152 | tf_op jit(solution)/shard_map/all_to_all | solution.py:538
  53.0 2.0 %add_convert_fusion = bf16[512,1024]{1,0:T(8,128)(2,1)S(1)} fusion(bf16[512,1024]{1,0:T(8,128)(2,1)} %copy-done.7, bf16[512,1024]{1,0:T(8,128)(2,1)} %get-tuple-element.47), kind=kLoop, calls=%fused_computation.1 | loop fusion | flops 2097152 | bytes 3145728 | tf_op jit(solution)/shard_map/convert_element_type | solution.py:544
  55.0 16.6 %all-to-all-done.1 = bf16[64,8,1024]{2,1,0:T(8,128)(2,1)S(1)} async-done(((bf16[64,8,1024]{2,1,0:T(8,128)(2,1)}), bf16[64,8,1024]{2,1,0:T(8,128)(2,1)S(1)}, u32[]{:S(2)}, u32[]{:S(2)}) %all-to-all-start.1) | async-done | bytes 1048608 | tf_op jit(solution)/shard_map/all_to_all | solution.py:538
  71.6 23.0 %all_to_all.25 = bf16[64,8,1024]{2,1,0:T(8,128)(2,1)S(1)} all-to-all(bf16[64,8,1024]{2,1,0:T(8,128)(2,1)S(1)} %bitcast.59), channel_id=1, replica_groups=mesh['sp_0'=4,'sp_1'=4,'sp_2'=4,'tp'=2] {'sp_0','sp_1','sp_2'}, dimensions={0} | all-to-all | bytes 2097152 | tf_op jit(solution)/shard_map/all_to_all | solution.py:546
  96.1 4.6 %shard_map.232 = (bf16[1024,128]{1,0:T(8,128)(2,1)}, f32[1024,128]{1,0:T(8,128)}, f32[1024,128]{1,0:T(8,128)}, f32[1024,128]{1,0:T(8,128)}, bf16[16,128,128]{2,1...) custom-call(bf16[128,1024]{1,0:T(8,128)(2,1)} %scan_in.1, ...), custom_call_target="tpu_custom_call" | custom-call | tf_op jit(solution)/shard_map/pallas_call | solution.py:334
  101.1 1.8 %collective-permute-start.8 = (bf16[1024,128]{1,0:T(8,128)(2,1)}, bf16[1024,128]{1,0:T(8,128)(2,1)S(1)}, u32[]{:S(2)}, u32[]{:S(2)}) collective-permute-start(bf16[1024,128]{1,0:T(8,128)(2,1)} %get-tuple-element.55), channel_id=1, source_target_pairs={{0,64},{32,96},{64,0},{96,32},{1,65},{33,97},{65,1},{97,33},{2,66}... | collective-permute-start | bytes 786440 | tf_op jit(solution)/shard_map/ppermute | solution.py:33
  105.4 2.0 %collective-permute-start.5 = (bf16[128,512]{1,0:T(8,128)(2,1)S(1)}, bf16[128,512]{1,0:T(8,128)(2,1)S(1)}, u32[]{:S(2)}, u32[]{:S(2)}) collective-permute-start(bf16[128,512]{1,0:T(8,128)(2,1)S(1)} %get-tuple-element.87), channel_id=1, source_target_pairs={{0,64},{32,96},{64,0},{96,32},{1,65},{33,97},{65,1},{97,33},{2,66}... | collective-permute-start | bytes 393224 | tf_op jit(solution)/shard_map/ppermute | solution.py:33
  107.4 9.5 %collective-permute-done.7 = bf16[1024,128]{1,0:T(8,128)(2,1)S(1)} collective-permute-done((bf16[1024,128]{1,0:T(8,128)(2,1)}, bf16[1024,128]{1,0:T(8,128)(2,1)S(1)}, u32[]{:S(2)}, u32[]{:S(2)}) %collective-permute-start.7) | collective-permute-done | bytes 262176 | tf_op jit(solution)/shard_map/ppermute | solution.py:33
  116.9 8.8 %backward.1 = (bf16[64,40,128]{2,1,0:T(8,128)(2,1)}, bf16[128,1024]{1,0:T(8,128)(2,1)}, f32[1024,128]{1,0:T(8,128)}, f32[128,512]{1,0:T(8,128)}, bf16[128,512]{1,0:T(8,128)(2,1)}, /*index=5*/f32[16,128]{1,0:T(8,128)}) custom-call(s32[1]{0:T(128)} %bitcast.side, bf16[128,1024]{1,0:T(8,128)(2,1)} %copy-done.4, bf16[128,1024]{1,0:T(8,128)(2,1)} %copy-done.8, ...), custom_call_target="tpu_custom_call" | custom-call | tf_op jit(solution)/shard_map/backward/pallas_call | solution.py:446
  125.8 5.1 %all-to-all-start.3 = ((bf16[64,40,128]{2,1,0:T(8,128)(2,1)}), bf16[64,40,128]{2,1,0:T(8,128)(2,1)S(1)}, u32[]{:S(2)}, u32[]{:S(2)}) async-start(bf16[64,40,128]{2,1,0:T(8,128)(2,1)} %get-tuple-element.65), calls=%async_computation.3 | async-start | bytes 1310720 | tf_op jit(solution)/shard_map/all_to_all | solution.py:571
  131.6 2.1 %convolution_convert_fusion.1 = bf16[512,1024]{1,0:T(8,128)(2,1)S(1)} fusion(bf16[1024,128]{1,0:T(8,128)(2,1)} %collective-permute-done.9, bf16[1024,128]{1,0:T(8,128)(2,1)} %copy-done.12, bf16[1024,128]{1,0:T(8,128)(2,1)} %copy-done.11, bf16[1024,128]{1,0:T(8,128)(2,1)} %get-tuple-element.55, bf16[128,512]{1,0:T(8,128)(2,1)} %collective-permute-done.6, ...), kind=kOutput, calls=%fused_computation.3 | convolution fusion | flops 543686656 | bytes 2621440 | tf_op jit(solution)/shard_map/dot_general | solution.py:23
  136.1 2.7 %collective-permute-start.11 = (bf16[128,1024]{1,0:T(8,128)(2,1)}, bf16[128,1024]{1,0:T(8,128)(2,1)}, u32[]{:S(2)}, u32[]{:S(2)}) collective-permute-start(bf16[128,1024]{1,0:T(8,128)(2,1)} %get-tuple-element.80), channel_id=1, source_target_pairs={{0,16},{8,24},{16,0},{24,8},{1,17},{9,25},{17,1},{25,9},{2,18},{10... | collective-permute-start | bytes 786440 | tf_op jit(solution)/shard_map/ppermute | solution.py:33
  140.3 6.4 %collective-permute-done.10 = bf16[128,1024]{1,0:T(8,128)(2,1)} collective-permute-done((bf16[128,1024]{1,0:T(8,128)(2,1)}, bf16[128,1024]{1,0:T(8,128)(2,1)}, u32[]{:S(2)}, u32[]{:S(2)}) %collective-permute-start.10) | collective-permute-done | bytes 262176 | tf_op jit(solution)/shard_map/ppermute | solution.py:33
  146.7 5.6 %collective-permute-done.11 = bf16[128,1024]{1,0:T(8,128)(2,1)} collective-permute-done((bf16[128,1024]{1,0:T(8,128)(2,1)}, bf16[128,1024]{1,0:T(8,128)(2,1)}, u32[]{:S(2)}, u32[]{:S(2)}) %collective-permute-start.11) | collective-permute-done | bytes 262176 | tf_op jit(solution)/shard_map/ppermute | solution.py:33
  157.1 7.5 %all-to-all-start.4 = ((bf16[64,24,128]{2,1,0:T(8,128)(2,1)}), bf16[64,24,128]{2,1,0:T(8,128)(2,1)S(1)}, u32[]{:S(2)}, u32[]{:S(2)}) async-start(bf16[64,24,128]{2,1,0:T(8,128)(2,1)} %pad_maximum_fusion), calls=%async_computation.4 | async-start | bytes 786432 | tf_op jit(solution)/shard_map/all_to_all | solution.py:574
  166.3 2.7 %collective-permute-start.14 = (bf16[32,1024]{1,0:T(8,128)(2,1)S(1)}, bf16[32,1024]{1,0:T(8,128)(2,1)S(1)}, u32[]{:S(2)}, u32[]{:S(2)}) collective-permute-start(bf16[32,1024]{1,0:T(8,128)(2,1)S(1)} %get-tuple-element.91), channel_id=1, source_target_pairs={{0,4},{2,6},{4,0},{6,2},{1,5},{3,7},{5,1},{7,3},{8,12},{10,14},{12... | collective-permute-start | bytes 196616 | tf_op jit(solution)/shard_map/ppermute | solution.py:33
  170.4 4.2 %down_weights.1 = bf16[512,2048]{1,0:T(8,128)(2,1)} custom-call(s32[1]{0:T(128)} %bitcast.side, bf16[512,512]{1,0:T(8,128)(2,1)} %get-tuple-element.53.active, bf16[512,1024]{1,0:T(8,128)(2,1)} %bitcast.52, bf16[512,1024]{1,0:T(8,128)(2,1)} %copy-done.2), custom_call_target="tpu_custom_call" | custom-call | tf_op jit(solution)/shard_map/down_weights/pallas_call | solution.py:143
  174.6 5.9 %tall_weights.1 = (bf16[2048,512]{1,0:T(8,128)(2,1)}, bf16[2048,512]{1,0:T(8,128)(2,1)}) custom-call(s32[1]{0:T(128)} %bitcast.side, bf16[512,512]{1,0:T(8,128)(2,1)} %get-tuple-element.45.gate_grad, bf16[512,512]{1,0:T(8,128)(2,1)} %get-tuple-element.46.up_grad, bf16[512,1024]{1,0:T(8,128)(2,1)} %bitcast.61, bf16[512,1024]{1,0:T(8,128)(2,1)} %collective-permute-done.2.other), custom_call_target="tpu_custom_call" | custom-call | tf_op jit(solution)/shard_map/tall_weights/pallas_call | solution.py:159
  181.9 2.6 %shard_map.233 = (bf16[128,1024]{1,0:T(8,128)(2,1)}, bf16[128,512]{1,0:T(8,128)(2,1)}, f32[16,128]{1,0:T(8,128)}) custom-call(bf16[64,24,128]{2,1,0:T(8,128)(2,1)} %copy-done.5, bf16[128,512]{1,0:T(8,128)(2,1)} %b_proj.5, bf16[1024,128]{1,0:T(8,128)(2,1)} %get-tuple-element.61.x_in, bf16[1024,128]{1,0:T(8,128)(2,1)} %get-tuple-element.66.tail_in, ...), custom_call_target="tpu_custom_call" | custom-call | tf_op jit(solution)/shard_map/pallas_call | solution.py:334
  (81 shorter events, 21.7 us)
Async XLA Ops:
  0.6 14.8 %copy-start = (bf16[128,2048]{1,0:T(8,128)(2,1)S(1)}, bf16[128,2048]{1,0:T(8,128)(2,1)}, u32[]{:S(2)}) copy-start(bf16[128,2048]{1,0:T(8,128)(2,1)} %param.17) | copy-start | bytes 1572868
  3.7 30.6 %all-to-all-start = ((bf16[64,8,1024]{2,1,0:T(8,128)(2,1)}), bf16[64,8,1024]{2,1,0:T(8,128)(2,1)S(1)}, u32[]{:S(2)}, u32[]{:S(2)}) async-start(bf16[64,8,1024]{2,1,0:T(8,128)(2,1)} %bitcast.69), calls=%async_computation | async-start | bytes 2097152 | tf_op jit(solution)/shard_map/all_to_all | solution.py:536
  34.3 2.7 %collective-permute-start = (bf16[512,1024]{1,0:T(8,128)(2,1)S(1)}, bf16[512,1024]{1,0:T(8,128)(2,1)S(1)}, u32[]{:S(2)}, u32[]{:S(2)}) collective-permute-start(bf16[512,1024]{1,0:T(8,128)(2,1)S(1)} %bitcast.50), channel_id=1, source_target_pairs={{0,1},{1,0},{2,3},{3,2},{4,5},{5,4},{6,7},{7,6},{8,9},{9,8},{10,11... | collective-permute-start | bytes 3145736 | tf_op jit(solution)/shard_map/ppermute | solution.py:27
  47.1 4.9 %collective-permute-start.1 = (bf16[512,1024]{1,0:T(8,128)(2,1)}, bf16[512,1024]{1,0:T(8,128)(2,1)S(1)}, u32[]{:S(2)}, u32[]{:S(2)}) collective-permute-start(bf16[512,1024]{1,0:T(8,128)(2,1)} %get-tuple-element.48), channel_id=1, source_target_pairs={{0,1},{1,0},{2,3},{3,2},{4,5},{5,4},{6,7},{7,6},{8,9},{9,8},{10,11... | collective-permute-start | bytes 3145736 | tf_op jit(solution)/shard_map/ppermute | solution.py:27
  47.3 24.4 %all-to-all-start.1 = ((bf16[64,8,1024]{2,1,0:T(8,128)(2,1)}), bf16[64,8,1024]{2,1,0:T(8,128)(2,1)S(1)}, u32[]{:S(2)}, u32[]{:S(2)}) async-start(bf16[64,8,1024]{2,1,0:T(8,128)(2,1)} %fusion), calls=%async_computation.1 | async-start | bytes 2097152 | tf_op jit(solution)/shard_map/all_to_all | solution.py:538
  53.0 41.7 %copy-start.6 = (bf16[128,2048]{1,0:T(8,128)(2,1)S(1)}, bf16[128,2048]{1,0:T(8,128)(2,1)}, u32[]{:S(2)}) copy-start(bf16[128,2048]{1,0:T(8,128)(2,1)} %cotangent.1) | copy-start | bytes 1572868
  55.0 40.1 %copy-start.10 = (bf16[1024]{0:T(1024)(128)(2,1)S(1)}, bf16[1024]{0:T(1024)(128)(2,1)}, u32[]{:S(2)}) copy-start(bf16[1024]{0:T(1024)(128)(2,1)} %param.27) | copy-start | bytes 6148
  71.6 68.6 %copy-start.3 = (bf16[64,8,1024]{2,1,0:T(8,128)(2,1)}, bf16[64,8,1024]{2,1,0:T(8,128)(2,1)S(1)}, u32[]{:S(2)}) copy-start(bf16[64,8,1024]{2,1,0:T(8,128)(2,1)S(1)} %all-to-all-done.1) | copy-start | bytes 3145732
  95.0 9.0 %collective-permute-start.3 = (bf16[128,1024]{1,0:T(8,128)(2,1)S(1)}, bf16[128,1024]{1,0:T(8,128)(2,1)S(1)}, u32[]{:S(2)}, u32[]{:S(2)}) collective-permute-start(bf16[128,1024]{1,0:T(8,128)(2,1)S(1)} %fusion.1.grad_own), channel_id=1, source_target_pairs={{0,1},{1,0},{2,3},{3,2},{4,5},{5,4},{6,7},{7,6},{8,9},{9,8},{10,11... | collective-permute-start | bytes 786440 | tf_op jit(solution)/shard_map/ppermute | solution.py:27
  100.7 16.2 %collective-permute-start.7 = (bf16[1024,128]{1,0:T(8,128)(2,1)}, bf16[1024,128]{1,0:T(8,128)(2,1)S(1)}, u32[]{:S(2)}, u32[]{:S(2)}) collective-permute-start(bf16[1024,128]{1,0:T(8,128)(2,1)} %get-tuple-element.55), channel_id=1, source_target_pairs={{0,32},{32,64},{64,96},{96,0},{1,33},{33,65},{65,97},{97,1},{2,34}... | collective-permute-start | bytes 786440 | tf_op jit(solution)/shard_map/ppermute | solution.py:33
  101.1 29.7 %collective-permute-start.8 = (bf16[1024,128]{1,0:T(8,128)(2,1)}, bf16[1024,128]{1,0:T(8,128)(2,1)S(1)}, u32[]{:S(2)}, u32[]{:S(2)}) collective-permute-start(bf16[1024,128]{1,0:T(8,128)(2,1)} %get-tuple-element.55), channel_id=1, source_target_pairs={{0,64},{32,96},{64,0},{96,32},{1,65},{33,97},{65,1},{97,33},{2,66}... | collective-permute-start | bytes 786440 | tf_op jit(solution)/shard_map/ppermute | solution.py:33
  103.0 27.9 %collective-permute-start.9 = (bf16[1024,128]{1,0:T(8,128)(2,1)}, bf16[1024,128]{1,0:T(8,128)(2,1)}, u32[]{:S(2)}, u32[]{:S(2)}) collective-permute-start(bf16[1024,128]{1,0:T(8,128)(2,1)} %get-tuple-element.55), channel_id=1, source_target_pairs={{0,96},{32,0},{64,32},{96,64},{1,97},{33,1},{65,33},{97,65},{2,98}... | collective-permute-start | bytes 786440 | tf_op jit(solution)/shard_map/ppermute | solution.py:33
  104.2 26.7 %collective-permute-start.4 = (bf16[128,512]{1,0:T(8,128)(2,1)S(1)}, bf16[128,512]{1,0:T(8,128)(2,1)S(1)}, u32[]{:S(2)}, u32[]{:S(2)}) collective-permute-start(bf16[128,512]{1,0:T(8,128)(2,1)S(1)} %get-tuple-element.88), channel_id=1, source_target_pairs={{0,32},{32,64},{64,96},{96,0},{1,33},{33,65},{65,97},{97,1},{2,34}... | collective-permute-start | bytes 393224 | tf_op jit(solution)/shard_map/ppermute | solution.py:33
  105.4 25.5 %collective-permute-start.5 = (bf16[128,512]{1,0:T(8,128)(2,1)S(1)}, bf16[128,512]{1,0:T(8,128)(2,1)S(1)}, u32[]{:S(2)}, u32[]{:S(2)}) collective-permute-start(bf16[128,512]{1,0:T(8,128)(2,1)S(1)} %get-tuple-element.87), channel_id=1, source_target_pairs={{0,64},{32,96},{64,0},{96,32},{1,65},{33,97},{65,1},{97,33},{2,66}... | collective-permute-start | bytes 393224 | tf_op jit(solution)/shard_map/ppermute | solution.py:33
  116.9 14.0 %collective-permute-start.6 = (bf16[128,512]{1,0:T(8,128)(2,1)S(1)}, bf16[128,512]{1,0:T(8,128)(2,1)}, u32[]{:S(2)}, u32[]{:S(2)}) collective-permute-start(bf16[128,512]{1,0:T(8,128)(2,1)S(1)} %get-tuple-element.86), channel_id=1, source_target_pairs={{0,96},{32,0},{64,32},{96,64},{1,97},{33,1},{65,33},{97,65},{2,98}... | collective-permute-start | bytes 393224 | tf_op jit(solution)/shard_map/ppermute | solution.py:33
  125.8 27.9 %all-to-all-start.3 = ((bf16[64,40,128]{2,1,0:T(8,128)(2,1)}), bf16[64,40,128]{2,1,0:T(8,128)(2,1)S(1)}, u32[]{:S(2)}, u32[]{:S(2)}) async-start(bf16[64,40,128]{2,1,0:T(8,128)(2,1)} %get-tuple-element.65), calls=%async_computation.3 | async-start | bytes 1310720 | tf_op jit(solution)/shard_map/all_to_all | solution.py:571
  134.6 12.1 %collective-permute-start.10 = (bf16[128,1024]{1,0:T(8,128)(2,1)}, bf16[128,1024]{1,0:T(8,128)(2,1)}, u32[]{:S(2)}, u32[]{:S(2)}) collective-permute-start(bf16[128,1024]{1,0:T(8,128)(2,1)} %get-tuple-element.78), channel_id=1, source_target_pairs={{0,8},{8,16},{16,24},{24,0},{1,9},{9,17},{17,25},{25,1},{2,10},{10... | collective-permute-start | bytes 786440 | tf_op jit(solution)/shard_map/ppermute | solution.py:33
  136.1 16.2 %collective-permute-start.11 = (bf16[128,1024]{1,0:T(8,128)(2,1)}, bf16[128,1024]{1,0:T(8,128)(2,1)}, u32[]{:S(2)}, u32[]{:S(2)}) collective-permute-start(bf16[128,1024]{1,0:T(8,128)(2,1)} %get-tuple-element.80), channel_id=1, source_target_pairs={{0,16},{8,24},{16,0},{24,8},{1,17},{9,25},{17,1},{25,9},{2,18},{10... | collective-permute-start | bytes 786440 | tf_op jit(solution)/shard_map/ppermute | solution.py:33
  138.8 13.5 %collective-permute-start.12 = (bf16[128,1024]{1,0:T(8,128)(2,1)S(1)}, bf16[128,1024]{1,0:T(8,128)(2,1)}, u32[]{:S(2)}, u32[]{:S(2)}) collective-permute-start(bf16[128,1024]{1,0:T(8,128)(2,1)S(1)} %get-tuple-element.79), channel_id=1, source_target_pairs={{0,24},{8,0},{16,8},{24,16},{1,25},{9,1},{17,9},{25,17},{2,26},{10... | collective-permute-start | bytes 786440 | tf_op jit(solution)/shard_map/ppermute | solution.py:33
  140.3 34.3 %collective-permute-start.2 = (bf16[512,1024]{1,0:T(8,128)(2,1)S(1)}, bf16[512,1024]{1,0:T(8,128)(2,1)}, u32[]{:S(2)}, u32[]{:S(2)}) collective-permute-start(bf16[512,1024]{1,0:T(8,128)(2,1)S(1)} %bitcast.60), channel_id=1, source_target_pairs={{0,1},{1,0},{2,3},{3,2},{4,5},{5,4},{6,7},{7,6},{8,9},{9,8},{10,11... | collective-permute-start | bytes 3145736 | tf_op jit(solution)/shard_map/ppermute | solution.py:27
  157.1 24.1 %all-to-all-start.4 = ((bf16[64,24,128]{2,1,0:T(8,128)(2,1)}), bf16[64,24,128]{2,1,0:T(8,128)(2,1)S(1)}, u32[]{:S(2)}, u32[]{:S(2)}) async-start(bf16[64,24,128]{2,1,0:T(8,128)(2,1)} %pad_maximum_fusion), calls=%async_computation.4 | async-start | bytes 786432 | tf_op jit(solution)/shard_map/all_to_all | solution.py:574
  164.6 15.8 %collective-permute-start.13 = (bf16[32,1024]{1,0:T(8,128)(2,1)S(1)}, bf16[32,1024]{1,0:T(8,128)(2,1)S(1)}, u32[]{:S(2)}, u32[]{:S(2)}) collective-permute-start(bf16[32,1024]{1,0:T(8,128)(2,1)S(1)} %get-tuple-element.89), channel_id=1, source_target_pairs={{0,2},{2,4},{4,6},{6,0},{1,3},{3,5},{5,7},{7,1},{8,10},{10,12},{12... | collective-permute-start | bytes 196616 | tf_op jit(solution)/shard_map/ppermute | solution.py:33
  166.3 14.2 %collective-permute-start.14 = (bf16[32,1024]{1,0:T(8,128)(2,1)S(1)}, bf16[32,1024]{1,0:T(8,128)(2,1)S(1)}, u32[]{:S(2)}, u32[]{:S(2)}) collective-permute-start(bf16[32,1024]{1,0:T(8,128)(2,1)S(1)} %get-tuple-element.91), channel_id=1, source_target_pairs={{0,4},{2,6},{4,0},{6,2},{1,5},{3,7},{5,1},{7,3},{8,12},{10,14},{12... | collective-permute-start | bytes 196616 | tf_op jit(solution)/shard_map/ppermute | solution.py:33
  168.9 11.5 %collective-permute-start.15 = (bf16[32,1024]{1,0:T(8,128)(2,1)S(1)}, bf16[32,1024]{1,0:T(8,128)(2,1)S(1)}, u32[]{:S(2)}, u32[]{:S(2)}) collective-permute-start(bf16[32,1024]{1,0:T(8,128)(2,1)S(1)} %get-tuple-element.90), channel_id=1, source_target_pairs={{0,6},{2,0},{4,2},{6,4},{1,7},{3,1},{5,3},{7,5},{8,14},{10,8},{12,... | collective-permute-start | bytes 196616 | tf_op jit(solution)/shard_map/ppermute | solution.py:33
  (10 other events, 49.4 us)

commit v4 on v3

--- a/solution.py
+++ b/solution.py
@@ -280,7 +280,7 @@
 def forward_kernel(
     scan_in, gate_in, b_proj, c_proj, log_decay, entry, gain,
     mixed, gated_out, silu_out, slope_out, mix_out, decay_out, x_out, tail_out, local_out,
-    rows_out, inverse_out,
+    rows_out, inverse_out, carry_out,
 ):
     tokens = scan_in.shape[0]
     groups = scan_in.shape[1] // GROUP
@@ -291,9 +291,7 @@
     total = cum_rows[:, tokens - 1 :]
     growth = jnp.exp(cum_rows)
     tail = jnp.exp(total - cum_rows)
-    rows_out[0] = growth
-    rows_out[1] = tail
-    rows_out[2] = jnp.broadcast_to(total, growth.shape)
+    totals = jnp.broadcast_to(total, growth.shape)
     causal = down >= across
     for g in range(groups):
         span = slice(g * GROUP, (g + 1) * GROUP)
@@ -313,7 +311,8 @@
             mix = (inner * decay).astype(bf16)
             mix_out[h] = mix
             within.append(dot(x_b[r * HEAD_DIM : (r + 1) * HEAD_DIM, :], mix, ((1,), (1,))))
-        scan_out = jnp.concatenate(within, axis=0) + carried * per_head(growth, first)
+        carried = carried * per_head(growth, first)
+        scan_out = jnp.concatenate(within, axis=0) + carried
         gate = jnp.transpose(gate_in[:, span].astype(f32))
         sig = jax.nn.sigmoid(gate)
         silu = gate * sig
@@ -323,7 +322,10 @@
         gated_out[span, :] = gated
         silu_out[span, :] = silu
         slope_out[span, :] = scan_out * sig * (1.0 + gate * (1.0 - sig))
-        inverse_out[g : g + 1, :] = inverse
+        carry_out[span, :] = carried * silu
+        inverse_out[g] = inverse
+        for k, part in enumerate((growth, tail, totals)):
+            rows_out[k, g] = part[first : first + PER_GROUP, :]
         x_out[span, :] = x_b
         x_tail = (x * per_head(tail, first)).astype(bf16)
         tail_out[span, :] = x_tail
@@ -349,8 +351,9 @@
             ((inner, tokens), bf16),
             ((inner, tokens), bf16),
             ((inner, STATE), bf16),
-            ((3, heads, tokens), f32),
-            ((inner // GROUP, tokens), f32),
+            ((3, inner // GROUP, PER_GROUP, tokens), f32),
+            ((inner // GROUP, 1, tokens), f32),
+            ((inner, tokens), f32),
         ],
         scan_in, gate_in, b_proj, c_proj, log_decay, entry, gain,
     )
@@ -369,36 +372,87 @@
     ]
 
 
-def backward_kernel(
-    side, grad_own, grad_far, out_own, out_far, gain, gated_in, silu_in, slope_in, mix_in, decay_in,
-    x_in, b_proj, c_proj, entry, local_in, rows_in, inverse_in,
-    message, gate_grad, x_grad, b_grad, c_grad, y_dots,
+def message_kernel(
+    side, grad_own, grad_far, out_own, out_far, gain, gated_in, silu_in, carry_in, c_proj, local_in,
+    rows_in, inverse_in,
+    message, grad_out,
 ):
-    groups = gain.shape[0] // GROUP
     pieces = GROUP // 16
-    tokens = grad_own.shape[0]
-    for g in range(groups):
+    grad_mixed = dot(out_own[...], grad_own[...], ((1,), (1,)))
+    grad_mixed = grad_mixed + dot(out_far[...], grad_far[...], ((1,), (1,)))
+    inverse = inverse_in[0]
+    unit = gated_in[...] * inverse
+    grad_unit = grad_mixed * gain[...]
+    mean = jnp.mean(grad_unit * unit, axis=0, keepdims=True)
+    grad_gated = inverse * (grad_unit - unit * mean)
+    grad_out[...] = grad_gated
+    grown = (grad_gated * silu_in[...] * per_head(rows_in[0, 0], 0)).astype(bf16)
+    block_state = dot(grown, c_proj[...], ((1,), (0,))).astype(bf16)
+    message[:, 0:16, :] = block_state.reshape(pieces, 16, STATE)
+    message[:, 16:32, :] = local_in[...].reshape(pieces, 16, STATE)
+    own = jnp.concatenate(head_sums(grad_gated * carry_in[...]), axis=0)
+    own = jnp.broadcast_to(jnp.sum(own, axis=1, keepdims=True), (PER_GROUP, STATE))
+    per = pieces // PER_GROUP
+    zero = jnp.zeros((pieces, 2, STATE), f32)
+    extra = jnp.concatenate(
+        spread_parts(rows_in[2, 0], PER_GROUP, per) + spread_parts(own, PER_GROUP, per) + [zero],
+        axis=1,
+    )
+    message[:, 32:40, :] = extra.astype(bf16)
+
+
+def state_message(side, grad_own, grad_far, w_out, gain, gated, silu, carry, c_proj, local, rows, inverse):
+    tokens, half = grad_own.shape
+    inner = gain.shape[0]
+    pieces = GROUP // 16
+    channels = pl.BlockSpec((GROUP, tokens), lambda i, side: (i, 0))
+    return pl.pallas_call(
+        message_kernel,
+        grid_spec=pltpu.PrefetchScalarGridSpec(
+            num_scalar_prefetch=1,
+            grid=(inner // GROUP,),
+            in_specs=[
+                whole_block(tokens, half),
+                whole_block(tokens, half),
+                pl.BlockSpec((GROUP, half), lambda i, side: (i, side[0])),
+                pl.BlockSpec((GROUP, half), lambda i, side: (i, 1 - side[0])),
+                pl.BlockSpec((GROUP, 1), lambda i, side: (i, 0)),
+                channels,
+                channels,
+                channels,
+                pl.BlockSpec((tokens, STATE), lambda i, side: (0, i)),
+                pl.BlockSpec((GROUP, STATE), lambda i, side: (i, 0)),
+                pl.BlockSpec((3, 1, PER_GROUP, tokens), lambda i, side: (0, i, 0, 0)),
+                pl.BlockSpec((1, 1, tokens), lambda i, side: (i, 0, 0)),
+            ],
+            out_specs=[
+                pl.BlockSpec((pieces, 40, STATE), lambda i, side: (i, 0, 0)),
+                channels,
+            ],
+        ),
+        out_shape=[
+            jax.ShapeDtypeStruct((inner // 16, 40, STATE), bf16),
+            jax.ShapeDtypeStruct((inner, tokens), f32),
+        ],
+        name="message",
+    )(side, grad_own, grad_far, w_out, w_out, gain, gated, silu, carry, c_proj, local, rows, inverse)
+
+
+def inside_kernel(
+    grad_in, gated_in, silu_in, slope_in, mix_in, decay_in, x_in, b_proj, c_proj, entry, rows_in,
+    gate_grad, x_grad, b_grad, c_grad, y_dots,
+):
+    tokens = x_in.shape[1]
+    for g in range(x_in.shape[0] // GROUP):
         span = slice(g * GROUP, (g + 1) * GROUP)
         states = slice(g * STATE, (g + 1) * STATE)
         first = g * PER_GROUP
-        grad_mixed = dot(out_own[span, :], grad_own[...], ((1,), (1,)))
-        grad_mixed = grad_mixed + dot(out_far[span, :], grad_far[...], ((1,), (1,)))
-        inverse = inverse_in[g : g + 1, :]
-        gated = gated_in[span, :]
-        unit = gated * inverse
-        grad_unit = grad_mixed * gain[span, :]
-        mean = jnp.mean(grad_unit * unit, axis=0, keepdims=True)
-        grad_gated = inverse * (grad_unit - unit * mean)
+        grad_gated = grad_in[span, :]
         gate_grad[:, span] = jnp.transpose(grad_gated * slope_in[span, :]).astype(bf16)
         grad_y = grad_gated * silu_in[span, :]
         grad_y_b = grad_y.astype(bf16)
-        grown = (grad_y * per_head(rows_in[0], first)).astype(bf16)
+        grown = (grad_y * per_head(rows_in[0, g], 0)).astype(bf16)
         b_group, c_group = b_proj[:, states], c_proj[:, states]
-        block_state = dot(grown, c_group, ((1,), (0,))).astype(bf16)
-        message[g * pieces : (g + 1) * pieces, 0:16, :] = block_state.reshape(pieces, 16, STATE)
-        message[g * pieces : (g + 1) * pieces, 16:32, :] = local_in[span, :].reshape(
-            pieces, 16, STATE
-        )
         x = x_in[span, :]
         weights = jnp.zeros((tokens, tokens), f32)
         inside = []
@@ -407,58 +461,31 @@
             head = slice(r * HEAD_DIM, (r + 1) * HEAD_DIM)
             inside.append(dot(grad_y_b[head, :], mix_in[h], ((1,), (0,))))
             weights = weights + decay_in[h] * dot(grad_y_b[head, :], x[head, :], ((0,), (0,)))
-        inside = jnp.concatenate(inside, axis=0)
-        x_grad[span, :] = inside
+        x_grad[span, :] = jnp.concatenate(inside, axis=0)
         weights = weights.astype(bf16)
         c_grad[:, states] = (
             dot(weights, b_group, ((1,), (0,)))
             + dot(grown, entry[span, :].astype(bf16), ((0,), (0,)))
         ).astype(bf16)
         b_grad[:, states] = dot(weights, c_group, ((0,), (0,)))
-        dots = jnp.concatenate(head_sums(grad_gated * gated), axis=0)
-        y_dots[first : first + PER_GROUP, :] = dots
-        own = dots - jnp.concatenate(head_sums(x.astype(f32) * inside), axis=0)
-        own = jnp.broadcast_to(jnp.sum(own, axis=1, keepdims=True), (PER_GROUP, STATE))
-        total = rows_in[2][first : first + PER_GROUP, :]
-        per = pieces // PER_GROUP
-        zero = jnp.zeros((pieces, 2, STATE), f32)
-        extra = jnp.concatenate(
-            spread_parts(total, PER_GROUP, per) + spread_parts(own, PER_GROUP, per) + [zero],
-            axis=1,
+        y_dots[first : first + PER_GROUP, :] = jnp.concatenate(
+            head_sums(grad_gated * gated_in[span, :]), axis=0
         )
-        message[g * pieces : (g + 1) * pieces, 32:40, :] = extra.astype(bf16)
-
-
-def backward(side, grad_own, grad_far, w_out, gain, saved, b_proj, c_proj, entry):
-    gated, silu, slope, mix, decay, x, local, rows, inverse = saved
-    tokens, half = grad_own.shape
-    inner = gain.shape[0]
-    heads = decay.shape[0]
-    wide = [gain, gated, silu, slope, mix, decay, x, b_proj, c_proj, entry, local, rows, inverse]
-    outs = [
-        ((inner // 16, 40, STATE), bf16),
-        ((tokens, inner), bf16),
-        ((inner, tokens), f32),
-        ((tokens, b_proj.shape[1]), f32),
-        ((tokens, b_proj.shape[1]), bf16),
-        ((heads, tokens), f32),
-    ]
-    return pl.pallas_call(
-        backward_kernel,
-        grid_spec=pltpu.PrefetchScalarGridSpec(
-            num_scalar_prefetch=1,
-            grid=(1,),
-            in_specs=[whole_block(tokens, half)] * 2
-            + [
-                pl.BlockSpec((inner, half), lambda i, side: (0, side[0])),
-                pl.BlockSpec((inner, half), lambda i, side: (0, 1 - side[0])),
-            ]
-            + [whole_block(*x.shape) for x in wide],
-            out_specs=[whole_block(*shape) for shape, _ in outs],
-        ),
-        out_shape=[jax.ShapeDtypeStruct(*x) for x in outs],
-        name="backward",
-    )(side, grad_own, grad_far, w_out, w_out, *wide)
+
+
+def inside_grads(grad, gated, silu, slope, mix, decay, x, b_proj, c_proj, entry, rows):
+    inner, tokens = grad.shape
+    return whole_call(
+        inside_kernel,
+        [
+            ((tokens, inner), bf16),
+            ((inner, tokens), f32),
+            (b_proj.shape, f32),
+            (b_proj.shape, bf16),
+            ((decay.shape[0], tokens), f32),
+        ],
+        grad, gated, silu, slope, mix, decay, x, b_proj, c_proj, entry, rows,
+    )
 
 
 def final_kernel(back, b_proj, x_in, tail_in, rows_in, x_inside, y_dots, b_inside, x_grad, b_grad, decay_grad):
@@ -470,10 +497,9 @@
     for g in range(groups):
         span = slice(g * GROUP, (g + 1) * GROUP)
         states = slice(g * STATE, (g + 1) * STATE)
-        first = g * PER_GROUP
         later = back[g * pieces : (g + 1) * pieces, 0:16, :].reshape(GROUP, STATE)
         carried = dot(later, b_proj[:, states], ((1,), (1,)))
-        grad = x_inside[span, :] + carried * per_head(rows_in[1], first)
+        grad = x_inside[span, :] + carried * per_head(rows_in[1, g], 0)
         x_grad[:, span] = jnp.transpose(grad).astype(bf16)
         b_grad[:, states] = (
             b_inside[:, states] + dot(tail_in[span, :], later, ((0,), (0,)))
@@ -560,17 +586,21 @@
     inner = scan_in.shape[1]
     gain = norm_gain.astype(f32)[:, None]
     entry = entry_state.reshape(inner, STATE)
-    mixed, *saved, x_tail, local, rows, inverse = forward(
+    mixed, *saved, x_tail, local, rows, inverse, carry = forward(
         scan_in, gate_in, b_proj, c_proj, log_decay.T, entry, gain
     )
     gated, silu, slope, mix, decay, x = saved
-    message, grad_gate_in, x_inside, b_inside, grad_c_proj, y_dots = backward(
-        side, grad_own, grad_far, w_out, gain,
-        (gated, silu, slope, mix, decay, x, local, rows, inverse), b_proj, c_proj, entry,
-    )
+    message, grad_gated = state_message(
+        side, grad_own, grad_far, w_out, gain, gated, silu, carry, c_proj, local, rows, inverse
+    )
+    grad_hidden, message = lax.optimization_barrier((grad_hidden, message))
     came_states = lax.all_to_all(message, SP, 0, 0, tiled=True)
     later, carried = scan_piece(came_states)
     back = jnp.concatenate([later, spread(list(three_parts(carried)), experts)], axis=1)
+    grad_gated, ready = lax.optimization_barrier((grad_gated, back))
+    grad_gate_in, x_inside, b_inside, grad_c_proj, y_dots = inside_grads(
+        grad_gated, gated, silu, slope, mix, decay, x, b_proj, c_proj, entry, rows
+    )
     back = lax.all_to_all(back, SP, 0, 0, tiled=True)
     grad_scan_in, grad_b_proj, decay_grad = final(
         back, b_proj, x, x_tail, rows, x_inside, y_dots, b_inside
@@ -578,14 +608,17 @@
     grad_log_decay = decay_grad.T
 
     line = lax.axis_size("sp_0")
+    mixed, gate_wgrad = lax.optimization_barrier((mixed, gate_wgrad))
     mixed_line = from_line([mixed] * line, "sp_0")
     grads_line = from_line(pieces_for(grad_hidden, "sp_0", 1), "sp_0")
-    grad_out_proj = dot(
+    product = dot(
         jnp.concatenate(grads_line, axis=0), jnp.concatenate(mixed_line, axis=1), ((0,), (1,))
-    )
-    for axis in ("sp_1", "sp_2"):
-        parts = from_line(pieces_for(grad_out_proj.astype(bf16), axis, 0), axis)
-        grad_out_proj = sum(part.astype(f32) for part in parts)
+    ).astype(bf16)
+    parts = from_line(pieces_for(product, "sp_1", 0), "sp_1")
+    parts, ready = lax.optimization_barrier((parts, ready))
+    product = sum(part.astype(f32) for part in parts).astype(bf16)
+    parts = from_line(pieces_for(product, "sp_2", 0), "sp_2")
+    grad_out_proj = sum(part.astype(f32) for part in parts)
 
     return (
         gate_wgrad[None],

time: 185 us -> 180 us (0.973)
  blocking collectives: 23 us -> 0 us
  waiting for transfers between devices: 58.4 us -> 73.2 us
  starting transfers between devices: 47.1 us -> 51.9 us
  Pallas kernels: 38.3 us -> 40.2 us
    all_to_all x1 -> x0, blocking collectives: 23 us -> none  [body(): lax.all_to_all(summed.reshape(experts, capacity, half), SP, 0, 0, tiled=T...]
    all_to_all x0 -> x1, waiting for transfers between devices: none -> 18.3 us  [body(): lax.all_to_all(summed.reshape(experts, capacity, half), SP, 0, 0, tiled=T...]
    all_to_all x0 -> x1, starting transfers between devices: none -> 4.76 us  [body(): lax.all_to_all(summed.reshape(experts, capacity, half), SP, 0, 0, tiled=T...]
    pallas_call x2 -> x3, Pallas kernels: 7.2 us -> 11.7 us  [whole_call(): pl.pallas_call(kernel, out_shape=[jax.ShapeDtypeStruct(*x) for x in out_s...]
    ppermute x12, waiting for transfers between devices: 21.6 us -> 17.9 us  [from_line(): lax.ppermute(parts[k], axis, [(i, (i + k) % size) for i in range(size)])]
    pallas_call x1, Pallas kernels: 8.83 us -> 6.16 us  [state_message(): pl.pallas_call(message_kernel, grid_spec=pltpu.PrefetchScalarGridSpec(num...]
  transfers between devices with their start and end apart: 20 -> 21, of which waited for: 6 -> 8; matrix products, arithmetic and copies ran while one was open for 7% -> 4% of each run, Pallas kernels for 13% -> 14%
where the time goes in v4:
time: 180 us; the launch traced here: 179 us
  waiting for transfers between devices  73.2 us (41%)
  starting transfers between devices  51.9 us (29%)
  Pallas kernels  40.2 us (22%)
  other arithmetic  5.2 us (3%)
  local copies, waits for them, and re-layouts  4.42 us (2%)
  matrix products  3.5 us (2%)
    all_to_all x1, waiting for transfers between devices, body(): lax.all_to_all(summed.reshape(experts, capacity, half), SP, 0, 0, tiled=T...  18.3 us
    ppermute x12, waiting for transfers between devices, from_line(): lax.ppermute(parts[k], axis, [(i, (i + k) % size) for i in range(size)])  17.9 us
    all_to_all x1, waiting for transfers between devices, body(): came_grads = lax.all_to_all(send_grads, SP, 0, 0, tiled=True)  17.5 us
    ppermute x12, starting transfers between devices, from_line(): lax.ppermute(parts[k], axis, [(i, (i + k) % size) for i in range(size)])  17.4 us
    all_to_all x1, waiting for transfers between devices, body(): came_hidden = lax.all_to_all(send_hidden, SP, 0, 0, tiled=True)  16.8 us
    pallas_call x3, Pallas kernels, whole_call(): pl.pallas_call(kernel, out_shape=[jax.ShapeDtypeStruct(*x) for x in out_s...  11.7 us
    all_to_all x1, starting transfers between devices, body(): came_grads = lax.all_to_all(send_grads, SP, 0, 0, tiled=True)  11.7 us
    pallas_call x1, Pallas kernels, expert_rows(): pl.pallas_call(expert_rows_kernel, grid_spec=pltpu.PrefetchScalarGridSpec...  9.19 us
  transfers between devices with their start and end apart: 21, of which 8 were waited for; matrix products, arithmetic and copies ran while one was open for 4% of the time, Pallas kernels for 14%

profile of v4, /device:TPU:0, one launch (start us, length us, event | category | flops | bytes accessed | tf_op | source)
XLA Modules:
  0.0 179.4 jit_solution(17780923078233890060)
XLA Ops:
  0.7 3.1 %route.1 = (bf16[512,1024]{1,0:T(8,128)(2,1)}, bf16[512,128]{1,0:T(8,128)(2,1)}) custom-call(s32[1]{0:T(128)} %bitcast.3.side, s32[2,128]{1,0:T(2,128)} %bitcast.73, f32[2,128]{1,0:T(2,128)} %bitcast.74, bf16[128,2048]{1,0:T(8,128)(2,1)} %cotangent.1), custom_call_target="tpu_custom_call" | custom-call | tf_op jit(solution)/shard_map/route/pallas_call | solution.py:239
  3.7 11.7 %all-to-all-start = ((bf16[64,8,1024]{2,1,0:T(8,128)(2,1)}), bf16[64,8,1024]{2,1,0:T(8,128)(2,1)S(1)}, u32[]{:S(2)}, u32[]{:S(2)}) async-start(bf16[64,8,1024]{2,1,0:T(8,128)(2,1)} %bitcast.68), calls=%async_computation | async-start | bytes 2097152 | tf_op jit(solution)/shard_map/all_to_all | solution.py:562
  16.8 17.5 %all-to-all-done = bf16[64,8,1024]{2,1,0:T(8,128)(2,1)S(1)} async-done(((bf16[64,8,1024]{2,1,0:T(8,128)(2,1)}), bf16[64,8,1024]{2,1,0:T(8,128)(2,1)S(1)}, u32[]{:S(2)}, u32[]{:S(2)}) %all-to-all-start) | async-done | bytes 1048608 | tf_op jit(solution)/shard_map/all_to_all | solution.py:562
  34.3 2.7 %collective-permute-done.other = bf16[512,1024]{1,0:T(8,128)(2,1)S(1)} collective-permute-done((bf16[512,1024]{1,0:T(8,128)(2,1)S(1)}, bf16[512,1024]{1,0:T(8,128)(2,1)S(1)}, u32[]{:S(2)}, u32[]{:S(2)}) %collective-permute-start) | collective-permute-done | bytes 1048608 | tf_op jit(solution)/shard_map/ppermute | solution.py:27
  37.9 9.2 %expert_rows.1 = (bf16[512,512]{1,0:T(8,128)(2,1)}, bf16[512,512]{1,0:T(8,128)(2,1)}, bf16[512,512]{1,0:T(8,128)(2,1)}, bf16[512,1024]{1,0:T(8,128)(2,1)}, bf16[512,1024]{1,0:T(8,128)(2,1)}) custom-call(s32[1]{0:T(128)} %bitcast.3.side, bf16[512,1024]{1,0:T(8,128)(2,1)} %bitcast.51, bf16[512,1024]{1,0:T(8,128)(2,1)} %copy-done.2, bf16[512,512]{1,0:T(8,128)(2,1)} %bitcast.69, ...), custom_call_target="tpu_custom_call" | custom-call | tf_op jit(solution)/shard_map/expert_rows/pallas_call | solution.py:99
  47.3 4.8 %all-to-all-start.1 = ((bf16[64,8,1024]{2,1,0:T(8,128)(2,1)}), bf16[64,8,1024]{2,1,0:T(8,128)(2,1)S(1)}, u32[]{:S(2)}, u32[]{:S(2)}) async-start(bf16[64,8,1024]{2,1,0:T(8,128)(2,1)} %fusion), calls=%async_computation.1 | async-start | bytes 2097152 | tf_op jit(solution)/shard_map/all_to_all | solution.py:564
  52.1 2.7 %add_convert_fusion = bf16[512,1024]{1,0:T(8,128)(2,1)} fusion(bf16[512,1024]{1,0:T(8,128)(2,1)} %collective-permute-done.1, bf16[512,1024]{1,0:T(8,128)(2,1)S(1)} %copy-done.7), kind=kLoop, calls=%fused_computation.1 | loop fusion | flops 2097152 | bytes 3145728 | tf_op jit(solution)/shard_map/convert_element_type | solution.py:570
  54.8 16.8 %all-to-all-done.1 = bf16[64,8,1024]{2,1,0:T(8,128)(2,1)S(1)} async-done(((bf16[64,8,1024]{2,1,0:T(8,128)(2,1)}), bf16[64,8,1024]{2,1,0:T(8,128)(2,1)S(1)}, u32[]{:S(2)}, u32[]{:S(2)}) %all-to-all-start.1) | async-done | bytes 1048608 | tf_op jit(solution)/shard_map/all_to_all | solution.py:564
  71.6 4.8 %all-to-all-start.2 = ((bf16[64,8,1024]{2,1,0:T(8,128)(2,1)}), bf16[64,8,1024]{2,1,0:T(8,128)(2,1)S(1)}, u32[]{:S(2)}, u32[]{:S(2)}) async-start(bf16[64,8,1024]{2,1,0:T(8,128)(2,1)} %bitcast.19), calls=%async_computation.2 | async-start | bytes 2097152 | tf_op jit(solution)/shard_map/all_to_all | solution.py:572
  76.5 18.3 %all-to-all-done.2 = bf16[64,8,1024]{2,1,0:T(8,128)(2,1)S(1)} async-done(((bf16[64,8,1024]{2,1,0:T(8,128)(2,1)}), bf16[64,8,1024]{2,1,0:T(8,128)(2,1)S(1)}, u32[]{:S(2)}, u32[]{:S(2)}) %all-to-all-start.2) | async-done | bytes 1048608 | tf_op jit(solution)/shard_map/all_to_all | solution.py:572
  96.6 4.8 %shard_map.232 = (bf16[1024,128]{1,0:T(8,128)(2,1)}, f32[1024,128]{1,0:T(8,128)}, f32[1024,128]{1,0:T(8,128)}, f32[1024,128]{1,0:T(8,128)}, bf16[16,128,128]{2,1...) custom-call(bf16[128,1024]{1,0:T(8,128)(2,1)} %scan_in.1, ...), custom_call_target="tpu_custom_call" | custom-call | tf_op jit(solution)/shard_map/pallas_call | solution.py:336
  101.4 5.9 %tall_weights.1 = (bf16[2048,512]{1,0:T(8,128)(2,1)}, bf16[2048,512]{1,0:T(8,128)(2,1)}) custom-call(s32[1]{0:T(128)} %bitcast.3.side, bf16[512,512]{1,0:T(8,128)(2,1)} %get-tuple-element.57.gate_grad, bf16[512,512]{1,0:T(8,128)(2,1)} %get-tuple-element.58.up_grad, bf16[512,1024]{1,0:T(8,128)(2,1)} %bitcast.60, bf16[512,1024]{1,0:T(8,128)(2,1)} %collective-permute-done.2.other), custom_call_target="tpu_custom_call" | custom-call | tf_op jit(solution)/shard_map/tall_weights/pallas_call | solution.py:159
  111.2 6.2 %message.1 = (bf16[64,40,128]{2,1,0:T(8,128)(2,1)}, f32[1024,128]{1,0:T(8,128)}) custom-call(s32[1]{0:T(128)} %bitcast.3.side, bf16[128,1024]{1,0:T(8,128)(2,1)} %copy-done.4, bf16[128,1024]{1,0:T(8,128)(2,1)} %copy-done.8, bf16[1024,2048]{1,0:T(8,128)(2,1)} %out_far.1, bf16[1024,2048]{1,0:T(8,128)(2,1)} %out_far.1, f32[1024,1]{1,0:T(8,128)} %copy.27.gain, ...), custom_call_target="tpu_custom_call" | custom-call | tf_op jit(solution)/shard_map/message/pallas_call | solution.py:409
  118.5 2.0 %collective-permute-start.5 = (bf16[128,512]{1,0:T(8,128)(2,1)S(1)}, bf16[128,512]{1,0:T(8,128)(2,1)S(1)}, u32[]{:S(2)}, u32[]{:S(2)}) collective-permute-start(bf16[128,512]{1,0:T(8,128)(2,1)S(1)} %get-tuple-element.110), channel_id=1, source_target_pairs={{0,64},{32,96},{64,0},{96,32},{1,65},{33,97},{65,1},{97,33},{2,66}... | collective-permute-start | bytes 393224 | tf_op jit(solution)/shard_map/ppermute | solution.py:33
  120.5 2.8 %collective-permute-done.7 = bf16[1024,128]{1,0:T(8,128)(2,1)S(1)} collective-permute-done((bf16[1024,128]{1,0:T(8,128)(2,1)S(1)}, bf16[1024,128]{1,0:T(8,128)(2,1)S(1)}, u32[]{:S(2)}, u32[]{:S(2)}) %collective-permute-start.7) | collective-permute-done | bytes 262176 | tf_op jit(solution)/shard_map/ppermute | solution.py:33
  123.3 5.1 %all-to-all-start.3 = ((bf16[64,40,128]{2,1,0:T(8,128)(2,1)}), bf16[64,40,128]{2,1,0:T(8,128)(2,1)S(1)}, u32[]{:S(2)}, u32[]{:S(2)}) async-start(bf16[64,40,128]{2,1,0:T(8,128)(2,1)} %get-tuple-element.81), calls=%async_computation.3 | async-start | bytes 1310720 | tf_op jit(solution)/shard_map/all_to_all | solution.py:597
  131.0 2.7 %collective-permute-start.11 = (bf16[128,1024]{1,0:T(8,128)(2,1)S(1)}, bf16[128,1024]{1,0:T(8,128)(2,1)S(1)}, u32[]{:S(2)}, u32[]{:S(2)}) collective-permute-start(bf16[128,1024]{1,0:T(8,128)(2,1)S(1)} %get-tuple-element.101), channel_id=1, source_target_pairs={{0,16},{8,24},{16,0},{24,8},{1,17},{9,25},{17,1},{25,9},{2,18},{10... | collective-permute-start | bytes 786440 | tf_op jit(solution)/shard_map/ppermute | solution.py:33
  135.1 9.9 %collective-permute-done.10 = bf16[128,1024]{1,0:T(8,128)(2,1)S(1)} collective-permute-done((bf16[128,1024]{1,0:T(8,128)(2,1)S(1)}, bf16[128,1024]{1,0:T(8,128)(2,1)S(1)}, u32[]{:S(2)}, u32[]{:S(2)}) %collective-permute-start.10) | collective-permute-done | bytes 262176 | tf_op jit(solution)/shard_map/ppermute | solution.py:33
  145.1 4.5 %collective-permute-done.11 = bf16[128,1024]{1,0:T(8,128)(2,1)S(1)} collective-permute-done((bf16[128,1024]{1,0:T(8,128)(2,1)S(1)}, bf16[128,1024]{1,0:T(8,128)(2,1)S(1)}, u32[]{:S(2)}, u32[]{:S(2)}) %collective-permute-start.11) | collective-permute-done | bytes 262176 | tf_op jit(solution)/shard_map/ppermute | solution.py:33
  153.2 7.6 %all-to-all-start.4 = ((bf16[64,24,128]{2,1,0:T(8,128)(2,1)}), bf16[64,24,128]{2,1,0:T(8,128)(2,1)S(1)}, u32[]{:S(2)}, u32[]{:S(2)}) async-start(bf16[64,24,128]{2,1,0:T(8,128)(2,1)} %pad_maximum_fusion), calls=%async_computation.4 | async-start | bytes 786432 | tf_op jit(solution)/shard_map/all_to_all | solution.py:604
  162.7 2.7 %collective-permute-start.14 = (bf16[32,1024]{1,0:T(8,128)(2,1)S(1)}, bf16[32,1024]{1,0:T(8,128)(2,1)S(1)}, u32[]{:S(2)}, u32[]{:S(2)}) collective-permute-start(bf16[32,1024]{1,0:T(8,128)(2,1)S(1)} %get-tuple-element.114), channel_id=1, source_target_pairs={{0,4},{2,6},{4,0},{6,2},{1,5},{3,7},{5,1},{7,3},{8,12},{10,14},{12... | collective-permute-start | bytes 196616 | tf_op jit(solution)/shard_map/ppermute | solution.py:33
  166.8 4.2 %down_weights.1 = bf16[512,2048]{1,0:T(8,128)(2,1)} custom-call(s32[1]{0:T(128)} %bitcast.3.side, bf16[512,512]{1,0:T(8,128)(2,1)} %get-tuple-element.66.active, bf16[512,1024]{1,0:T(8,128)(2,1)} %bitcast.52, bf16[512,1024]{1,0:T(8,128)(2,1)} %copy-done.2), custom_call_target="tpu_custom_call" | custom-call | tf_op jit(solution)/shard_map/down_weights/pallas_call | solution.py:143
  171.7 4.3 %shard_map.233 = (bf16[128,1024]{1,0:T(8,128)(2,1)}, f32[1024,128]{1,0:T(8,128)}, f32[128,512]{1,0:T(8,128)}, bf16[128,512]{1,0:T(8,128)(2,1)}, f32[16,128]{1,0:T(8,128)}) custom-call(f32[1024,128]{1,0:T(8,128)} %get-tuple-element.85.grad_in, f32[1024,128]{1,0:T(8,128)} %get-tuple-element.68.gated_in, f32[1024,128]{1,0:T(8,128)} %get-tuple-element.69.silu_in, ...), custom_call_target="tpu_custom_call" | custom-call | tf_op jit(solution)/shard_map/pallas_call | solution.py:336
  176.8 2.6 %shard_map.234 = (bf16[128,1024]{1,0:T(8,128)(2,1)}, bf16[128,512]{1,0:T(8,128)(2,1)}, f32[16,128]{1,0:T(8,128)}) custom-call(bf16[64,24,128]{2,1,0:T(8,128)(2,1)} %copy-done.5, bf16[128,512]{1,0:T(8,128)(2,1)} %b_proj.5, bf16[1024,128]{1,0:T(8,128)(2,1)} %get-tuple-element.82.x_in, bf16[1024,128]{1,0:T(8,128)(2,1)} %get-tuple-element.83.tail_in, ...), custom_call_target="tpu_custom_call" | custom-call | tf_op jit(solution)/shard_map/pallas_call | solution.py:336
  (79 shorter events, 21.8 us)
Async XLA Ops:
  3.7 30.6 %all-to-all-start = ((bf16[64,8,1024]{2,1,0:T(8,128)(2,1)}), bf16[64,8,1024]{2,1,0:T(8,128)(2,1)S(1)}, u32[]{:S(2)}, u32[]{:S(2)}) async-start(bf16[64,8,1024]{2,1,0:T(8,128)(2,1)} %bitcast.68), calls=%async_computation | async-start | bytes 2097152 | tf_op jit(solution)/shard_map/all_to_all | solution.py:562
  34.3 2.7 %collective-permute-start = (bf16[512,1024]{1,0:T(8,128)(2,1)S(1)}, bf16[512,1024]{1,0:T(8,128)(2,1)S(1)}, u32[]{:S(2)}, u32[]{:S(2)}) collective-permute-start(bf16[512,1024]{1,0:T(8,128)(2,1)S(1)} %bitcast.50), channel_id=1, source_target_pairs={{0,1},{1,0},{2,3},{3,2},{4,5},{5,4},{6,7},{7,6},{8,9},{9,8},{10,11... | collective-permute-start | bytes 3145736 | tf_op jit(solution)/shard_map/ppermute | solution.py:27
  47.1 5.0 %collective-permute-start.1 = (bf16[512,1024]{1,0:T(8,128)(2,1)}, bf16[512,1024]{1,0:T(8,128)(2,1)}, u32[]{:S(2)}, u32[]{:S(2)}) collective-permute-start(bf16[512,1024]{1,0:T(8,128)(2,1)} %get-tuple-element.60), channel_id=1, source_target_pairs={{0,1},{1,0},{2,3},{3,2},{4,5},{5,4},{6,7},{7,6},{8,9},{9,8},{10,11... | collective-permute-start | bytes 3145736 | tf_op jit(solution)/shard_map/ppermute | solution.py:27
  47.3 24.4 %all-to-all-start.1 = ((bf16[64,8,1024]{2,1,0:T(8,128)(2,1)}), bf16[64,8,1024]{2,1,0:T(8,128)(2,1)S(1)}, u32[]{:S(2)}, u32[]{:S(2)}) async-start(bf16[64,8,1024]{2,1,0:T(8,128)(2,1)} %fusion), calls=%async_computation.1 | async-start | bytes 2097152 | tf_op jit(solution)/shard_map/all_to_all | solution.py:564
  52.1 42.7 %copy-start.6 = (bf16[128,2048]{1,0:T(8,128)(2,1)S(1)}, bf16[128,2048]{1,0:T(8,128)(2,1)}, u32[]{:S(2)}) copy-start(bf16[128,2048]{1,0:T(8,128)(2,1)} %cotangent.1) | copy-start | bytes 1572868
  54.8 40.7 %copy-start.10 = (bf16[1024]{0:T(1024)(128)(2,1)S(1)}, bf16[1024]{0:T(1024)(128)(2,1)}, u32[]{:S(2)}) copy-start(bf16[1024]{0:T(1024)(128)(2,1)} %param.27) | copy-start | bytes 6148
  71.6 25.0 %copy-start.3 = (bf16[64,8,1024]{2,1,0:T(8,128)(2,1)}, bf16[64,8,1024]{2,1,0:T(8,128)(2,1)S(1)}, u32[]{:S(2)}) copy-start(bf16[64,8,1024]{2,1,0:T(8,128)(2,1)S(1)} %all-to-all-done.1) | copy-start | bytes 3145732
  71.6 23.2 %all-to-all-start.2 = ((bf16[64,8,1024]{2,1,0:T(8,128)(2,1)}), bf16[64,8,1024]{2,1,0:T(8,128)(2,1)S(1)}, u32[]{:S(2)}, u32[]{:S(2)}) async-start(bf16[64,8,1024]{2,1,0:T(8,128)(2,1)} %bitcast.19), calls=%async_computation.2 | async-start | bytes 2097152 | tf_op jit(solution)/shard_map/all_to_all | solution.py:572
  76.4 25.0 %collective-permute-start.2 = (bf16[512,1024]{1,0:T(8,128)(2,1)S(1)}, bf16[512,1024]{1,0:T(8,128)(2,1)}, u32[]{:S(2)}, u32[]{:S(2)}) collective-permute-start(bf16[512,1024]{1,0:T(8,128)(2,1)S(1)} %bitcast.59), channel_id=1, source_target_pairs={{0,1},{1,0},{2,3},{3,2},{4,5},{5,4},{6,7},{7,6},{8,9},{9,8},{10,11... | collective-permute-start | bytes 3145736 | tf_op jit(solution)/shard_map/ppermute | solution.py:27
  95.2 15.3 %collective-permute-start.3 = (bf16[128,1024]{1,0:T(8,128)(2,1)S(1)}, bf16[128,1024]{1,0:T(8,128)(2,1)S(1)}, u32[]{:S(2)}, u32[]{:S(2)}) collective-permute-start(bf16[128,1024]{1,0:T(8,128)(2,1)S(1)} %fusion.1.grad_own), channel_id=1, source_target_pairs={{0,1},{1,0},{2,3},{3,2},{4,5},{5,4},{6,7},{7,6},{8,9},{9,8},{10,11... | collective-permute-start | bytes 786440 | tf_op jit(solution)/shard_map/ppermute | solution.py:27
  107.3 16.0 %collective-permute-start.7 = (bf16[1024,128]{1,0:T(8,128)(2,1)S(1)}, bf16[1024,128]{1,0:T(8,128)(2,1)S(1)}, u32[]{:S(2)}, u32[]{:S(2)}) collective-permute-start(bf16[1024,128]{1,0:T(8,128)(2,1)S(1)} %copy-done.11), channel_id=1, source_target_pairs={{0,32},{32,64},{64,96},{96,0},{1,33},{33,65},{65,97},{97,1},{2,34}... | collective-permute-start | bytes 786440 | tf_op jit(solution)/shard_map/ppermute | solution.py:33
  107.7 20.8 %collective-permute-start.8 = (bf16[1024,128]{1,0:T(8,128)(2,1)S(1)}, bf16[1024,128]{1,0:T(8,128)(2,1)S(1)}, u32[]{:S(2)}, u32[]{:S(2)}) collective-permute-start(bf16[1024,128]{1,0:T(8,128)(2,1)S(1)} %copy-done.11), channel_id=1, source_target_pairs={{0,64},{32,96},{64,0},{96,32},{1,65},{33,97},{65,1},{97,33},{2,66}... | collective-permute-start | bytes 786440 | tf_op jit(solution)/shard_map/ppermute | solution.py:33
  109.5 18.9 %collective-permute-start.9 = (bf16[1024,128]{1,0:T(8,128)(2,1)S(1)}, bf16[1024,128]{1,0:T(8,128)(2,1)S(1)}, u32[]{:S(2)}, u32[]{:S(2)}) collective-permute-start(bf16[1024,128]{1,0:T(8,128)(2,1)S(1)} %copy-done.11), channel_id=1, source_target_pairs={{0,96},{32,0},{64,32},{96,64},{1,97},{33,1},{65,33},{97,65},{2,98}... | collective-permute-start | bytes 786440 | tf_op jit(solution)/shard_map/ppermute | solution.py:33
  117.4 11.0 %collective-permute-start.4 = (bf16[128,512]{1,0:T(8,128)(2,1)S(1)}, bf16[128,512]{1,0:T(8,128)(2,1)S(1)}, u32[]{:S(2)}, u32[]{:S(2)}) collective-permute-start(bf16[128,512]{1,0:T(8,128)(2,1)S(1)} %get-tuple-element.111), channel_id=1, source_target_pairs={{0,32},{32,64},{64,96},{96,0},{1,33},{33,65},{65,97},{97,1},{2,34}... | collective-permute-start | bytes 393224 | tf_op jit(solution)/shard_map/ppermute | solution.py:33
  118.5 9.9 %collective-permute-start.5 = (bf16[128,512]{1,0:T(8,128)(2,1)S(1)}, bf16[128,512]{1,0:T(8,128)(2,1)S(1)}, u32[]{:S(2)}, u32[]{:S(2)}) collective-permute-start(bf16[128,512]{1,0:T(8,128)(2,1)S(1)} %get-tuple-element.110), channel_id=1, source_target_pairs={{0,64},{32,96},{64,0},{96,32},{1,65},{33,97},{65,1},{97,33},{2,66}... | collective-permute-start | bytes 393224 | tf_op jit(solution)/shard_map/ppermute | solution.py:33
  123.3 5.9 %collective-permute-start.6 = (bf16[128,512]{1,0:T(8,128)(2,1)S(1)}, bf16[128,512]{1,0:T(8,128)(2,1)S(1)}, u32[]{:S(2)}, u32[]{:S(2)}) collective-permute-start(bf16[128,512]{1,0:T(8,128)(2,1)S(1)} %get-tuple-element.109), channel_id=1, source_target_pairs={{0,96},{32,0},{64,32},{96,64},{1,97},{33,1},{65,33},{97,65},{2,98}... | collective-permute-start | bytes 393224 | tf_op jit(solution)/shard_map/ppermute | solution.py:33
  123.3 26.4 %all-to-all-start.3 = ((bf16[64,40,128]{2,1,0:T(8,128)(2,1)}), bf16[64,40,128]{2,1,0:T(8,128)(2,1)S(1)}, u32[]{:S(2)}, u32[]{:S(2)}) async-start(bf16[64,40,128]{2,1,0:T(8,128)(2,1)} %get-tuple-element.81), calls=%async_computation.3 | async-start | bytes 1310720 | tf_op jit(solution)/shard_map/all_to_all | solution.py:597
  130.0 15.0 %collective-permute-start.10 = (bf16[128,1024]{1,0:T(8,128)(2,1)S(1)}, bf16[128,1024]{1,0:T(8,128)(2,1)S(1)}, u32[]{:S(2)}, u32[]{:S(2)}) collective-permute-start(bf16[128,1024]{1,0:T(8,128)(2,1)S(1)} %get-tuple-element.102), channel_id=1, source_target_pairs={{0,8},{8,16},{16,24},{24,0},{1,9},{9,17},{17,25},{25,1},{2,10},{10... | collective-permute-start | bytes 786440 | tf_op jit(solution)/shard_map/ppermute | solution.py:33
  131.0 18.5 %collective-permute-start.11 = (bf16[128,1024]{1,0:T(8,128)(2,1)S(1)}, bf16[128,1024]{1,0:T(8,128)(2,1)S(1)}, u32[]{:S(2)}, u32[]{:S(2)}) collective-permute-start(bf16[128,1024]{1,0:T(8,128)(2,1)S(1)} %get-tuple-element.101), channel_id=1, source_target_pairs={{0,16},{8,24},{16,0},{24,8},{1,17},{9,25},{17,1},{25,9},{2,18},{10... | collective-permute-start | bytes 786440 | tf_op jit(solution)/shard_map/ppermute | solution.py:33
  133.7 15.9 %collective-permute-start.12 = (bf16[128,1024]{1,0:T(8,128)(2,1)S(1)}, bf16[128,1024]{1,0:T(8,128)(2,1)S(1)}, u32[]{:S(2)}, u32[]{:S(2)}) collective-permute-start(bf16[128,1024]{1,0:T(8,128)(2,1)S(1)} %get-tuple-element.100), channel_id=1, source_target_pairs={{0,24},{8,0},{16,8},{24,16},{1,25},{9,1},{17,9},{25,17},{2,26},{10... | collective-permute-start | bytes 786440 | tf_op jit(solution)/shard_map/ppermute | solution.py:33
  153.2 22.8 %all-to-all-start.4 = ((bf16[64,24,128]{2,1,0:T(8,128)(2,1)}), bf16[64,24,128]{2,1,0:T(8,128)(2,1)S(1)}, u32[]{:S(2)}, u32[]{:S(2)}) async-start(bf16[64,24,128]{2,1,0:T(8,128)(2,1)} %pad_maximum_fusion), calls=%async_computation.4 | async-start | bytes 786432 | tf_op jit(solution)/shard_map/all_to_all | solution.py:604
  160.8 10.2 %collective-permute-start.13 = (bf16[32,1024]{1,0:T(8,128)(2,1)S(1)}, bf16[32,1024]{1,0:T(8,128)(2,1)S(1)}, u32[]{:S(2)}, u32[]{:S(2)}) collective-permute-start(bf16[32,1024]{1,0:T(8,128)(2,1)S(1)} %get-tuple-element.112), channel_id=1, source_target_pairs={{0,2},{2,4},{4,6},{6,0},{1,3},{3,5},{5,7},{7,1},{8,10},{10,12},{12... | collective-permute-start | bytes 196616 | tf_op jit(solution)/shard_map/ppermute | solution.py:33
  162.7 8.3 %collective-permute-start.14 = (bf16[32,1024]{1,0:T(8,128)(2,1)S(1)}, bf16[32,1024]{1,0:T(8,128)(2,1)S(1)}, u32[]{:S(2)}, u32[]{:S(2)}) collective-permute-start(bf16[32,1024]{1,0:T(8,128)(2,1)S(1)} %get-tuple-element.114), channel_id=1, source_target_pairs={{0,4},{2,6},{4,0},{6,2},{1,5},{3,7},{5,1},{7,3},{8,12},{10,14},{12... | collective-permute-start | bytes 196616 | tf_op jit(solution)/shard_map/ppermute | solution.py:33
  165.3 5.7 %collective-permute-start.15 = (bf16[32,1024]{1,0:T(8,128)(2,1)S(1)}, bf16[32,1024]{1,0:T(8,128)(2,1)S(1)}, u32[]{:S(2)}, u32[]{:S(2)}) collective-permute-start(bf16[32,1024]{1,0:T(8,128)(2,1)S(1)} %get-tuple-element.113), channel_id=1, source_target_pairs={{0,6},{2,0},{4,2},{6,4},{1,7},{3,1},{5,3},{7,5},{8,14},{10,8},{12,... | collective-permute-start | bytes 196616 | tf_op jit(solution)/shard_map/ppermute | solution.py:33
  (9 other events, 57.8 us)

commit v5 on v4

--- a/solution.py
+++ b/solution.py
@@ -278,9 +278,9 @@
 
 
 def forward_kernel(
-    scan_in, gate_in, b_proj, c_proj, log_decay, entry, gain,
+    scan_in, gate_in, b_proj, c_proj, log_decay, entry, gain, cotangent,
     mixed, gated_out, silu_out, slope_out, mix_out, decay_out, x_out, tail_out, local_out,
-    rows_out, inverse_out, carry_out,
+    rows_out, inverse_out, carry_out, cotangent_out,
 ):
     tokens = scan_in.shape[0]
     groups = scan_in.shape[1] // GROUP
@@ -323,6 +323,7 @@
         silu_out[span, :] = silu
         slope_out[span, :] = scan_out * sig * (1.0 + gate * (1.0 - sig))
         carry_out[span, :] = carried * silu
+        cotangent_out[span, :] = jnp.transpose(cotangent[:, span].astype(f32)).astype(bf16)
         inverse_out[g] = inverse
         for k, part in enumerate((growth, tail, totals)):
             rows_out[k, g] = part[first : first + PER_GROUP, :]
@@ -336,7 +337,7 @@
     return pl.pallas_call(kernel, out_shape=[jax.ShapeDtypeStruct(*x) for x in out_shape])(*args)
 
 
-def forward(scan_in, gate_in, b_proj, c_proj, log_decay, entry, gain):
+def forward(scan_in, gate_in, b_proj, c_proj, log_decay, entry, gain, cotangent):
     tokens, inner = scan_in.shape
     heads = log_decay.shape[0]
     return whole_call(
@@ -354,8 +355,9 @@
             ((3, inner // GROUP, PER_GROUP, tokens), f32),
             ((inner // GROUP, 1, tokens), f32),
             ((inner, tokens), f32),
+            ((cotangent.shape[1], tokens), bf16),
         ],
-        scan_in, gate_in, b_proj, c_proj, log_decay, entry, gain,
+        scan_in, gate_in, b_proj, c_proj, log_decay, entry, gain, cotangent,
     )
 
 
@@ -378,8 +380,8 @@
     message, grad_out,
 ):
     pieces = GROUP // 16
-    grad_mixed = dot(out_own[...], grad_own[...], ((1,), (1,)))
-    grad_mixed = grad_mixed + dot(out_far[...], grad_far[...], ((1,), (1,)))
+    grad_mixed = dot(out_own[...], grad_own[...], ((1,), (0,)))
+    grad_mixed = grad_mixed + dot(out_far[...], grad_far[...], ((1,), (0,)))
     inverse = inverse_in[0]
     unit = gated_in[...] * inverse
     grad_unit = grad_mixed * gain[...]
@@ -402,7 +404,7 @@
 
 
 def state_message(side, grad_own, grad_far, w_out, gain, gated, silu, carry, c_proj, local, rows, inverse):
-    tokens, half = grad_own.shape
+    half, tokens = grad_own.shape
     inner = gain.shape[0]
     pieces = GROUP // 16
     channels = pl.BlockSpec((GROUP, tokens), lambda i, side: (i, 0))
@@ -412,8 +414,8 @@
             num_scalar_prefetch=1,
             grid=(inner // GROUP,),
             in_specs=[
-                whole_block(tokens, half),
-                whole_block(tokens, half),
+                whole_block(half, tokens),
+                whole_block(half, tokens),
                 pl.BlockSpec((GROUP, half), lambda i, side: (i, side[0])),
                 pl.BlockSpec((GROUP, half), lambda i, side: (i, 1 - side[0])),
                 pl.BlockSpec((GROUP, 1), lambda i, side: (i, 0)),
@@ -559,6 +561,13 @@
     send_hidden = dot(either, hidden_half, ((1,), (0,))).astype(bf16)
     send_grads = send_grads.reshape(experts, capacity, half)
     send_hidden = send_hidden.reshape(experts, capacity, half)
+    inner = scan_in.shape[1]
+    gain = norm_gain.astype(f32)[:, None]
+    entry = entry_state.reshape(inner, STATE)
+    mixed, *saved, x_tail, local, rows, inverse, carry, cotangent_rows = forward(
+        scan_in, gate_in, b_proj, c_proj, log_decay.T, entry, gain, cotangent_half
+    )
+    gated, silu, slope, mix, decay, x = saved
     came_grads = lax.all_to_all(send_grads, SP, 0, 0, tiled=True)
     send_hidden, came_grads = lax.optimization_barrier((send_hidden, came_grads))
     came_hidden = lax.all_to_all(send_hidden, SP, 0, 0, tiled=True)
@@ -574,30 +583,21 @@
     hidden_far = swapped(hidden_own)
     down_wgrad = down_weights(side, active, grads_own, grads_far)
     gate_wgrad, up_wgrad = tall_weights(side, gate_grad, up_grad, hidden_own, hidden_far)
-    moe_terms = dot(either, returned.reshape(-1, half), ((0,), (0,)))
-    grad_own = (cotangent_half.astype(f32) + moe_terms).astype(bf16)
+    moe_terms = dot(returned.reshape(-1, half), either, ((0,), (0,)))
+    grad_own = (cotangent_rows.astype(f32) + moe_terms).astype(bf16)
     grad_far = swapped(grad_own)
     grad_hidden = jnp.where(
         side == 0,
-        jnp.concatenate([grad_own, grad_far], axis=1),
-        jnp.concatenate([grad_far, grad_own], axis=1),
-    )
-
-    inner = scan_in.shape[1]
-    gain = norm_gain.astype(f32)[:, None]
-    entry = entry_state.reshape(inner, STATE)
-    mixed, *saved, x_tail, local, rows, inverse, carry = forward(
-        scan_in, gate_in, b_proj, c_proj, log_decay.T, entry, gain
-    )
-    gated, silu, slope, mix, decay, x = saved
+        jnp.concatenate([grad_own, grad_far], axis=0),
+        jnp.concatenate([grad_far, grad_own], axis=0),
+    )
+
     message, grad_gated = state_message(
         side, grad_own, grad_far, w_out, gain, gated, silu, carry, c_proj, local, rows, inverse
     )
-    grad_hidden, message = lax.optimization_barrier((grad_hidden, message))
     came_states = lax.all_to_all(message, SP, 0, 0, tiled=True)
     later, carried = scan_piece(came_states)
     back = jnp.concatenate([later, spread(list(three_parts(carried)), experts)], axis=1)
-    grad_gated, ready = lax.optimization_barrier((grad_gated, back))
     grad_gate_in, x_inside, b_inside, grad_c_proj, y_dots = inside_grads(
         grad_gated, gated, silu, slope, mix, decay, x, b_proj, c_proj, entry, rows
     )
@@ -610,12 +610,11 @@
     line = lax.axis_size("sp_0")
     mixed, gate_wgrad = lax.optimization_barrier((mixed, gate_wgrad))
     mixed_line = from_line([mixed] * line, "sp_0")
-    grads_line = from_line(pieces_for(grad_hidden, "sp_0", 1), "sp_0")
+    grads_line = from_line(pieces_for(grad_hidden, "sp_0", 0), "sp_0")
     product = dot(
-        jnp.concatenate(grads_line, axis=0), jnp.concatenate(mixed_line, axis=1), ((0,), (1,))
+        jnp.concatenate(grads_line, axis=1), jnp.concatenate(mixed_line, axis=1), ((1,), (1,))
     ).astype(bf16)
     parts = from_line(pieces_for(product, "sp_1", 0), "sp_1")
-    parts, ready = lax.optimization_barrier((parts, ready))
     product = sum(part.astype(f32) for part in parts).astype(bf16)
     parts = from_line(pieces_for(product, "sp_2", 0), "sp_2")
     grad_out_proj = sum(part.astype(f32) for part in parts)

time: 180 us -> 182 us (1.011)
  waiting for transfers between devices: 73.2 us -> 70.5 us
  matrix products: 3.5 us -> 5.61 us
    all_to_all x1, waiting for transfers between devices: 18.3 us -> 11.7 us  [body(): lax.all_to_all(summed.reshape(experts, capacity, half), SP, 0, 0, tiled=T...]
    ppermute x12, waiting for transfers between devices: 17.9 us -> 21.7 us  [from_line(): lax.ppermute(parts[k], axis, [(i, (i + k) % size) for i in range(size)])]
    dot_general x8, matrix products: 3.5 us -> 5.61 us  [dot(): return lax.dot_general(a, b, (dims, ((), ())), preferred_element_type=f32)]
  transfers between devices with their start and end apart: 21 -> 21, of which waited for: 8 -> 7; matrix products, arithmetic and copies ran while one was open for 4% -> 6% of each run, Pallas kernels for 14% -> 14%
where the time goes in v5:
time: 182 us; the launch traced here: 181 us
  waiting for transfers between devices  70.5 us (39%)
  starting transfers between devices  52.2 us (29%)
  Pallas kernels  40.1 us (22%)
  other arithmetic  6.1 us (3%)
  local copies, waits for them, and re-layouts  5.84 us (3%)
  matrix products  5.61 us (3%)
    ppermute x12, waiting for transfers between devices, from_line(): lax.ppermute(parts[k], axis, [(i, (i + k) % size) for i in range(size)])  21.7 us
    ppermute x12, starting transfers between devices, from_line(): lax.ppermute(parts[k], axis, [(i, (i + k) % size) for i in range(size)])  17.9 us
    all_to_all x1, waiting for transfers between devices, body(): came_grads = lax.all_to_all(send_grads, SP, 0, 0, tiled=True)  17.5 us
    all_to_all x1, waiting for transfers between devices, body(): came_hidden = lax.all_to_all(send_hidden, SP, 0, 0, tiled=True)  16.9 us
    pallas_call x3, Pallas kernels, whole_call(): pl.pallas_call(kernel, out_shape=[jax.ShapeDtypeStruct(*x) for x in out_s...  11.8 us
    all_to_all x1, waiting for transfers between devices, body(): lax.all_to_all(summed.reshape(experts, capacity, half), SP, 0, 0, tiled=T...  11.7 us
    all_to_all x1, starting transfers between devices, body(): came_grads = lax.all_to_all(send_grads, SP, 0, 0, tiled=True)  11.7 us
    pallas_call x1, Pallas kernels, expert_rows(): pl.pallas_call(expert_rows_kernel, grid_spec=pltpu.PrefetchScalarGridSpec...  9.2 us
  transfers between devices with their start and end apart: 21, of which 7 were waited for; matrix products, arithmetic and copies ran while one was open for 6% of the time, Pallas kernels for 14%

profile of v5, /device:TPU:0, one launch (start us, length us, event | category | flops | bytes accessed | tf_op | source)
XLA Modules:
  0.0 181.4 jit_solution(3020820673426396038)
XLA Ops:
  0.7 3.1 %route.1 = (bf16[512,1024]{1,0:T(8,128)(2,1)}, bf16[512,128]{1,0:T(8,128)(2,1)}) custom-call(s32[1]{0:T(128)} %bitcast.3.side, s32[2,128]{1,0:T(2,128)} %bitcast.73, f32[2,128]{1,0:T(2,128)} %bitcast.74, bf16[128,2048]{1,0:T(8,128)(2,1)} %cotangent.1), custom_call_target="tpu_custom_call" | custom-call | tf_op jit(solution)/shard_map/route/pallas_call | solution.py:239
  3.7 11.7 %all-to-all-start = ((bf16[64,8,1024]{2,1,0:T(8,128)(2,1)}), bf16[64,8,1024]{2,1,0:T(8,128)(2,1)S(1)}, u32[]{:S(2)}, u32[]{:S(2)}) async-start(bf16[64,8,1024]{2,1,0:T(8,128)(2,1)} %bitcast.68), calls=%async_computation | async-start | bytes 2097152 | tf_op jit(solution)/shard_map/all_to_all | solution.py:571
  16.8 17.5 %all-to-all-done = bf16[64,8,1024]{2,1,0:T(8,128)(2,1)S(1)} async-done(((bf16[64,8,1024]{2,1,0:T(8,128)(2,1)}), bf16[64,8,1024]{2,1,0:T(8,128)(2,1)S(1)}, u32[]{:S(2)}, u32[]{:S(2)}) %all-to-all-start) | async-done | bytes 1048608 | tf_op jit(solution)/shard_map/all_to_all | solution.py:571
  34.3 2.7 %collective-permute-done.other = bf16[512,1024]{1,0:T(8,128)(2,1)S(1)} collective-permute-done((bf16[512,1024]{1,0:T(8,128)(2,1)S(1)}, bf16[512,1024]{1,0:T(8,128)(2,1)S(1)}, u32[]{:S(2)}, u32[]{:S(2)}) %collective-permute-start) | collective-permute-done | bytes 1048608 | tf_op jit(solution)/shard_map/ppermute | solution.py:27
  37.9 9.2 %expert_rows.1 = (bf16[512,512]{1,0:T(8,128)(2,1)}, bf16[512,512]{1,0:T(8,128)(2,1)}, bf16[512,512]{1,0:T(8,128)(2,1)}, bf16[512,1024]{1,0:T(8,128)(2,1)}, bf16[512,1024]{1,0:T(8,128)(2,1)}) custom-call(s32[1]{0:T(128)} %bitcast.3.side, bf16[512,1024]{1,0:T(8,128)(2,1)} %bitcast.51, bf16[512,1024]{1,0:T(8,128)(2,1)} %copy-done.2, bf16[512,512]{1,0:T(8,128)(2,1)} %bitcast.69, ...), custom_call_target="tpu_custom_call" | custom-call | tf_op jit(solution)/shard_map/expert_rows/pallas_call | solution.py:99
  47.2 4.8 %all-to-all-start.1 = ((bf16[64,8,1024]{2,1,0:T(8,128)(2,1)}), bf16[64,8,1024]{2,1,0:T(8,128)(2,1)S(1)}, u32[]{:S(2)}, u32[]{:S(2)}) async-start(bf16[64,8,1024]{2,1,0:T(8,128)(2,1)} %fusion), calls=%async_computation.1 | async-start | bytes 2097152 | tf_op jit(solution)/shard_map/all_to_all | solution.py:573
  52.1 2.6 %add_convert_fusion = bf16[512,1024]{1,0:T(8,128)(2,1)} fusion(bf16[512,1024]{1,0:T(8,128)(2,1)} %collective-permute-done.1, bf16[512,1024]{1,0:T(8,128)(2,1)S(1)} %copy-done.7), kind=kLoop, calls=%fused_computation.1 | loop fusion | flops 2097152 | bytes 3145728 | tf_op jit(solution)/shard_map/convert_element_type | solution.py:579
  54.7 16.9 %all-to-all-done.1 = bf16[64,8,1024]{2,1,0:T(8,128)(2,1)S(1)} async-done(((bf16[64,8,1024]{2,1,0:T(8,128)(2,1)}), bf16[64,8,1024]{2,1,0:T(8,128)(2,1)S(1)}, u32[]{:S(2)}, u32[]{:S(2)}) %all-to-all-start.1) | async-done | bytes 1048608 | tf_op jit(solution)/shard_map/all_to_all | solution.py:573
  71.6 4.8 %all-to-all-start.2 = ((bf16[64,8,1024]{2,1,0:T(8,128)(2,1)}), bf16[64,8,1024]{2,1,0:T(8,128)(2,1)S(1)}, u32[]{:S(2)}, u32[]{:S(2)}) async-start(bf16[64,8,1024]{2,1,0:T(8,128)(2,1)} %bitcast.19), calls=%async_computation.2 | async-start | bytes 2097152 | tf_op jit(solution)/shard_map/all_to_all | solution.py:581
  78.3 4.8 %shard_map.232 = (bf16[1024,128]{1,0:T(8,128)(2,1)}, f32[1024,128]{1,0:T(8,128)}, f32[1024,128]{1,0:T(8,128)}, f32[1024,128]{1,0:T(8,128)}, bf16[16,128,128]{2,1...) custom-call(bf16[128,1024]{1,0:T(8,128)(2,1)} %scan_in.1, ...), custom_call_target="tpu_custom_call" | custom-call | tf_op jit(solution)/shard_map/pallas_call | solution.py:337
  83.1 11.7 %all-to-all-done.2 = bf16[64,8,1024]{2,1,0:T(8,128)(2,1)S(1)} async-done(((bf16[64,8,1024]{2,1,0:T(8,128)(2,1)}), bf16[64,8,1024]{2,1,0:T(8,128)(2,1)S(1)}, u32[]{:S(2)}, u32[]{:S(2)}) %all-to-all-start.2) | async-done | bytes 1048608 | tf_op jit(solution)/shard_map/all_to_all | solution.py:581
  96.6 5.9 %tall_weights.1 = (bf16[2048,512]{1,0:T(8,128)(2,1)}, bf16[2048,512]{1,0:T(8,128)(2,1)}) custom-call(s32[1]{0:T(128)} %bitcast.3.side, bf16[512,512]{1,0:T(8,128)(2,1)} %get-tuple-element.51.gate_grad, bf16[512,512]{1,0:T(8,128)(2,1)} %get-tuple-element.52.up_grad, bf16[512,1024]{1,0:T(8,128)(2,1)} %bitcast.60, bf16[512,1024]{1,0:T(8,128)(2,1)} %collective-permute-done.2.other), custom_call_target="tpu_custom_call" | custom-call | tf_op jit(solution)/shard_map/tall_weights/pallas_call | solution.py:159
  107.1 2.0 %collective-permute-start.5 = (bf16[512,128]{1,0:T(8,128)(2,1)S(1)}, bf16[512,128]{1,0:T(8,128)(2,1)S(1)}, u32[]{:S(2)}, u32[]{:S(2)}) collective-permute-start(bf16[512,128]{1,0:T(8,128)(2,1)S(1)} %get-tuple-element.97), channel_id=1, source_target_pairs={{0,64},{32,96},{64,0},{96,32},{1,65},{33,97},{65,1},{97,33},{2,66}... | collective-permute-start | bytes 393224 | tf_op jit(solution)/shard_map/ppermute | solution.py:33
  109.1 9.5 %collective-permute-done.7 = bf16[1024,128]{1,0:T(8,128)(2,1)S(1)} collective-permute-done((bf16[1024,128]{1,0:T(8,128)(2,1)S(1)}, bf16[1024,128]{1,0:T(8,128)(2,1)S(1)}, u32[]{:S(2)}, u32[]{:S(2)}) %collective-permute-start.7) | collective-permute-done | bytes 262176 | tf_op jit(solution)/shard_map/ppermute | solution.py:33
  118.5 6.1 %message.1 = (bf16[64,40,128]{2,1,0:T(8,128)(2,1)}, f32[1024,128]{1,0:T(8,128)}) custom-call(s32[1]{0:T(128)} %bitcast.3.side, bf16[1024,128]{1,0:T(8,128)(2,1)} %copy-done.4, bf16[1024,128]{1,0:T(8,128)(2,1)} %copy-done.8, bf16[1024,2048]{1,0:T(8,128)(2,1)} %out_far.1, bf16[1024,2048]{1,0:T(8,128)(2,1)} %out_far.1, f32[1024,1]{1,0:T(8,128)} %copy.27.gain, ...), custom_call_target="tpu_custom_call" | custom-call | tf_op jit(solution)/shard_map/message/pallas_call | solution.py:411
  124.6 5.2 %all-to-all-start.3 = ((bf16[64,40,128]{2,1,0:T(8,128)(2,1)}), bf16[64,40,128]{2,1,0:T(8,128)(2,1)S(1)}, u32[]{:S(2)}, u32[]{:S(2)}) async-start(bf16[64,40,128]{2,1,0:T(8,128)(2,1)} %get-tuple-element.70), calls=%async_computation.3 | async-start | bytes 1310720 | tf_op jit(solution)/shard_map/all_to_all | solution.py:598
  134.6 2.7 %collective-permute-start.11 = (bf16[128,1024]{1,0:T(8,128)(2,1)S(1)}, bf16[128,1024]{1,0:T(8,128)(2,1)S(1)}, u32[]{:S(2)}, u32[]{:S(2)}) collective-permute-start(bf16[128,1024]{1,0:T(8,128)(2,1)S(1)} %get-tuple-element.90), channel_id=1, source_target_pairs={{0,16},{8,24},{16,0},{24,8},{1,17},{9,25},{17,1},{25,9},{2,18},{10... | collective-permute-start | bytes 786440 | tf_op jit(solution)/shard_map/ppermute | solution.py:33
  138.7 6.7 %collective-permute-done.10 = bf16[128,1024]{1,0:T(8,128)(2,1)S(1)} collective-permute-done((bf16[128,1024]{1,0:T(8,128)(2,1)S(1)}, bf16[128,1024]{1,0:T(8,128)(2,1)S(1)}, u32[]{:S(2)}, u32[]{:S(2)}) %collective-permute-start.10) | collective-permute-done | bytes 262176 | tf_op jit(solution)/shard_map/ppermute | solution.py:33
  145.4 5.5 %collective-permute-done.11 = bf16[128,1024]{1,0:T(8,128)(2,1)S(1)} collective-permute-done((bf16[128,1024]{1,0:T(8,128)(2,1)S(1)}, bf16[128,1024]{1,0:T(8,128)(2,1)S(1)}, u32[]{:S(2)}, u32[]{:S(2)}) %collective-permute-start.11) | collective-permute-done | bytes 262176 | tf_op jit(solution)/shard_map/ppermute | solution.py:33
  155.6 7.4 %all-to-all-start.4 = ((bf16[64,24,128]{2,1,0:T(8,128)(2,1)}), bf16[64,24,128]{2,1,0:T(8,128)(2,1)S(1)}, u32[]{:S(2)}, u32[]{:S(2)}) async-start(bf16[64,24,128]{2,1,0:T(8,128)(2,1)} %pad_maximum_fusion), calls=%async_computation.4 | async-start | bytes 786432 | tf_op jit(solution)/shard_map/all_to_all | solution.py:604
  164.6 2.7 %collective-permute-start.14 = (bf16[32,1024]{1,0:T(8,128)(2,1)S(1)}, bf16[32,1024]{1,0:T(8,128)(2,1)S(1)}, u32[]{:S(2)}, u32[]{:S(2)}) collective-permute-start(bf16[32,1024]{1,0:T(8,128)(2,1)S(1)} %get-tuple-element.101), channel_id=1, source_target_pairs={{0,4},{2,6},{4,0},{6,2},{1,5},{3,7},{5,1},{7,3},{8,12},{10,14},{12... | collective-permute-start | bytes 196616 | tf_op jit(solution)/shard_map/ppermute | solution.py:33
  168.7 4.2 %down_weights.1 = bf16[512,2048]{1,0:T(8,128)(2,1)} custom-call(s32[1]{0:T(128)} %bitcast.3.side, bf16[512,512]{1,0:T(8,128)(2,1)} %get-tuple-element.60.active, bf16[512,1024]{1,0:T(8,128)(2,1)} %bitcast.52, bf16[512,1024]{1,0:T(8,128)(2,1)} %copy-done.2), custom_call_target="tpu_custom_call" | custom-call | tf_op jit(solution)/shard_map/down_weights/pallas_call | solution.py:143
  172.9 4.4 %shard_map.233 = (bf16[128,1024]{1,0:T(8,128)(2,1)}, f32[1024,128]{1,0:T(8,128)}, f32[128,512]{1,0:T(8,128)}, bf16[128,512]{1,0:T(8,128)(2,1)}, f32[16,128]{1,0:T(8,128)}) custom-call(f32[1024,128]{1,0:T(8,128)} %get-tuple-element.73.grad_in, f32[1024,128]{1,0:T(8,128)} %get-tuple-element.64.gated_in, f32[1024,128]{1,0:T(8,128)} %get-tuple-element.65.silu_in, ...), custom_call_target="tpu_custom_call" | custom-call | tf_op jit(solution)/shard_map/pallas_call | solution.py:337
  178.8 2.6 %shard_map.234 = (bf16[128,1024]{1,0:T(8,128)(2,1)}, bf16[128,512]{1,0:T(8,128)(2,1)}, f32[16,128]{1,0:T(8,128)}) custom-call(bf16[64,24,128]{2,1,0:T(8,128)(2,1)} %copy-done.5, bf16[128,512]{1,0:T(8,128)(2,1)} %b_proj.5, bf16[1024,128]{1,0:T(8,128)(2,1)} %get-tuple-element.71.x_in, bf16[1024,128]{1,0:T(8,128)(2,1)} %get-tuple-element.72.tail_in, ...), custom_call_target="tpu_custom_call" | custom-call | tf_op jit(solution)/shard_map/pallas_call | solution.py:337
  (84 shorter events, 26.1 us)
Async XLA Ops:
  0.6 14.8 %copy-start = (bf16[128,2048]{1,0:T(8,128)(2,1)S(1)}, bf16[128,2048]{1,0:T(8,128)(2,1)}, u32[]{:S(2)}) copy-start(bf16[128,2048]{1,0:T(8,128)(2,1)} %param.17) | copy-start | bytes 1572868
  3.7 30.6 %all-to-all-start = ((bf16[64,8,1024]{2,1,0:T(8,128)(2,1)}), bf16[64,8,1024]{2,1,0:T(8,128)(2,1)S(1)}, u32[]{:S(2)}, u32[]{:S(2)}) async-start(bf16[64,8,1024]{2,1,0:T(8,128)(2,1)} %bitcast.68), calls=%async_computation | async-start | bytes 2097152 | tf_op jit(solution)/shard_map/all_to_all | solution.py:571
  34.3 2.7 %collective-permute-start = (bf16[512,1024]{1,0:T(8,128)(2,1)S(1)}, bf16[512,1024]{1,0:T(8,128)(2,1)S(1)}, u32[]{:S(2)}, u32[]{:S(2)}) collective-permute-start(bf16[512,1024]{1,0:T(8,128)(2,1)S(1)} %bitcast.50), channel_id=1, source_target_pairs={{0,1},{1,0},{2,3},{3,2},{4,5},{5,4},{6,7},{7,6},{8,9},{9,8},{10,11... | collective-permute-start | bytes 3145736 | tf_op jit(solution)/shard_map/ppermute | solution.py:27
  47.1 5.0 %collective-permute-start.1 = (bf16[512,1024]{1,0:T(8,128)(2,1)}, bf16[512,1024]{1,0:T(8,128)(2,1)}, u32[]{:S(2)}, u32[]{:S(2)}) collective-permute-start(bf16[512,1024]{1,0:T(8,128)(2,1)} %get-tuple-element.54), channel_id=1, source_target_pairs={{0,1},{1,0},{2,3},{3,2},{4,5},{5,4},{6,7},{7,6},{8,9},{9,8},{10,11... | collective-permute-start | bytes 3145736 | tf_op jit(solution)/shard_map/ppermute | solution.py:27
  47.2 24.4 %all-to-all-start.1 = ((bf16[64,8,1024]{2,1,0:T(8,128)(2,1)}), bf16[64,8,1024]{2,1,0:T(8,128)(2,1)S(1)}, u32[]{:S(2)}, u32[]{:S(2)}) async-start(bf16[64,8,1024]{2,1,0:T(8,128)(2,1)} %fusion), calls=%async_computation.1 | async-start | bytes 2097152 | tf_op jit(solution)/shard_map/all_to_all | solution.py:573
  52.1 24.4 %copy-start.10 = (bf16[1024]{0:T(1024)(128)(2,1)S(1)}, bf16[1024]{0:T(1024)(128)(2,1)}, u32[]{:S(2)}) copy-start(bf16[1024]{0:T(1024)(128)(2,1)} %param.27) | copy-start | bytes 6148
  54.7 22.9 %copy-start.6 = (bf16[128,2048]{1,0:T(8,128)(2,1)S(1)}, bf16[128,2048]{1,0:T(8,128)(2,1)}, u32[]{:S(2)}) copy-start(bf16[128,2048]{1,0:T(8,128)(2,1)} %cotangent.1) | copy-start | bytes 1572868
  71.6 23.2 %all-to-all-start.2 = ((bf16[64,8,1024]{2,1,0:T(8,128)(2,1)}), bf16[64,8,1024]{2,1,0:T(8,128)(2,1)S(1)}, u32[]{:S(2)}, u32[]{:S(2)}) async-start(bf16[64,8,1024]{2,1,0:T(8,128)(2,1)} %bitcast.19), calls=%async_computation.2 | async-start | bytes 2097152 | tf_op jit(solution)/shard_map/all_to_all | solution.py:581
  76.4 20.2 %collective-permute-start.2 = (bf16[512,1024]{1,0:T(8,128)(2,1)S(1)}, bf16[512,1024]{1,0:T(8,128)(2,1)}, u32[]{:S(2)}, u32[]{:S(2)}) collective-permute-start(bf16[512,1024]{1,0:T(8,128)(2,1)S(1)} %bitcast.59), channel_id=1, source_target_pairs={{0,1},{1,0},{2,3},{3,2},{4,5},{5,4},{6,7},{7,6},{8,9},{9,8},{10,11... | collective-permute-start | bytes 3145736 | tf_op jit(solution)/shard_map/ppermute | solution.py:27
  96.3 9.5 %collective-permute-start.3 = (bf16[1024,128]{1,0:T(8,128)(2,1)S(1)}, bf16[1024,128]{1,0:T(8,128)(2,1)S(1)}, u32[]{:S(2)}, u32[]{:S(2)}) collective-permute-start(bf16[1024,128]{1,0:T(8,128)(2,1)S(1)} %fusion.1.grad_own), channel_id=1, source_target_pairs={{0,1},{1,0},{2,3},{3,2},{4,5},{5,4},{6,7},{7,6},{8,9},{9,8},{10,11... | collective-permute-start | bytes 786440 | tf_op jit(solution)/shard_map/ppermute | solution.py:27
  102.5 16.0 %collective-permute-start.7 = (bf16[1024,128]{1,0:T(8,128)(2,1)S(1)}, bf16[1024,128]{1,0:T(8,128)(2,1)S(1)}, u32[]{:S(2)}, u32[]{:S(2)}) collective-permute-start(bf16[1024,128]{1,0:T(8,128)(2,1)S(1)} %copy-done.11), channel_id=1, source_target_pairs={{0,32},{32,64},{64,96},{96,0},{1,33},{33,65},{65,97},{97,1},{2,34}... | collective-permute-start | bytes 786440 | tf_op jit(solution)/shard_map/ppermute | solution.py:33
  102.9 26.8 %collective-permute-start.8 = (bf16[1024,128]{1,0:T(8,128)(2,1)S(1)}, bf16[1024,128]{1,0:T(8,128)(2,1)S(1)}, u32[]{:S(2)}, u32[]{:S(2)}) collective-permute-start(bf16[1024,128]{1,0:T(8,128)(2,1)S(1)} %copy-done.11), channel_id=1, source_target_pairs={{0,64},{32,96},{64,0},{96,32},{1,65},{33,97},{65,1},{97,33},{2,66}... | collective-permute-start | bytes 786440 | tf_op jit(solution)/shard_map/ppermute | solution.py:33
  104.8 25.0 %collective-permute-start.9 = (bf16[1024,128]{1,0:T(8,128)(2,1)S(1)}, bf16[1024,128]{1,0:T(8,128)(2,1)S(1)}, u32[]{:S(2)}, u32[]{:S(2)}) collective-permute-start(bf16[1024,128]{1,0:T(8,128)(2,1)S(1)} %copy-done.11), channel_id=1, source_target_pairs={{0,96},{32,0},{64,32},{96,64},{1,97},{33,1},{65,33},{97,65},{2,98}... | collective-permute-start | bytes 786440 | tf_op jit(solution)/shard_map/ppermute | solution.py:33
  106.0 23.8 %collective-permute-start.4 = (bf16[512,128]{1,0:T(8,128)(2,1)S(1)}, bf16[512,128]{1,0:T(8,128)(2,1)S(1)}, u32[]{:S(2)}, u32[]{:S(2)}) collective-permute-start(bf16[512,128]{1,0:T(8,128)(2,1)S(1)} %get-tuple-element.98), channel_id=1, source_target_pairs={{0,32},{32,64},{64,96},{96,0},{1,33},{33,65},{65,97},{97,1},{2,34}... | collective-permute-start | bytes 393224 | tf_op jit(solution)/shard_map/ppermute | solution.py:33
  107.1 22.7 %collective-permute-start.5 = (bf16[512,128]{1,0:T(8,128)(2,1)S(1)}, bf16[512,128]{1,0:T(8,128)(2,1)S(1)}, u32[]{:S(2)}, u32[]{:S(2)}) collective-permute-start(bf16[512,128]{1,0:T(8,128)(2,1)S(1)} %get-tuple-element.97), channel_id=1, source_target_pairs={{0,64},{32,96},{64,0},{96,32},{1,65},{33,97},{65,1},{97,33},{2,66}... | collective-permute-start | bytes 393224 | tf_op jit(solution)/shard_map/ppermute | solution.py:33
  118.5 11.3 %collective-permute-start.6 = (bf16[512,128]{1,0:T(8,128)(2,1)S(1)}, bf16[512,128]{1,0:T(8,128)(2,1)S(1)}, u32[]{:S(2)}, u32[]{:S(2)}) collective-permute-start(bf16[512,128]{1,0:T(8,128)(2,1)S(1)} %get-tuple-element.96), channel_id=1, source_target_pairs={{0,96},{32,0},{64,32},{96,64},{1,97},{33,1},{65,33},{97,65},{2,98}... | collective-permute-start | bytes 393224 | tf_op jit(solution)/shard_map/ppermute | solution.py:33
  124.6 27.5 %all-to-all-start.3 = ((bf16[64,40,128]{2,1,0:T(8,128)(2,1)}), bf16[64,40,128]{2,1,0:T(8,128)(2,1)S(1)}, u32[]{:S(2)}, u32[]{:S(2)}) async-start(bf16[64,40,128]{2,1,0:T(8,128)(2,1)} %get-tuple-element.70), calls=%async_computation.3 | async-start | bytes 1310720 | tf_op jit(solution)/shard_map/all_to_all | solution.py:598
  132.9 12.5 %collective-permute-start.10 = (bf16[128,1024]{1,0:T(8,128)(2,1)S(1)}, bf16[128,1024]{1,0:T(8,128)(2,1)S(1)}, u32[]{:S(2)}, u32[]{:S(2)}) collective-permute-start(bf16[128,1024]{1,0:T(8,128)(2,1)S(1)} %get-tuple-element.88), channel_id=1, source_target_pairs={{0,8},{8,16},{16,24},{24,0},{1,9},{9,17},{17,25},{25,1},{2,10},{10... | collective-permute-start | bytes 786440 | tf_op jit(solution)/shard_map/ppermute | solution.py:33
  134.6 16.4 %collective-permute-start.11 = (bf16[128,1024]{1,0:T(8,128)(2,1)S(1)}, bf16[128,1024]{1,0:T(8,128)(2,1)S(1)}, u32[]{:S(2)}, u32[]{:S(2)}) collective-permute-start(bf16[128,1024]{1,0:T(8,128)(2,1)S(1)} %get-tuple-element.90), channel_id=1, source_target_pairs={{0,16},{8,24},{16,0},{24,8},{1,17},{9,25},{17,1},{25,9},{2,18},{10... | collective-permute-start | bytes 786440 | tf_op jit(solution)/shard_map/ppermute | solution.py:33
  137.2 13.7 %collective-permute-start.12 = (bf16[128,1024]{1,0:T(8,128)(2,1)S(1)}, bf16[128,1024]{1,0:T(8,128)(2,1)}, u32[]{:S(2)}, u32[]{:S(2)}) collective-permute-start(bf16[128,1024]{1,0:T(8,128)(2,1)S(1)} %get-tuple-element.89), channel_id=1, source_target_pairs={{0,24},{8,0},{16,8},{24,16},{1,25},{9,1},{17,9},{25,17},{2,26},{10... | collective-permute-start | bytes 786440 | tf_op jit(solution)/shard_map/ppermute | solution.py:33
  155.6 22.5 %all-to-all-start.4 = ((bf16[64,24,128]{2,1,0:T(8,128)(2,1)}), bf16[64,24,128]{2,1,0:T(8,128)(2,1)S(1)}, u32[]{:S(2)}, u32[]{:S(2)}) async-start(bf16[64,24,128]{2,1,0:T(8,128)(2,1)} %pad_maximum_fusion), calls=%async_computation.4 | async-start | bytes 786432 | tf_op jit(solution)/shard_map/all_to_all | solution.py:604
  163.0 14.3 %collective-permute-start.13 = (bf16[32,1024]{1,0:T(8,128)(2,1)S(1)}, bf16[32,1024]{1,0:T(8,128)(2,1)S(1)}, u32[]{:S(2)}, u32[]{:S(2)}) collective-permute-start(bf16[32,1024]{1,0:T(8,128)(2,1)S(1)} %get-tuple-element.99), channel_id=1, source_target_pairs={{0,2},{2,4},{4,6},{6,0},{1,3},{3,5},{5,7},{7,1},{8,10},{10,12},{12... | collective-permute-start | bytes 196616 | tf_op jit(solution)/shard_map/ppermute | solution.py:33
  164.6 12.7 %collective-permute-start.14 = (bf16[32,1024]{1,0:T(8,128)(2,1)S(1)}, bf16[32,1024]{1,0:T(8,128)(2,1)S(1)}, u32[]{:S(2)}, u32[]{:S(2)}) collective-permute-start(bf16[32,1024]{1,0:T(8,128)(2,1)S(1)} %get-tuple-element.101), channel_id=1, source_target_pairs={{0,4},{2,6},{4,0},{6,2},{1,5},{3,7},{5,1},{7,3},{8,12},{10,14},{12... | collective-permute-start | bytes 196616 | tf_op jit(solution)/shard_map/ppermute | solution.py:33
  167.3 10.0 %collective-permute-start.15 = (bf16[32,1024]{1,0:T(8,128)(2,1)S(1)}, bf16[32,1024]{1,0:T(8,128)(2,1)S(1)}, u32[]{:S(2)}, u32[]{:S(2)}) collective-permute-start(bf16[32,1024]{1,0:T(8,128)(2,1)S(1)} %get-tuple-element.100), channel_id=1, source_target_pairs={{0,6},{2,0},{4,2},{6,4},{1,7},{3,1},{5,3},{7,5},{8,14},{10,8},{12,... | collective-permute-start | bytes 196616 | tf_op jit(solution)/shard_map/ppermute | solution.py:33
  (11 other events, 63.9 us)

commit v6 on v5

--- a/solution.py
+++ b/solution.py
@@ -41,13 +41,6 @@
     return [
         lax.dynamic_slice_in_dim(x, lax.rem(spot + k, size) * span, span, dim) for k in range(size)
     ]
-
-
-def three_parts(x):
-    high = lax.reduce_precision(x, 8, 7)
-    rest = x - high
-    middle = lax.reduce_precision(rest, 8, 7)
-    return high.astype(bf16), middle.astype(bf16), (rest - middle).astype(bf16)
 
 
 def expert_rows_kernel(
@@ -109,94 +102,50 @@
     )(side, mine, other, gate_value, up_value, w_down, w_down, w_gate, w_gate, w_up, w_up)
 
 
-def down_kernel(side, active, mine, other, out):
-    @pl.when(pl.program_id(0) == 0)
+def weights_kernel(
+    side, active, gate_grad, up_grad, grads_own, grads_far, hidden_own, hidden_far,
+    down_out, gate_out, up_out,
+):
+    def write(grads, hidden):
+        down_out[...] = dot(active[...], grads, ((0,), (0,))).astype(bf16)
+        gate_out[...] = dot(hidden, gate_grad[...], ((0,), (0,))).astype(bf16)
+        up_out[...] = dot(hidden, up_grad[...], ((0,), (0,))).astype(bf16)
+
+    @pl.when(pl.program_id(0) < 2)
     def _():
-        out[...] = dot(active[...], mine[...], ((0,), (0,))).astype(bf16)
-
-    @pl.when(pl.program_id(0) == 1)
+        write(grads_own[...], hidden_own[...])
+
+    @pl.when(pl.program_id(0) >= 2)
     def _():
-        out[...] = dot(active[...], other[...], ((0,), (0,))).astype(bf16)
-
-
-def tall_kernel(side, gate_grad, up_grad, mine, other, gate_out, up_out):
-    def write(rows):
-        gate_out[...] = dot(rows, gate_grad[...], ((0,), (0,))).astype(bf16)
-        up_out[...] = dot(rows, up_grad[...], ((0,), (0,))).astype(bf16)
-
-    @pl.when(pl.program_id(0) == 0)
-    def _():
-        write(mine[...])
-
-    @pl.when(pl.program_id(0) == 1)
-    def _():
-        write(other[...])
-
-
-def half_of(i, side):
-    return lax.rem(i + side[0], 2)
-
-
-def down_weights(side, active, mine, other):
-    rows, half = mine.shape
+        write(grads_far[...], hidden_far[...])
+
+
+def expert_weights(side, active, gate_grad, up_grad, grads_own, grads_far, hidden_own, hidden_far):
+    rows, half = grads_own.shape
     hidden = active.shape[1]
+    own = pl.BlockSpec((rows, half // 2), lambda i, side: (0, jnp.minimum(i, 1)))
+    far = pl.BlockSpec((rows, half // 2), lambda i, side: (0, jnp.maximum(i - 2, 0)))
+
+    def place(i, side):
+        return lax.rem(i + 2 * side[0], 4)
+
+    tall = pl.BlockSpec((half // 2, hidden), lambda i, side: (place(i, side), 0))
     return pl.pallas_call(
-        down_kernel,
+        weights_kernel,
         grid_spec=pltpu.PrefetchScalarGridSpec(
             num_scalar_prefetch=1,
-            grid=(2,),
-            in_specs=[whole_block(rows, hidden)] + [whole_block(rows, half)] * 2,
-            out_specs=pl.BlockSpec((hidden, half), lambda i, side: (0, half_of(i, side))),
+            grid=(4,),
+            in_specs=[whole_block(rows, hidden)] * 3 + [own, far, own, far],
+            out_specs=[
+                pl.BlockSpec((hidden, half // 2), lambda i, side: (0, place(i, side))),
+                tall,
+                tall,
+            ],
         ),
-        out_shape=jax.ShapeDtypeStruct((hidden, 2 * half), bf16),
-        name="down_weights",
-    )(side, active, mine, other)
-
-
-def tall_weights(side, gate_grad, up_grad, mine, other):
-    rows, half = mine.shape
-    hidden = gate_grad.shape[1]
-    return pl.pallas_call(
-        tall_kernel,
-        grid_spec=pltpu.PrefetchScalarGridSpec(
-            num_scalar_prefetch=1,
-            grid=(2,),
-            in_specs=[whole_block(rows, hidden)] * 2 + [whole_block(rows, half)] * 2,
-            out_specs=[pl.BlockSpec((half, hidden), lambda i, side: (half_of(i, side), 0))] * 2,
-        ),
-        out_shape=[jax.ShapeDtypeStruct((2 * half, hidden), bf16)] * 2,
-        name="tall_weights",
-    )(side, gate_grad, up_grad, mine, other)
-
-
-def scan_piece(came):
-    blocks = came.shape[0]
-    values = came[:, :16].reshape(blocks, -1)
-    local = came[:, 16:32].reshape(blocks, -1).astype(f32)
-    pieces = 4
-    lead = lax.rem(lax.axis_index(SP), pieces) == 0
-    sums = jnp.where(lead, came[:, 35:38, 0].astype(f32).sum(axis=1), 0.0)
-    at = jnp.arange(blocks)
-    after = at[None, :] > at[:, None]
-    gaps = jnp.zeros((blocks, blocks), f32)
-    for k in range(3):
-        part = jnp.where(after, came[:, 32 + k, 0][None, :], 0).astype(bf16)
-        gaps = gaps + dot(part, after.astype(bf16), ((1,), (0,)))
-    weights = jnp.where(after, jnp.exp(gaps), 0.0)
-    high = lax.reduce_precision(weights, 8, 7)
-    low = weights - high
-    later = dot(high.astype(bf16), values, ((1,), (0,))) + dot(
-        low.astype(bf16), values, ((1,), (0,))
-    )
-    own = sums - jnp.sum(later * local, axis=1)
-    carried = jnp.sum(jnp.where(after, own[None, :], 0.0), axis=1)
-    return later.astype(bf16).reshape(blocks, 16, STATE), carried
-
-
-def spread(parts, blocks):
-    rows = jnp.stack(parts, axis=1)
-    rows = jnp.pad(rows, ((0, 0), (0, 8 - len(parts))))
-    return jnp.broadcast_to(rows[:, :, None], (blocks, 8, STATE)).astype(bf16)
+        out_shape=[jax.ShapeDtypeStruct((hidden, 2 * half), bf16)]
+        + [jax.ShapeDtypeStruct((2 * half, hidden), bf16)] * 2,
+        name="weights",
+    )(side, active, gate_grad, up_grad, grads_own, grads_far, hidden_own, hidden_far)
 
 
 def exact_dot(a, b, dims):
@@ -445,56 +394,112 @@
     gate_grad, x_grad, b_grad, c_grad, y_dots,
 ):
     tokens = x_in.shape[1]
-    for g in range(x_in.shape[0] // GROUP):
-        span = slice(g * GROUP, (g + 1) * GROUP)
-        states = slice(g * STATE, (g + 1) * STATE)
-        first = g * PER_GROUP
-        grad_gated = grad_in[span, :]
-        gate_grad[:, span] = jnp.transpose(grad_gated * slope_in[span, :]).astype(bf16)
-        grad_y = grad_gated * silu_in[span, :]
-        grad_y_b = grad_y.astype(bf16)
-        grown = (grad_y * per_head(rows_in[0, g], 0)).astype(bf16)
-        b_group, c_group = b_proj[:, states], c_proj[:, states]
-        x = x_in[span, :]
-        weights = jnp.zeros((tokens, tokens), f32)
-        inside = []
-        for r in range(PER_GROUP):
-            h = first + r
-            head = slice(r * HEAD_DIM, (r + 1) * HEAD_DIM)
-            inside.append(dot(grad_y_b[head, :], mix_in[h], ((1,), (0,))))
-            weights = weights + decay_in[h] * dot(grad_y_b[head, :], x[head, :], ((0,), (0,)))
-        x_grad[span, :] = jnp.concatenate(inside, axis=0)
-        weights = weights.astype(bf16)
-        c_grad[:, states] = (
-            dot(weights, b_group, ((1,), (0,)))
-            + dot(grown, entry[span, :].astype(bf16), ((0,), (0,)))
-        ).astype(bf16)
-        b_grad[:, states] = dot(weights, c_group, ((0,), (0,)))
-        y_dots[first : first + PER_GROUP, :] = jnp.concatenate(
-            head_sums(grad_gated * gated_in[span, :]), axis=0
-        )
+    grad_gated = grad_in[...]
+    gate_grad[...] = jnp.transpose(grad_gated * slope_in[...]).astype(bf16)
+    grad_y = grad_gated * silu_in[...]
+    grad_y_b = grad_y.astype(bf16)
+    grown = (grad_y * per_head(rows_in[0, 0], 0)).astype(bf16)
+    x = x_in[...]
+    weights = jnp.zeros((tokens, tokens), f32)
+    inside = []
+    for r in range(PER_GROUP):
+        head = slice(r * HEAD_DIM, (r + 1) * HEAD_DIM)
+        inside.append(dot(grad_y_b[head, :], mix_in[r], ((1,), (0,))))
+        weights = weights + decay_in[r] * dot(grad_y_b[head, :], x[head, :], ((0,), (0,)))
+    x_grad[...] = jnp.concatenate(inside, axis=0)
+    weights = weights.astype(bf16)
+    c_grad[...] = (
+        dot(weights, b_proj[...], ((1,), (0,)))
+        + dot(grown, entry[...].astype(bf16), ((0,), (0,)))
+    ).astype(bf16)
+    b_grad[...] = dot(weights, c_proj[...], ((0,), (0,)))
+    y_dots[0] = jnp.concatenate(head_sums(grad_gated * gated_in[...]), axis=0)
 
 
 def inside_grads(grad, gated, silu, slope, mix, decay, x, b_proj, c_proj, entry, rows):
     inner, tokens = grad.shape
-    return whole_call(
+    channels = pl.BlockSpec((GROUP, tokens), lambda i: (i, 0))
+    tokens_by = pl.BlockSpec((tokens, STATE), lambda i: (0, i))
+    square = pl.BlockSpec((PER_GROUP, tokens, tokens), lambda i: (i, 0, 0))
+    outs = [
+        ((tokens, inner), bf16),
+        ((inner, tokens), f32),
+        (b_proj.shape, f32),
+        (b_proj.shape, bf16),
+        ((inner // GROUP, PER_GROUP, tokens), f32),
+    ]
+    return pl.pallas_call(
         inside_kernel,
-        [
-            ((tokens, inner), bf16),
-            ((inner, tokens), f32),
-            (b_proj.shape, f32),
-            (b_proj.shape, bf16),
-            ((decay.shape[0], tokens), f32),
+        grid=(inner // GROUP,),
+        in_specs=[channels] * 4
+        + [square] * 2
+        + [channels, tokens_by, tokens_by, pl.BlockSpec((GROUP, STATE), lambda i: (i, 0))]
+        + [pl.BlockSpec((3, 1, PER_GROUP, tokens), lambda i: (0, i, 0, 0))],
+        out_specs=[
+            pl.BlockSpec((tokens, GROUP), lambda i: (0, i)),
+            channels,
+            tokens_by,
+            tokens_by,
+            pl.BlockSpec((1, PER_GROUP, tokens), lambda i: (i, 0, 0)),
         ],
-        grad, gated, silu, slope, mix, decay, x, b_proj, c_proj, entry, rows,
-    )
+        out_shape=[jax.ShapeDtypeStruct(*x) for x in outs],
+        name="inside",
+    )(grad, gated, silu, slope, mix, decay, x, b_proj, c_proj, entry, rows)
+
+
+def owner_kernel(lead, came, back, values, local, later):
+    blocks = came.shape[0]
+    values[...] = came[:, 0:16, :].astype(f32)
+    local[...] = came[:, 16:32, :].astype(f32)
+    extra = came[:, 32:40, :].astype(f32)
+    first, second = grid_of(blocks, blocks, 0), grid_of(blocks, blocks, 1)
+    after = (second > first).astype(bf16)
+    gaps = jnp.zeros((blocks, blocks), f32)
+    for k in range(3):
+        part = jnp.where(first < second, extra[:, k, :blocks], 0.0).astype(bf16)
+        gaps = gaps + dot(after, part, ((1,), (0,)))
+    weights = jnp.where(second > first, jnp.exp(gaps), 0.0)
+    high = weights.astype(bf16)
+    low = (weights - high.astype(f32)).astype(bf16)
+    total = jnp.zeros((blocks, STATE), f32)
+    for r in range(16):
+        piece = values[:, r, :].astype(bf16)
+        found = dot(high, piece, ((1,), (0,))) + dot(low, piece, ((1,), (0,)))
+        later[:, r, :] = found
+        total = total + found * local[:, r, :]
+    total = jnp.broadcast_to(jnp.sum(total, axis=1, keepdims=True), (blocks, STATE))
+    sums = extra[:, 3, :] + extra[:, 4, :] + extra[:, 5, :]
+    own = jnp.where(lead[0] == 1, sums, 0.0) - total
+    carried = exact_dot(after.astype(f32), own, ((1,), (0,)))
+    back[:, 0:16, :] = later[...].astype(bf16)
+    zero = jnp.zeros((blocks, 5, STATE), f32)
+    back[:, 16:24, :] = jnp.concatenate(spread_parts(carried, blocks, 1) + [zero], axis=1).astype(
+        bf16
+    )
+
+
+def owner_scan(lead, came):
+    blocks = came.shape[0]
+    scratch = pltpu.VMEM((blocks, 16, STATE), f32)
+    return pl.pallas_call(
+        owner_kernel,
+        grid_spec=pltpu.PrefetchScalarGridSpec(
+            num_scalar_prefetch=1,
+            grid=(1,),
+            in_specs=[whole_block(*came.shape)],
+            out_specs=whole_block(blocks, 24, STATE),
+            scratch_shapes=[scratch] * 3,
+        ),
+        out_shape=jax.ShapeDtypeStruct((blocks, 24, STATE), bf16),
+        name="owner",
+    )(lead, came)
 
 
 def final_kernel(back, b_proj, x_in, tail_in, rows_in, x_inside, y_dots, b_inside, x_grad, b_grad, decay_grad):
     groups = x_in.shape[0] // GROUP
     pieces = GROUP // 16
     tokens = x_in.shape[1]
-    heads = y_dots.shape[0]
+    heads = groups * PER_GROUP
     dots = []
     for g in range(groups):
         span = slice(g * GROUP, (g + 1) * GROUP)
@@ -507,7 +512,8 @@
             b_inside[:, states] + dot(tail_in[span, :], later, ((0,), (0,)))
         ).astype(bf16)
         dots = dots + head_sums(x_in[span, :].astype(f32) * grad)
-    own = y_dots[...] - jnp.concatenate(dots, axis=0)
+    own = jnp.concatenate([y_dots[g] for g in range(groups)], axis=0)
+    own = own - jnp.concatenate(dots, axis=0)
     after = (grid_of(tokens, tokens, 0) >= grid_of(tokens, tokens, 1)).astype(f32)
     extra = jnp.sum(back[:, 16:24, :].astype(f32), axis=1)
     extra = jnp.sum(extra.reshape(heads, extra.shape[0] // heads, STATE), axis=1)
@@ -521,7 +527,7 @@
         [
             ((tokens, inner), bf16),
             (b_proj.shape, bf16),
-            (y_dots.shape, f32),
+            ((inner // HEAD_DIM, tokens), f32),
         ],
         back, b_proj, x, x_tail, rows, x_inside, y_dots, b_inside,
     )
@@ -581,8 +587,9 @@
     returned = lax.all_to_all(summed.reshape(experts, capacity, half), SP, 0, 0, tiled=True)
     hidden_own = came_hidden.reshape(-1, half)
     hidden_far = swapped(hidden_own)
-    down_wgrad = down_weights(side, active, grads_own, grads_far)
-    gate_wgrad, up_wgrad = tall_weights(side, gate_grad, up_grad, hidden_own, hidden_far)
+    down_wgrad, gate_wgrad, up_wgrad = expert_weights(
+        side, active, gate_grad, up_grad, grads_own, grads_far, hidden_own, hidden_far
+    )
     moe_terms = dot(returned.reshape(-1, half), either, ((0,), (0,)))
     grad_own = (cotangent_rows.astype(f32) + moe_terms).astype(bf16)
     grad_far = swapped(grad_own)
@@ -596,8 +603,8 @@
         side, grad_own, grad_far, w_out, gain, gated, silu, carry, c_proj, local, rows, inverse
     )
     came_states = lax.all_to_all(message, SP, 0, 0, tiled=True)
-    later, carried = scan_piece(came_states)
-    back = jnp.concatenate([later, spread(list(three_parts(carried)), experts)], axis=1)
+    lead = lax.rem(lax.axis_index(SP), HEAD_DIM // 16) == 0
+    back = owner_scan(lead.astype(jnp.int32)[None], came_states)
     grad_gate_in, x_inside, b_inside, grad_c_proj, y_dots = inside_grads(
         grad_gated, gated, silu, slope, mix, decay, x, b_proj, c_proj, entry, rows
     )

time: 182 us -> 184 us (1.011)
  waiting for transfers between devices: 70.5 us -> 72.7 us
  Pallas kernels: 40.1 us -> 42.1 us
    pallas_call x2 -> x3, Pallas kernels: 10 us -> 16.4 us  [the longest x1 8.16 us: expert_weights(): pl.pallas_call(weights_kernel, grid_spec=pltpu.PrefetchScalarGridSpec(num...]
    pallas_call x3 -> x2, Pallas kernels: 11.8 us -> 7.39 us  [whole_call(): pl.pallas_call(kernel, out_shape=[jax.ShapeDtypeStruct(*x) for x in out_s...]
    all_to_all x1, waiting for transfers between devices: 0.01 us -> 2.13 us  [body(): back = lax.all_to_all(back, SP, 0, 0, tiled=True)]
    dot_general x8 -> x3, matrix products: 5.61 us -> 4.54 us  [dot(): return lax.dot_general(a, b, (dims, ((), ())), preferred_element_type=f32)]
  transfers between devices with their start and end apart: 21 -> 21, of which waited for: 7 -> 8; matrix products, arithmetic and copies ran while one was open for 6% -> 6% of each run, Pallas kernels for 14% -> 13%
where the time goes in v6:
time: 184 us; the launch traced here: 183 us
  waiting for transfers between devices  72.7 us (40%)
  starting transfers between devices  52.3 us (28%)
  Pallas kernels  42.1 us (23%)
  local copies, waits for them, and re-layouts  5.77 us (3%)
  other arithmetic  4.56 us (2%)
  matrix products  4.54 us (2%)
    ppermute x12, waiting for transfers between devices, from_line(): lax.ppermute(parts[k], axis, [(i, (i + k) % size) for i in range(size)])  21.8 us
    ppermute x12, starting transfers between devices, from_line(): lax.ppermute(parts[k], axis, [(i, (i + k) % size) for i in range(size)])  17.9 us
    all_to_all x1, waiting for transfers between devices, body(): came_grads = lax.all_to_all(send_grads, SP, 0, 0, tiled=True)  17.5 us
    all_to_all x1, waiting for transfers between devices, body(): came_hidden = lax.all_to_all(send_hidden, SP, 0, 0, tiled=True)  16.9 us
    all_to_all x1, waiting for transfers between devices, body(): lax.all_to_all(summed.reshape(experts, capacity, half), SP, 0, 0, tiled=T...  11.8 us
    all_to_all x1, starting transfers between devices, body(): came_grads = lax.all_to_all(send_grads, SP, 0, 0, tiled=True)  11.7 us
    pallas_call x1, Pallas kernels, expert_rows(): pl.pallas_call(expert_rows_kernel, grid_spec=pltpu.PrefetchScalarGridSpec...  9.19 us
    pallas_call x1, Pallas kernels, expert_weights(): pl.pallas_call(weights_kernel, grid_spec=pltpu.PrefetchScalarGridSpec(num...  8.16 us
  transfers between devices with their start and end apart: 21, of which 8 were waited for; matrix products, arithmetic and copies ran while one was open for 6% of the time, Pallas kernels for 13%

profile of v6, /device:TPU:0, one launch (start us, length us, event | category | flops | bytes accessed | tf_op | source)
XLA Modules:
  0.0 183.0 jit_solution(14907343666117761294)
XLA Ops:
  0.7 3.1 %route.1 = (bf16[512,1024]{1,0:T(8,128)(2,1)}, bf16[512,128]{1,0:T(8,128)(2,1)}) custom-call(s32[1]{0:T(128)} %bitcast.3.side, s32[2,128]{1,0:T(2,128)} %bitcast.46, f32[2,128]{1,0:T(2,128)} %bitcast.47, bf16[128,2048]{1,0:T(8,128)(2,1)} %cotangent.1), custom_call_target="tpu_custom_call" | custom-call | tf_op jit(solution)/shard_map/route/pallas_call | solution.py:188
  3.7 11.7 %all-to-all-start = ((bf16[64,8,1024]{2,1,0:T(8,128)(2,1)}), bf16[64,8,1024]{2,1,0:T(8,128)(2,1)S(1)}, u32[]{:S(2)}, u32[]{:S(2)}) async-start(bf16[64,8,1024]{2,1,0:T(8,128)(2,1)} %bitcast.41), calls=%async_computation | async-start | bytes 2097152 | tf_op jit(solution)/shard_map/all_to_all | solution.py:577
  16.8 17.5 %all-to-all-done = bf16[64,8,1024]{2,1,0:T(8,128)(2,1)S(1)} async-done(((bf16[64,8,1024]{2,1,0:T(8,128)(2,1)}), bf16[64,8,1024]{2,1,0:T(8,128)(2,1)S(1)}, u32[]{:S(2)}, u32[]{:S(2)}) %all-to-all-start) | async-done | bytes 1048608 | tf_op jit(solution)/shard_map/all_to_all | solution.py:577
  34.3 2.7 %collective-permute-done.other.grads_far = bf16[512,1024]{1,0:T(8,128)(2,1)S(1)} collective-permute-done((bf16[512,1024]{1,0:T(8,128)(2,1)S(1)}, bf16[512,1024]{1,0:T(8,128)(2,1)S(1)}, u32[]{:S(2)}, u32[]{:S(2)}) %collective-permute-start) | collective-permute-done | bytes 1048608 | tf_op jit(solution)/shard_map/ppermute | solution.py:27
  37.9 9.2 %expert_rows.1 = (bf16[512,512]{1,0:T(8,128)(2,1)}, bf16[512,512]{1,0:T(8,128)(2,1)}, bf16[512,512]{1,0:T(8,128)(2,1)}, bf16[512,1024]{1,0:T(8,128)(2,1)}, bf16[512,1024]{1,0:T(8,128)(2,1)}) custom-call(s32[1]{0:T(128)} %bitcast.3.side, bf16[512,1024]{1,0:T(8,128)(2,1)} %bitcast.29, bf16[512,1024]{1,0:T(8,128)(2,1)} %copy-done.2, bf16[512,512]{1,0:T(8,128)(2,1)} %bitcast.42, ...), custom_call_target="tpu_custom_call" | custom-call | tf_op jit(solution)/shard_map/expert_rows/pallas_call | solution.py:92
  47.3 4.8 %all-to-all-start.1 = ((bf16[64,8,1024]{2,1,0:T(8,128)(2,1)}), bf16[64,8,1024]{2,1,0:T(8,128)(2,1)S(1)}, u32[]{:S(2)}, u32[]{:S(2)}) async-start(bf16[64,8,1024]{2,1,0:T(8,128)(2,1)} %fusion), calls=%async_computation.1 | async-start | bytes 2097152 | tf_op jit(solution)/shard_map/all_to_all | solution.py:579
  52.1 2.6 %add_convert_fusion = bf16[512,1024]{1,0:T(8,128)(2,1)} fusion(bf16[512,1024]{1,0:T(8,128)(2,1)} %collective-permute-done.1, bf16[512,1024]{1,0:T(8,128)(2,1)S(1)} %copy-done.8), kind=kLoop, calls=%fused_computation | loop fusion | flops 2097152 | bytes 3145728 | tf_op jit(solution)/shard_map/convert_element_type | solution.py:585
  54.7 16.9 %all-to-all-done.1 = bf16[64,8,1024]{2,1,0:T(8,128)(2,1)S(1)} async-done(((bf16[64,8,1024]{2,1,0:T(8,128)(2,1)}), bf16[64,8,1024]{2,1,0:T(8,128)(2,1)S(1)}, u32[]{:S(2)}, u32[]{:S(2)}) %all-to-all-start.1) | async-done | bytes 1048608 | tf_op jit(solution)/shard_map/all_to_all | solution.py:579
  71.6 4.8 %all-to-all-start.2 = ((bf16[64,8,1024]{2,1,0:T(8,128)(2,1)}), bf16[64,8,1024]{2,1,0:T(8,128)(2,1)S(1)}, u32[]{:S(2)}, u32[]{:S(2)}) async-start(bf16[64,8,1024]{2,1,0:T(8,128)(2,1)} %bitcast.19), calls=%async_computation.2 | async-start | bytes 2097152 | tf_op jit(solution)/shard_map/all_to_all | solution.py:587
  78.3 4.8 %shard_map.232 = (bf16[1024,128]{1,0:T(8,128)(2,1)}, f32[1024,128]{1,0:T(8,128)}, f32[1024,128]{1,0:T(8,128)}, f32[1024,128]{1,0:T(8,128)}, bf16[16,128,128]{2,1...) custom-call(bf16[128,1024]{1,0:T(8,128)(2,1)} %scan_in.1, ...), custom_call_target="tpu_custom_call" | custom-call | tf_op jit(solution)/shard_map/pallas_call | solution.py:286
  83.0 11.8 %all-to-all-done.2 = bf16[64,8,1024]{2,1,0:T(8,128)(2,1)S(1)} async-done(((bf16[64,8,1024]{2,1,0:T(8,128)(2,1)}), bf16[64,8,1024]{2,1,0:T(8,128)(2,1)S(1)}, u32[]{:S(2)}, u32[]{:S(2)}) %all-to-all-start.2) | async-done | bytes 1048608 | tf_op jit(solution)/shard_map/all_to_all | solution.py:587
  96.6 8.2 %weights.1 = (bf16[512,2048]{1,0:T(8,128)(2,1)}, bf16[2048,512]{1,0:T(8,128)(2,1)}, bf16[2048,512]{1,0:T(8,128)(2,1)}) custom-call(s32[1]{0:T(128)} %bitcast.3.side, bf16[512,512]{1,0:T(8,128)(2,1)} %get-tuple-element.52.active, bf16[512,512]{1,0:T(8,128)(2,1)} %get-tuple-element.53.gate_grad, bf16[512,512]{1,0:T(8,128)(2,1)} %get-tuple-element.54.up_grad, ...), custom_call_target="tpu_custom_call" | custom-call | tf_op jit(solution)/shard_map/weights/pallas_call | solution.py:133
  111.4 9.5 %collective-permute-done.7 = bf16[1024,128]{1,0:T(8,128)(2,1)S(1)} collective-permute-done((bf16[1024,128]{1,0:T(8,128)(2,1)S(1)}, bf16[1024,128]{1,0:T(8,128)(2,1)S(1)}, u32[]{:S(2)}, u32[]{:S(2)}) %collective-permute-start.7) | collective-permute-done | bytes 262176 | tf_op jit(solution)/shard_map/ppermute | solution.py:33
  120.9 6.1 %message.1 = (bf16[64,40,128]{2,1,0:T(8,128)(2,1)}, f32[1024,128]{1,0:T(8,128)}) custom-call(s32[1]{0:T(128)} %bitcast.3.side, bf16[1024,128]{1,0:T(8,128)(2,1)} %copy-done.5, bf16[1024,128]{1,0:T(8,128)(2,1)} %copy-done.9, bf16[1024,2048]{1,0:T(8,128)(2,1)} %out_far.1, bf16[1024,2048]{1,0:T(8,128)(2,1)} %out_far.1, f32[1024,1]{1,0:T(8,128)} %copy.26.gain, ...), custom_call_target="tpu_custom_call" | custom-call | tf_op jit(solution)/shard_map/message/pallas_call | solution.py:360
  126.9 5.2 %all-to-all-start.3 = ((bf16[64,40,128]{2,1,0:T(8,128)(2,1)}), bf16[64,40,128]{2,1,0:T(8,128)(2,1)S(1)}, u32[]{:S(2)}, u32[]{:S(2)}) async-start(bf16[64,40,128]{2,1,0:T(8,128)(2,1)} %get-tuple-element.72), calls=%async_computation.3 | async-start | bytes 1310720 | tf_op jit(solution)/shard_map/all_to_all | solution.py:605
  136.9 2.7 %collective-permute-start.11 = (bf16[128,1024]{1,0:T(8,128)(2,1)S(1)}, bf16[128,1024]{1,0:T(8,128)(2,1)S(1)}, u32[]{:S(2)}, u32[]{:S(2)}) collective-permute-start(bf16[128,1024]{1,0:T(8,128)(2,1)S(1)} %get-tuple-element.89), channel_id=1, source_target_pairs={{0,16},{8,24},{16,0},{24,8},{1,17},{9,25},{17,1},{25,9},{2,18},{10... | collective-permute-start | bytes 786440 | tf_op jit(solution)/shard_map/ppermute | solution.py:33
  141.0 6.8 %collective-permute-done.10 = bf16[128,1024]{1,0:T(8,128)(2,1)S(1)} collective-permute-done((bf16[128,1024]{1,0:T(8,128)(2,1)S(1)}, bf16[128,1024]{1,0:T(8,128)(2,1)S(1)}, u32[]{:S(2)}, u32[]{:S(2)}) %collective-permute-start.10) | collective-permute-done | bytes 262176 | tf_op jit(solution)/shard_map/ppermute | solution.py:33
  147.9 5.4 %collective-permute-done.11 = bf16[128,1024]{1,0:T(8,128)(2,1)S(1)} collective-permute-done((bf16[128,1024]{1,0:T(8,128)(2,1)S(1)}, bf16[128,1024]{1,0:T(8,128)(2,1)S(1)}, u32[]{:S(2)}, u32[]{:S(2)}) %collective-permute-start.11) | collective-permute-done | bytes 262176 | tf_op jit(solution)/shard_map/ppermute | solution.py:33
  155.3 3.6 %owner.1 = bf16[64,24,128]{2,1,0:T(8,128)(2,1)} custom-call(s32[1]{0:T(128)} %bitcast.21.lead, bf16[64,40,128]{2,1,0:T(8,128)(2,1)} %copy-done.4), custom_call_target="tpu_custom_call" | custom-call | tf_op jit(solution)/shard_map/owner/pallas_call | solution.py:484
  158.9 7.5 %all-to-all-start.4 = ((bf16[64,24,128]{2,1,0:T(8,128)(2,1)}), bf16[64,24,128]{2,1,0:T(8,128)(2,1)S(1)}, u32[]{:S(2)}, u32[]{:S(2)}) async-start(bf16[64,24,128]{2,1,0:T(8,128)(2,1)} %owner.1), calls=%async_computation.4 | async-start | bytes 786432 | tf_op jit(solution)/shard_map/all_to_all | solution.py:611
  168.0 2.7 %collective-permute-start.14 = (bf16[32,1024]{1,0:T(8,128)(2,1)S(1)}, bf16[32,1024]{1,0:T(8,128)(2,1)S(1)}, u32[]{:S(2)}, u32[]{:S(2)}) collective-permute-start(bf16[32,1024]{1,0:T(8,128)(2,1)S(1)} %get-tuple-element.96), channel_id=1, source_target_pairs={{0,4},{2,6},{4,0},{6,2},{1,5},{3,7},{5,1},{7,3},{8,12},{10,14},{12... | collective-permute-start | bytes 196616 | tf_op jit(solution)/shard_map/ppermute | solution.py:33
  172.2 4.7 %inside.1 = (bf16[128,1024]{1,0:T(8,128)(2,1)}, f32[1024,128]{1,0:T(8,128)}, f32[128,512]{1,0:T(8,128)}, bf16[128,512]{1,0:T(8,128)(2,1)}, f32[4,4,128]{2,1,0:T(4,128)}) custom-call(f32[1024,128]{1,0:T(8,128)} %get-tuple-element.75.grad_in, f32[1024,128]{1,0:T(8,128)} %get-tuple-element.66.gated_in, f32[1024,128]{1,0:T(8,128)} %get-tuple-element.67.silu_in, ...), custom_call_target="tpu_custom_call" | custom-call | tf_op jit(solution)/shard_map/inside/pallas_call | solution.py:431
  177.5 2.1 %all-to-all-done.4.back = bf16[64,24,128]{2,1,0:T(8,128)(2,1)S(1)} async-done(((bf16[64,24,128]{2,1,0:T(8,128)(2,1)}), bf16[64,24,128]{2,1,0:T(8,128)(2,1)S(1)}, u32[]{:S(2)}, u32[]{:S(2)}) %all-to-all-start.4) | async-done | bytes 393248 | tf_op jit(solution)/shard_map/all_to_all | solution.py:611
  180.4 2.6 %shard_map.233 = (bf16[128,1024]{1,0:T(8,128)(2,1)}, bf16[128,512]{1,0:T(8,128)(2,1)}, f32[16,128]{1,0:T(8,128)}) custom-call(bf16[64,24,128]{2,1,0:T(8,128)(2,1)} %copy-done.6, bf16[128,512]{1,0:T(8,128)(2,1)} %b_proj.5, bf16[1024,128]{1,0:T(8,128)(2,1)} %get-tuple-element.73.x_in, bf16[1024,128]{1,0:T(8,128)(2,1)} %get-tuple-element.74.tail_in, ...), custom_call_target="tpu_custom_call" | custom-call | tf_op jit(solution)/shard_map/pallas_call | solution.py:286
  (69 shorter events, 25.4 us)
Async XLA Ops:
  0.6 14.8 %copy-start = (bf16[128,2048]{1,0:T(8,128)(2,1)S(1)}, bf16[128,2048]{1,0:T(8,128)(2,1)}, u32[]{:S(2)}) copy-start(bf16[128,2048]{1,0:T(8,128)(2,1)} %param.17) | copy-start | bytes 1572868
  3.7 30.6 %all-to-all-start = ((bf16[64,8,1024]{2,1,0:T(8,128)(2,1)}), bf16[64,8,1024]{2,1,0:T(8,128)(2,1)S(1)}, u32[]{:S(2)}, u32[]{:S(2)}) async-start(bf16[64,8,1024]{2,1,0:T(8,128)(2,1)} %bitcast.41), calls=%async_computation | async-start | bytes 2097152 | tf_op jit(solution)/shard_map/all_to_all | solution.py:577
  34.3 2.7 %collective-permute-start = (bf16[512,1024]{1,0:T(8,128)(2,1)S(1)}, bf16[512,1024]{1,0:T(8,128)(2,1)S(1)}, u32[]{:S(2)}, u32[]{:S(2)}) collective-permute-start(bf16[512,1024]{1,0:T(8,128)(2,1)S(1)} %bitcast.28), channel_id=1, source_target_pairs={{0,1},{1,0},{2,3},{3,2},{4,5},{5,4},{6,7},{7,6},{8,9},{9,8},{10,11... | collective-permute-start | bytes 3145736 | tf_op jit(solution)/shard_map/ppermute | solution.py:27
  47.1 5.0 %collective-permute-start.1 = (bf16[512,1024]{1,0:T(8,128)(2,1)}, bf16[512,1024]{1,0:T(8,128)(2,1)}, u32[]{:S(2)}, u32[]{:S(2)}) collective-permute-start(bf16[512,1024]{1,0:T(8,128)(2,1)} %get-tuple-element.56), channel_id=1, source_target_pairs={{0,1},{1,0},{2,3},{3,2},{4,5},{5,4},{6,7},{7,6},{8,9},{9,8},{10,11... | collective-permute-start | bytes 3145736 | tf_op jit(solution)/shard_map/ppermute | solution.py:27
  47.3 24.4 %all-to-all-start.1 = ((bf16[64,8,1024]{2,1,0:T(8,128)(2,1)}), bf16[64,8,1024]{2,1,0:T(8,128)(2,1)S(1)}, u32[]{:S(2)}, u32[]{:S(2)}) async-start(bf16[64,8,1024]{2,1,0:T(8,128)(2,1)} %fusion), calls=%async_computation.1 | async-start | bytes 2097152 | tf_op jit(solution)/shard_map/all_to_all | solution.py:579
  52.1 24.4 %copy-start.11 = (bf16[1024]{0:T(1024)(128)(2,1)S(1)}, bf16[1024]{0:T(1024)(128)(2,1)}, u32[]{:S(2)}) copy-start(bf16[1024]{0:T(1024)(128)(2,1)} %param.27) | copy-start | bytes 6148
  54.7 22.8 %copy-start.7 = (bf16[128,2048]{1,0:T(8,128)(2,1)S(1)}, bf16[128,2048]{1,0:T(8,128)(2,1)}, u32[]{:S(2)}) copy-start(bf16[128,2048]{1,0:T(8,128)(2,1)} %cotangent.1) | copy-start | bytes 1572868
  71.6 23.2 %all-to-all-start.2 = ((bf16[64,8,1024]{2,1,0:T(8,128)(2,1)}), bf16[64,8,1024]{2,1,0:T(8,128)(2,1)S(1)}, u32[]{:S(2)}, u32[]{:S(2)}) async-start(bf16[64,8,1024]{2,1,0:T(8,128)(2,1)} %bitcast.19), calls=%async_computation.2 | async-start | bytes 2097152 | tf_op jit(solution)/shard_map/all_to_all | solution.py:587
  76.4 20.2 %collective-permute-start.2 = (bf16[512,1024]{1,0:T(8,128)(2,1)S(1)}, bf16[512,1024]{1,0:T(8,128)(2,1)}, u32[]{:S(2)}, u32[]{:S(2)}) collective-permute-start(bf16[512,1024]{1,0:T(8,128)(2,1)S(1)} %bitcast.37), channel_id=1, source_target_pairs={{0,1},{1,0},{2,3},{3,2},{4,5},{5,4},{6,7},{7,6},{8,9},{9,8},{10,11... | collective-permute-start | bytes 3145736 | tf_op jit(solution)/shard_map/ppermute | solution.py:27
  96.3 11.8 %collective-permute-start.3 = (bf16[1024,128]{1,0:T(8,128)(2,1)S(1)}, bf16[1024,128]{1,0:T(8,128)(2,1)S(1)}, u32[]{:S(2)}, u32[]{:S(2)}) collective-permute-start(bf16[1024,128]{1,0:T(8,128)(2,1)S(1)} %fusion.1.grad_own), channel_id=1, source_target_pairs={{0,1},{1,0},{2,3},{3,2},{4,5},{5,4},{6,7},{7,6},{8,9},{9,8},{10,11... | collective-permute-start | bytes 786440 | tf_op jit(solution)/shard_map/ppermute | solution.py:27
  104.8 16.1 %collective-permute-start.7 = (bf16[1024,128]{1,0:T(8,128)(2,1)S(1)}, bf16[1024,128]{1,0:T(8,128)(2,1)S(1)}, u32[]{:S(2)}, u32[]{:S(2)}) collective-permute-start(bf16[1024,128]{1,0:T(8,128)(2,1)S(1)} %copy-done.12), channel_id=1, source_target_pairs={{0,32},{32,64},{64,96},{96,0},{1,33},{33,65},{65,97},{97,1},{2,34}... | collective-permute-start | bytes 786440 | tf_op jit(solution)/shard_map/ppermute | solution.py:33
  105.3 26.8 %collective-permute-start.8 = (bf16[1024,128]{1,0:T(8,128)(2,1)S(1)}, bf16[1024,128]{1,0:T(8,128)(2,1)S(1)}, u32[]{:S(2)}, u32[]{:S(2)}) collective-permute-start(bf16[1024,128]{1,0:T(8,128)(2,1)S(1)} %copy-done.12), channel_id=1, source_target_pairs={{0,64},{32,96},{64,0},{96,32},{1,65},{33,97},{65,1},{97,33},{2,66}... | collective-permute-start | bytes 786440 | tf_op jit(solution)/shard_map/ppermute | solution.py:33
  107.1 25.0 %collective-permute-start.9 = (bf16[1024,128]{1,0:T(8,128)(2,1)S(1)}, bf16[1024,128]{1,0:T(8,128)(2,1)S(1)}, u32[]{:S(2)}, u32[]{:S(2)}) collective-permute-start(bf16[1024,128]{1,0:T(8,128)(2,1)S(1)} %copy-done.12), channel_id=1, source_target_pairs={{0,96},{32,0},{64,32},{96,64},{1,97},{33,1},{65,33},{97,65},{2,98}... | collective-permute-start | bytes 786440 | tf_op jit(solution)/shard_map/ppermute | solution.py:33
  108.3 23.8 %collective-permute-start.4 = (bf16[512,128]{1,0:T(8,128)(2,1)S(1)}, bf16[512,128]{1,0:T(8,128)(2,1)S(1)}, u32[]{:S(2)}, u32[]{:S(2)}) collective-permute-start(bf16[512,128]{1,0:T(8,128)(2,1)S(1)} %get-tuple-element.93), channel_id=1, source_target_pairs={{0,32},{32,64},{64,96},{96,0},{1,33},{33,65},{65,97},{97,1},{2,34}... | collective-permute-start | bytes 393224 | tf_op jit(solution)/shard_map/ppermute | solution.py:33
  109.4 22.7 %collective-permute-start.5 = (bf16[512,128]{1,0:T(8,128)(2,1)S(1)}, bf16[512,128]{1,0:T(8,128)(2,1)S(1)}, u32[]{:S(2)}, u32[]{:S(2)}) collective-permute-start(bf16[512,128]{1,0:T(8,128)(2,1)S(1)} %get-tuple-element.92), channel_id=1, source_target_pairs={{0,64},{32,96},{64,0},{96,32},{1,65},{33,97},{65,1},{97,33},{2,66}... | collective-permute-start | bytes 393224 | tf_op jit(solution)/shard_map/ppermute | solution.py:33
  120.9 11.3 %collective-permute-start.6 = (bf16[512,128]{1,0:T(8,128)(2,1)S(1)}, bf16[512,128]{1,0:T(8,128)(2,1)S(1)}, u32[]{:S(2)}, u32[]{:S(2)}) collective-permute-start(bf16[512,128]{1,0:T(8,128)(2,1)S(1)} %get-tuple-element.91), channel_id=1, source_target_pairs={{0,96},{32,0},{64,32},{96,64},{1,97},{33,1},{65,33},{97,65},{2,98}... | collective-permute-start | bytes 393224 | tf_op jit(solution)/shard_map/ppermute | solution.py:33
  126.9 27.5 %all-to-all-start.3 = ((bf16[64,40,128]{2,1,0:T(8,128)(2,1)}), bf16[64,40,128]{2,1,0:T(8,128)(2,1)S(1)}, u32[]{:S(2)}, u32[]{:S(2)}) async-start(bf16[64,40,128]{2,1,0:T(8,128)(2,1)} %get-tuple-element.72), calls=%async_computation.3 | async-start | bytes 1310720 | tf_op jit(solution)/shard_map/all_to_all | solution.py:605
  135.3 12.6 %collective-permute-start.10 = (bf16[128,1024]{1,0:T(8,128)(2,1)S(1)}, bf16[128,1024]{1,0:T(8,128)(2,1)S(1)}, u32[]{:S(2)}, u32[]{:S(2)}) collective-permute-start(bf16[128,1024]{1,0:T(8,128)(2,1)S(1)} %get-tuple-element.87), channel_id=1, source_target_pairs={{0,8},{8,16},{16,24},{24,0},{1,9},{9,17},{17,25},{25,1},{2,10},{10... | collective-permute-start | bytes 786440 | tf_op jit(solution)/shard_map/ppermute | solution.py:33
  136.9 16.4 %collective-permute-start.11 = (bf16[128,1024]{1,0:T(8,128)(2,1)S(1)}, bf16[128,1024]{1,0:T(8,128)(2,1)S(1)}, u32[]{:S(2)}, u32[]{:S(2)}) collective-permute-start(bf16[128,1024]{1,0:T(8,128)(2,1)S(1)} %get-tuple-element.89), channel_id=1, source_target_pairs={{0,16},{8,24},{16,0},{24,8},{1,17},{9,25},{17,1},{25,9},{2,18},{10... | collective-permute-start | bytes 786440 | tf_op jit(solution)/shard_map/ppermute | solution.py:33
  139.6 13.7 %collective-permute-start.12 = (bf16[128,1024]{1,0:T(8,128)(2,1)S(1)}, bf16[128,1024]{1,0:T(8,128)(2,1)}, u32[]{:S(2)}, u32[]{:S(2)}) collective-permute-start(bf16[128,1024]{1,0:T(8,128)(2,1)S(1)} %get-tuple-element.88), channel_id=1, source_target_pairs={{0,24},{8,0},{16,8},{24,16},{1,25},{9,1},{17,9},{25,17},{2,26},{10... | collective-permute-start | bytes 786440 | tf_op jit(solution)/shard_map/ppermute | solution.py:33
  158.9 20.8 %all-to-all-start.4 = ((bf16[64,24,128]{2,1,0:T(8,128)(2,1)}), bf16[64,24,128]{2,1,0:T(8,128)(2,1)S(1)}, u32[]{:S(2)}, u32[]{:S(2)}) async-start(bf16[64,24,128]{2,1,0:T(8,128)(2,1)} %owner.1), calls=%async_computation.4 | async-start | bytes 786432 | tf_op jit(solution)/shard_map/all_to_all | solution.py:611
  166.4 10.4 %collective-permute-start.13 = (bf16[32,1024]{1,0:T(8,128)(2,1)S(1)}, bf16[32,1024]{1,0:T(8,128)(2,1)S(1)}, u32[]{:S(2)}, u32[]{:S(2)}) collective-permute-start(bf16[32,1024]{1,0:T(8,128)(2,1)S(1)} %get-tuple-element.94), channel_id=1, source_target_pairs={{0,2},{2,4},{4,6},{6,0},{1,3},{3,5},{5,7},{7,1},{8,10},{10,12},{12... | collective-permute-start | bytes 196616 | tf_op jit(solution)/shard_map/ppermute | solution.py:33
  168.0 8.8 %collective-permute-start.14 = (bf16[32,1024]{1,0:T(8,128)(2,1)S(1)}, bf16[32,1024]{1,0:T(8,128)(2,1)S(1)}, u32[]{:S(2)}, u32[]{:S(2)}) collective-permute-start(bf16[32,1024]{1,0:T(8,128)(2,1)S(1)} %get-tuple-element.96), channel_id=1, source_target_pairs={{0,4},{2,6},{4,0},{6,2},{1,5},{3,7},{5,1},{7,3},{8,12},{10,14},{12... | collective-permute-start | bytes 196616 | tf_op jit(solution)/shard_map/ppermute | solution.py:33
  170.7 6.1 %collective-permute-start.15 = (bf16[32,1024]{1,0:T(8,128)(2,1)S(1)}, bf16[32,1024]{1,0:T(8,128)(2,1)S(1)}, u32[]{:S(2)}, u32[]{:S(2)}) collective-permute-start(bf16[32,1024]{1,0:T(8,128)(2,1)S(1)} %get-tuple-element.95), channel_id=1, source_target_pairs={{0,6},{2,0},{4,2},{6,4},{1,7},{3,1},{5,3},{7,5},{8,14},{10,8},{12,... | collective-permute-start | bytes 196616 | tf_op jit(solution)/shard_map/ppermute | solution.py:33
  (12 other events, 67.4 us)

commit v7 on v6

--- a/solution.py
+++ b/solution.py
@@ -99,6 +99,7 @@
         ),
         out_shape=[act] * 3 + [out] * 2,
         name="expert_rows",
+        compiler_params=pltpu.CompilerParams(vmem_limit_bytes=24 << 20),
     )(side, mine, other, gate_value, up_value, w_down, w_down, w_gate, w_gate, w_up, w_up)
 
 
@@ -145,6 +146,7 @@
         out_shape=[jax.ShapeDtypeStruct((hidden, 2 * half), bf16)]
         + [jax.ShapeDtypeStruct((2 * half, hidden), bf16)] * 2,
         name="weights",
+        compiler_params=pltpu.CompilerParams(vmem_limit_bytes=20 << 20),
     )(side, active, gate_grad, up_grad, grads_own, grads_far, hidden_own, hidden_far)
 
 
@@ -202,6 +204,7 @@
             jax.ShapeDtypeStruct((slots, tokens), bf16),
         ],
         name="route",
+        compiler_params=pltpu.CompilerParams(vmem_limit_bytes=10 << 20),
     )(side, choice, weight, cotangent)
 
 
@@ -282,8 +285,12 @@
         local_out[span, :] = dot(x_tail, b_group, ((1,), (0,))).astype(bf16)
 
 
-def whole_call(kernel, out_shape, *args):
-    return pl.pallas_call(kernel, out_shape=[jax.ShapeDtypeStruct(*x) for x in out_shape])(*args)
+def whole_call(kernel, limit, out_shape, *args):
+    return pl.pallas_call(
+        kernel,
+        out_shape=[jax.ShapeDtypeStruct(*x) for x in out_shape],
+        compiler_params=pltpu.CompilerParams(vmem_limit_bytes=limit << 20),
+    )(*args)
 
 
 def forward(scan_in, gate_in, b_proj, c_proj, log_decay, entry, gain, cotangent):
@@ -291,6 +298,7 @@
     heads = log_decay.shape[0]
     return whole_call(
         forward_kernel,
+        12,
         [
             ((inner, tokens), bf16),
             ((inner, tokens), f32),
@@ -386,6 +394,7 @@
             jax.ShapeDtypeStruct((inner, tokens), f32),
         ],
         name="message",
+        compiler_params=pltpu.CompilerParams(vmem_limit_bytes=8 << 20),
     )(side, grad_own, grad_far, w_out, w_out, gain, gated, silu, carry, c_proj, local, rows, inverse)
 
 
@@ -444,6 +453,7 @@
         ],
         out_shape=[jax.ShapeDtypeStruct(*x) for x in outs],
         name="inside",
+        compiler_params=pltpu.CompilerParams(vmem_limit_bytes=8 << 20),
     )(grad, gated, silu, slope, mix, decay, x, b_proj, c_proj, entry, rows)
 
 
@@ -492,6 +502,7 @@
         ),
         out_shape=jax.ShapeDtypeStruct((blocks, 24, STATE), bf16),
         name="owner",
+        compiler_params=pltpu.CompilerParams(vmem_limit_bytes=6 << 20),
     )(lead, came)
 
 
@@ -524,6 +535,7 @@
     inner, tokens = x.shape
     return whole_call(
         final_kernel,
+        6,
         [
             ((tokens, inner), bf16),
             (b_proj.shape, bf16),

time: 184 us -> 198 us (1.076)
  local copies, waits for them, and re-layouts: 5.77 us -> 43.1 us
  Pallas kernels: 42.1 us -> 25.6 us
  waiting for transfers between devices: 72.7 us -> 58.8 us
  starting transfers between devices: 52.3 us -> 55 us
  other arithmetic: 4.56 us -> 7.08 us
    unnamed x30 -> x114, local copies, waits for them, and re-layouts: 3.87 us -> 39.6 us
    all_to_all x1, waiting for transfers between devices: 11.8 us -> 3.34 us  [body(): lax.all_to_all(summed.reshape(experts, capacity, half), SP, 0, 0, tiled=T...]
    pallas_call x1, Pallas kernels: 9.19 us -> 4.19 us  [expert_rows(): pl.pallas_call(expert_rows_kernel, grid_spec=pltpu.PrefetchScalarGridSpec...]
    pallas_call x2, Pallas kernels: 7.39 us -> 3.34 us  [whole_call(): pl.pallas_call(kernel, out_shape=[jax.ShapeDtypeStruct(*x) for x in out_s...]
    ppermute x12, waiting for transfers between devices: 21.8 us -> 18.7 us  [from_line(): lax.ppermute(parts[k], axis, [(i, (i + k) % size) for i in range(size)])]
    pallas_call x1, Pallas kernels: 6.06 us -> 3.86 us  [state_message(): pl.pallas_call(message_kernel, grid_spec=pltpu.PrefetchScalarGridSpec(num...]
    dynamic_slice x3, local copies, waits for them, and re-layouts: 0.14 us -> 2.3 us  [pieces_for(): lax.dynamic_slice_in_dim(x, lax.rem(spot + k, size) * span, span, dim)]
    all_to_all x1, waiting for transfers between devices: 2.13 us -> 0.01 us  [body(): back = lax.all_to_all(back, SP, 0, 0, tiled=True)]
  transfers between devices with their start and end apart: 21 -> 21, of which waited for: 8 -> 7; matrix products, arithmetic and copies ran while one was open for 6% -> 8% of each run, Pallas kernels for 13% -> 8%
where the time goes in v7:
time: 198 us; the launch traced here: 196 us
  waiting for transfers between devices  58.8 us (30%)
  starting transfers between devices  55 us (28%)
  local copies, waits for them, and re-layouts  43.1 us (22%)
  Pallas kernels  25.6 us (13%)
  other arithmetic  7.08 us (4%)
  matrix products  5.3 us (3%)
    unnamed x114, local copies, waits for them, and re-layouts  39.6 us
    ppermute x12, waiting for transfers between devices, from_line(): lax.ppermute(parts[k], axis, [(i, (i + k) % size) for i in range(size)])  18.7 us
    ppermute x12, starting transfers between devices, from_line(): lax.ppermute(parts[k], axis, [(i, (i + k) % size) for i in range(size)])  17.7 us
    all_to_all x1, waiting for transfers between devices, body(): came_grads = lax.all_to_all(send_grads, SP, 0, 0, tiled=True)  17.5 us
    all_to_all x1, waiting for transfers between devices, body(): came_hidden = lax.all_to_all(send_hidden, SP, 0, 0, tiled=True)  16.6 us
    all_to_all x1, starting transfers between devices, body(): came_grads = lax.all_to_all(send_grads, SP, 0, 0, tiled=True)  11.5 us
    all_to_all x1, starting transfers between devices, body(): back = lax.all_to_all(back, SP, 0, 0, tiled=True)  7.56 us
    pallas_call x1, Pallas kernels, expert_weights(): pl.pallas_call(weights_kernel, grid_spec=pltpu.PrefetchScalarGridSpec(num...  7.09 us
  transfers between devices with their start and end apart: 21, of which 7 were waited for; matrix products, arithmetic and copies ran while one was open for 8% of the time, Pallas kernels for 8%

profile of v7, /device:TPU:0, one launch (start us, length us, event | category | flops | bytes accessed | tf_op | source)
XLA Modules:
  0.0 196.0 jit_solution(1531200502980495829)
XLA Ops:
  3.1 2.0 %route.1 = (bf16[512,1024]{1,0:T(8,128)(2,1)}, bf16[512,128]{1,0:T(8,128)(2,1)S(1)}) custom-call(s32[1]{0:T(128)} %bitcast.3.side, s32[2,128]{1,0:T(2,128)S(1)} %bitcast.42, f32[2,128]{1,0:T(2,128)S(1)} %bitcast.43, bf16[128,2048]{1,0:T(8,128)(2,1)S(1)} %copy-done.14), custom_call_target="tpu_custom_call" | custom-call | tf_op jit(solution)/shard_map/route/pallas_call | solution.py:190
  5.1 11.5 %all-to-all-start = ((bf16[64,8,1024]{2,1,0:T(8,128)(2,1)}), bf16[64,8,1024]{2,1,0:T(8,128)(2,1)S(1)}, u32[]{:S(2)}, u32[]{:S(2)}) async-start(bf16[64,8,1024]{2,1,0:T(8,128)(2,1)} %bitcast.7), calls=%async_computation | async-start | bytes 2097152 | tf_op jit(solution)/shard_map/all_to_all | solution.py:589
  18.1 17.5 %all-to-all-done = bf16[64,8,1024]{2,1,0:T(8,128)(2,1)S(1)} async-done(((bf16[64,8,1024]{2,1,0:T(8,128)(2,1)}), bf16[64,8,1024]{2,1,0:T(8,128)(2,1)S(1)}, u32[]{:S(2)}, u32[]{:S(2)}) %all-to-all-start) | async-done | bytes 1048608 | tf_op jit(solution)/shard_map/all_to_all | solution.py:589
  35.6 2.7 %collective-permute-done.other.grads_far = bf16[512,1024]{1,0:T(8,128)(2,1)S(1)} collective-permute-done((bf16[512,1024]{1,0:T(8,128)(2,1)S(1)}, bf16[512,1024]{1,0:T(8,128)(2,1)S(1)}, u32[]{:S(2)}, u32[]{:S(2)}) %collective-permute-start) | collective-permute-done | bytes 1048608 | tf_op jit(solution)/shard_map/ppermute | solution.py:27
  44.1 4.2 %expert_rows.1 = (bf16[512,512]{1,0:T(8,128)(2,1)S(1)}, bf16[512,512]{1,0:T(8,128)(2,1)S(1)}, bf16[512,512]{1,0:T(8,128)(2,1)S(1)}, bf16[512,1024]{1,0:T(8,128)(2,1)S(1)}, bf16[512,1024]{1,0:T(8,128)(2,1)}) custom-call(s32[1]{0:T(128)} %bitcast.3.side, bf16[512,1024]{1,0:T(8,128)(2,1)S(1)} %bitcast.29, ...), custom_call_target="tpu_custom_call" | custom-call | tf_op jit(solution)/shard_map/expert_rows/pallas_call | solution.py:92
  51.9 5.5 %all-to-all-start.1 = ((bf16[64,8,1024]{2,1,0:T(8,128)(2,1)}), bf16[64,8,1024]{2,1,0:T(8,128)(2,1)}, u32[]{:S(2)}, u32[]{:S(2)}) async-start(bf16[64,8,1024]{2,1,0:T(8,128)(2,1)} %fusion), calls=%async_computation.1 | async-start | bytes 2097152 | tf_op jit(solution)/shard_map/all_to_all | solution.py:591
  57.5 2.9 %add_convert_fusion = bf16[512,1024]{1,0:T(8,128)(2,1)} fusion(bf16[512,1024]{1,0:T(8,128)(2,1)} %collective-permute-done.1, bf16[512,1024]{1,0:T(8,128)(2,1)} %copy-done.15), kind=kLoop, calls=%fused_computation | loop fusion | flops 2097152 | bytes 3145728 | tf_op jit(solution)/shard_map/convert_element_type | solution.py:597
  60.4 16.6 %all-to-all-done.1 = bf16[64,8,1024]{2,1,0:T(8,128)(2,1)} async-done(((bf16[64,8,1024]{2,1,0:T(8,128)(2,1)}), bf16[64,8,1024]{2,1,0:T(8,128)(2,1)}, u32[]{:S(2)}, u32[]{:S(2)}) %all-to-all-start.1) | async-done | bytes 1048608 | tf_op jit(solution)/shard_map/all_to_all | solution.py:591
  77.0 5.5 %all-to-all-start.2 = ((bf16[64,8,1024]{2,1,0:T(8,128)(2,1)}), bf16[64,8,1024]{2,1,0:T(8,128)(2,1)}, u32[]{:S(2)}, u32[]{:S(2)}) async-start(bf16[64,8,1024]{2,1,0:T(8,128)(2,1)} %bitcast.44), calls=%async_computation.2 | async-start | bytes 2097152 | tf_op jit(solution)/shard_map/all_to_all | solution.py:599
  86.8 2.1 %shard_map.232 = (bf16[1024,128]{1,0:T(8,128)(2,1)}, f32[1024,128]{1,0:T(8,128)S(1)}, f32[1024,128]{1,0:T(8,128)S(1)}, f32[1024,128]{1,0:T(8,128)S(1)}, bf16[16,...) custom-call(bf16[128,1024]{1,0:T(8,128)(2,1)S(1)} %copy-done.45, ...), custom_call_target="tpu_custom_call" | custom-call | tf_op jit(solution)/shard_map/pallas_call | solution.py:289
  97.4 3.3 %all-to-all-done.2 = bf16[64,8,1024]{2,1,0:T(8,128)(2,1)} async-done(((bf16[64,8,1024]{2,1,0:T(8,128)(2,1)}), bf16[64,8,1024]{2,1,0:T(8,128)(2,1)}, u32[]{:S(2)}, u32[]{:S(2)}) %all-to-all-start.2) | async-done | bytes 1048608 | tf_op jit(solution)/shard_map/all_to_all | solution.py:599
  106.0 7.1 %weights.1 = (bf16[512,2048]{1,0:T(8,128)(2,1)}, bf16[2048,512]{1,0:T(8,128)(2,1)}, bf16[2048,512]{1,0:T(8,128)(2,1)}) custom-call(s32[1]{0:T(128)} %bitcast.3.side, bf16[512,512]{1,0:T(8,128)(2,1)S(1)} %copy-done.32, bf16[512,512]{1,0:T(8,128)(2,1)S(1)} %copy-done.34, bf16[512,512]{1,0:T(8,128)(2,1)S(1)} %copy-done.36, bf16[512,1024]{1,0:T(8,128)(2,1)S(1)} %bitcast.30, ...), custom_call_target="tpu_custom_call" | custom-call | tf_op jit(solution)/shard_map/weights/pallas_call | solution.py:134
  121.3 8.2 %collective-permute-done.7 = bf16[1024,128]{1,0:T(8,128)(2,1)} collective-permute-done((bf16[1024,128]{1,0:T(8,128)(2,1)}, bf16[1024,128]{1,0:T(8,128)(2,1)}, u32[]{:S(2)}, u32[]{:S(2)}) %collective-permute-start.7) | collective-permute-done | bytes 262176 | tf_op jit(solution)/shard_map/ppermute | solution.py:33
  129.6 2.2 %copy-done.1 = bf16[1024,2048]{1,0:T(8,128)(2,1)S(1)} copy-done((bf16[1024,2048]{1,0:T(8,128)(2,1)S(1)}, bf16[1024,2048]{1,0:T(8,128)(2,1)}, u32[]{:S(2)}) %copy-start.1) | copy-done | bytes 4194328
  131.8 3.9 %message.1 = (bf16[64,40,128]{2,1,0:T(8,128)(2,1)S(1)}, f32[1024,128]{1,0:T(8,128)S(1)}) custom-call(s32[1]{0:T(128)} %bitcast.3.side, bf16[1024,128]{1,0:T(8,128)(2,1)S(1)} %fusion.1.grad_own, bf16[1024,128]{1,0:T(8,128)(2,1)} %collective-permute-done.3.grad_far, bf16[1024,2048]{1,0:T(8,128)(2,1)S(1)} %copy-done.1, bf16[1024,2048]{1,0:T(8,128)(2,1)S(1)} %copy-done.1, ...), custom_call_target="tpu_custom_call" | custom-call | tf_op jit(solution)/shard_map/message/pallas_call | solution.py:368
  137.3 6.7 %all-to-all-start.3 = ((bf16[64,40,128]{2,1,0:T(8,128)(2,1)}), bf16[64,40,128]{2,1,0:T(8,128)(2,1)S(1)}, u32[]{:S(2)}, u32[]{:S(2)}) async-start(bf16[64,40,128]{2,1,0:T(8,128)(2,1)} %copy-done.20), calls=%async_computation.3 | async-start | bytes 1310720 | tf_op jit(solution)/shard_map/all_to_all | solution.py:617
  144.0 2.1 %convolution_convert_fusion.1 = bf16[512,1024]{1,0:T(8,128)(2,1)S(1)} fusion(bf16[1024,128]{1,0:T(8,128)(2,1)} %collective-permute-done.9, bf16[1024,128]{1,0:T(8,128)(2,1)} %collective-permute-done.8, bf16[1024,128]{1,0:T(8,128)(2,1)} %collective-permute-done.7, bf16[1024,128]{1,0:T(8,128)(2,1)} %get-tuple-element.65, ...), kind=kOutput, calls=%fused_computation.2 | convolution fusion | flops 543686656 | bytes 2621440 | tf_op jit(solution)/shard_map/dot_general | solution.py:23
  149.6 2.7 %collective-permute-start.11 = (bf16[128,1024]{1,0:T(8,128)(2,1)}, bf16[128,1024]{1,0:T(8,128)(2,1)}, u32[]{:S(2)}, u32[]{:S(2)}) collective-permute-start(bf16[128,1024]{1,0:T(8,128)(2,1)} %get-tuple-element.89), channel_id=1, source_target_pairs={{0,16},{8,24},{16,0},{24,8},{1,17},{9,25},{17,1},{25,9},{2,18},{10... | collective-permute-start | bytes 786440 | tf_op jit(solution)/shard_map/ppermute | solution.py:33
  153.7 5.9 %collective-permute-done.10 = bf16[128,1024]{1,0:T(8,128)(2,1)} collective-permute-done((bf16[128,1024]{1,0:T(8,128)(2,1)}, bf16[128,1024]{1,0:T(8,128)(2,1)}, u32[]{:S(2)}, u32[]{:S(2)}) %collective-permute-start.10) | collective-permute-done | bytes 262176 | tf_op jit(solution)/shard_map/ppermute | solution.py:33
  159.6 4.6 %collective-permute-done.11 = bf16[128,1024]{1,0:T(8,128)(2,1)} collective-permute-done((bf16[128,1024]{1,0:T(8,128)(2,1)}, bf16[128,1024]{1,0:T(8,128)(2,1)}, u32[]{:S(2)}, u32[]{:S(2)}) %collective-permute-start.11) | collective-permute-done | bytes 262176 | tf_op jit(solution)/shard_map/ppermute | solution.py:33
  165.6 2.5 %owner.1 = bf16[64,24,128]{2,1,0:T(8,128)(2,1)} custom-call(s32[1]{0:T(128)} %bitcast.21.lead, bf16[64,40,128]{2,1,0:T(8,128)(2,1)S(1)} %all-to-all-done.3.came), custom_call_target="tpu_custom_call" | custom-call | tf_op jit(solution)/shard_map/owner/pallas_call | solution.py:494
  168.1 7.6 %all-to-all-start.4 = ((bf16[64,24,128]{2,1,0:T(8,128)(2,1)}), bf16[64,24,128]{2,1,0:T(8,128)(2,1)S(1)}, u32[]{:S(2)}, u32[]{:S(2)}) async-start(bf16[64,24,128]{2,1,0:T(8,128)(2,1)} %owner.1), calls=%async_computation.4 | async-start | bytes 786432 | tf_op jit(solution)/shard_map/all_to_all | solution.py:623
  177.9 2.7 %collective-permute-start.14 = (bf16[32,1024]{1,0:T(8,128)(2,1)}, bf16[32,1024]{1,0:T(8,128)(2,1)}, u32[]{:S(2)}, u32[]{:S(2)}) collective-permute-start(bf16[32,1024]{1,0:T(8,128)(2,1)} %get-tuple-element.96), channel_id=1, source_target_pairs={{0,4},{2,6},{4,0},{6,2},{1,5},{3,7},{5,1},{7,3},{8,12},{10,14},{12... | collective-permute-start | bytes 196616 | tf_op jit(solution)/shard_map/ppermute | solution.py:33
  187.2 2.6 %inside.1 = (bf16[128,1024]{1,0:T(8,128)(2,1)}, f32[1024,128]{1,0:T(8,128)S(1)}, f32[128,512]{1,0:T(8,128)S(1)}, bf16[128,512]{1,0:T(8,128)(2,1)}, f32[4,4,128]{2,1,0:T(4,128)S(1)}) custom-call(f32[1024,128]{1,0:T(8,128)S(1)} %copy-done.28, f32[1024,128]{1,0:T(8,128)S(1)} %copy-done.6, f32[1024,128]{1,0:T(8,128)S(1)} %copy-done.8, ...), custom_call_target="tpu_custom_call" | custom-call | tf_op jit(solution)/shard_map/inside/pallas_call | solution.py:440
  (153 shorter events, 62.3 us)
Async XLA Ops:
  3.1 35.1 %copy-start.21 = (bf16[1,512,512]{2,1,0:T(8,128)(2,1)S(1)}, bf16[1,512,512]{2,1,0:T(8,128)(2,1)}, u32[]{:S(2)}) copy-start(bf16[1,512,512]{2,1,0:T(8,128)(2,1)} %param.21) | copy-start | bytes 1572868
  5.1 43.1 %copy-start.37 = (bf16[512,128]{1,0:T(8,128)(2,1)}, bf16[512,128]{1,0:T(8,128)(2,1)S(1)}, u32[]{:S(2)}) copy-start(bf16[512,128]{1,0:T(8,128)(2,1)S(1)} %get-tuple-element.49) | copy-start | bytes 393220
  5.1 30.4 %all-to-all-start = ((bf16[64,8,1024]{2,1,0:T(8,128)(2,1)}), bf16[64,8,1024]{2,1,0:T(8,128)(2,1)S(1)}, u32[]{:S(2)}, u32[]{:S(2)}) async-start(bf16[64,8,1024]{2,1,0:T(8,128)(2,1)} %bitcast.7), calls=%async_computation | async-start | bytes 2097152 | tf_op jit(solution)/shard_map/all_to_all | solution.py:589
  35.6 2.7 %collective-permute-start = (bf16[512,1024]{1,0:T(8,128)(2,1)S(1)}, bf16[512,1024]{1,0:T(8,128)(2,1)S(1)}, u32[]{:S(2)}, u32[]{:S(2)}) collective-permute-start(bf16[512,1024]{1,0:T(8,128)(2,1)S(1)} %bitcast.28), channel_id=1, source_target_pairs={{0,1},{1,0},{2,3},{3,2},{4,5},{5,4},{6,7},{7,6},{8,9},{9,8},{10,11... | collective-permute-start | bytes 3145736 | tf_op jit(solution)/shard_map/ppermute | solution.py:27
  51.8 5.7 %collective-permute-start.1 = (bf16[512,1024]{1,0:T(8,128)(2,1)}, bf16[512,1024]{1,0:T(8,128)(2,1)}, u32[]{:S(2)}, u32[]{:S(2)}) collective-permute-start(bf16[512,1024]{1,0:T(8,128)(2,1)} %get-tuple-element.56), channel_id=1, source_target_pairs={{0,1},{1,0},{2,3},{3,2},{4,5},{5,4},{6,7},{7,6},{8,9},{9,8},{10,11... | collective-permute-start | bytes 3145736 | tf_op jit(solution)/shard_map/ppermute | solution.py:27
  51.9 25.1 %all-to-all-start.1 = ((bf16[64,8,1024]{2,1,0:T(8,128)(2,1)}), bf16[64,8,1024]{2,1,0:T(8,128)(2,1)}, u32[]{:S(2)}, u32[]{:S(2)}) async-start(bf16[64,8,1024]{2,1,0:T(8,128)(2,1)} %fusion), calls=%async_computation.1 | async-start | bytes 2097152 | tf_op jit(solution)/shard_map/all_to_all | solution.py:591
  77.0 23.8 %all-to-all-start.2 = ((bf16[64,8,1024]{2,1,0:T(8,128)(2,1)}), bf16[64,8,1024]{2,1,0:T(8,128)(2,1)}, u32[]{:S(2)}, u32[]{:S(2)}) async-start(bf16[64,8,1024]{2,1,0:T(8,128)(2,1)} %bitcast.44), calls=%async_computation.2 | async-start | bytes 2097152 | tf_op jit(solution)/shard_map/all_to_all | solution.py:599
  82.5 20.4 %collective-permute-start.2 = (bf16[512,1024]{1,0:T(8,128)(2,1)}, bf16[512,1024]{1,0:T(8,128)(2,1)}, u32[]{:S(2)}, u32[]{:S(2)}) collective-permute-start(bf16[512,1024]{1,0:T(8,128)(2,1)} %bitcast.14.hidden_own), channel_id=1, source_target_pairs={{0,1},{1,0},{2,3},{3,2},{4,5},{5,4},{6,7},{7,6},{8,9},{9,8},{10,11... | collective-permute-start | bytes 3145736 | tf_op jit(solution)/shard_map/ppermute | solution.py:27
  102.6 13.9 %collective-permute-start.3 = (bf16[1024,128]{1,0:T(8,128)(2,1)S(1)}, bf16[1024,128]{1,0:T(8,128)(2,1)}, u32[]{:S(2)}, u32[]{:S(2)}) collective-permute-start(bf16[1024,128]{1,0:T(8,128)(2,1)S(1)} %fusion.1.grad_own), channel_id=1, source_target_pairs={{0,1},{1,0},{2,3},{3,2},{4,5},{5,4},{6,7},{7,6},{8,9},{9,8},{10,11... | collective-permute-start | bytes 786440 | tf_op jit(solution)/shard_map/ppermute | solution.py:27
  113.2 16.4 %collective-permute-start.7 = (bf16[1024,128]{1,0:T(8,128)(2,1)}, bf16[1024,128]{1,0:T(8,128)(2,1)}, u32[]{:S(2)}, u32[]{:S(2)}) collective-permute-start(bf16[1024,128]{1,0:T(8,128)(2,1)} %get-tuple-element.65), channel_id=1, source_target_pairs={{0,32},{32,64},{64,96},{96,0},{1,33},{33,65},{65,97},{97,1},{2,34}... | collective-permute-start | bytes 786440 | tf_op jit(solution)/shard_map/ppermute | solution.py:33
  113.6 30.4 %collective-permute-start.8 = (bf16[1024,128]{1,0:T(8,128)(2,1)}, bf16[1024,128]{1,0:T(8,128)(2,1)}, u32[]{:S(2)}, u32[]{:S(2)}) collective-permute-start(bf16[1024,128]{1,0:T(8,128)(2,1)} %get-tuple-element.65), channel_id=1, source_target_pairs={{0,64},{32,96},{64,0},{96,32},{1,65},{33,97},{65,1},{97,33},{2,66}... | collective-permute-start | bytes 786440 | tf_op jit(solution)/shard_map/ppermute | solution.py:33
  115.5 28.5 %collective-permute-start.9 = (bf16[1024,128]{1,0:T(8,128)(2,1)}, bf16[1024,128]{1,0:T(8,128)(2,1)}, u32[]{:S(2)}, u32[]{:S(2)}) collective-permute-start(bf16[1024,128]{1,0:T(8,128)(2,1)} %get-tuple-element.65), channel_id=1, source_target_pairs={{0,96},{32,0},{64,32},{96,64},{1,97},{33,1},{65,33},{97,65},{2,98}... | collective-permute-start | bytes 786440 | tf_op jit(solution)/shard_map/ppermute | solution.py:33
  118.4 25.6 %collective-permute-start.4 = (bf16[512,128]{1,0:T(8,128)(2,1)}, bf16[512,128]{1,0:T(8,128)(2,1)}, u32[]{:S(2)}, u32[]{:S(2)}) collective-permute-start(bf16[512,128]{1,0:T(8,128)(2,1)} %get-tuple-element.93), channel_id=1, source_target_pairs={{0,32},{32,64},{64,96},{96,0},{1,33},{33,65},{65,97},{97,1},{2,34}... | collective-permute-start | bytes 393224 | tf_op jit(solution)/shard_map/ppermute | solution.py:33
  119.5 24.6 %collective-permute-start.5 = (bf16[512,128]{1,0:T(8,128)(2,1)}, bf16[512,128]{1,0:T(8,128)(2,1)}, u32[]{:S(2)}, u32[]{:S(2)}) collective-permute-start(bf16[512,128]{1,0:T(8,128)(2,1)} %get-tuple-element.92), channel_id=1, source_target_pairs={{0,64},{32,96},{64,0},{96,32},{1,65},{33,97},{65,1},{97,33},{2,66}... | collective-permute-start | bytes 393224 | tf_op jit(solution)/shard_map/ppermute | solution.py:33
  129.5 14.5 %collective-permute-start.6 = (bf16[512,128]{1,0:T(8,128)(2,1)}, bf16[512,128]{1,0:T(8,128)(2,1)}, u32[]{:S(2)}, u32[]{:S(2)}) collective-permute-start(bf16[512,128]{1,0:T(8,128)(2,1)} %get-tuple-element.91), channel_id=1, source_target_pairs={{0,96},{32,0},{64,32},{96,64},{1,97},{33,1},{65,33},{97,65},{2,98}... | collective-permute-start | bytes 393224 | tf_op jit(solution)/shard_map/ppermute | solution.py:33
  137.3 28.3 %all-to-all-start.3 = ((bf16[64,40,128]{2,1,0:T(8,128)(2,1)}), bf16[64,40,128]{2,1,0:T(8,128)(2,1)S(1)}, u32[]{:S(2)}, u32[]{:S(2)}) async-start(bf16[64,40,128]{2,1,0:T(8,128)(2,1)} %copy-done.20), calls=%async_computation.3 | async-start | bytes 1310720 | tf_op jit(solution)/shard_map/all_to_all | solution.py:617
  148.0 34.1 %copy-start.17 = (bf16[1024,128]{1,0:T(8,128)(2,1)S(1)}, bf16[1024,128]{1,0:T(8,128)(2,1)}, u32[]{:S(2)}) copy-start(bf16[1024,128]{1,0:T(8,128)(2,1)} %copy-done.16) | copy-start | bytes 786436
  148.0 11.6 %collective-permute-start.10 = (bf16[128,1024]{1,0:T(8,128)(2,1)}, bf16[128,1024]{1,0:T(8,128)(2,1)}, u32[]{:S(2)}, u32[]{:S(2)}) collective-permute-start(bf16[128,1024]{1,0:T(8,128)(2,1)} %get-tuple-element.87), channel_id=1, source_target_pairs={{0,8},{8,16},{16,24},{24,0},{1,9},{9,17},{17,25},{25,1},{2,10},{10... | collective-permute-start | bytes 786440 | tf_op jit(solution)/shard_map/ppermute | solution.py:33
  149.6 14.6 %collective-permute-start.11 = (bf16[128,1024]{1,0:T(8,128)(2,1)}, bf16[128,1024]{1,0:T(8,128)(2,1)}, u32[]{:S(2)}, u32[]{:S(2)}) collective-permute-start(bf16[128,1024]{1,0:T(8,128)(2,1)} %get-tuple-element.89), channel_id=1, source_target_pairs={{0,16},{8,24},{16,0},{24,8},{1,17},{9,25},{17,1},{25,9},{2,18},{10... | collective-permute-start | bytes 786440 | tf_op jit(solution)/shard_map/ppermute | solution.py:33
  152.3 11.9 %collective-permute-start.12 = (bf16[128,1024]{1,0:T(8,128)(2,1)S(1)}, bf16[128,1024]{1,0:T(8,128)(2,1)}, u32[]{:S(2)}, u32[]{:S(2)}) collective-permute-start(bf16[128,1024]{1,0:T(8,128)(2,1)S(1)} %get-tuple-element.88), channel_id=1, source_target_pairs={{0,24},{8,0},{16,8},{24,16},{1,25},{9,1},{17,9},{25,17},{2,26},{10... | collective-permute-start | bytes 786440 | tf_op jit(solution)/shard_map/ppermute | solution.py:33
  168.1 24.0 %all-to-all-start.4 = ((bf16[64,24,128]{2,1,0:T(8,128)(2,1)}), bf16[64,24,128]{2,1,0:T(8,128)(2,1)S(1)}, u32[]{:S(2)}, u32[]{:S(2)}) async-start(bf16[64,24,128]{2,1,0:T(8,128)(2,1)} %owner.1), calls=%async_computation.4 | async-start | bytes 786432 | tf_op jit(solution)/shard_map/all_to_all | solution.py:623
  176.4 14.1 %collective-permute-start.13 = (bf16[32,1024]{1,0:T(8,128)(2,1)}, bf16[32,1024]{1,0:T(8,128)(2,1)}, u32[]{:S(2)}, u32[]{:S(2)}) collective-permute-start(bf16[32,1024]{1,0:T(8,128)(2,1)} %get-tuple-element.94), channel_id=1, source_target_pairs={{0,2},{2,4},{4,6},{6,0},{1,3},{3,5},{5,7},{7,1},{8,10},{10,12},{12... | collective-permute-start | bytes 196616 | tf_op jit(solution)/shard_map/ppermute | solution.py:33
  177.9 12.6 %collective-permute-start.14 = (bf16[32,1024]{1,0:T(8,128)(2,1)}, bf16[32,1024]{1,0:T(8,128)(2,1)}, u32[]{:S(2)}, u32[]{:S(2)}) collective-permute-start(bf16[32,1024]{1,0:T(8,128)(2,1)} %get-tuple-element.96), channel_id=1, source_target_pairs={{0,4},{2,6},{4,0},{6,2},{1,5},{3,7},{5,1},{7,3},{8,12},{10,14},{12... | collective-permute-start | bytes 196616 | tf_op jit(solution)/shard_map/ppermute | solution.py:33
  180.6 9.9 %collective-permute-start.15 = (bf16[32,1024]{1,0:T(8,128)(2,1)}, bf16[32,1024]{1,0:T(8,128)(2,1)}, u32[]{:S(2)}, u32[]{:S(2)}) collective-permute-start(bf16[32,1024]{1,0:T(8,128)(2,1)} %get-tuple-element.95), channel_id=1, source_target_pairs={{0,6},{2,0},{4,2},{6,4},{1,7},{3,1},{5,3},{7,5},{8,14},{10,8},{12,... | collective-permute-start | bytes 196616 | tf_op jit(solution)/shard_map/ppermute | solution.py:33
  (54 other events, 318.1 us)

commit v8 on v7

--- a/solution.py
+++ b/solution.py
@@ -99,7 +99,6 @@
         ),
         out_shape=[act] * 3 + [out] * 2,
         name="expert_rows",
-        compiler_params=pltpu.CompilerParams(vmem_limit_bytes=24 << 20),
     )(side, mine, other, gate_value, up_value, w_down, w_down, w_gate, w_gate, w_up, w_up)
 
 
@@ -146,7 +145,6 @@
         out_shape=[jax.ShapeDtypeStruct((hidden, 2 * half), bf16)]
         + [jax.ShapeDtypeStruct((2 * half, hidden), bf16)] * 2,
         name="weights",
-        compiler_params=pltpu.CompilerParams(vmem_limit_bytes=20 << 20),
     )(side, active, gate_grad, up_grad, grads_own, grads_far, hidden_own, hidden_far)
 
 
@@ -204,7 +202,6 @@
             jax.ShapeDtypeStruct((slots, tokens), bf16),
         ],
         name="route",
-        compiler_params=pltpu.CompilerParams(vmem_limit_bytes=10 << 20),
     )(side, choice, weight, cotangent)
 
 
@@ -289,7 +286,7 @@
     return pl.pallas_call(
         kernel,
         out_shape=[jax.ShapeDtypeStruct(*x) for x in out_shape],
-        compiler_params=pltpu.CompilerParams(vmem_limit_bytes=limit << 20),
+        compiler_params=pltpu.CompilerParams(vmem_limit_bytes=limit),
     )(*args)
 
 
@@ -298,7 +295,7 @@
     heads = log_decay.shape[0]
     return whole_call(
         forward_kernel,
-        12,
+        None,
         [
             ((inner, tokens), bf16),
             ((inner, tokens), f32),
@@ -394,7 +391,6 @@
             jax.ShapeDtypeStruct((inner, tokens), f32),
         ],
         name="message",
-        compiler_params=pltpu.CompilerParams(vmem_limit_bytes=8 << 20),
     )(side, grad_own, grad_far, w_out, w_out, gain, gated, silu, carry, c_proj, local, rows, inverse)
 
 
@@ -453,7 +449,6 @@
         ],
         out_shape=[jax.ShapeDtypeStruct(*x) for x in outs],
         name="inside",
-        compiler_params=pltpu.CompilerParams(vmem_limit_bytes=8 << 20),
     )(grad, gated, silu, slope, mix, decay, x, b_proj, c_proj, entry, rows)
 
 
@@ -535,7 +530,7 @@
     inner, tokens = x.shape
     return whole_call(
         final_kernel,
-        6,
+        6 << 20,
         [
             ((tokens, inner), bf16),
             (b_proj.shape, bf16),

time: 198 us -> 183 us (0.924)
  local copies, waits for them, and re-layouts: 43.1 us -> 6.91 us
  Pallas kernels: 25.6 us -> 39.7 us
  waiting for transfers between devices: 58.8 us -> 72.6 us
  starting transfers between devices: 55 us -> 52.4 us
  other arithmetic: 7.08 us -> 4.56 us
    unnamed x114 -> x40, local copies, waits for them, and re-layouts: 39.6 us -> 5.01 us
    all_to_all x1, waiting for transfers between devices: 3.34 us -> 11.8 us  [body(): lax.all_to_all(summed.reshape(experts, capacity, half), SP, 0, 0, tiled=T...]
    pallas_call x1, Pallas kernels: 4.19 us -> 9.19 us  [expert_rows(): pl.pallas_call(expert_rows_kernel, grid_spec=pltpu.PrefetchScalarGridSpec...]
    ppermute x12, waiting for transfers between devices: 18.7 us -> 21.8 us  [from_line(): lax.ppermute(parts[k], axis, [(i, (i + k) % size) for i in range(size)])]
    pallas_call x2, Pallas kernels: 3.34 us -> 5.97 us  [whole_call(): pl.pallas_call(kernel, out_shape=[jax.ShapeDtypeStruct(*x) for x in out_s...]
    pallas_call x1, Pallas kernels: 3.86 us -> 6.06 us  [state_message(): pl.pallas_call(message_kernel, grid_spec=pltpu.PrefetchScalarGridSpec(num...]
    dynamic_slice x3, local copies, waits for them, and re-layouts: 2.3 us -> 0.14 us  [pieces_for(): lax.dynamic_slice_in_dim(x, lax.rem(spot + k, size) * span, span, dim)]
    pallas_call x1, Pallas kernels: 2.61 us -> 4.72 us  [inside_grads(): pl.pallas_call(inside_kernel, grid=(inner // GROUP,), in_specs=[channels]...]
  transfers between devices with their start and end apart: 21 -> 21, of which waited for: 7 -> 8; matrix products, arithmetic and copies ran while one was open for 8% -> 6% of each run, Pallas kernels for 8% -> 13%
where the time goes in v8:
time: 183 us; the launch traced here: 182 us
  waiting for transfers between devices  72.6 us (40%)
  starting transfers between devices  52.4 us (29%)
  Pallas kernels  39.7 us (22%)
  local copies, waits for them, and re-layouts  6.91 us (4%)
  other arithmetic  4.56 us (2%)
  matrix products  4.54 us (2%)
    ppermute x12, waiting for transfers between devices, from_line(): lax.ppermute(parts[k], axis, [(i, (i + k) % size) for i in range(size)])  21.8 us
    ppermute x12, starting transfers between devices, from_line(): lax.ppermute(parts[k], axis, [(i, (i + k) % size) for i in range(size)])  17.9 us
    all_to_all x1, waiting for transfers between devices, body(): came_grads = lax.all_to_all(send_grads, SP, 0, 0, tiled=True)  17.5 us
    all_to_all x1, waiting for transfers between devices, body(): came_hidden = lax.all_to_all(send_hidden, SP, 0, 0, tiled=True)  16.9 us
    all_to_all x1, waiting for transfers between devices, body(): lax.all_to_all(summed.reshape(experts, capacity, half), SP, 0, 0, tiled=T...  11.8 us
    all_to_all x1, starting transfers between devices, body(): came_grads = lax.all_to_all(send_grads, SP, 0, 0, tiled=True)  11.7 us
    pallas_call x1, Pallas kernels, expert_rows(): pl.pallas_call(expert_rows_kernel, grid_spec=pltpu.PrefetchScalarGridSpec...  9.19 us
    pallas_call x1, Pallas kernels, expert_weights(): pl.pallas_call(weights_kernel, grid_spec=pltpu.PrefetchScalarGridSpec(num...  8.16 us
  transfers between devices with their start and end apart: 21, of which 8 were waited for; matrix products, arithmetic and copies ran while one was open for 6% of the time, Pallas kernels for 13%

profile of v8, /device:TPU:0, one launch (start us, length us, event | category | flops | bytes accessed | tf_op | source)
XLA Modules:
  0.0 181.7 jit_solution(13004818649279820330)
XLA Ops:
  0.7 3.1 %route.1 = (bf16[512,1024]{1,0:T(8,128)(2,1)}, bf16[512,128]{1,0:T(8,128)(2,1)}) custom-call(s32[1]{0:T(128)} %bitcast.3.side, s32[2,128]{1,0:T(2,128)} %bitcast.46, f32[2,128]{1,0:T(2,128)} %bitcast.47, bf16[128,2048]{1,0:T(8,128)(2,1)} %cotangent.1), custom_call_target="tpu_custom_call" | custom-call | tf_op jit(solution)/shard_map/route/pallas_call | solution.py:188
  3.7 11.7 %all-to-all-start = ((bf16[64,8,1024]{2,1,0:T(8,128)(2,1)}), bf16[64,8,1024]{2,1,0:T(8,128)(2,1)S(1)}, u32[]{:S(2)}, u32[]{:S(2)}) async-start(bf16[64,8,1024]{2,1,0:T(8,128)(2,1)} %bitcast.41), calls=%async_computation | async-start | bytes 2097152 | tf_op jit(solution)/shard_map/all_to_all | solution.py:584
  16.8 17.5 %all-to-all-done = bf16[64,8,1024]{2,1,0:T(8,128)(2,1)S(1)} async-done(((bf16[64,8,1024]{2,1,0:T(8,128)(2,1)}), bf16[64,8,1024]{2,1,0:T(8,128)(2,1)S(1)}, u32[]{:S(2)}, u32[]{:S(2)}) %all-to-all-start) | async-done | bytes 1048608 | tf_op jit(solution)/shard_map/all_to_all | solution.py:584
  34.3 2.7 %collective-permute-done.other.grads_far = bf16[512,1024]{1,0:T(8,128)(2,1)S(1)} collective-permute-done((bf16[512,1024]{1,0:T(8,128)(2,1)S(1)}, bf16[512,1024]{1,0:T(8,128)(2,1)S(1)}, u32[]{:S(2)}, u32[]{:S(2)}) %collective-permute-start) | collective-permute-done | bytes 1048608 | tf_op jit(solution)/shard_map/ppermute | solution.py:27
  37.9 9.2 %expert_rows.1 = (bf16[512,512]{1,0:T(8,128)(2,1)}, bf16[512,512]{1,0:T(8,128)(2,1)}, bf16[512,512]{1,0:T(8,128)(2,1)}, bf16[512,1024]{1,0:T(8,128)(2,1)}, bf16[512,1024]{1,0:T(8,128)(2,1)}) custom-call(s32[1]{0:T(128)} %bitcast.3.side, bf16[512,1024]{1,0:T(8,128)(2,1)} %bitcast.29, bf16[512,1024]{1,0:T(8,128)(2,1)} %copy-done.9, bf16[512,512]{1,0:T(8,128)(2,1)} %bitcast.42, ...), custom_call_target="tpu_custom_call" | custom-call | tf_op jit(solution)/shard_map/expert_rows/pallas_call | solution.py:92
  47.3 4.8 %all-to-all-start.1 = ((bf16[64,8,1024]{2,1,0:T(8,128)(2,1)}), bf16[64,8,1024]{2,1,0:T(8,128)(2,1)S(1)}, u32[]{:S(2)}, u32[]{:S(2)}) async-start(bf16[64,8,1024]{2,1,0:T(8,128)(2,1)} %fusion), calls=%async_computation.1 | async-start | bytes 2097152 | tf_op jit(solution)/shard_map/all_to_all | solution.py:586
  52.1 2.6 %add_convert_fusion = bf16[512,1024]{1,0:T(8,128)(2,1)} fusion(bf16[512,1024]{1,0:T(8,128)(2,1)} %collective-permute-done.1, bf16[512,1024]{1,0:T(8,128)(2,1)S(1)} %copy-done.13), kind=kLoop, calls=%fused_computation | loop fusion | flops 2097152 | bytes 3145728 | tf_op jit(solution)/shard_map/convert_element_type | solution.py:592
  54.8 16.9 %all-to-all-done.1 = bf16[64,8,1024]{2,1,0:T(8,128)(2,1)S(1)} async-done(((bf16[64,8,1024]{2,1,0:T(8,128)(2,1)}), bf16[64,8,1024]{2,1,0:T(8,128)(2,1)S(1)}, u32[]{:S(2)}, u32[]{:S(2)}) %all-to-all-start.1) | async-done | bytes 1048608 | tf_op jit(solution)/shard_map/all_to_all | solution.py:586
  71.6 4.8 %all-to-all-start.2 = ((bf16[64,8,1024]{2,1,0:T(8,128)(2,1)}), bf16[64,8,1024]{2,1,0:T(8,128)(2,1)S(1)}, u32[]{:S(2)}, u32[]{:S(2)}) async-start(bf16[64,8,1024]{2,1,0:T(8,128)(2,1)} %bitcast.19), calls=%async_computation.2 | async-start | bytes 2097152 | tf_op jit(solution)/shard_map/all_to_all | solution.py:594
  78.3 4.8 %shard_map.232 = (bf16[1024,128]{1,0:T(8,128)(2,1)}, f32[1024,128]{1,0:T(8,128)}, f32[1024,128]{1,0:T(8,128)}, f32[1024,128]{1,0:T(8,128)}, bf16[16,128,128]{2,1...) custom-call(bf16[128,1024]{1,0:T(8,128)(2,1)} %scan_in.1, ...), custom_call_target="tpu_custom_call" | custom-call | tf_op jit(solution)/shard_map/pallas_call | solution.py:286
  83.1 11.8 %all-to-all-done.2 = bf16[64,8,1024]{2,1,0:T(8,128)(2,1)S(1)} async-done(((bf16[64,8,1024]{2,1,0:T(8,128)(2,1)}), bf16[64,8,1024]{2,1,0:T(8,128)(2,1)S(1)}, u32[]{:S(2)}, u32[]{:S(2)}) %all-to-all-start.2) | async-done | bytes 1048608 | tf_op jit(solution)/shard_map/all_to_all | solution.py:594
  96.6 8.2 %weights.1 = (bf16[512,2048]{1,0:T(8,128)(2,1)}, bf16[2048,512]{1,0:T(8,128)(2,1)}, bf16[2048,512]{1,0:T(8,128)(2,1)}) custom-call(s32[1]{0:T(128)} %bitcast.3.side, bf16[512,512]{1,0:T(8,128)(2,1)} %get-tuple-element.52.active, bf16[512,512]{1,0:T(8,128)(2,1)} %get-tuple-element.53.gate_grad, bf16[512,512]{1,0:T(8,128)(2,1)} %get-tuple-element.54.up_grad, ...), custom_call_target="tpu_custom_call" | custom-call | tf_op jit(solution)/shard_map/weights/pallas_call | solution.py:133
  109.4 2.0 %collective-permute-start.5 = (bf16[512,128]{1,0:T(8,128)(2,1)S(1)}, bf16[512,128]{1,0:T(8,128)(2,1)S(1)}, u32[]{:S(2)}, u32[]{:S(2)}) collective-permute-start(bf16[512,128]{1,0:T(8,128)(2,1)S(1)} %get-tuple-element.92), channel_id=1, source_target_pairs={{0,64},{32,96},{64,0},{96,32},{1,65},{33,97},{65,1},{97,33},{2,66}... | collective-permute-start | bytes 393224 | tf_op jit(solution)/shard_map/ppermute | solution.py:33
  111.4 9.5 %collective-permute-done.7 = bf16[1024,128]{1,0:T(8,128)(2,1)S(1)} collective-permute-done((bf16[1024,128]{1,0:T(8,128)(2,1)S(1)}, bf16[1024,128]{1,0:T(8,128)(2,1)S(1)}, u32[]{:S(2)}, u32[]{:S(2)}) %collective-permute-start.7) | collective-permute-done | bytes 262176 | tf_op jit(solution)/shard_map/ppermute | solution.py:33
  120.9 6.1 %message.1 = (bf16[64,40,128]{2,1,0:T(8,128)(2,1)}, f32[1024,128]{1,0:T(8,128)}) custom-call(s32[1]{0:T(128)} %bitcast.3.side, bf16[1024,128]{1,0:T(8,128)(2,1)} %copy-done.11, bf16[1024,128]{1,0:T(8,128)(2,1)} %copy-done.14, bf16[1024,2048]{1,0:T(8,128)(2,1)} %out_far.1, bf16[1024,2048]{1,0:T(8,128)(2,1)} %out_far.1, f32[1024,1]{1,0:T(8,128)} %copy.26.gain, ...), custom_call_target="tpu_custom_call" | custom-call | tf_op jit(solution)/shard_map/message/pallas_call | solution.py:365
  126.9 5.2 %all-to-all-start.3 = ((bf16[64,40,128]{2,1,0:T(8,128)(2,1)}), bf16[64,40,128]{2,1,0:T(8,128)(2,1)S(1)}, u32[]{:S(2)}, u32[]{:S(2)}) async-start(bf16[64,40,128]{2,1,0:T(8,128)(2,1)} %get-tuple-element.72), calls=%async_computation.3 | async-start | bytes 1310720 | tf_op jit(solution)/shard_map/all_to_all | solution.py:612
  136.9 2.7 %collective-permute-start.11 = (bf16[128,1024]{1,0:T(8,128)(2,1)S(1)}, bf16[128,1024]{1,0:T(8,128)(2,1)S(1)}, u32[]{:S(2)}, u32[]{:S(2)}) collective-permute-start(bf16[128,1024]{1,0:T(8,128)(2,1)S(1)} %get-tuple-element.89), channel_id=1, source_target_pairs={{0,16},{8,24},{16,0},{24,8},{1,17},{9,25},{17,1},{25,9},{2,18},{10... | collective-permute-start | bytes 786440 | tf_op jit(solution)/shard_map/ppermute | solution.py:33
  141.0 6.8 %collective-permute-done.10 = bf16[128,1024]{1,0:T(8,128)(2,1)S(1)} collective-permute-done((bf16[128,1024]{1,0:T(8,128)(2,1)S(1)}, bf16[128,1024]{1,0:T(8,128)(2,1)S(1)}, u32[]{:S(2)}, u32[]{:S(2)}) %collective-permute-start.10) | collective-permute-done | bytes 262176 | tf_op jit(solution)/shard_map/ppermute | solution.py:33
  147.9 5.4 %collective-permute-done.11 = bf16[128,1024]{1,0:T(8,128)(2,1)S(1)} collective-permute-done((bf16[128,1024]{1,0:T(8,128)(2,1)S(1)}, bf16[128,1024]{1,0:T(8,128)(2,1)S(1)}, u32[]{:S(2)}, u32[]{:S(2)}) %collective-permute-start.11) | collective-permute-done | bytes 262176 | tf_op jit(solution)/shard_map/ppermute | solution.py:33
  154.5 2.5 %owner.1 = bf16[64,24,128]{2,1,0:T(8,128)(2,1)} custom-call(s32[1]{0:T(128)} %bitcast.21.lead, bf16[64,40,128]{2,1,0:T(8,128)(2,1)S(1)} %all-to-all-done.3.came), custom_call_target="tpu_custom_call" | custom-call | tf_op jit(solution)/shard_map/owner/pallas_call | solution.py:489
  157.0 7.5 %all-to-all-start.4 = ((bf16[64,24,128]{2,1,0:T(8,128)(2,1)}), bf16[64,24,128]{2,1,0:T(8,128)(2,1)S(1)}, u32[]{:S(2)}, u32[]{:S(2)}) async-start(bf16[64,24,128]{2,1,0:T(8,128)(2,1)} %owner.1), calls=%async_computation.4 | async-start | bytes 786432 | tf_op jit(solution)/shard_map/all_to_all | solution.py:618
  166.1 2.7 %collective-permute-start.14 = (bf16[32,1024]{1,0:T(8,128)(2,1)S(1)}, bf16[32,1024]{1,0:T(8,128)(2,1)S(1)}, u32[]{:S(2)}, u32[]{:S(2)}) collective-permute-start(bf16[32,1024]{1,0:T(8,128)(2,1)S(1)} %get-tuple-element.96), channel_id=1, source_target_pairs={{0,4},{2,6},{4,0},{6,2},{1,5},{3,7},{5,1},{7,3},{8,12},{10,14},{12... | collective-permute-start | bytes 196616 | tf_op jit(solution)/shard_map/ppermute | solution.py:33
  170.3 4.7 %inside.1 = (bf16[128,1024]{1,0:T(8,128)(2,1)}, f32[1024,128]{1,0:T(8,128)}, f32[128,512]{1,0:T(8,128)}, bf16[128,512]{1,0:T(8,128)(2,1)}, f32[4,4,128]{2,1,0:T(4,128)}) custom-call(f32[1024,128]{1,0:T(8,128)} %get-tuple-element.75.grad_in, f32[1024,128]{1,0:T(8,128)} %get-tuple-element.66.gated_in, f32[1024,128]{1,0:T(8,128)} %get-tuple-element.67.silu_in, ...), custom_call_target="tpu_custom_call" | custom-call | tf_op jit(solution)/shard_map/inside/pallas_call | solution.py:436
  175.7 2.1 %all-to-all-done.4.back = bf16[64,24,128]{2,1,0:T(8,128)(2,1)S(1)} async-done(((bf16[64,24,128]{2,1,0:T(8,128)(2,1)}), bf16[64,24,128]{2,1,0:T(8,128)(2,1)S(1)}, u32[]{:S(2)}, u32[]{:S(2)}) %all-to-all-start.4) | async-done | bytes 393248 | tf_op jit(solution)/shard_map/all_to_all | solution.py:618
  (79 shorter events, 25.8 us)
Async XLA Ops:
  0.6 14.8 %copy-start = (bf16[128,2048]{1,0:T(8,128)(2,1)S(1)}, bf16[128,2048]{1,0:T(8,128)(2,1)}, u32[]{:S(2)}) copy-start(bf16[128,2048]{1,0:T(8,128)(2,1)} %param.17) | copy-start | bytes 1572868
  3.7 30.6 %all-to-all-start = ((bf16[64,8,1024]{2,1,0:T(8,128)(2,1)}), bf16[64,8,1024]{2,1,0:T(8,128)(2,1)S(1)}, u32[]{:S(2)}, u32[]{:S(2)}) async-start(bf16[64,8,1024]{2,1,0:T(8,128)(2,1)} %bitcast.41), calls=%async_computation | async-start | bytes 2097152 | tf_op jit(solution)/shard_map/all_to_all | solution.py:584
  34.3 2.7 %collective-permute-start = (bf16[512,1024]{1,0:T(8,128)(2,1)S(1)}, bf16[512,1024]{1,0:T(8,128)(2,1)S(1)}, u32[]{:S(2)}, u32[]{:S(2)}) collective-permute-start(bf16[512,1024]{1,0:T(8,128)(2,1)S(1)} %bitcast.28), channel_id=1, source_target_pairs={{0,1},{1,0},{2,3},{3,2},{4,5},{5,4},{6,7},{7,6},{8,9},{9,8},{10,11... | collective-permute-start | bytes 3145736 | tf_op jit(solution)/shard_map/ppermute | solution.py:27
  47.1 5.0 %collective-permute-start.1 = (bf16[512,1024]{1,0:T(8,128)(2,1)}, bf16[512,1024]{1,0:T(8,128)(2,1)}, u32[]{:S(2)}, u32[]{:S(2)}) collective-permute-start(bf16[512,1024]{1,0:T(8,128)(2,1)} %get-tuple-element.56), channel_id=1, source_target_pairs={{0,1},{1,0},{2,3},{3,2},{4,5},{5,4},{6,7},{7,6},{8,9},{9,8},{10,11... | collective-permute-start | bytes 3145736 | tf_op jit(solution)/shard_map/ppermute | solution.py:27
  47.3 24.4 %all-to-all-start.1 = ((bf16[64,8,1024]{2,1,0:T(8,128)(2,1)}), bf16[64,8,1024]{2,1,0:T(8,128)(2,1)S(1)}, u32[]{:S(2)}, u32[]{:S(2)}) async-start(bf16[64,8,1024]{2,1,0:T(8,128)(2,1)} %fusion), calls=%async_computation.1 | async-start | bytes 2097152 | tf_op jit(solution)/shard_map/all_to_all | solution.py:586
  52.1 24.4 %copy-start.16 = (bf16[1024]{0:T(1024)(128)(2,1)S(1)}, bf16[1024]{0:T(1024)(128)(2,1)}, u32[]{:S(2)}) copy-start(bf16[1024]{0:T(1024)(128)(2,1)} %param.27) | copy-start | bytes 6148
  54.7 22.8 %copy-start.12 = (bf16[128,2048]{1,0:T(8,128)(2,1)S(1)}, bf16[128,2048]{1,0:T(8,128)(2,1)}, u32[]{:S(2)}) copy-start(bf16[128,2048]{1,0:T(8,128)(2,1)} %cotangent.1) | copy-start | bytes 1572868
  71.6 23.2 %all-to-all-start.2 = ((bf16[64,8,1024]{2,1,0:T(8,128)(2,1)}), bf16[64,8,1024]{2,1,0:T(8,128)(2,1)S(1)}, u32[]{:S(2)}, u32[]{:S(2)}) async-start(bf16[64,8,1024]{2,1,0:T(8,128)(2,1)} %bitcast.19), calls=%async_computation.2 | async-start | bytes 2097152 | tf_op jit(solution)/shard_map/all_to_all | solution.py:594
  76.4 20.2 %collective-permute-start.2 = (bf16[512,1024]{1,0:T(8,128)(2,1)S(1)}, bf16[512,1024]{1,0:T(8,128)(2,1)}, u32[]{:S(2)}, u32[]{:S(2)}) collective-permute-start(bf16[512,1024]{1,0:T(8,128)(2,1)S(1)} %bitcast.37), channel_id=1, source_target_pairs={{0,1},{1,0},{2,3},{3,2},{4,5},{5,4},{6,7},{7,6},{8,9},{9,8},{10,11... | collective-permute-start | bytes 3145736 | tf_op jit(solution)/shard_map/ppermute | solution.py:27
  96.3 11.8 %collective-permute-start.3 = (bf16[1024,128]{1,0:T(8,128)(2,1)S(1)}, bf16[1024,128]{1,0:T(8,128)(2,1)S(1)}, u32[]{:S(2)}, u32[]{:S(2)}) collective-permute-start(bf16[1024,128]{1,0:T(8,128)(2,1)S(1)} %fusion.1.grad_own), channel_id=1, source_target_pairs={{0,1},{1,0},{2,3},{3,2},{4,5},{5,4},{6,7},{7,6},{8,9},{9,8},{10,11... | collective-permute-start | bytes 786440 | tf_op jit(solution)/shard_map/ppermute | solution.py:27
  104.8 16.1 %collective-permute-start.7 = (bf16[1024,128]{1,0:T(8,128)(2,1)S(1)}, bf16[1024,128]{1,0:T(8,128)(2,1)S(1)}, u32[]{:S(2)}, u32[]{:S(2)}) collective-permute-start(bf16[1024,128]{1,0:T(8,128)(2,1)S(1)} %copy-done.17), channel_id=1, source_target_pairs={{0,32},{32,64},{64,96},{96,0},{1,33},{33,65},{65,97},{97,1},{2,34}... | collective-permute-start | bytes 786440 | tf_op jit(solution)/shard_map/ppermute | solution.py:33
  105.3 26.8 %collective-permute-start.8 = (bf16[1024,128]{1,0:T(8,128)(2,1)S(1)}, bf16[1024,128]{1,0:T(8,128)(2,1)S(1)}, u32[]{:S(2)}, u32[]{:S(2)}) collective-permute-start(bf16[1024,128]{1,0:T(8,128)(2,1)S(1)} %copy-done.17), channel_id=1, source_target_pairs={{0,64},{32,96},{64,0},{96,32},{1,65},{33,97},{65,1},{97,33},{2,66}... | collective-permute-start | bytes 786440 | tf_op jit(solution)/shard_map/ppermute | solution.py:33
  107.1 25.0 %collective-permute-start.9 = (bf16[1024,128]{1,0:T(8,128)(2,1)S(1)}, bf16[1024,128]{1,0:T(8,128)(2,1)S(1)}, u32[]{:S(2)}, u32[]{:S(2)}) collective-permute-start(bf16[1024,128]{1,0:T(8,128)(2,1)S(1)} %copy-done.17), channel_id=1, source_target_pairs={{0,96},{32,0},{64,32},{96,64},{1,97},{33,1},{65,33},{97,65},{2,98}... | collective-permute-start | bytes 786440 | tf_op jit(solution)/shard_map/ppermute | solution.py:33
  108.3 23.8 %collective-permute-start.4 = (bf16[512,128]{1,0:T(8,128)(2,1)S(1)}, bf16[512,128]{1,0:T(8,128)(2,1)S(1)}, u32[]{:S(2)}, u32[]{:S(2)}) collective-permute-start(bf16[512,128]{1,0:T(8,128)(2,1)S(1)} %get-tuple-element.93), channel_id=1, source_target_pairs={{0,32},{32,64},{64,96},{96,0},{1,33},{33,65},{65,97},{97,1},{2,34}... | collective-permute-start | bytes 393224 | tf_op jit(solution)/shard_map/ppermute | solution.py:33
  109.4 22.7 %collective-permute-start.5 = (bf16[512,128]{1,0:T(8,128)(2,1)S(1)}, bf16[512,128]{1,0:T(8,128)(2,1)S(1)}, u32[]{:S(2)}, u32[]{:S(2)}) collective-permute-start(bf16[512,128]{1,0:T(8,128)(2,1)S(1)} %get-tuple-element.92), channel_id=1, source_target_pairs={{0,64},{32,96},{64,0},{96,32},{1,65},{33,97},{65,1},{97,33},{2,66}... | collective-permute-start | bytes 393224 | tf_op jit(solution)/shard_map/ppermute | solution.py:33
  120.9 11.3 %collective-permute-start.6 = (bf16[512,128]{1,0:T(8,128)(2,1)S(1)}, bf16[512,128]{1,0:T(8,128)(2,1)S(1)}, u32[]{:S(2)}, u32[]{:S(2)}) collective-permute-start(bf16[512,128]{1,0:T(8,128)(2,1)S(1)} %get-tuple-element.91), channel_id=1, source_target_pairs={{0,96},{32,0},{64,32},{96,64},{1,97},{33,1},{65,33},{97,65},{2,98}... | collective-permute-start | bytes 393224 | tf_op jit(solution)/shard_map/ppermute | solution.py:33
  126.9 27.5 %all-to-all-start.3 = ((bf16[64,40,128]{2,1,0:T(8,128)(2,1)}), bf16[64,40,128]{2,1,0:T(8,128)(2,1)S(1)}, u32[]{:S(2)}, u32[]{:S(2)}) async-start(bf16[64,40,128]{2,1,0:T(8,128)(2,1)} %get-tuple-element.72), calls=%async_computation.3 | async-start | bytes 1310720 | tf_op jit(solution)/shard_map/all_to_all | solution.py:612
  135.3 12.6 %collective-permute-start.10 = (bf16[128,1024]{1,0:T(8,128)(2,1)S(1)}, bf16[128,1024]{1,0:T(8,128)(2,1)S(1)}, u32[]{:S(2)}, u32[]{:S(2)}) collective-permute-start(bf16[128,1024]{1,0:T(8,128)(2,1)S(1)} %get-tuple-element.87), channel_id=1, source_target_pairs={{0,8},{8,16},{16,24},{24,0},{1,9},{9,17},{17,25},{25,1},{2,10},{10... | collective-permute-start | bytes 786440 | tf_op jit(solution)/shard_map/ppermute | solution.py:33
  136.9 16.4 %collective-permute-start.11 = (bf16[128,1024]{1,0:T(8,128)(2,1)S(1)}, bf16[128,1024]{1,0:T(8,128)(2,1)S(1)}, u32[]{:S(2)}, u32[]{:S(2)}) collective-permute-start(bf16[128,1024]{1,0:T(8,128)(2,1)S(1)} %get-tuple-element.89), channel_id=1, source_target_pairs={{0,16},{8,24},{16,0},{24,8},{1,17},{9,25},{17,1},{25,9},{2,18},{10... | collective-permute-start | bytes 786440 | tf_op jit(solution)/shard_map/ppermute | solution.py:33
  139.6 13.7 %collective-permute-start.12 = (bf16[128,1024]{1,0:T(8,128)(2,1)S(1)}, bf16[128,1024]{1,0:T(8,128)(2,1)}, u32[]{:S(2)}, u32[]{:S(2)}) collective-permute-start(bf16[128,1024]{1,0:T(8,128)(2,1)S(1)} %get-tuple-element.88), channel_id=1, source_target_pairs={{0,24},{8,0},{16,8},{24,16},{1,25},{9,1},{17,9},{25,17},{2,26},{10... | collective-permute-start | bytes 786440 | tf_op jit(solution)/shard_map/ppermute | solution.py:33
  157.0 20.8 %all-to-all-start.4 = ((bf16[64,24,128]{2,1,0:T(8,128)(2,1)}), bf16[64,24,128]{2,1,0:T(8,128)(2,1)S(1)}, u32[]{:S(2)}, u32[]{:S(2)}) async-start(bf16[64,24,128]{2,1,0:T(8,128)(2,1)} %owner.1), calls=%async_computation.4 | async-start | bytes 786432 | tf_op jit(solution)/shard_map/all_to_all | solution.py:618
  164.5 10.5 %collective-permute-start.13 = (bf16[32,1024]{1,0:T(8,128)(2,1)S(1)}, bf16[32,1024]{1,0:T(8,128)(2,1)S(1)}, u32[]{:S(2)}, u32[]{:S(2)}) collective-permute-start(bf16[32,1024]{1,0:T(8,128)(2,1)S(1)} %get-tuple-element.94), channel_id=1, source_target_pairs={{0,2},{2,4},{4,6},{6,0},{1,3},{3,5},{5,7},{7,1},{8,10},{10,12},{12... | collective-permute-start | bytes 196616 | tf_op jit(solution)/shard_map/ppermute | solution.py:33
  166.1 8.9 %collective-permute-start.14 = (bf16[32,1024]{1,0:T(8,128)(2,1)S(1)}, bf16[32,1024]{1,0:T(8,128)(2,1)S(1)}, u32[]{:S(2)}, u32[]{:S(2)}) collective-permute-start(bf16[32,1024]{1,0:T(8,128)(2,1)S(1)} %get-tuple-element.96), channel_id=1, source_target_pairs={{0,4},{2,6},{4,0},{6,2},{1,5},{3,7},{5,1},{7,3},{8,12},{10,14},{12... | collective-permute-start | bytes 196616 | tf_op jit(solution)/shard_map/ppermute | solution.py:33
  168.8 6.2 %collective-permute-start.15 = (bf16[32,1024]{1,0:T(8,128)(2,1)S(1)}, bf16[32,1024]{1,0:T(8,128)(2,1)S(1)}, u32[]{:S(2)}, u32[]{:S(2)}) collective-permute-start(bf16[32,1024]{1,0:T(8,128)(2,1)S(1)} %get-tuple-element.95), channel_id=1, source_target_pairs={{0,6},{2,0},{4,2},{6,4},{1,7},{3,1},{5,3},{7,5},{8,14},{10,8},{12,... | collective-permute-start | bytes 196616 | tf_op jit(solution)/shard_map/ppermute | solution.py:33
  (17 other events, 98.6 us)

commit v9 on v8

--- a/solution.py
+++ b/solution.py
@@ -600,12 +600,18 @@
     moe_terms = dot(returned.reshape(-1, half), either, ((0,), (0,)))
     grad_own = (cotangent_rows.astype(f32) + moe_terms).astype(bf16)
     grad_far = swapped(grad_own)
-    grad_hidden = jnp.where(
-        side == 0,
-        jnp.concatenate([grad_own, grad_far], axis=0),
-        jnp.concatenate([grad_far, grad_own], axis=0),
-    )
-
+    line, spot = lax.axis_size("sp_0"), lax.axis_index("sp_0")
+    span = width // line
+    near = lax.axis_index("tp") * (line // 2)
+    grads_line = from_line(
+        [
+            lax.dynamic_slice_in_dim(
+                grad_own, (lax.rem(spot + k, line) - near) * span, span, 0
+            )
+            for k in range(line)
+        ],
+        "sp_0",
+    )
     message, grad_gated = state_message(
         side, grad_own, grad_far, w_out, gain, gated, silu, carry, c_proj, local, rows, inverse
     )
@@ -621,13 +627,12 @@
     )
     grad_log_decay = decay_grad.T
 
-    line = lax.axis_size("sp_0")
     mixed, gate_wgrad = lax.optimization_barrier((mixed, gate_wgrad))
     mixed_line = from_line([mixed] * line, "sp_0")
-    grads_line = from_line(pieces_for(grad_hidden, "sp_0", 0), "sp_0")
-    product = dot(
-        jnp.concatenate(grads_line, axis=1), jnp.concatenate(mixed_line, axis=1), ((1,), (1,))
-    ).astype(bf16)
+    own_line = jnp.concatenate(grads_line, axis=1)
+    far_line = swapped(own_line)
+    chosen = jnp.where(spot // 2 == lax.axis_index("tp"), own_line, far_line)
+    product = dot(chosen, jnp.concatenate(mixed_line, axis=1), ((1,), (1,))).astype(bf16)
     parts = from_line(pieces_for(product, "sp_1", 0), "sp_1")
     product = sum(part.astype(f32) for part in parts).astype(bf16)
     parts = from_line(pieces_for(product, "sp_2", 0), "sp_2")

time: 183 us -> 169 us (0.923)
  waiting for transfers between devices: 72.6 us -> 60.8 us
  starting transfers between devices: 52.4 us -> 49.6 us
    ppermute x12, waiting for transfers between devices: 21.8 us -> 6.21 us  [from_line(): lax.ppermute(parts[k], axis, [(i, (i + k) % size) for i in range(size)])]
    all_to_all x1, waiting for transfers between devices: 0.01 us -> 5.62 us  [body(): came_states = lax.all_to_all(message, SP, 0, 0, tiled=True)]
    all_to_all x1, starting transfers between devices: 7.47 us -> 4.93 us  [body(): back = lax.all_to_all(back, SP, 0, 0, tiled=True)]
    all_to_all x1, waiting for transfers between devices: 2.05 us -> 0.16 us  [body(): back = lax.all_to_all(back, SP, 0, 0, tiled=True)]
    ppermute x12, starting transfers between devices: 17.9 us -> 16.1 us  [from_line(): lax.ppermute(parts[k], axis, [(i, (i + k) % size) for i in range(size)])]
    unnamed x40 -> x42, local copies, waits for them, and re-layouts: 5.01 us -> 5.89 us
  transfers between devices with their start and end apart: 21 -> 22, of which waited for: 8 -> 9; matrix products, arithmetic and copies ran while one was open for 6% -> 7% of each run, Pallas kernels for 13% -> 16%
where the time goes in v9:
time: 169 us; the launch traced here: 168 us
  waiting for transfers between devices  60.8 us (36%)
  starting transfers between devices  49.6 us (29%)
  Pallas kernels  39.7 us (23%)
  local copies, waits for them, and re-layouts  7.78 us (5%)
  matrix products  4.69 us (3%)
  other arithmetic  4.48 us (3%)
    all_to_all x1, waiting for transfers between devices, body(): came_grads = lax.all_to_all(send_grads, SP, 0, 0, tiled=True)  17.5 us
    all_to_all x1, waiting for transfers between devices, body(): came_hidden = lax.all_to_all(send_hidden, SP, 0, 0, tiled=True)  16.9 us
    ppermute x12, starting transfers between devices, from_line(): lax.ppermute(parts[k], axis, [(i, (i + k) % size) for i in range(size)])  16.1 us
    all_to_all x1, waiting for transfers between devices, body(): lax.all_to_all(summed.reshape(experts, capacity, half), SP, 0, 0, tiled=T...  11.8 us
    all_to_all x1, starting transfers between devices, body(): came_grads = lax.all_to_all(send_grads, SP, 0, 0, tiled=True)  11.7 us
    pallas_call x1, Pallas kernels, expert_rows(): pl.pallas_call(expert_rows_kernel, grid_spec=pltpu.PrefetchScalarGridSpec...  9.19 us
    pallas_call x1, Pallas kernels, expert_weights(): pl.pallas_call(weights_kernel, grid_spec=pltpu.PrefetchScalarGridSpec(num...  8.16 us
    all_to_all x1, starting transfers between devices, body(): came_states = lax.all_to_all(message, SP, 0, 0, tiled=True)  6.54 us
  transfers between devices with their start and end apart: 22, of which 9 were waited for; matrix products, arithmetic and copies ran while one was open for 7% of the time, Pallas kernels for 16%

profile of v9, /device:TPU:0, one launch (start us, length us, event | category | flops | bytes accessed | tf_op | source)
XLA Modules:
  0.0 168.0 jit_solution(10994851237994051004)
XLA Ops:
  0.7 3.1 %route.1 = (bf16[512,1024]{1,0:T(8,128)(2,1)}, bf16[512,128]{1,0:T(8,128)(2,1)}) custom-call(s32[1]{0:T(128)} %bitcast.3.side, s32[2,128]{1,0:T(2,128)} %bitcast.45, f32[2,128]{1,0:T(2,128)} %bitcast.46, bf16[128,2048]{1,0:T(8,128)(2,1)} %cotangent.1), custom_call_target="tpu_custom_call" | custom-call | tf_op jit(solution)/shard_map/route/pallas_call | solution.py:188
  3.7 11.7 %all-to-all-start = ((bf16[64,8,1024]{2,1,0:T(8,128)(2,1)}), bf16[64,8,1024]{2,1,0:T(8,128)(2,1)S(1)}, u32[]{:S(2)}, u32[]{:S(2)}) async-start(bf16[64,8,1024]{2,1,0:T(8,128)(2,1)} %bitcast.40), calls=%async_computation | async-start | bytes 2097152 | tf_op jit(solution)/shard_map/all_to_all | solution.py:584
  16.8 17.5 %all-to-all-done = bf16[64,8,1024]{2,1,0:T(8,128)(2,1)S(1)} async-done(((bf16[64,8,1024]{2,1,0:T(8,128)(2,1)}), bf16[64,8,1024]{2,1,0:T(8,128)(2,1)S(1)}, u32[]{:S(2)}, u32[]{:S(2)}) %all-to-all-start) | async-done | bytes 1048608 | tf_op jit(solution)/shard_map/all_to_all | solution.py:584
  34.3 2.7 %collective-permute-done.other.grads_far = bf16[512,1024]{1,0:T(8,128)(2,1)S(1)} collective-permute-done((bf16[512,1024]{1,0:T(8,128)(2,1)S(1)}, bf16[512,1024]{1,0:T(8,128)(2,1)S(1)}, u32[]{:S(2)}, u32[]{:S(2)}) %collective-permute-start) | collective-permute-done | bytes 1048608 | tf_op jit(solution)/shard_map/ppermute | solution.py:27
  37.9 9.2 %expert_rows.1 = (bf16[512,512]{1,0:T(8,128)(2,1)}, bf16[512,512]{1,0:T(8,128)(2,1)}, bf16[512,512]{1,0:T(8,128)(2,1)}, bf16[512,1024]{1,0:T(8,128)(2,1)}, bf16[512,1024]{1,0:T(8,128)(2,1)}) custom-call(s32[1]{0:T(128)} %bitcast.3.side, bf16[512,1024]{1,0:T(8,128)(2,1)} %bitcast.28, bf16[512,1024]{1,0:T(8,128)(2,1)} %copy-done.9, bf16[512,512]{1,0:T(8,128)(2,1)} %bitcast.41, ...), custom_call_target="tpu_custom_call" | custom-call | tf_op jit(solution)/shard_map/expert_rows/pallas_call | solution.py:92
  47.3 4.8 %all-to-all-start.1 = ((bf16[64,8,1024]{2,1,0:T(8,128)(2,1)}), bf16[64,8,1024]{2,1,0:T(8,128)(2,1)S(1)}, u32[]{:S(2)}, u32[]{:S(2)}) async-start(bf16[64,8,1024]{2,1,0:T(8,128)(2,1)} %fusion), calls=%async_computation.1 | async-start | bytes 2097152 | tf_op jit(solution)/shard_map/all_to_all | solution.py:586
  52.2 2.6 %add_convert_fusion = bf16[512,1024]{1,0:T(8,128)(2,1)} fusion(bf16[512,1024]{1,0:T(8,128)(2,1)} %collective-permute-done.1, bf16[512,1024]{1,0:T(8,128)(2,1)S(1)} %copy-done.13), kind=kLoop, calls=%fused_computation | loop fusion | flops 2097152 | bytes 3145728 | tf_op jit(solution)/shard_map/convert_element_type | solution.py:592
  54.8 16.9 %all-to-all-done.1 = bf16[64,8,1024]{2,1,0:T(8,128)(2,1)S(1)} async-done(((bf16[64,8,1024]{2,1,0:T(8,128)(2,1)}), bf16[64,8,1024]{2,1,0:T(8,128)(2,1)S(1)}, u32[]{:S(2)}, u32[]{:S(2)}) %all-to-all-start.1) | async-done | bytes 1048608 | tf_op jit(solution)/shard_map/all_to_all | solution.py:586
  71.6 4.8 %all-to-all-start.2 = ((bf16[64,8,1024]{2,1,0:T(8,128)(2,1)}), bf16[64,8,1024]{2,1,0:T(8,128)(2,1)S(1)}, u32[]{:S(2)}, u32[]{:S(2)}) async-start(bf16[64,8,1024]{2,1,0:T(8,128)(2,1)} %bitcast.18), calls=%async_computation.2 | async-start | bytes 2097152 | tf_op jit(solution)/shard_map/all_to_all | solution.py:594
  78.3 4.8 %shard_map.232 = (bf16[1024,128]{1,0:T(8,128)(2,1)}, f32[1024,128]{1,0:T(8,128)}, f32[1024,128]{1,0:T(8,128)}, f32[1024,128]{1,0:T(8,128)}, bf16[16,128,128]{2,1...) custom-call(bf16[128,1024]{1,0:T(8,128)(2,1)} %scan_in.1, ...), custom_call_target="tpu_custom_call" | custom-call | tf_op jit(solution)/shard_map/pallas_call | solution.py:286
  83.1 11.8 %all-to-all-done.2 = bf16[64,8,1024]{2,1,0:T(8,128)(2,1)S(1)} async-done(((bf16[64,8,1024]{2,1,0:T(8,128)(2,1)}), bf16[64,8,1024]{2,1,0:T(8,128)(2,1)S(1)}, u32[]{:S(2)}, u32[]{:S(2)}) %all-to-all-start.2) | async-done | bytes 1048608 | tf_op jit(solution)/shard_map/all_to_all | solution.py:594
  97.2 1.7 %collective-permute-start.4 = (bf16[512,128]{1,0:T(8,128)(2,1)S(1)}, bf16[512,128]{1,0:T(8,128)(2,1)S(1)}, u32[]{:S(2)}, u32[]{:S(2)}) collective-permute-start(bf16[512,128]{1,0:T(8,128)(2,1)S(1)} %get-tuple-element.95), channel_id=1, source_target_pairs={{0,64},{32,96},{64,0},{96,32},{1,65},{33,97},{65,1},{97,33},{2,66}... | collective-permute-start | bytes 393224 | tf_op jit(solution)/shard_map/ppermute | solution.py:33
  98.9 2.5 %collective-permute-done.5 = bf16[512,128]{1,0:T(8,128)(2,1)S(1)} collective-permute-done((bf16[512,128]{1,0:T(8,128)(2,1)S(1)}, bf16[512,128]{1,0:T(8,128)(2,1)S(1)}, u32[]{:S(2)}, u32[]{:S(2)}) %collective-permute-start.5) | collective-permute-done | bytes 131104 | tf_op jit(solution)/shard_map/ppermute | solution.py:33
  101.4 2.3 %collective-permute-done.4 = bf16[512,128]{1,0:T(8,128)(2,1)S(1)} collective-permute-done((bf16[512,128]{1,0:T(8,128)(2,1)S(1)}, bf16[512,128]{1,0:T(8,128)(2,1)S(1)}, u32[]{:S(2)}, u32[]{:S(2)}) %collective-permute-start.4) | collective-permute-done | bytes 131104 | tf_op jit(solution)/shard_map/ppermute | solution.py:33
  105.8 8.2 %weights.1 = (bf16[512,2048]{1,0:T(8,128)(2,1)}, bf16[2048,512]{1,0:T(8,128)(2,1)}, bf16[2048,512]{1,0:T(8,128)(2,1)}) custom-call(s32[1]{0:T(128)} %bitcast.3.side, bf16[512,512]{1,0:T(8,128)(2,1)} %get-tuple-element.52.active, bf16[512,512]{1,0:T(8,128)(2,1)} %get-tuple-element.53.gate_grad, bf16[512,512]{1,0:T(8,128)(2,1)} %get-tuple-element.54.up_grad, ...), custom_call_target="tpu_custom_call" | custom-call | tf_op jit(solution)/shard_map/weights/pallas_call | solution.py:133
  117.8 6.1 %message.1 = (bf16[64,40,128]{2,1,0:T(8,128)(2,1)}, f32[1024,128]{1,0:T(8,128)}) custom-call(s32[1]{0:T(128)} %bitcast.3.side, bf16[1024,128]{1,0:T(8,128)(2,1)} %copy-done.10, bf16[1024,128]{1,0:T(8,128)(2,1)} %copy-done.15, bf16[1024,2048]{1,0:T(8,128)(2,1)} %out_far.1, bf16[1024,2048]{1,0:T(8,128)(2,1)} %out_far.1, f32[1024,1]{1,0:T(8,128)} %copy.27.gain, ...), custom_call_target="tpu_custom_call" | custom-call | tf_op jit(solution)/shard_map/message/pallas_call | solution.py:365
  123.9 6.5 %all-to-all-start.3 = ((bf16[64,40,128]{2,1,0:T(8,128)(2,1)}), bf16[64,40,128]{2,1,0:T(8,128)(2,1)S(1)}, u32[]{:S(2)}, u32[]{:S(2)}) async-start(bf16[64,40,128]{2,1,0:T(8,128)(2,1)} %get-tuple-element.72), calls=%async_computation.3 | async-start | bytes 1310720 | tf_op jit(solution)/shard_map/all_to_all | solution.py:618
  132.0 1.9 %convolution_convert_fusion.1 = bf16[512,1024]{1,0:T(8,128)(2,1)S(1)} fusion(bf16[1024,128]{1,0:T(8,128)(2,1)} %copy-done.18, bf16[1024,128]{1,0:T(8,128)(2,1)} %copy-done.19, bf16[1024,128]{1,0:T(8,128)(2,1)} %copy-done.20, bf16[1024,128]{1,0:T(8,128)(2,1)S(1)} %copy-done.17, bf16[512,512]{1,0:T(8,128)(2,1)} %collective-permute-done.6, pred[]{:T(512)S(6)} %eq.6, ...), kind=kOutput, calls=%fused_computation.2 | convolution fusion | flops 543948800 | bytes 3145729 | tf_op jit(solution)/shard_map/dot_general | solution.py:23
  137.2 1.9 %collective-permute-start.11 = (bf16[128,1024]{1,0:T(8,128)(2,1)S(1)}, bf16[128,1024]{1,0:T(8,128)(2,1)}, u32[]{:S(2)}, u32[]{:S(2)}) collective-permute-start(bf16[128,1024]{1,0:T(8,128)(2,1)S(1)} %get-tuple-element.89), channel_id=1, source_target_pairs={{0,16},{8,24},{16,0},{24,8},{1,17},{9,25},{17,1},{25,9},{2,18},{10... | collective-permute-start | bytes 786440 | tf_op jit(solution)/shard_map/ppermute | solution.py:33
  139.1 5.6 %all-to-all-done.3.came = bf16[64,40,128]{2,1,0:T(8,128)(2,1)S(1)} async-done(((bf16[64,40,128]{2,1,0:T(8,128)(2,1)}), bf16[64,40,128]{2,1,0:T(8,128)(2,1)S(1)}, u32[]{:S(2)}, u32[]{:S(2)}) %all-to-all-start.3) | async-done | bytes 655392 | tf_op jit(solution)/shard_map/all_to_all | solution.py:618
  144.7 2.5 %owner.1 = bf16[64,24,128]{2,1,0:T(8,128)(2,1)} custom-call(s32[1]{0:T(128)} %bitcast.20.lead, bf16[64,40,128]{2,1,0:T(8,128)(2,1)S(1)} %all-to-all-done.3.came), custom_call_target="tpu_custom_call" | custom-call | tf_op jit(solution)/shard_map/owner/pallas_call | solution.py:489
  147.2 4.9 %all-to-all-start.4 = ((bf16[64,24,128]{2,1,0:T(8,128)(2,1)}), bf16[64,24,128]{2,1,0:T(8,128)(2,1)S(1)}, u32[]{:S(2)}, u32[]{:S(2)}) async-start(bf16[64,24,128]{2,1,0:T(8,128)(2,1)} %owner.1), calls=%async_computation.4 | async-start | bytes 786432 | tf_op jit(solution)/shard_map/all_to_all | solution.py:624
  156.6 1.9 %collective-permute-start.14 = (bf16[32,1024]{1,0:T(8,128)(2,1)S(1)}, bf16[32,1024]{1,0:T(8,128)(2,1)S(1)}, u32[]{:S(2)}, u32[]{:S(2)}) collective-permute-start(bf16[32,1024]{1,0:T(8,128)(2,1)S(1)} %get-tuple-element.92), channel_id=1, source_target_pairs={{0,4},{2,6},{4,0},{6,2},{1,5},{3,7},{5,1},{7,3},{8,12},{10,14},{12... | collective-permute-start | bytes 196616 | tf_op jit(solution)/shard_map/ppermute | solution.py:33
  158.5 4.7 %inside.1 = (bf16[128,1024]{1,0:T(8,128)(2,1)}, f32[1024,128]{1,0:T(8,128)}, f32[128,512]{1,0:T(8,128)}, bf16[128,512]{1,0:T(8,128)(2,1)}, f32[4,4,128]{2,1,0:T(4,128)}) custom-call(f32[1024,128]{1,0:T(8,128)} %get-tuple-element.75.grad_in, f32[1024,128]{1,0:T(8,128)} %get-tuple-element.66.gated_in, f32[1024,128]{1,0:T(8,128)} %get-tuple-element.67.silu_in, ...), custom_call_target="tpu_custom_call" | custom-call | tf_op jit(solution)/shard_map/inside/pallas_call | solution.py:436
  (83 shorter events, 26.8 us)
Async XLA Ops:
  3.7 30.6 %all-to-all-start = ((bf16[64,8,1024]{2,1,0:T(8,128)(2,1)}), bf16[64,8,1024]{2,1,0:T(8,128)(2,1)S(1)}, u32[]{:S(2)}, u32[]{:S(2)}) async-start(bf16[64,8,1024]{2,1,0:T(8,128)(2,1)} %bitcast.40), calls=%async_computation | async-start | bytes 2097152 | tf_op jit(solution)/shard_map/all_to_all | solution.py:584
  34.3 2.7 %collective-permute-start = (bf16[512,1024]{1,0:T(8,128)(2,1)S(1)}, bf16[512,1024]{1,0:T(8,128)(2,1)S(1)}, u32[]{:S(2)}, u32[]{:S(2)}) collective-permute-start(bf16[512,1024]{1,0:T(8,128)(2,1)S(1)} %bitcast.27), channel_id=1, source_target_pairs={{0,1},{1,0},{2,3},{3,2},{4,5},{5,4},{6,7},{7,6},{8,9},{9,8},{10,11... | collective-permute-start | bytes 3145736 | tf_op jit(solution)/shard_map/ppermute | solution.py:27
  47.1 5.0 %collective-permute-start.1 = (bf16[512,1024]{1,0:T(8,128)(2,1)}, bf16[512,1024]{1,0:T(8,128)(2,1)}, u32[]{:S(2)}, u32[]{:S(2)}) collective-permute-start(bf16[512,1024]{1,0:T(8,128)(2,1)} %get-tuple-element.56), channel_id=1, source_target_pairs={{0,1},{1,0},{2,3},{3,2},{4,5},{5,4},{6,7},{7,6},{8,9},{9,8},{10,11... | collective-permute-start | bytes 3145736 | tf_op jit(solution)/shard_map/ppermute | solution.py:27
  47.3 24.4 %all-to-all-start.1 = ((bf16[64,8,1024]{2,1,0:T(8,128)(2,1)}), bf16[64,8,1024]{2,1,0:T(8,128)(2,1)S(1)}, u32[]{:S(2)}, u32[]{:S(2)}) async-start(bf16[64,8,1024]{2,1,0:T(8,128)(2,1)} %fusion), calls=%async_computation.1 | async-start | bytes 2097152 | tf_op jit(solution)/shard_map/all_to_all | solution.py:586
  52.1 24.4 %copy-start.16 = (bf16[1024]{0:T(1024)(128)(2,1)S(1)}, bf16[1024]{0:T(1024)(128)(2,1)}, u32[]{:S(2)}) copy-start(bf16[1024]{0:T(1024)(128)(2,1)} %param.27) | copy-start | bytes 6148
  54.8 22.8 %copy-start.12 = (bf16[128,2048]{1,0:T(8,128)(2,1)S(1)}, bf16[128,2048]{1,0:T(8,128)(2,1)}, u32[]{:S(2)}) copy-start(bf16[128,2048]{1,0:T(8,128)(2,1)} %cotangent.1) | copy-start | bytes 1572868
  71.6 23.2 %all-to-all-start.2 = ((bf16[64,8,1024]{2,1,0:T(8,128)(2,1)}), bf16[64,8,1024]{2,1,0:T(8,128)(2,1)S(1)}, u32[]{:S(2)}, u32[]{:S(2)}) async-start(bf16[64,8,1024]{2,1,0:T(8,128)(2,1)} %bitcast.18), calls=%async_computation.2 | async-start | bytes 2097152 | tf_op jit(solution)/shard_map/all_to_all | solution.py:594
  76.4 29.3 %collective-permute-start.2 = (bf16[512,1024]{1,0:T(8,128)(2,1)S(1)}, bf16[512,1024]{1,0:T(8,128)(2,1)}, u32[]{:S(2)}, u32[]{:S(2)}) collective-permute-start(bf16[512,1024]{1,0:T(8,128)(2,1)S(1)} %bitcast.36), channel_id=1, source_target_pairs={{0,1},{1,0},{2,3},{3,2},{4,5},{5,4},{6,7},{7,6},{8,9},{9,8},{10,11... | collective-permute-start | bytes 3145736 | tf_op jit(solution)/shard_map/ppermute | solution.py:27
  96.4 5.0 %collective-permute-start.5 = (bf16[512,128]{1,0:T(8,128)(2,1)S(1)}, bf16[512,128]{1,0:T(8,128)(2,1)S(1)}, u32[]{:S(2)}, u32[]{:S(2)}) collective-permute-start(bf16[512,128]{1,0:T(8,128)(2,1)S(1)} %get-tuple-element.94), channel_id=1, source_target_pairs={{0,96},{32,0},{64,32},{96,64},{1,97},{33,1},{65,33},{97,65},{2,98}... | collective-permute-start | bytes 393224 | tf_op jit(solution)/shard_map/ppermute | solution.py:33
  97.2 6.5 %collective-permute-start.4 = (bf16[512,128]{1,0:T(8,128)(2,1)S(1)}, bf16[512,128]{1,0:T(8,128)(2,1)S(1)}, u32[]{:S(2)}, u32[]{:S(2)}) collective-permute-start(bf16[512,128]{1,0:T(8,128)(2,1)S(1)} %get-tuple-element.95), channel_id=1, source_target_pairs={{0,64},{32,96},{64,0},{96,32},{1,65},{33,97},{65,1},{97,33},{2,66}... | collective-permute-start | bytes 393224 | tf_op jit(solution)/shard_map/ppermute | solution.py:33
  98.9 6.2 %collective-permute-start.3 = (bf16[512,128]{1,0:T(8,128)(2,1)S(1)}, bf16[512,128]{1,0:T(8,128)(2,1)S(1)}, u32[]{:S(2)}, u32[]{:S(2)}) collective-permute-start(bf16[512,128]{1,0:T(8,128)(2,1)S(1)} %get-tuple-element.96), channel_id=1, source_target_pairs={{0,32},{32,64},{64,96},{96,0},{1,33},{33,65},{65,97},{97,1},{2,34}... | collective-permute-start | bytes 393224 | tf_op jit(solution)/shard_map/ppermute | solution.py:33
  105.2 26.8 %collective-permute-start.6 = (bf16[512,512]{1,0:T(8,128)(2,1)S(1)}, bf16[512,512]{1,0:T(8,128)(2,1)}, u32[]{:S(2)}, u32[]{:S(2)}) collective-permute-start(bf16[512,512]{1,0:T(8,128)(2,1)S(1)} %pad_maximum_fusion), channel_id=1, source_target_pairs={{0,1},{1,0},{2,3},{3,2},{4,5},{5,4},{6,7},{7,6},{8,9},{9,8},{10,11... | collective-permute-start | bytes 1572872 | tf_op jit(solution)/shard_map/ppermute | solution.py:27
  105.3 11.9 %collective-permute-start.16 = (bf16[1024,128]{1,0:T(8,128)(2,1)S(1)}, bf16[1024,128]{1,0:T(8,128)(2,1)S(1)}, u32[]{:S(2)}, u32[]{:S(2)}) collective-permute-start(bf16[1024,128]{1,0:T(8,128)(2,1)S(1)} %fusion.1.grad_own), channel_id=1, source_target_pairs={{0,1},{1,0},{2,3},{3,2},{4,5},{5,4},{6,7},{7,6},{8,9},{9,8},{10,11... | collective-permute-start | bytes 786440 | tf_op jit(solution)/shard_map/ppermute | solution.py:27
  113.9 16.5 %collective-permute-start.9 = (bf16[1024,128]{1,0:T(8,128)(2,1)S(1)}, bf16[1024,128]{1,0:T(8,128)(2,1)S(1)}, u32[]{:S(2)}, u32[]{:S(2)}) collective-permute-start(bf16[1024,128]{1,0:T(8,128)(2,1)S(1)} %copy-done.17), channel_id=1, source_target_pairs={{0,96},{32,0},{64,32},{96,64},{1,97},{33,1},{65,33},{97,65},{2,98}... | collective-permute-start | bytes 786440 | tf_op jit(solution)/shard_map/ppermute | solution.py:33
  115.0 15.5 %collective-permute-start.8 = (bf16[1024,128]{1,0:T(8,128)(2,1)S(1)}, bf16[1024,128]{1,0:T(8,128)(2,1)S(1)}, u32[]{:S(2)}, u32[]{:S(2)}) collective-permute-start(bf16[1024,128]{1,0:T(8,128)(2,1)S(1)} %copy-done.17), channel_id=1, source_target_pairs={{0,64},{32,96},{64,0},{96,32},{1,65},{33,97},{65,1},{97,33},{2,66}... | collective-permute-start | bytes 786440 | tf_op jit(solution)/shard_map/ppermute | solution.py:33
  116.2 14.2 %collective-permute-start.7 = (bf16[1024,128]{1,0:T(8,128)(2,1)S(1)}, bf16[1024,128]{1,0:T(8,128)(2,1)S(1)}, u32[]{:S(2)}, u32[]{:S(2)}) collective-permute-start(bf16[1024,128]{1,0:T(8,128)(2,1)S(1)} %copy-done.17), channel_id=1, source_target_pairs={{0,32},{32,64},{64,96},{96,0},{1,33},{33,65},{65,97},{97,1},{2,34}... | collective-permute-start | bytes 786440 | tf_op jit(solution)/shard_map/ppermute | solution.py:33
  123.9 20.8 %all-to-all-start.3 = ((bf16[64,40,128]{2,1,0:T(8,128)(2,1)}), bf16[64,40,128]{2,1,0:T(8,128)(2,1)S(1)}, u32[]{:S(2)}, u32[]{:S(2)}) async-start(bf16[64,40,128]{2,1,0:T(8,128)(2,1)} %get-tuple-element.72), calls=%async_computation.3 | async-start | bytes 1310720 | tf_op jit(solution)/shard_map/all_to_all | solution.py:618
  133.9 18.2 %collective-permute-start.10 = (bf16[128,1024]{1,0:T(8,128)(2,1)S(1)}, bf16[128,1024]{1,0:T(8,128)(2,1)S(1)}, u32[]{:S(2)}, u32[]{:S(2)}) collective-permute-start(bf16[128,1024]{1,0:T(8,128)(2,1)S(1)} %get-tuple-element.87), channel_id=1, source_target_pairs={{0,8},{8,16},{16,24},{24,0},{1,9},{9,17},{17,25},{25,1},{2,10},{10... | collective-permute-start | bytes 786440 | tf_op jit(solution)/shard_map/ppermute | solution.py:33
  135.5 16.6 %collective-permute-start.12 = (bf16[128,1024]{1,0:T(8,128)(2,1)S(1)}, bf16[128,1024]{1,0:T(8,128)(2,1)S(1)}, u32[]{:S(2)}, u32[]{:S(2)}) collective-permute-start(bf16[128,1024]{1,0:T(8,128)(2,1)S(1)} %get-tuple-element.88), channel_id=1, source_target_pairs={{0,24},{8,0},{16,8},{24,16},{1,25},{9,1},{17,9},{25,17},{2,26},{10... | collective-permute-start | bytes 786440 | tf_op jit(solution)/shard_map/ppermute | solution.py:33
  137.2 15.0 %collective-permute-start.11 = (bf16[128,1024]{1,0:T(8,128)(2,1)S(1)}, bf16[128,1024]{1,0:T(8,128)(2,1)}, u32[]{:S(2)}, u32[]{:S(2)}) collective-permute-start(bf16[128,1024]{1,0:T(8,128)(2,1)S(1)} %get-tuple-element.89), channel_id=1, source_target_pairs={{0,16},{8,24},{16,0},{24,8},{1,17},{9,25},{17,1},{25,9},{2,18},{10... | collective-permute-start | bytes 786440 | tf_op jit(solution)/shard_map/ppermute | solution.py:33
  147.2 16.9 %all-to-all-start.4 = ((bf16[64,24,128]{2,1,0:T(8,128)(2,1)}), bf16[64,24,128]{2,1,0:T(8,128)(2,1)S(1)}, u32[]{:S(2)}, u32[]{:S(2)}) async-start(bf16[64,24,128]{2,1,0:T(8,128)(2,1)} %owner.1), calls=%async_computation.4 | async-start | bytes 786432 | tf_op jit(solution)/shard_map/all_to_all | solution.py:624
  153.3 9.9 %collective-permute-start.13 = (bf16[32,1024]{1,0:T(8,128)(2,1)S(1)}, bf16[32,1024]{1,0:T(8,128)(2,1)S(1)}, u32[]{:S(2)}, u32[]{:S(2)}) collective-permute-start(bf16[32,1024]{1,0:T(8,128)(2,1)S(1)} %get-tuple-element.90), channel_id=1, source_target_pairs={{0,2},{2,4},{4,6},{6,0},{1,3},{3,5},{5,7},{7,1},{8,10},{10,12},{12... | collective-permute-start | bytes 196616 | tf_op jit(solution)/shard_map/ppermute | solution.py:33
  155.0 8.3 %collective-permute-start.15 = (bf16[32,1024]{1,0:T(8,128)(2,1)S(1)}, bf16[32,1024]{1,0:T(8,128)(2,1)S(1)}, u32[]{:S(2)}, u32[]{:S(2)}) collective-permute-start(bf16[32,1024]{1,0:T(8,128)(2,1)S(1)} %get-tuple-element.91), channel_id=1, source_target_pairs={{0,6},{2,0},{4,2},{6,4},{1,7},{3,1},{5,3},{7,5},{8,14},{10,8},{12,... | collective-permute-start | bytes 196616 | tf_op jit(solution)/shard_map/ppermute | solution.py:33
  156.6 6.6 %collective-permute-start.14 = (bf16[32,1024]{1,0:T(8,128)(2,1)S(1)}, bf16[32,1024]{1,0:T(8,128)(2,1)S(1)}, u32[]{:S(2)}, u32[]{:S(2)}) collective-permute-start(bf16[32,1024]{1,0:T(8,128)(2,1)S(1)} %get-tuple-element.92), channel_id=1, source_target_pairs={{0,4},{2,6},{4,0},{6,2},{1,5},{3,7},{5,1},{7,3},{8,12},{10,14},{12... | collective-permute-start | bytes 196616 | tf_op jit(solution)/shard_map/ppermute | solution.py:33
  (19 other events, 100.5 us)

commit v10 on v9

--- a/solution.py
+++ b/solution.py
@@ -396,7 +396,7 @@
 
 def inside_kernel(
     grad_in, gated_in, silu_in, slope_in, mix_in, decay_in, x_in, b_proj, c_proj, entry, rows_in,
-    gate_grad, x_grad, b_grad, c_grad, y_dots,
+    gate_grad, packed, c_grad,
 ):
     tokens = x_in.shape[1]
     grad_gated = grad_in[...]
@@ -411,14 +411,16 @@
         head = slice(r * HEAD_DIM, (r + 1) * HEAD_DIM)
         inside.append(dot(grad_y_b[head, :], mix_in[r], ((1,), (0,))))
         weights = weights + decay_in[r] * dot(grad_y_b[head, :], x[head, :], ((0,), (0,)))
-    x_grad[...] = jnp.concatenate(inside, axis=0)
+    packed[0, :GROUP, :] = jnp.concatenate(inside, axis=0)
     weights = weights.astype(bf16)
     c_grad[...] = (
         dot(weights, b_proj[...], ((1,), (0,)))
         + dot(grown, entry[...].astype(bf16), ((0,), (0,)))
     ).astype(bf16)
-    b_grad[...] = dot(weights, c_proj[...], ((0,), (0,)))
-    y_dots[0] = jnp.concatenate(head_sums(grad_gated * gated_in[...]), axis=0)
+    packed[0, GROUP : GROUP + tokens, :] = dot(weights, c_proj[...], ((0,), (0,)))
+    dots = head_sums(grad_gated * gated_in[...])
+    zero = jnp.zeros((8 - PER_GROUP, tokens), f32)
+    packed[0, GROUP + tokens :, :] = jnp.concatenate(dots + [zero], axis=0)
 
 
 def inside_grads(grad, gated, silu, slope, mix, decay, x, b_proj, c_proj, entry, rows):
@@ -428,10 +430,8 @@
     square = pl.BlockSpec((PER_GROUP, tokens, tokens), lambda i: (i, 0, 0))
     outs = [
         ((tokens, inner), bf16),
-        ((inner, tokens), f32),
-        (b_proj.shape, f32),
+        ((inner // GROUP, GROUP + tokens + 8, tokens), f32),
         (b_proj.shape, bf16),
-        ((inner // GROUP, PER_GROUP, tokens), f32),
     ]
     return pl.pallas_call(
         inside_kernel,
@@ -442,10 +442,8 @@
         + [pl.BlockSpec((3, 1, PER_GROUP, tokens), lambda i: (0, i, 0, 0))],
         out_specs=[
             pl.BlockSpec((tokens, GROUP), lambda i: (0, i)),
-            channels,
+            pl.BlockSpec((1, GROUP + tokens + 8, tokens), lambda i: (i, 0, 0)),
             tokens_by,
-            tokens_by,
-            pl.BlockSpec((1, PER_GROUP, tokens), lambda i: (i, 0, 0)),
         ],
         out_shape=[jax.ShapeDtypeStruct(*x) for x in outs],
         name="inside",
@@ -501,7 +499,7 @@
     )(lead, came)
 
 
-def final_kernel(back, b_proj, x_in, tail_in, rows_in, x_inside, y_dots, b_inside, x_grad, b_grad, decay_grad):
+def final_kernel(back, b_proj, x_in, tail_in, rows_in, packed, x_grad, b_grad, decay_grad):
     groups = x_in.shape[0] // GROUP
     pieces = GROUP // 16
     tokens = x_in.shape[1]
@@ -512,13 +510,16 @@
         states = slice(g * STATE, (g + 1) * STATE)
         later = back[g * pieces : (g + 1) * pieces, 0:16, :].reshape(GROUP, STATE)
         carried = dot(later, b_proj[:, states], ((1,), (1,)))
-        grad = x_inside[span, :] + carried * per_head(rows_in[1, g], 0)
+        grad = packed[g, :GROUP, :] + carried * per_head(rows_in[1, g], 0)
         x_grad[:, span] = jnp.transpose(grad).astype(bf16)
         b_grad[:, states] = (
-            b_inside[:, states] + dot(tail_in[span, :], later, ((0,), (0,)))
+            packed[g, GROUP : GROUP + tokens, :] + dot(tail_in[span, :], later, ((0,), (0,)))
         ).astype(bf16)
         dots = dots + head_sums(x_in[span, :].astype(f32) * grad)
-    own = jnp.concatenate([y_dots[g] for g in range(groups)], axis=0)
+    lowest = GROUP + tokens
+    own = jnp.concatenate(
+        [packed[g, lowest : lowest + PER_GROUP, :] for g in range(groups)], axis=0
+    )
     own = own - jnp.concatenate(dots, axis=0)
     after = (grid_of(tokens, tokens, 0) >= grid_of(tokens, tokens, 1)).astype(f32)
     extra = jnp.sum(back[:, 16:24, :].astype(f32), axis=1)
@@ -526,7 +527,7 @@
     decay_grad[...] = exact_dot(own, after, ((1,), (0,))) + extra
 
 
-def final(back, b_proj, x, x_tail, rows, x_inside, y_dots, b_inside):
+def final(back, b_proj, x, x_tail, rows, packed):
     inner, tokens = x.shape
     return whole_call(
         final_kernel,
@@ -536,7 +537,7 @@
             (b_proj.shape, bf16),
             ((inner // HEAD_DIM, tokens), f32),
         ],
-        back, b_proj, x, x_tail, rows, x_inside, y_dots, b_inside,
+        back, b_proj, x, x_tail, rows, packed,
     )
 
 
@@ -618,12 +619,12 @@
     came_states = lax.all_to_all(message, SP, 0, 0, tiled=True)
     lead = lax.rem(lax.axis_index(SP), HEAD_DIM // 16) == 0
     back = owner_scan(lead.astype(jnp.int32)[None], came_states)
-    grad_gate_in, x_inside, b_inside, grad_c_proj, y_dots = inside_grads(
+    grad_gate_in, packed, grad_c_proj = inside_grads(
         grad_gated, gated, silu, slope, mix, decay, x, b_proj, c_proj, entry, rows
     )
     back = lax.all_to_all(back, SP, 0, 0, tiled=True)
     grad_scan_in, grad_b_proj, decay_grad = final(
-        back, b_proj, x, x_tail, rows, x_inside, y_dots, b_inside
+        back, b_proj, x, x_tail, rows, packed
     )
     grad_log_decay = decay_grad.T
 

time: 169 us -> 167 us (0.988)
    unnamed x42 -> x38, local copies, waits for them, and re-layouts: 5.89 us -> 4.33 us
  transfers between devices with their start and end apart: 22 -> 22, of which waited for: 9 -> 8; matrix products, arithmetic and copies ran while one was open for 7% -> 7% of each run, Pallas kernels for 16% -> 16%
where the time goes in v10:
time: 167 us; the launch traced here: 166 us
  waiting for transfers between devices  60.7 us (36%)
  starting transfers between devices  49.6 us (30%)
  Pallas kernels  39.8 us (24%)
  local copies, waits for them, and re-layouts  6.22 us (4%)
  matrix products  4.69 us (3%)
  other arithmetic  4.48 us (3%)
    all_to_all x1, waiting for transfers between devices, body(): came_grads = lax.all_to_all(send_grads, SP, 0, 0, tiled=True)  17.5 us
    all_to_all x1, waiting for transfers between devices, body(): came_hidden = lax.all_to_all(send_hidden, SP, 0, 0, tiled=True)  16.9 us
    ppermute x12, starting transfers between devices, from_line(): lax.ppermute(parts[k], axis, [(i, (i + k) % size) for i in range(size)])  16.1 us
    all_to_all x1, waiting for transfers between devices, body(): lax.all_to_all(summed.reshape(experts, capacity, half), SP, 0, 0, tiled=T...  11.8 us
    all_to_all x1, starting transfers between devices, body(): came_grads = lax.all_to_all(send_grads, SP, 0, 0, tiled=True)  11.7 us
    pallas_call x1, Pallas kernels, expert_rows(): pl.pallas_call(expert_rows_kernel, grid_spec=pltpu.PrefetchScalarGridSpec...  9.19 us
    pallas_call x1, Pallas kernels, expert_weights(): pl.pallas_call(weights_kernel, grid_spec=pltpu.PrefetchScalarGridSpec(num...  8.15 us
    all_to_all x1, starting transfers between devices, body(): came_states = lax.all_to_all(message, SP, 0, 0, tiled=True)  6.55 us
  transfers between devices with their start and end apart: 22, of which 8 were waited for; matrix products, arithmetic and copies ran while one was open for 7% of the time, Pallas kernels for 16%

profile of v10, /device:TPU:0, one launch (start us, length us, event | category | flops | bytes accessed | tf_op | source)
XLA Modules:
  0.0 166.5 jit_solution(5935105234479416526)
XLA Ops:
  0.7 3.1 %route.1 = (bf16[512,1024]{1,0:T(8,128)(2,1)}, bf16[512,128]{1,0:T(8,128)(2,1)}) custom-call(s32[1]{0:T(128)} %bitcast.3.side, s32[2,128]{1,0:T(2,128)} %bitcast.45, f32[2,128]{1,0:T(2,128)} %bitcast.46, bf16[128,2048]{1,0:T(8,128)(2,1)} %cotangent.1), custom_call_target="tpu_custom_call" | custom-call | tf_op jit(solution)/shard_map/route/pallas_call | solution.py:188
  3.7 11.7 %all-to-all-start = ((bf16[64,8,1024]{2,1,0:T(8,128)(2,1)}), bf16[64,8,1024]{2,1,0:T(8,128)(2,1)S(1)}, u32[]{:S(2)}, u32[]{:S(2)}) async-start(bf16[64,8,1024]{2,1,0:T(8,128)(2,1)} %bitcast.40), calls=%async_computation | async-start | bytes 2097152 | tf_op jit(solution)/shard_map/all_to_all | solution.py:585
  16.8 17.5 %all-to-all-done = bf16[64,8,1024]{2,1,0:T(8,128)(2,1)S(1)} async-done(((bf16[64,8,1024]{2,1,0:T(8,128)(2,1)}), bf16[64,8,1024]{2,1,0:T(8,128)(2,1)S(1)}, u32[]{:S(2)}, u32[]{:S(2)}) %all-to-all-start) | async-done | bytes 1048608 | tf_op jit(solution)/shard_map/all_to_all | solution.py:585
  34.3 2.7 %collective-permute-done.other.grads_far = bf16[512,1024]{1,0:T(8,128)(2,1)S(1)} collective-permute-done((bf16[512,1024]{1,0:T(8,128)(2,1)S(1)}, bf16[512,1024]{1,0:T(8,128)(2,1)S(1)}, u32[]{:S(2)}, u32[]{:S(2)}) %collective-permute-start) | collective-permute-done | bytes 1048608 | tf_op jit(solution)/shard_map/ppermute | solution.py:27
  37.9 9.2 %expert_rows.1 = (bf16[512,512]{1,0:T(8,128)(2,1)}, bf16[512,512]{1,0:T(8,128)(2,1)}, bf16[512,512]{1,0:T(8,128)(2,1)}, bf16[512,1024]{1,0:T(8,128)(2,1)}, bf16[512,1024]{1,0:T(8,128)(2,1)}) custom-call(s32[1]{0:T(128)} %bitcast.3.side, bf16[512,1024]{1,0:T(8,128)(2,1)} %bitcast.28, bf16[512,1024]{1,0:T(8,128)(2,1)} %copy-done.7, bf16[512,512]{1,0:T(8,128)(2,1)} %bitcast.41, ...), custom_call_target="tpu_custom_call" | custom-call | tf_op jit(solution)/shard_map/expert_rows/pallas_call | solution.py:92
  47.3 4.8 %all-to-all-start.1 = ((bf16[64,8,1024]{2,1,0:T(8,128)(2,1)}), bf16[64,8,1024]{2,1,0:T(8,128)(2,1)S(1)}, u32[]{:S(2)}, u32[]{:S(2)}) async-start(bf16[64,8,1024]{2,1,0:T(8,128)(2,1)} %fusion), calls=%async_computation.1 | async-start | bytes 2097152 | tf_op jit(solution)/shard_map/all_to_all | solution.py:587
  52.1 2.6 %add_convert_fusion = bf16[512,1024]{1,0:T(8,128)(2,1)} fusion(bf16[512,1024]{1,0:T(8,128)(2,1)} %collective-permute-done.1, bf16[512,1024]{1,0:T(8,128)(2,1)S(1)} %copy-done.11), kind=kLoop, calls=%fused_computation | loop fusion | flops 2097152 | bytes 3145728 | tf_op jit(solution)/shard_map/convert_element_type | solution.py:593
  54.8 16.9 %all-to-all-done.1 = bf16[64,8,1024]{2,1,0:T(8,128)(2,1)S(1)} async-done(((bf16[64,8,1024]{2,1,0:T(8,128)(2,1)}), bf16[64,8,1024]{2,1,0:T(8,128)(2,1)S(1)}, u32[]{:S(2)}, u32[]{:S(2)}) %all-to-all-start.1) | async-done | bytes 1048608 | tf_op jit(solution)/shard_map/all_to_all | solution.py:587
  71.6 4.8 %all-to-all-start.2 = ((bf16[64,8,1024]{2,1,0:T(8,128)(2,1)}), bf16[64,8,1024]{2,1,0:T(8,128)(2,1)S(1)}, u32[]{:S(2)}, u32[]{:S(2)}) async-start(bf16[64,8,1024]{2,1,0:T(8,128)(2,1)} %bitcast.18), calls=%async_computation.2 | async-start | bytes 2097152 | tf_op jit(solution)/shard_map/all_to_all | solution.py:595
  78.3 4.8 %shard_map.232 = (bf16[1024,128]{1,0:T(8,128)(2,1)}, f32[1024,128]{1,0:T(8,128)}, f32[1024,128]{1,0:T(8,128)}, f32[1024,128]{1,0:T(8,128)}, bf16[16,128,128]{2,1...) custom-call(bf16[128,1024]{1,0:T(8,128)(2,1)} %scan_in.1, ...), custom_call_target="tpu_custom_call" | custom-call | tf_op jit(solution)/shard_map/pallas_call | solution.py:286
  83.1 11.8 %all-to-all-done.2 = bf16[64,8,1024]{2,1,0:T(8,128)(2,1)S(1)} async-done(((bf16[64,8,1024]{2,1,0:T(8,128)(2,1)}), bf16[64,8,1024]{2,1,0:T(8,128)(2,1)S(1)}, u32[]{:S(2)}, u32[]{:S(2)}) %all-to-all-start.2) | async-done | bytes 1048608 | tf_op jit(solution)/shard_map/all_to_all | solution.py:595
  97.2 1.7 %collective-permute-start.4 = (bf16[512,128]{1,0:T(8,128)(2,1)S(1)}, bf16[512,128]{1,0:T(8,128)(2,1)S(1)}, u32[]{:S(2)}, u32[]{:S(2)}) collective-permute-start(bf16[512,128]{1,0:T(8,128)(2,1)S(1)} %get-tuple-element.91), channel_id=1, source_target_pairs={{0,64},{32,96},{64,0},{96,32},{1,65},{33,97},{65,1},{97,33},{2,66}... | collective-permute-start | bytes 393224 | tf_op jit(solution)/shard_map/ppermute | solution.py:33
  98.9 2.5 %collective-permute-done.5 = bf16[512,128]{1,0:T(8,128)(2,1)S(1)} collective-permute-done((bf16[512,128]{1,0:T(8,128)(2,1)S(1)}, bf16[512,128]{1,0:T(8,128)(2,1)S(1)}, u32[]{:S(2)}, u32[]{:S(2)}) %collective-permute-start.5) | collective-permute-done | bytes 131104 | tf_op jit(solution)/shard_map/ppermute | solution.py:33
  101.4 2.3 %collective-permute-done.4 = bf16[512,128]{1,0:T(8,128)(2,1)S(1)} collective-permute-done((bf16[512,128]{1,0:T(8,128)(2,1)S(1)}, bf16[512,128]{1,0:T(8,128)(2,1)S(1)}, u32[]{:S(2)}, u32[]{:S(2)}) %collective-permute-start.4) | collective-permute-done | bytes 131104 | tf_op jit(solution)/shard_map/ppermute | solution.py:33
  105.8 8.1 %weights.1 = (bf16[512,2048]{1,0:T(8,128)(2,1)}, bf16[2048,512]{1,0:T(8,128)(2,1)}, bf16[2048,512]{1,0:T(8,128)(2,1)}) custom-call(s32[1]{0:T(128)} %bitcast.3.side, bf16[512,512]{1,0:T(8,128)(2,1)} %get-tuple-element.50.active, bf16[512,512]{1,0:T(8,128)(2,1)} %get-tuple-element.51.gate_grad, bf16[512,512]{1,0:T(8,128)(2,1)} %get-tuple-element.52.up_grad, ...), custom_call_target="tpu_custom_call" | custom-call | tf_op jit(solution)/shard_map/weights/pallas_call | solution.py:133
  117.8 6.1 %message.1 = (bf16[64,40,128]{2,1,0:T(8,128)(2,1)}, f32[1024,128]{1,0:T(8,128)}) custom-call(s32[1]{0:T(128)} %bitcast.3.side, bf16[1024,128]{1,0:T(8,128)(2,1)} %copy-done.8, bf16[1024,128]{1,0:T(8,128)(2,1)} %copy-done.13, bf16[1024,2048]{1,0:T(8,128)(2,1)} %out_far.1, bf16[1024,2048]{1,0:T(8,128)(2,1)} %out_far.1, f32[1024,1]{1,0:T(8,128)} %copy.27.gain, ...), custom_call_target="tpu_custom_call" | custom-call | tf_op jit(solution)/shard_map/message/pallas_call | solution.py:365
  123.9 6.6 %all-to-all-start.3 = ((bf16[64,40,128]{2,1,0:T(8,128)(2,1)}), bf16[64,40,128]{2,1,0:T(8,128)(2,1)S(1)}, u32[]{:S(2)}, u32[]{:S(2)}) async-start(bf16[64,40,128]{2,1,0:T(8,128)(2,1)} %get-tuple-element.70), calls=%async_computation.3 | async-start | bytes 1310720 | tf_op jit(solution)/shard_map/all_to_all | solution.py:619
  131.9 1.9 %convolution_convert_fusion.1 = bf16[512,1024]{1,0:T(8,128)(2,1)S(1)} fusion(bf16[1024,128]{1,0:T(8,128)(2,1)} %copy-done.16, bf16[1024,128]{1,0:T(8,128)(2,1)} %copy-done.17, bf16[1024,128]{1,0:T(8,128)(2,1)} %copy-done.18, bf16[1024,128]{1,0:T(8,128)(2,1)S(1)} %copy-done.15, bf16[512,512]{1,0:T(8,128)(2,1)} %collective-permute-done.6, pred[]{:T(512)S(6)} %eq.6, ...), kind=kOutput, calls=%fused_computation.2 | convolution fusion | flops 543948800 | bytes 3145729 | tf_op jit(solution)/shard_map/dot_general | solution.py:23
  137.2 1.9 %collective-permute-start.11 = (bf16[128,1024]{1,0:T(8,128)(2,1)S(1)}, bf16[128,1024]{1,0:T(8,128)(2,1)}, u32[]{:S(2)}, u32[]{:S(2)}) collective-permute-start(bf16[128,1024]{1,0:T(8,128)(2,1)S(1)} %get-tuple-element.85), channel_id=1, source_target_pairs={{0,16},{8,24},{16,0},{24,8},{1,17},{9,25},{17,1},{25,9},{2,18},{10... | collective-permute-start | bytes 786440 | tf_op jit(solution)/shard_map/ppermute | solution.py:33
  139.0 5.6 %all-to-all-done.3.came = bf16[64,40,128]{2,1,0:T(8,128)(2,1)S(1)} async-done(((bf16[64,40,128]{2,1,0:T(8,128)(2,1)}), bf16[64,40,128]{2,1,0:T(8,128)(2,1)S(1)}, u32[]{:S(2)}, u32[]{:S(2)}) %all-to-all-start.3) | async-done | bytes 655392 | tf_op jit(solution)/shard_map/all_to_all | solution.py:619
  144.7 2.5 %owner.1 = bf16[64,24,128]{2,1,0:T(8,128)(2,1)} custom-call(s32[1]{0:T(128)} %bitcast.20.lead, bf16[64,40,128]{2,1,0:T(8,128)(2,1)S(1)} %all-to-all-done.3.came), custom_call_target="tpu_custom_call" | custom-call | tf_op jit(solution)/shard_map/owner/pallas_call | solution.py:487
  147.2 4.9 %all-to-all-start.4 = ((bf16[64,24,128]{2,1,0:T(8,128)(2,1)}), bf16[64,24,128]{2,1,0:T(8,128)(2,1)S(1)}, u32[]{:S(2)}, u32[]{:S(2)}) async-start(bf16[64,24,128]{2,1,0:T(8,128)(2,1)} %owner.1), calls=%async_computation.4 | async-start | bytes 786432 | tf_op jit(solution)/shard_map/all_to_all | solution.py:625
  156.6 1.9 %collective-permute-start.14 = (bf16[32,1024]{1,0:T(8,128)(2,1)S(1)}, bf16[32,1024]{1,0:T(8,128)(2,1)S(1)}, u32[]{:S(2)}, u32[]{:S(2)}) collective-permute-start(bf16[32,1024]{1,0:T(8,128)(2,1)S(1)} %get-tuple-element.88), channel_id=1, source_target_pairs={{0,4},{2,6},{4,0},{6,2},{1,5},{3,7},{5,1},{7,3},{8,12},{10,14},{12... | collective-permute-start | bytes 196616 | tf_op jit(solution)/shard_map/ppermute | solution.py:33
  158.5 4.8 %inside.1 = (bf16[128,1024]{1,0:T(8,128)(2,1)}, f32[4,392,128]{2,1,0:T(8,128)}, bf16[128,512]{1,0:T(8,128)(2,1)}) custom-call(f32[1024,128]{1,0:T(8,128)} %get-tuple-element.73.grad_in, f32[1024,128]{1,0:T(8,128)} %get-tuple-element.64.gated_in, f32[1024,128]{1,0:T(8,128)} %get-tuple-element.65.silu_in, f32[1024,128]{1,0:T(8,128)} %get-tuple-element.74.slope_in, ...), custom_call_target="tpu_custom_call" | custom-call | tf_op jit(solution)/shard_map/inside/pallas_call | solution.py:436
  (79 shorter events, 25.1 us)
Async XLA Ops:
  3.7 30.6 %all-to-all-start = ((bf16[64,8,1024]{2,1,0:T(8,128)(2,1)}), bf16[64,8,1024]{2,1,0:T(8,128)(2,1)S(1)}, u32[]{:S(2)}, u32[]{:S(2)}) async-start(bf16[64,8,1024]{2,1,0:T(8,128)(2,1)} %bitcast.40), calls=%async_computation | async-start | bytes 2097152 | tf_op jit(solution)/shard_map/all_to_all | solution.py:585
  34.3 2.7 %collective-permute-start = (bf16[512,1024]{1,0:T(8,128)(2,1)S(1)}, bf16[512,1024]{1,0:T(8,128)(2,1)S(1)}, u32[]{:S(2)}, u32[]{:S(2)}) collective-permute-start(bf16[512,1024]{1,0:T(8,128)(2,1)S(1)} %bitcast.27), channel_id=1, source_target_pairs={{0,1},{1,0},{2,3},{3,2},{4,5},{5,4},{6,7},{7,6},{8,9},{9,8},{10,11... | collective-permute-start | bytes 3145736 | tf_op jit(solution)/shard_map/ppermute | solution.py:27
  47.1 5.0 %collective-permute-start.1 = (bf16[512,1024]{1,0:T(8,128)(2,1)}, bf16[512,1024]{1,0:T(8,128)(2,1)}, u32[]{:S(2)}, u32[]{:S(2)}) collective-permute-start(bf16[512,1024]{1,0:T(8,128)(2,1)} %get-tuple-element.54), channel_id=1, source_target_pairs={{0,1},{1,0},{2,3},{3,2},{4,5},{5,4},{6,7},{7,6},{8,9},{9,8},{10,11... | collective-permute-start | bytes 3145736 | tf_op jit(solution)/shard_map/ppermute | solution.py:27
  47.3 24.4 %all-to-all-start.1 = ((bf16[64,8,1024]{2,1,0:T(8,128)(2,1)}), bf16[64,8,1024]{2,1,0:T(8,128)(2,1)S(1)}, u32[]{:S(2)}, u32[]{:S(2)}) async-start(bf16[64,8,1024]{2,1,0:T(8,128)(2,1)} %fusion), calls=%async_computation.1 | async-start | bytes 2097152 | tf_op jit(solution)/shard_map/all_to_all | solution.py:587
  52.1 24.4 %copy-start.14 = (bf16[1024]{0:T(1024)(128)(2,1)S(1)}, bf16[1024]{0:T(1024)(128)(2,1)}, u32[]{:S(2)}) copy-start(bf16[1024]{0:T(1024)(128)(2,1)} %param.27) | copy-start | bytes 6148
  54.7 22.8 %copy-start.10 = (bf16[128,2048]{1,0:T(8,128)(2,1)S(1)}, bf16[128,2048]{1,0:T(8,128)(2,1)}, u32[]{:S(2)}) copy-start(bf16[128,2048]{1,0:T(8,128)(2,1)} %cotangent.1) | copy-start | bytes 1572868
  71.6 23.2 %all-to-all-start.2 = ((bf16[64,8,1024]{2,1,0:T(8,128)(2,1)}), bf16[64,8,1024]{2,1,0:T(8,128)(2,1)S(1)}, u32[]{:S(2)}, u32[]{:S(2)}) async-start(bf16[64,8,1024]{2,1,0:T(8,128)(2,1)} %bitcast.18), calls=%async_computation.2 | async-start | bytes 2097152 | tf_op jit(solution)/shard_map/all_to_all | solution.py:595
  76.4 29.3 %collective-permute-start.2 = (bf16[512,1024]{1,0:T(8,128)(2,1)S(1)}, bf16[512,1024]{1,0:T(8,128)(2,1)}, u32[]{:S(2)}, u32[]{:S(2)}) collective-permute-start(bf16[512,1024]{1,0:T(8,128)(2,1)S(1)} %bitcast.36), channel_id=1, source_target_pairs={{0,1},{1,0},{2,3},{3,2},{4,5},{5,4},{6,7},{7,6},{8,9},{9,8},{10,11... | collective-permute-start | bytes 3145736 | tf_op jit(solution)/shard_map/ppermute | solution.py:27
  96.4 5.0 %collective-permute-start.5 = (bf16[512,128]{1,0:T(8,128)(2,1)S(1)}, bf16[512,128]{1,0:T(8,128)(2,1)S(1)}, u32[]{:S(2)}, u32[]{:S(2)}) collective-permute-start(bf16[512,128]{1,0:T(8,128)(2,1)S(1)} %get-tuple-element.90), channel_id=1, source_target_pairs={{0,96},{32,0},{64,32},{96,64},{1,97},{33,1},{65,33},{97,65},{2,98}... | collective-permute-start | bytes 393224 | tf_op jit(solution)/shard_map/ppermute | solution.py:33
  97.2 6.5 %collective-permute-start.4 = (bf16[512,128]{1,0:T(8,128)(2,1)S(1)}, bf16[512,128]{1,0:T(8,128)(2,1)S(1)}, u32[]{:S(2)}, u32[]{:S(2)}) collective-permute-start(bf16[512,128]{1,0:T(8,128)(2,1)S(1)} %get-tuple-element.91), channel_id=1, source_target_pairs={{0,64},{32,96},{64,0},{96,32},{1,65},{33,97},{65,1},{97,33},{2,66}... | collective-permute-start | bytes 393224 | tf_op jit(solution)/shard_map/ppermute | solution.py:33
  98.9 6.2 %collective-permute-start.3 = (bf16[512,128]{1,0:T(8,128)(2,1)S(1)}, bf16[512,128]{1,0:T(8,128)(2,1)S(1)}, u32[]{:S(2)}, u32[]{:S(2)}) collective-permute-start(bf16[512,128]{1,0:T(8,128)(2,1)S(1)} %get-tuple-element.92), channel_id=1, source_target_pairs={{0,32},{32,64},{64,96},{96,0},{1,33},{33,65},{65,97},{97,1},{2,34}... | collective-permute-start | bytes 393224 | tf_op jit(solution)/shard_map/ppermute | solution.py:33
  105.2 26.8 %collective-permute-start.6 = (bf16[512,512]{1,0:T(8,128)(2,1)S(1)}, bf16[512,512]{1,0:T(8,128)(2,1)}, u32[]{:S(2)}, u32[]{:S(2)}) collective-permute-start(bf16[512,512]{1,0:T(8,128)(2,1)S(1)} %pad_maximum_fusion), channel_id=1, source_target_pairs={{0,1},{1,0},{2,3},{3,2},{4,5},{5,4},{6,7},{7,6},{8,9},{9,8},{10,11... | collective-permute-start | bytes 1572872 | tf_op jit(solution)/shard_map/ppermute | solution.py:27
  105.3 11.8 %collective-permute-start.16 = (bf16[1024,128]{1,0:T(8,128)(2,1)S(1)}, bf16[1024,128]{1,0:T(8,128)(2,1)S(1)}, u32[]{:S(2)}, u32[]{:S(2)}) collective-permute-start(bf16[1024,128]{1,0:T(8,128)(2,1)S(1)} %fusion.1.grad_own), channel_id=1, source_target_pairs={{0,1},{1,0},{2,3},{3,2},{4,5},{5,4},{6,7},{7,6},{8,9},{9,8},{10,11... | collective-permute-start | bytes 786440 | tf_op jit(solution)/shard_map/ppermute | solution.py:27
  113.9 16.5 %collective-permute-start.9 = (bf16[1024,128]{1,0:T(8,128)(2,1)S(1)}, bf16[1024,128]{1,0:T(8,128)(2,1)S(1)}, u32[]{:S(2)}, u32[]{:S(2)}) collective-permute-start(bf16[1024,128]{1,0:T(8,128)(2,1)S(1)} %copy-done.15), channel_id=1, source_target_pairs={{0,96},{32,0},{64,32},{96,64},{1,97},{33,1},{65,33},{97,65},{2,98}... | collective-permute-start | bytes 786440 | tf_op jit(solution)/shard_map/ppermute | solution.py:33
  115.0 15.5 %collective-permute-start.8 = (bf16[1024,128]{1,0:T(8,128)(2,1)S(1)}, bf16[1024,128]{1,0:T(8,128)(2,1)S(1)}, u32[]{:S(2)}, u32[]{:S(2)}) collective-permute-start(bf16[1024,128]{1,0:T(8,128)(2,1)S(1)} %copy-done.15), channel_id=1, source_target_pairs={{0,64},{32,96},{64,0},{96,32},{1,65},{33,97},{65,1},{97,33},{2,66}... | collective-permute-start | bytes 786440 | tf_op jit(solution)/shard_map/ppermute | solution.py:33
  116.2 14.2 %collective-permute-start.7 = (bf16[1024,128]{1,0:T(8,128)(2,1)S(1)}, bf16[1024,128]{1,0:T(8,128)(2,1)S(1)}, u32[]{:S(2)}, u32[]{:S(2)}) collective-permute-start(bf16[1024,128]{1,0:T(8,128)(2,1)S(1)} %copy-done.15), channel_id=1, source_target_pairs={{0,32},{32,64},{64,96},{96,0},{1,33},{33,65},{65,97},{97,1},{2,34}... | collective-permute-start | bytes 786440 | tf_op jit(solution)/shard_map/ppermute | solution.py:33
  123.9 20.8 %all-to-all-start.3 = ((bf16[64,40,128]{2,1,0:T(8,128)(2,1)}), bf16[64,40,128]{2,1,0:T(8,128)(2,1)S(1)}, u32[]{:S(2)}, u32[]{:S(2)}) async-start(bf16[64,40,128]{2,1,0:T(8,128)(2,1)} %get-tuple-element.70), calls=%async_computation.3 | async-start | bytes 1310720 | tf_op jit(solution)/shard_map/all_to_all | solution.py:619
  133.9 18.3 %collective-permute-start.10 = (bf16[128,1024]{1,0:T(8,128)(2,1)S(1)}, bf16[128,1024]{1,0:T(8,128)(2,1)S(1)}, u32[]{:S(2)}, u32[]{:S(2)}) collective-permute-start(bf16[128,1024]{1,0:T(8,128)(2,1)S(1)} %get-tuple-element.83), channel_id=1, source_target_pairs={{0,8},{8,16},{16,24},{24,0},{1,9},{9,17},{17,25},{25,1},{2,10},{10... | collective-permute-start | bytes 786440 | tf_op jit(solution)/shard_map/ppermute | solution.py:33
  135.5 16.6 %collective-permute-start.12 = (bf16[128,1024]{1,0:T(8,128)(2,1)S(1)}, bf16[128,1024]{1,0:T(8,128)(2,1)S(1)}, u32[]{:S(2)}, u32[]{:S(2)}) collective-permute-start(bf16[128,1024]{1,0:T(8,128)(2,1)S(1)} %get-tuple-element.84), channel_id=1, source_target_pairs={{0,24},{8,0},{16,8},{24,16},{1,25},{9,1},{17,9},{25,17},{2,26},{10... | collective-permute-start | bytes 786440 | tf_op jit(solution)/shard_map/ppermute | solution.py:33
  137.2 15.0 %collective-permute-start.11 = (bf16[128,1024]{1,0:T(8,128)(2,1)S(1)}, bf16[128,1024]{1,0:T(8,128)(2,1)}, u32[]{:S(2)}, u32[]{:S(2)}) collective-permute-start(bf16[128,1024]{1,0:T(8,128)(2,1)S(1)} %get-tuple-element.85), channel_id=1, source_target_pairs={{0,16},{8,24},{16,0},{24,8},{1,17},{9,25},{17,1},{25,9},{2,18},{10... | collective-permute-start | bytes 786440 | tf_op jit(solution)/shard_map/ppermute | solution.py:33
  147.2 16.9 %all-to-all-start.4 = ((bf16[64,24,128]{2,1,0:T(8,128)(2,1)}), bf16[64,24,128]{2,1,0:T(8,128)(2,1)S(1)}, u32[]{:S(2)}, u32[]{:S(2)}) async-start(bf16[64,24,128]{2,1,0:T(8,128)(2,1)} %owner.1), calls=%async_computation.4 | async-start | bytes 786432 | tf_op jit(solution)/shard_map/all_to_all | solution.py:625
  153.3 10.0 %collective-permute-start.13 = (bf16[32,1024]{1,0:T(8,128)(2,1)S(1)}, bf16[32,1024]{1,0:T(8,128)(2,1)S(1)}, u32[]{:S(2)}, u32[]{:S(2)}) collective-permute-start(bf16[32,1024]{1,0:T(8,128)(2,1)S(1)} %get-tuple-element.86), channel_id=1, source_target_pairs={{0,2},{2,4},{4,6},{6,0},{1,3},{3,5},{5,7},{7,1},{8,10},{10,12},{12... | collective-permute-start | bytes 196616 | tf_op jit(solution)/shard_map/ppermute | solution.py:33
  155.0 8.4 %collective-permute-start.15 = (bf16[32,1024]{1,0:T(8,128)(2,1)S(1)}, bf16[32,1024]{1,0:T(8,128)(2,1)S(1)}, u32[]{:S(2)}, u32[]{:S(2)}) collective-permute-start(bf16[32,1024]{1,0:T(8,128)(2,1)S(1)} %get-tuple-element.87), channel_id=1, source_target_pairs={{0,6},{2,0},{4,2},{6,4},{1,7},{3,1},{5,3},{7,5},{8,14},{10,8},{12,... | collective-permute-start | bytes 196616 | tf_op jit(solution)/shard_map/ppermute | solution.py:33
  156.6 6.7 %collective-permute-start.14 = (bf16[32,1024]{1,0:T(8,128)(2,1)S(1)}, bf16[32,1024]{1,0:T(8,128)(2,1)S(1)}, u32[]{:S(2)}, u32[]{:S(2)}) collective-permute-start(bf16[32,1024]{1,0:T(8,128)(2,1)S(1)} %get-tuple-element.88), channel_id=1, source_target_pairs={{0,4},{2,6},{4,0},{6,2},{1,5},{3,7},{5,1},{7,3},{8,12},{10,14},{12... | collective-permute-start | bytes 196616 | tf_op jit(solution)/shard_map/ppermute | solution.py:33
  (17 other events, 98.9 us)
